TPU v7x, 256 devices: a whole 4x4x8 slice. The times are simulated.
256 devices in a mesh: sp: 32 (over z, x), tp: 8 (over y, core).
Axes of the slice: x: 4, y: 4, z: 8, core: 2. Of those that a mesh axis runs over, the one named last changes fastest.
Arguments:
- tokens: bfloat16 [8192, 1024], P(('sp', 'tp')), may hold values from -6 to 6
- doc_ids: int32 [8192], P('sp'), may hold values from 0 to 31, never falling along the last dimension, each value on 1 to 4608 neighbouring positions
- down_query: bfloat16 [1024, 256], P('sp'), may hold values from -0.1875 to 0.1875
- down_key: bfloat16 [1024, 256], P('sp'), may hold values from -0.1875 to 0.1875
- down_rotary: bfloat16 [1024, 32], P('sp'), may hold values from -0.1875 to 0.1875
- query_gain: float32 [256], replicated, may hold values from 0.1 to 1.9
- key_gain: float32 [256], replicated, may hold values from 0.1 to 1.9
- up_query: bfloat16 [256, 1536], P('sp', 'tp'), may hold values from -0.375 to 0.375
- up_key: bfloat16 [256, 1024], P('sp', 'tp'), may hold values from -0.375 to 0.375
- up_value: bfloat16 [256, 1024], P('sp', 'tp'), may hold values from -0.375 to 0.375
- output_weight: bfloat16 [1024, 1024], P('tp', 'sp'), may hold values from -0.1875 to 0.1875
- out_gain: float32 [1024], replicated, may hold values from 0.1 to 1.9
Outputs:
- mixed: bfloat16 [8192, 1024], P(('sp', 'tp'))
- log_sums: float32 [8192, 16], P('sp', 'tp')
Inputs may be any that keep to these rules, and one draw needn't show every extreme that they name: doc_ids never fall along the sequence and run from 0 to at most the number of devices along sp minus one; each document has 1 to 4608 positions, and one document has exactly that many.
All inputs are finite; a program needn't handle non-finite values.
Results may differ from a plain program's by a relative error of at most 0.02.
Values may be sent and summed in bfloat16 or wider, within the bound.
No kernel may reach another device: no remote copies, remote signals or barrier semaphores. Data moves between devices by JAX's collectives and lax.ppermute only.
A program may use at most 64 MiB of HBM per device.

v0:
```python
import math

import jax
import jax.numpy as jnp
from jax import lax
from jax.experimental import pallas as pl
from jax.experimental.pallas import tpu as pltpu
from jax.sharding import Mesh
from jax.sharding import PartitionSpec as P


NOPE = 64
ROPE = 32
NZ, NX, NY, NC = 8, 4, 4, 2
NS = NZ * NX
AXES = ("z", "x", "y", "c")
SP = ("z", "x")
TP = ("y", "c")
NEG_BIG = -1e30
FLOOR = -1e20
THETA = 10000.0
EPS = 1e-06
LN2 = math.log(2.0)
SCALE2 = 1.0 / math.sqrt(NOPE + ROPE) / LN2
BF = jnp.bfloat16
F32 = jnp.float32


VMEM = pltpu.VMEM
SMEM_SPEC = pl.BlockSpec(memory_space=pltpu.SMEM)
VMEM_SPEC = pl.BlockSpec(memory_space=pltpu.VMEM)
ANY_SPEC = pl.BlockSpec(memory_space=pl.ANY)


def call(body, outs, n_smem, n_in, scratch=(), any_from=None, cost=None):
    specs = [SMEM_SPEC] * n_smem
    for i in range(n_in):
        specs.append(ANY_SPEC if any_from is not None and i >= any_from else VMEM_SPEC)
    single = not isinstance(outs, tuple)
    return pl.pallas_call(
        body,
        out_shape=outs,
        in_specs=specs,
        out_specs=VMEM_SPEC if single else tuple(VMEM_SPEC for _ in outs),
        scratch_shapes=list(scratch),
        compiler_params=pltpu.CompilerParams(vmem_limit_bytes=50 * 1024 * 1024),
        cost_estimate=cost,
    )


def lanes(shape):
    return lax.broadcasted_iota(jnp.int32, shape, len(shape) - 1)


def column(row):
    return jnp.transpose(jnp.broadcast_to(row, (128, 128)))


def pack(where, dq, dk, dr, out, flipped):
    y = where[2]

    def chosen(ref):
        block = ref[:, 0:64]
        for k in range(1, NY):
            block = jnp.where(y == k, ref[:, 64 * k : 64 * (k + 1)], block)
        return block

    block = jnp.concatenate([chosen(dq), chosen(dk)], axis=1)
    rope = dr[...].astype(F32)
    rope = jnp.concatenate([rope, jnp.zeros((32, 96), F32)], axis=1)
    flipped[...] = jnp.transpose(jnp.concatenate([rope] * 4, axis=0))
    turned = jnp.concatenate([flipped[pl.ds(4 * y, 4), :], flipped[pl.ds(16 + 4 * y, 4), :]], axis=0)
    turned = turned.astype(BF)
    for s in range(NS):
        out[s, 0:32, :] = block
        out[s, 32:40, :] = turned


def project(where, t0, t1, t2, t3, gathered, cos_ref, sin_ref, q_ref, k_ref, tok):
    y = where[2]
    for j, part in enumerate((t0, t1, t2, t3)):
        at = lax.rem(y - j + NY, NY)
        tok[pl.ds(pl.multiple_of(at * 32, 32), 32), :] = part[...]
    rows = tok[...]
    weights = gathered[:, 0:32, :].reshape(NS * 32, 128)
    both = jnp.dot(rows, weights, preferred_element_type=F32)
    turned = jnp.transpose(both).astype(BF)
    for t in range(NY * NC):
        q_ref[t] = turned[0:64, :]
    for t in range(NZ):
        k_ref[t, 0:64, :] = turned[64:128, :]
    group = lanes((8, 128)) // 32
    pieces = []
    for z in range(NZ):
        piece = gathered[4 * z, 32:40, :].astype(F32)
        for g in range(1, 4):
            piece = jnp.where(group == g, gathered[4 * z + g, 32:40, :].astype(F32), piece)
        pieces.append(piece)
    rope = jnp.concatenate(pieces, axis=1)
    rope = jnp.concatenate([rope, jnp.zeros_like(rope)], axis=0).astype(BF)
    raw = lax.dot_general(rope, rows, (((1,), (1,)), ((), ())), preferred_element_type=F32)
    raw = raw[0:8, :].astype(BF).astype(F32)
    rotated = raw * cos_ref[...] + pltpu.roll(raw, 4, 0) * sin_ref[...]
    rotated = rotated.astype(BF)
    for t in range(NZ):
        k_ref[t, 64:72, :] = rotated


def make_queries(q_in, up_own, up_other, gain, cos_ref, low_ref, high_ref, out):
    blocks = []
    for y in range(NY):
        blocks.append(
            jnp.concatenate([q_in[2 * y].astype(F32), q_in[2 * y + 1].astype(F32)], axis=1)
        )
    total = blocks[0] * blocks[0]
    for b in blocks[1:]:
        total = total + b * b
    mean = jnp.sum(total, axis=0, keepdims=True) * (1.0 / 256.0)
    inverse = lax.rsqrt(mean + EPS)
    gains = jnp.concatenate([column(gain[0:1, :]), column(gain[1:2, :])], axis=0)
    gains = jnp.concatenate([gains, gains], axis=1)
    latent = jnp.concatenate(blocks, axis=0) * inverse * gains
    latent = jnp.transpose(latent).astype(BF)
    lane = lanes((256, 128))
    for p, up in enumerate((up_own, up_other)):
        wide = up[...].astype(F32)
        plain_w = wide[:, 0:8, :].reshape(256, 128).astype(BF)
        rope_w = wide[:, 24:32, :].reshape(256, 128).astype(BF)
        plain = jnp.dot(latent, plain_w, preferred_element_type=F32) * SCALE2
        raw = jnp.dot(latent, rope_w, preferred_element_type=F32) * SCALE2
        rope = (
            raw * cos_ref[...]
            + pltpu.roll(raw, 124, 1) * low_ref[...]
            + pltpu.roll(raw, 4, 1) * high_ref[...]
        )
        for i in range(2):
            own = slice(256 * i, 256 * (i + 1))
            out[p, own, 0:128] = jnp.where(lane // 64 == i, plain, 0.0).astype(BF)
            out[p, own, 128:256] = jnp.where(lane // 32 == i, rope, 0.0).astype(BF)


def attend(
    where, q_ref, up_own, up_other, gain, key_docs, query_docs, b0, b1, b2, b3,
    keep_ref, send_ref, ml_ref, kb, s_buf, v_buf, mx, total, acc, uk, uv, gains, docs_col, sems,
):
    x0, y0, c, low, high = where[1], where[2], where[3], where[4], where[5]
    copies = [
        pltpu.make_async_copy(part, kb.at[j], sems.at[j]) for j, part in enumerate((b0, b1, b2, b3))
    ]
    for copy in copies:
        copy.start()
    for p, up in enumerate((up_own, up_other)):
        wide = up[...].astype(F32)
        own = slice(128 * p, 128 * (p + 1))
        uk[own, :] = jnp.transpose(wide[:, 8:16, :].reshape(256, 128)).astype(BF)
        uv[own, :] = jnp.transpose(wide[:, 16:24, :].reshape(256, 128)).astype(BF)
    for i in range(2):
        gains[128 * i : 128 * (i + 1), :] = column(gain[i : i + 1, :])
        docs_col[128 * i : 128 * (i + 1), :] = column(query_docs[i : i + 1, :])
    mx[...] = jnp.full(mx.shape, NEG_BIG, F32)
    total[...] = jnp.zeros(total.shape, F32)
    acc[...] = jnp.zeros(acc.shape, F32)
    for copy in copies:
        copy.wait()
    first = low // 2
    last = high // 2 + 1

    def scores(tile, carry):
        z = tile // 2
        latents, ropes = [], []
        for half in range(2):
            x = 2 * lax.rem(tile, 2) + half
            jx = lax.rem(x0 - x + NX, NX)
            parts, turned = [], []
            for y in range(NY):
                jy = lax.rem(y0 - y + NY, NY)
                third = jnp.where(c == 0, jy, jx)
                second = jnp.where(c == 0, jx, jy)
                slab = kb[third, second, z].astype(F32)
                parts.append(slab[0:64, :])
                turned.append(slab[64:72, :])
            squares = parts[0] * parts[0]
            for part in parts[1:]:
                squares = squares + part * part
            mean = jnp.sum(squares, axis=0, keepdims=True) * (1.0 / 256.0)
            inverse = lax.rsqrt(mean + EPS)
            latent = jnp.concatenate(parts, axis=0) * inverse * gains[...]
            latents.append(latent.astype(BF))
            ropes.append(jnp.concatenate(turned, axis=0).astype(BF))
        latent = jnp.concatenate(latents, axis=1)
        rope = jnp.concatenate(ropes, axis=1)
        keys = jnp.dot(uk[...], latent, preferred_element_type=F32).astype(BF)
        values = jnp.dot(uv[...], latent, preferred_element_type=F32)
        v_buf[tile] = jnp.transpose(values).astype(BF)
        blank = jnp.zeros((64, 256), BF)
        same = []
        for half in range(2):
            docs_row = key_docs[pl.ds(2 * tile + half, 1), :]
            same.append(docs_col[...] == docs_row)
        for p in range(2):
            stack = jnp.concatenate([keys[128 * p : 128 * (p + 1), :], rope, rope, blank], axis=0)
            for i in range(2):
                own = slice(256 * i, 256 * (i + 1))
                got = jnp.dot(q_ref[p, own, :], stack, preferred_element_type=F32)
                lhs = jnp.where(same[0], got[:, 0:128], NEG_BIG)
                rhs = jnp.where(same[1], got[:, 128:256], NEG_BIG)
                s_buf[tile, 2 * p + i, :, 0:128] = lhs
                s_buf[tile, 2 * p + i, :, 128:256] = rhs
                mx[2 * p + i] = jnp.maximum(mx[2 * p + i], jnp.maximum(lhs, rhs))
        return carry

    lax.fori_loop(first, last, scores, 0)
    tops = []
    for h in range(4):
        top = jnp.max(mx[h], axis=1, keepdims=True)
        top = jnp.maximum(top, FLOOR)
        mx[h] = jnp.broadcast_to(top, (256, 128))
        tops.append(top)

    def weigh(tile, carry):
        v = v_buf[tile]
        lane = lanes((256, 256)) // 64
        result = acc[...]
        for h in range(4):
            top = mx[h]
            lhs = jnp.exp2(s_buf[tile, h, :, 0:128] - top)
            rhs = jnp.exp2(s_buf[tile, h, :, 128:256] - top)
            total[h] = total[h] + lhs + rhs
            weights = jnp.concatenate([lhs.astype(BF), rhs.astype(BF)], axis=1)
            own = jnp.where(lane == h, v, jnp.zeros_like(v))
            result = result + jnp.dot(weights, own, preferred_element_type=F32)
        acc[...] = result
        return carry

    lax.fori_loop(first, last, weigh, 0)
    lane = lanes((256, 128))
    packed = jnp.zeros((256, 128), F32)
    for h in range(4):
        packed = jnp.where(lane == h, tops[h], packed)
        packed = jnp.where(lane == 4 + h, jnp.sum(total[h], axis=1, keepdims=True), packed)
    ml_ref[...] = packed
    keep_ref[...] = acc[pl.ds(pl.multiple_of(c * 128, 128), 128), :]
    send_ref[...] = acc[pl.ds(pl.multiple_of((1 - c) * 128, 128), 128), :].astype(BF)


def combine(where, keep, got, ml_own, ml_got, w_own, w_other, part_ref, lse_ref, f_own, f_got):
    c = where[3]
    own = ml_own[...]
    other = ml_got[...]
    for h in range(4):
        k = (h + 2) % 4
        m0, l0 = own[:, h : h + 1], own[:, 4 + h : 5 + h]
        m1, l1 = other[:, k : k + 1], other[:, 4 + k : 5 + k]
        top = jnp.maximum(m0, m1)
        e0 = jnp.exp2(m0 - top)
        e1 = jnp.exp2(m1 - top)
        weight_sum = l0 * e0 + l1 * e1
        if h < 2:
            lse = (top + jnp.log2(weight_sum)) * LN2
            for half in range(2):
                for y in range(NY):
                    lse_ref[64 * y + 32 * half : 64 * y + 32 * half + 32, h : h + 1] = lse[
                        128 * half + 32 * y : 128 * half + 32 * y + 32, :
                    ]
        f_own[h] = jnp.broadcast_to(e0 / weight_sum, (256, 128))
        f_got[h] = jnp.broadcast_to(e1 / weight_sum, (256, 128))
    rows = pl.ds(pl.multiple_of(c * 128, 128), 128)
    lane = lanes((128, 128)) // 64
    result = jnp.zeros((128, 1024), F32)
    for p, w in enumerate((w_own, w_other)):
        a = jnp.where(lane == 0, f_own[2 * p, rows, :], f_own[2 * p + 1, rows, :])
        b = jnp.where(lane == 0, f_got[2 * p, rows, :], f_got[2 * p + 1, rows, :])
        mine = keep[:, 128 * p : 128 * (p + 1)]
        theirs = got[:, 128 * (1 - p) : 128 * (2 - p)].astype(F32)
        attended = (mine * a + theirs * b).astype(BF)
        result = result + lax.dot_general(
            attended, w[:, 32:64, :].reshape(1024, 128), (((1,), (1,)), ((), ())),
            preferred_element_type=F32,
        )
    part_ref[...] = result.astype(BF).reshape(NY, 32, 1024)


def finish(parts, gain, out):
    summed = parts[0].astype(F32)
    for y in range(1, NY):
        summed = summed + parts[y].astype(F32)
    wide = summed.astype(BF).astype(F32)
    mean = jnp.mean(wide * wide, axis=1, keepdims=True)
    out[...] = (wide * lax.rsqrt(mean + EPS) * gain[...]).astype(BF)


def flat(z, x, y, c):
    return ((z * NX + x) * NY + y) * NC + c


def shift_pairs(stage, j):
    pairs = []
    for z in range(NZ):
        for x in range(NX):
            for y in range(NY):
                for c in range(NC):
                    along_x = (c == 0) == (stage == 2)
                    to = flat(z, (x + j) % NX, y, c) if along_x else flat(z, x, (y + j) % NY, c)
                    pairs.append((flat(z, x, y, c), to))
    return pairs


def layer(
    tokens, doc_ids, down_query, down_key, down_rotary, query_gain, key_gain,
    up_query, up_key, up_value, output_weight, out_gain,
):
    z = lax.axis_index("z")
    x = lax.axis_index("x")
    y = lax.axis_index("y")
    c = lax.axis_index("c")
    sp = z * NX + x
    here = jnp.stack([z, x, y, c]).astype(jnp.int32)
    swap = [(0, 1), (1, 0)]

    message = call(
        pack, jax.ShapeDtypeStruct((NS, 40, 128), BF), 1, 3, scratch=[VMEM((128, 128), F32)]
    )(here, down_query, down_key, down_rotary)
    gathered = lax.all_to_all(message, SP, 0, 0)

    shifted = [
        lax.ppermute(tokens, "y", [(i, (i + j) % NY) for i in range(NY)]) for j in range(1, NY)
    ]

    heads = up_query.reshape(8, 2, NOPE + ROPE)
    plain = heads[:, :, :NOPE].reshape(8, 128)
    turning = heads[:, :, NOPE:].reshape(8, 2, 2, 4, 4).transpose(0, 1, 3, 2, 4).reshape(8, 64)
    docs = doc_ids.astype(BF).reshape(8, 32)
    mixed_rows = jnp.concatenate([turning, docs, jnp.zeros((8, 32), BF)], axis=1)
    later = jnp.concatenate([plain, up_key, up_value, mixed_rows, output_weight.T], axis=0)
    later = jnp.broadcast_to(later[None], (NS, 64, 128))

    f32_base = (sp * 256).astype(F32)
    key_tok = lax.broadcasted_iota(jnp.int32, (8, 128), 1)
    key_row = lax.broadcasted_iota(jnp.int32, (8, 128), 0)
    key_pos = f32_base + (64 * (key_tok // 32) + 32 * c + key_tok % 32).astype(F32)
    key_freq = THETA ** (-(4 * y + key_row % 4).astype(F32) / 16)
    key_angle = key_pos * key_freq
    key_cos = jnp.cos(key_angle)
    key_sin = jnp.sin(key_angle) * jnp.where(key_row < 4, -1.0, 1.0)
    tok = lax.broadcasted_iota(jnp.int32, (256, 128), 0)
    lane = lax.broadcasted_iota(jnp.int32, (256, 128), 1)
    pos = f32_base + (64 * ((tok % 128) // 32) + 32 * (tok // 128) + tok % 32).astype(F32)
    freq = THETA ** (-(4 * ((lane % 32) // 8) + lane % 4).astype(F32) / 16)
    angle = pos * freq
    used = lane < 64
    is_low = (lane // 4) % 2 == 0
    cos = jnp.where(used, jnp.cos(angle), 0.0)
    sine = jnp.sin(angle)
    low_sin = jnp.where(used & is_low, -sine, 0.0)
    high_sin = jnp.where(used & ~is_low, sine, 0.0)

    q_part, k_part = call(
        project,
        (jax.ShapeDtypeStruct((NY * NC, 64, 128), BF), jax.ShapeDtypeStruct((NZ, 72, 128), BF)),
        1, 7, scratch=[VMEM((128, 1024), BF)],
    )(here, tokens, *shifted, gathered, key_cos, key_sin)

    stage1 = lax.all_to_all(k_part, "z", 0, 0)
    stage2 = [lax.ppermute(stage1, AXES, shift_pairs(2, j)) for j in range(1, 4)]
    held = jnp.stack([stage1] + stage2)
    stage3 = [lax.ppermute(held, AXES, shift_pairs(3, j)) for j in range(1, 4)]

    up_own = lax.all_to_all(later, SP, 0, 0)
    up_other = lax.ppermute(up_own, "c", swap)
    q_all = lax.all_to_all(q_part, TP, 0, 0)
    queries = call(
        make_queries, jax.ShapeDtypeStruct((2, 512, 256), BF), 0, 7
    )(q_all, up_own, up_other, query_gain.reshape(2, 128), cos, low_sin, high_sin)

    all_docs = up_own[:, 24:32, 64:96].astype(F32)
    key_docs = lax.dynamic_index_in_dim(
        all_docs.reshape(NS, 4, 2, 32), c, 2, keepdims=False
    ).reshape(NS, 128)
    query_docs = doc_ids.astype(F32).reshape(4, 2, 32).transpose(1, 0, 2).reshape(2, 128)
    own_first = doc_ids[0].astype(F32)
    own_last = doc_ids[255].astype(F32)
    low = jnp.sum((all_docs[:, 7, 31] < own_first).astype(jnp.int32))
    high = NS - 1 - jnp.sum((all_docs[:, 0, 0] > own_last).astype(jnp.int32))
    where = jnp.stack([z, x, y, c, low, high]).astype(jnp.int32)

    keep, send, ml = call(
        attend,
        (
            jax.ShapeDtypeStruct((128, 256), F32),
            jax.ShapeDtypeStruct((128, 256), BF),
            jax.ShapeDtypeStruct((256, 128), F32),
        ),
        1, 10, any_from=6,
        scratch=[
            VMEM((4, 4, NZ, 72, 128), BF),
            VMEM((16, 4, 256, 256), F32),
            VMEM((16, 256, 256), BF),
            VMEM((4, 256, 128), F32),
            VMEM((4, 256, 128), F32),
            VMEM((256, 256), F32),
            VMEM((256, 256), BF),
            VMEM((256, 256), BF),
            VMEM((256, 128), F32),
            VMEM((256, 128), F32),
            pltpu.SemaphoreType.DMA((4,)),
        ],
    )(where, queries, up_own, up_other, key_gain.reshape(2, 128), key_docs, query_docs, held, *stage3)

    got = lax.ppermute(send, "c", swap)
    ml_got = lax.ppermute(ml, "c", swap)
    part, log_sums = call(
        combine,
        (jax.ShapeDtypeStruct((NY, 32, 1024), BF), jax.ShapeDtypeStruct((256, 2), F32)),
        1, 6, scratch=[VMEM((4, 256, 128), F32), VMEM((4, 256, 128), F32)],
    )(here, keep, got, ml, ml_got, up_own, up_other)
    parts = lax.all_to_all(part, "y", 0, 0)
    mixed = call(finish, jax.ShapeDtypeStruct((32, 1024), BF), 0, 2)(
        parts, out_gain.reshape(1, 1024)
    )
    return mixed, log_sums


def solution(mesh):
    finer = Mesh(mesh.devices.reshape(NZ, NX, NY, NC), AXES)
    return jax.shard_map(
        layer,
        mesh=finer,
        in_specs=(
            P(AXES, None), P(SP), P(SP, None), P(SP, None), P(SP, None), P(), P(),
            P(SP, TP), P(SP, TP), P(SP, TP), P(TP, SP), P(),
        ),
        out_specs=(P(AXES, None), P(SP, TP)),
        check_vma=False,
    )
```

profile of v0, /device:TPU:1, one launch (start us, length us, event | category | flops | bytes accessed | tf_op | source)
XLA Modules:
  0.0 123.4 jit_solution(14742681583001220729)
XLA Ops:
  0.6 3.8 %collective-permute-start.1 = (bf16[32,1024]{1,0:T(8,128)(2,1)}, bf16[32,1024]{1,0:T(8,128)(2,1)S(1)}, u32[]{:S(2)}, u32[]{:S(2)}) collective-permute-start(bf16[32,1024]{1,0:T(8,128)(2,1)} %t0.1), channel_id=1, source_target_pairs={{0,4},{2,6},{4,0},{6,2},{1,5},{3,7},{5,1},{7,3},{8,12},{10,14},{12... | collective-permute-start | bytes 196616 | tf_op jit(solution)/shard_map/ppermute | solution.py:326
  4.9 2.3 %collective-permute-start.2 = (bf16[32,1024]{1,0:T(8,128)(2,1)}, bf16[32,1024]{1,0:T(8,128)(2,1)S(1)}, u32[]{:S(2)}, u32[]{:S(2)}) collective-permute-start(bf16[32,1024]{1,0:T(8,128)(2,1)} %t0.1), channel_id=1, source_target_pairs={{0,6},{2,0},{4,2},{6,4},{1,7},{3,1},{5,3},{7,5},{8,14},{10,8},{12,... | collective-permute-start | bytes 196616 | tf_op jit(solution)/shard_map/ppermute | solution.py:326
  7.9 1.6 %shard_map.131 = bf16[32,40,128]{2,1,0:T(8,128)(2,1)} custom-call(s32[4]{0:T(128)S(1)} %pad_add_fusion.where, bf16[32,256]{1,0:T(8,128)(2,1)S(1)} %copy-done.1, bf16[32,256]{1,0:T(8,128)(2,1)S(1)} %copy-done.2, bf16[32,32]{1,0:T(8,128)(2,1)S(1)} %copy-done.3), custom_call_target="tpu_custom_call" | custom-call | tf_op jit(solution)/shard_map/pallas_call | solution.py:320
  9.5 11.0 %all-to-all-start.1 = ((bf16[32,40,128]{2,1,0:T(8,128)(2,1)}), bf16[32,40,128]{2,1,0:T(8,128)(2,1)S(1)}, u32[]{:S(2)}, u32[]{:S(2)}) async-start(bf16[32,40,128]{2,1,0:T(8,128)(2,1)} %shard_map.131), calls=%async_computation.1 | async-start | bytes 655360 | tf_op jit(solution)/shard_map/all_to_all | solution.py:323
  24.1 7.7 %all-to-all-done.1.gathered = bf16[32,40,128]{2,1,0:T(8,128)(2,1)S(1)} async-done(((bf16[32,40,128]{2,1,0:T(8,128)(2,1)}), bf16[32,40,128]{2,1,0:T(8,128)(2,1)S(1)}, u32[]{:S(2)}, u32[]{:S(2)}) %all-to-all-start.1) | async-done | bytes 327712 | tf_op jit(solution)/shard_map/all_to_all | solution.py:323
  31.8 1.6 %shard_map.132 = (bf16[8,64,128]{2,1,0:T(8,128)(2,1)}, bf16[8,72,128]{2,1,0:T(8,128)(2,1)}) custom-call(s32[4]{0:T(128)S(1)} %pad_add_fusion.where, bf16[32,1024]{1,0:T(8,128)(2,1)S(1)} %copy-done, bf16[32,1024]{1,0:T(8,128)(2,1)S(1)} %collective-permute-done.t1, bf16[32,1024]{1,0:T(8,128)(2,1)S(1)} %collective-permute-done.1.t2, ...), custom_call_target="tpu_custom_call" | custom-call | tf_op jit(solution)/shard_map/pallas_call | solution.py:357
  33.3 3.5 %all-to-all-start.3 = ((bf16[8,72,128]{2,1,0:T(8,128)(2,1)}), bf16[8,72,128]{2,1,0:T(8,128)(2,1)S(1)}, u32[]{:S(2)}, u32[]{:S(2)}) async-start(bf16[8,72,128]{2,1,0:T(8,128)(2,1)} %get-tuple-element.10), calls=%async_computation.3 | async-start | bytes 294912 | tf_op jit(solution)/shard_map/all_to_all | solution.py:363
  38.3 6.6 %all-to-all-done.3 = bf16[8,72,128]{2,1,0:T(8,128)(2,1)S(1)} async-done(((bf16[8,72,128]{2,1,0:T(8,128)(2,1)}), bf16[8,72,128]{2,1,0:T(8,128)(2,1)S(1)}, u32[]{:S(2)}, u32[]{:S(2)}) %all-to-all-start.3) | async-done | bytes 147488 | tf_op jit(solution)/shard_map/all_to_all | solution.py:363
  44.9 1.0 broadcast_in_dim.24
  45.9 4.1 %all-to-all-start = ((bf16[32,64,128]{2,1,0:T(8,128)(2,1)}), bf16[32,64,128]{2,1,0:T(8,128)(2,1)S(1)}, u32[]{:S(2)}, u32[]{:S(2)}) async-start(bf16[32,64,128]{2,1,0:T(8,128)(2,1)} %broadcast_in_dim.24), calls=%async_computation | async-start | bytes 1048576 | tf_op jit(solution)/shard_map/all_to_all | solution.py:368
  52.9 1.9 %collective-permute-done.6 = bf16[8,72,128]{2,1,0:T(8,128)(2,1)S(1)} collective-permute-done((bf16[8,72,128]{2,1,0:T(8,128)(2,1)S(1)}, bf16[8,72,128]{2,1,0:T(8,128)(2,1)S(1)}, u32[]{:S(2)}, u32[]{:S(2)}) %collective-permute-start.6) | collective-permute-done | bytes 147488 | tf_op jit(solution)/shard_map/ppermute | solution.py:364
  54.8 1.9 %collective-permute-done.5 = bf16[8,72,128]{2,1,0:T(8,128)(2,1)S(1)} collective-permute-done((bf16[8,72,128]{2,1,0:T(8,128)(2,1)S(1)}, bf16[8,72,128]{2,1,0:T(8,128)(2,1)S(1)}, u32[]{:S(2)}, u32[]{:S(2)}) %collective-permute-start.5) | collective-permute-done | bytes 147488 | tf_op jit(solution)/shard_map/ppermute | solution.py:364
  56.7 1.5 %collective-permute-done.4 = bf16[8,72,128]{2,1,0:T(8,128)(2,1)S(1)} collective-permute-done((bf16[8,72,128]{2,1,0:T(8,128)(2,1)S(1)}, bf16[8,72,128]{2,1,0:T(8,128)(2,1)S(1)}, u32[]{:S(2)}, u32[]{:S(2)}) %collective-permute-start.4) | collective-permute-done | bytes 147488 | tf_op jit(solution)/shard_map/ppermute | solution.py:364
  58.2 2.7 %collective-permute-start.9 = (bf16[4,8,72,128]{3,2,1,0:T(8,128)(2,1)S(1)}, bf16[4,8,72,128]{3,2,1,0:T(8,128)(2,1)}, u32[]{:S(2)}, u32[]{:S(2)}) collective-permute-start(bf16[4,8,72,128]{3,2,1,0:T(8,128)(2,1)S(1)} %pad_maximum_fusion.b0), channel_id=1, source_target_pairs={{0,6},{1,25},{2,0},{3,27},{4,2},{5,29},{6,4},{7,31},{8,14},{9,1},{... | collective-permute-start | bytes 1769480 | tf_op jit(solution)/shard_map/ppermute | solution.py:366
  62.8 15.8 %collective-permute-start.3 = (bf16[32,64,128]{2,1,0:T(8,128)(2,1)S(1)}, bf16[32,64,128]{2,1,0:T(8,128)(2,1)S(1)}, u32[]{:S(2)}, u32[]{:S(2)}) collective-permute-start(bf16[32,64,128]{2,1,0:T(8,128)(2,1)S(1)} %all-to-all-done.up_own.w_own), channel_id=1, source_target_pairs={{0,1},{1,0},{2,3},{3,2},{4,5},{5,4},{6,7},{7,6},{8,9},{9,8},{10,11... | collective-permute-start | bytes 1572872 | tf_op jit(solution)/shard_map/ppermute | solution.py:369
  79.2 5.5 %all-to-all-start.2 = ((bf16[8,64,128]{2,1,0:T(8,128)(2,1)}), bf16[8,64,128]{2,1,0:T(8,128)(2,1)S(1)}, u32[]{:S(2)}, u32[]{:S(2)}) async-start(bf16[8,64,128]{2,1,0:T(8,128)(2,1)} %get-tuple-element.9), calls=%async_computation.2 | async-start | bytes 262144 | tf_op jit(solution)/shard_map/all_to_all | solution.py:370
  85.7 0.9 reshape.58.key_docs
  88.9 6.4 %all-to-all-done.2.q_in = bf16[8,64,128]{2,1,0:T(8,128)(2,1)S(1)} async-done(((bf16[8,64,128]{2,1,0:T(8,128)(2,1)}), bf16[8,64,128]{2,1,0:T(8,128)(2,1)S(1)}, u32[]{:S(2)}, u32[]{:S(2)}) %all-to-all-start.2) | async-done | bytes 131104 | tf_op jit(solution)/shard_map/all_to_all | solution.py:370
  96.4 11.3 %shard_map.134 = (f32[128,256]{1,0:T(8,128)S(1)}, bf16[128,256]{1,0:T(8,128)(2,1)S(1)}, f32[256,128]{1,0:T(8,128)S(1)}) custom-call(s32[6]{0:T(128)S(1)} %stack.50.where, bf16[2,512,256]{2,1,0:T(8,128)(2,1)S(1)} %shard_map.133.q_ref, bf16[32,64,128]{2,1,0:T(8,128)(2,1)S(1)} %all-to-all-done.up_own.w_own, ...), custom_call_target="tpu_custom_call" | custom-call | tf_op jit(solution)/shard_map/pallas_call | solution.py:386
  107.8 1.0 collective-permute-start.11
  108.8 1.2 collective-permute-done.10.got
  110.0 2.7 %shard_map.135 = (bf16[4,32,1024]{2,1,0:T(8,128)(2,1)}, f32[256,2]{1,0:T(8,128)S(1)}) custom-call(s32[4]{0:T(128)S(1)} %pad_add_fusion.where, f32[128,256]{1,0:T(8,128)S(1)} %get-tuple-element.11.keep, bf16[128,256]{1,0:T(8,128)(2,1)S(1)} %collective-permute-done.10.got, f32[256,128]{1,0:T(8,128)S(1)} %get-tuple-element.13.ml_own, ...), custom_call_target="tpu_custom_call" | custom-call | tf_op jit(solution)/shard_map/pallas_call | solution.py:411
  112.7 3.4 %all-to-all-start.4 = ((bf16[4,32,1024]{2,1,0:T(8,128)(2,1)}), bf16[4,32,1024]{2,1,0:T(8,128)(2,1)S(1)}, u32[]{:S(2)}, u32[]{:S(2)}) async-start(bf16[4,32,1024]{2,1,0:T(8,128)(2,1)} %get-tuple-element.14), calls=%async_computation.4 | async-start | bytes 524288 | tf_op jit(solution)/shard_map/all_to_all | solution.py:416
  116.8 5.9 %all-to-all-done.4.parts = bf16[4,32,1024]{2,1,0:T(8,128)(2,1)S(1)} async-done(((bf16[4,32,1024]{2,1,0:T(8,128)(2,1)}), bf16[4,32,1024]{2,1,0:T(8,128)(2,1)S(1)}, u32[]{:S(2)}, u32[]{:S(2)}) %all-to-all-start.4) | async-done | bytes 262176 | tf_op jit(solution)/shard_map/all_to_all | solution.py:416
  (88 shorter events, 15.3 us)
Async XLA Ops:
  0.6 6.6 %copy-start.2 = (bf16[32,256]{1,0:T(8,128)(2,1)S(1)}, bf16[32,256]{1,0:T(8,128)(2,1)}, u32[]{:S(2)}) copy-start(bf16[32,256]{1,0:T(8,128)(2,1)} %dk.1) | copy-start | bytes 49156
  0.6 6.6 %copy-start.1 = (bf16[32,256]{1,0:T(8,128)(2,1)S(1)}, bf16[32,256]{1,0:T(8,128)(2,1)}, u32[]{:S(2)}) copy-start(bf16[32,256]{1,0:T(8,128)(2,1)} %dq.1) | copy-start | bytes 49156
  0.6 23.4 %collective-permute-start.1 = (bf16[32,1024]{1,0:T(8,128)(2,1)}, bf16[32,1024]{1,0:T(8,128)(2,1)S(1)}, u32[]{:S(2)}, u32[]{:S(2)}) collective-permute-start(bf16[32,1024]{1,0:T(8,128)(2,1)} %t0.1), channel_id=1, source_target_pairs={{0,4},{2,6},{4,0},{6,2},{1,5},{3,7},{5,1},{7,3},{8,12},{10,14},{12... | collective-permute-start | bytes 196616 | tf_op jit(solution)/shard_map/ppermute | solution.py:326
  4.5 19.6 %collective-permute-start = (bf16[32,1024]{1,0:T(8,128)(2,1)}, bf16[32,1024]{1,0:T(8,128)(2,1)S(1)}, u32[]{:S(2)}, u32[]{:S(2)}) collective-permute-start(bf16[32,1024]{1,0:T(8,128)(2,1)} %t0.1), channel_id=1, source_target_pairs={{0,2},{2,4},{4,6},{6,0},{1,3},{3,5},{5,7},{7,1},{8,10},{10,12},{12... | collective-permute-start | bytes 196616 | tf_op jit(solution)/shard_map/ppermute | solution.py:326
  4.9 19.2 %collective-permute-start.2 = (bf16[32,1024]{1,0:T(8,128)(2,1)}, bf16[32,1024]{1,0:T(8,128)(2,1)S(1)}, u32[]{:S(2)}, u32[]{:S(2)}) collective-permute-start(bf16[32,1024]{1,0:T(8,128)(2,1)} %t0.1), channel_id=1, source_target_pairs={{0,6},{2,0},{4,2},{6,4},{1,7},{3,1},{5,3},{7,5},{8,14},{10,8},{12,... | collective-permute-start | bytes 196616 | tf_op jit(solution)/shard_map/ppermute | solution.py:326
  9.5 22.2 %all-to-all-start.1 = ((bf16[32,40,128]{2,1,0:T(8,128)(2,1)}), bf16[32,40,128]{2,1,0:T(8,128)(2,1)S(1)}, u32[]{:S(2)}, u32[]{:S(2)}) async-start(bf16[32,40,128]{2,1,0:T(8,128)(2,1)} %shard_map.131), calls=%async_computation.1 | async-start | bytes 655360 | tf_op jit(solution)/shard_map/all_to_all | solution.py:323
  20.7 1.3 %copy-start.9 = (bf16[8,192]{1,0:T(8,128)(2,1)S(1)}, bf16[8,192]{1,0:T(8,128)(2,1)}, u32[]{:S(2)}) copy-start(bf16[8,192]{1,0:T(8,128)(2,1)} %param.19) | copy-start | bytes 9220
  22.2 9.5 %copy-start = (bf16[32,1024]{1,0:T(8,128)(2,1)S(1)}, bf16[32,1024]{1,0:T(8,128)(2,1)}, u32[]{:S(2)}) copy-start(bf16[32,1024]{1,0:T(8,128)(2,1)} %t0.1) | copy-start | bytes 196612
  33.3 11.6 %all-to-all-start.3 = ((bf16[8,72,128]{2,1,0:T(8,128)(2,1)}), bf16[8,72,128]{2,1,0:T(8,128)(2,1)S(1)}, u32[]{:S(2)}, u32[]{:S(2)}) async-start(bf16[8,72,128]{2,1,0:T(8,128)(2,1)} %get-tuple-element.10), calls=%async_computation.3 | async-start | bytes 294912 | tf_op jit(solution)/shard_map/all_to_all | solution.py:363
  36.8 1.4 %copy-start.7 = (bf16[128,32]{0,1:T(8,128)(2,1)S(1)}, bf16[128,32]{0,1:T(8,128)(2,1)}, u32[]{:S(2)}) copy-start(bf16[128,32]{0,1:T(8,128)(2,1)} %param.22) | copy-start | bytes 24580
  45.9 16.9 %all-to-all-start = ((bf16[32,64,128]{2,1,0:T(8,128)(2,1)}), bf16[32,64,128]{2,1,0:T(8,128)(2,1)S(1)}, u32[]{:S(2)}, u32[]{:S(2)}) async-start(bf16[32,64,128]{2,1,0:T(8,128)(2,1)} %broadcast_in_dim.24), calls=%async_computation | async-start | bytes 1048576 | tf_op jit(solution)/shard_map/all_to_all | solution.py:368
  50.7 4.1 %collective-permute-start.6 = (bf16[8,72,128]{2,1,0:T(8,128)(2,1)S(1)}, bf16[8,72,128]{2,1,0:T(8,128)(2,1)S(1)}, u32[]{:S(2)}, u32[]{:S(2)}) collective-permute-start(bf16[8,72,128]{2,1,0:T(8,128)(2,1)S(1)} %all-to-all-done.3), channel_id=1, source_target_pairs={{0,24},{1,7},{2,26},{3,1},{4,28},{5,3},{6,30},{7,5},{8,0},{9,15},{... | collective-permute-start | bytes 442376 | tf_op jit(solution)/shard_map/ppermute | solution.py:364
  51.1 5.6 %collective-permute-start.5 = (bf16[8,72,128]{2,1,0:T(8,128)(2,1)S(1)}, bf16[8,72,128]{2,1,0:T(8,128)(2,1)S(1)}, u32[]{:S(2)}, u32[]{:S(2)}) collective-permute-start(bf16[8,72,128]{2,1,0:T(8,128)(2,1)S(1)} %all-to-all-done.3), channel_id=1, source_target_pairs={{0,16},{1,5},{2,18},{3,7},{4,20},{5,1},{6,22},{7,3},{8,24},{9,13},... | collective-permute-start | bytes 442376 | tf_op jit(solution)/shard_map/ppermute | solution.py:364
  51.7 6.4 %collective-permute-start.4 = (bf16[8,72,128]{2,1,0:T(8,128)(2,1)S(1)}, bf16[8,72,128]{2,1,0:T(8,128)(2,1)S(1)}, u32[]{:S(2)}, u32[]{:S(2)}) collective-permute-start(bf16[8,72,128]{2,1,0:T(8,128)(2,1)S(1)} %all-to-all-done.3), channel_id=1, source_target_pairs={{0,8},{1,3},{2,10},{3,5},{4,12},{5,7},{6,14},{7,1},{8,16},{9,11},{... | collective-permute-start | bytes 442376 | tf_op jit(solution)/shard_map/ppermute | solution.py:364
  58.2 37.5 %collective-permute-start.9 = (bf16[4,8,72,128]{3,2,1,0:T(8,128)(2,1)S(1)}, bf16[4,8,72,128]{3,2,1,0:T(8,128)(2,1)}, u32[]{:S(2)}, u32[]{:S(2)}) collective-permute-start(bf16[4,8,72,128]{3,2,1,0:T(8,128)(2,1)S(1)} %pad_maximum_fusion.b0), channel_id=1, source_target_pairs={{0,6},{1,25},{2,0},{3,27},{4,2},{5,29},{6,4},{7,31},{8,14},{9,1},{... | collective-permute-start | bytes 1769480 | tf_op jit(solution)/shard_map/ppermute | solution.py:366
  60.9 34.8 %collective-permute-start.8 = (bf16[4,8,72,128]{3,2,1,0:T(8,128)(2,1)S(1)}, bf16[4,8,72,128]{3,2,1,0:T(8,128)(2,1)S(1)}, u32[]{:S(2)}, u32[]{:S(2)}) collective-permute-start(bf16[4,8,72,128]{3,2,1,0:T(8,128)(2,1)S(1)} %pad_maximum_fusion.b0), channel_id=1, source_target_pairs={{0,4},{1,17},{2,6},{3,19},{4,0},{5,21},{6,2},{7,23},{8,12},{9,25},... | collective-permute-start | bytes 1769480 | tf_op jit(solution)/shard_map/ppermute | solution.py:366
  61.3 34.5 %collective-permute-start.7 = (bf16[4,8,72,128]{3,2,1,0:T(8,128)(2,1)S(1)}, bf16[4,8,72,128]{3,2,1,0:T(8,128)(2,1)S(1)}, u32[]{:S(2)}, u32[]{:S(2)}) collective-permute-start(bf16[4,8,72,128]{3,2,1,0:T(8,128)(2,1)S(1)} %pad_maximum_fusion.b0), channel_id=1, source_target_pairs={{0,2},{1,9},{2,4},{3,11},{4,6},{5,13},{6,0},{7,15},{8,10},{9,17},{... | collective-permute-start | bytes 1769480 | tf_op jit(solution)/shard_map/ppermute | solution.py:366
  62.8 32.5 %collective-permute-start.3 = (bf16[32,64,128]{2,1,0:T(8,128)(2,1)S(1)}, bf16[32,64,128]{2,1,0:T(8,128)(2,1)S(1)}, u32[]{:S(2)}, u32[]{:S(2)}) collective-permute-start(bf16[32,64,128]{2,1,0:T(8,128)(2,1)S(1)} %all-to-all-done.up_own.w_own), channel_id=1, source_target_pairs={{0,1},{1,0},{2,3},{3,2},{4,5},{5,4},{6,7},{7,6},{8,9},{9,8},{10,11... | collective-permute-start | bytes 1572872 | tf_op jit(solution)/shard_map/ppermute | solution.py:369
  79.2 16.0 %all-to-all-start.2 = ((bf16[8,64,128]{2,1,0:T(8,128)(2,1)}), bf16[8,64,128]{2,1,0:T(8,128)(2,1)S(1)}, u32[]{:S(2)}, u32[]{:S(2)}) async-start(bf16[8,64,128]{2,1,0:T(8,128)(2,1)} %get-tuple-element.9), calls=%async_computation.2 | async-start | bytes 262144 | tf_op jit(solution)/shard_map/all_to_all | solution.py:370
  88.9 6.4 %copy-start.5 = (f32[256]{0:T(256)S(1)}, f32[256]{0:T(256)}, u32[]{:S(2)}) copy-start(f32[256]{0:T(256)} %param.17) | copy-start | bytes 3076
  107.8 2.2 %collective-permute-start.11 = (f32[256,128]{1,0:T(8,128)S(1)}, f32[256,128]{1,0:T(8,128)S(1)}, u32[]{:S(2)}, u32[]{:S(2)}) collective-permute-start(f32[256,128]{1,0:T(8,128)S(1)} %get-tuple-element.13.ml_own), channel_id=1, source_target_pairs={{0,1},{1,0},{2,3},{3,2},{4,5},{5,4},{6,7},{7,6},{8,9},{9,8},{10,11... | collective-permute-start | bytes 393224 | tf_op jit(solution)/shard_map/ppermute | solution.py:410
  108.7 1.3 %collective-permute-start.10 = (bf16[128,256]{1,0:T(8,128)(2,1)S(1)}, bf16[128,256]{1,0:T(8,128)(2,1)S(1)}, u32[]{:S(2)}, u32[]{:S(2)}) collective-permute-start(bf16[128,256]{1,0:T(8,128)(2,1)S(1)} %get-tuple-element.12), channel_id=1, source_target_pairs={{0,1},{1,0},{2,3},{3,2},{4,5},{5,4},{6,7},{7,6},{8,9},{9,8},{10,11... | collective-permute-start | bytes 196616 | tf_op jit(solution)/shard_map/ppermute | solution.py:409
  112.7 10.0 %all-to-all-start.4 = ((bf16[4,32,1024]{2,1,0:T(8,128)(2,1)}), bf16[4,32,1024]{2,1,0:T(8,128)(2,1)S(1)}, u32[]{:S(2)}, u32[]{:S(2)}) async-start(bf16[4,32,1024]{2,1,0:T(8,128)(2,1)} %get-tuple-element.14), calls=%async_computation.4 | async-start | bytes 524288 | tf_op jit(solution)/shard_map/all_to_all | solution.py:416
  116.1 6.5 %copy-start.4 = (f32[1024]{0:T(1024)S(1)}, f32[1024]{0:T(1024)}, u32[]{:S(2)}) copy-start(f32[1024]{0:T(1024)} %param.23) | copy-start | bytes 12292
  (5 other events, 3.4 us)
where the time goes:
time: 124 us; the launch traced here: 123 us
  starting transfers between devices  56.1 us (45%)
  waiting for transfers between devices  33.9 us (27%)
  Pallas kernels  18.4 us (15%)
  local copies, waits for them, and re-layouts  8.77 us (7%)
  other arithmetic  3.29 us (3%)
  between operations  2.98 us (2%)
    ppermute x1, starting transfers between devices, layer(): up_other = lax.ppermute(up_own, 'c', swap)  15.8 us
    pallas_call x1, Pallas kernels, layer(): call(attend, (jax.ShapeDtypeStruct((128, 256), F32), jax.ShapeDtypeStruct...  11.3 us
    all_to_all x1, starting transfers between devices, layer(): gathered = lax.all_to_all(message, SP, 0, 0)  11 us
    all_to_all x1, waiting for transfers between devices, layer(): gathered = lax.all_to_all(message, SP, 0, 0)  7.71 us
    all_to_all x1, waiting for transfers between devices, layer(): stage1 = lax.all_to_all(k_part, 'z', 0, 0)  6.64 us
    ppermute x3, starting transfers between devices, layer(): lax.ppermute(tokens, 'y', [(i, (i + j) % NY) for i in range(NY)])  6.5 us
    all_to_all x1, waiting for transfers between devices, layer(): q_all = lax.all_to_all(q_part, TP, 0, 0)  6.38 us
    all_to_all x1, waiting for transfers between devices, layer(): parts = lax.all_to_all(part, 'y', 0, 0)  5.87 us
  transfers between devices with their start and end apart: 17, of which 9 were waited for; matrix products, arithmetic and copies ran while one was open for 6% of the time, Pallas kernels for 2%

commit v1 on v0

--- a/solution.py
+++ b/solution.py
@@ -85,8 +85,7 @@
     weights = gathered[:, 0:32, :].reshape(NS * 32, 128)
     both = jnp.dot(rows, weights, preferred_element_type=F32)
     turned = jnp.transpose(both).astype(BF)
-    for t in range(NY * NC):
-        q_ref[t] = turned[0:64, :]
+    q_ref[...] = turned[0:64, :]
     for t in range(NZ):
         k_ref[t, 0:64, :] = turned[64:128, :]
     group = lanes((8, 128)) // 32
@@ -106,20 +105,21 @@
         k_ref[t, 64:72, :] = rotated
 
 
-def make_queries(q_in, up_own, up_other, gain, cos_ref, low_ref, high_ref, out):
-    blocks = []
-    for y in range(NY):
-        blocks.append(
-            jnp.concatenate([q_in[2 * y].astype(F32), q_in[2 * y + 1].astype(F32)], axis=1)
-        )
-    total = blocks[0] * blocks[0]
-    for b in blocks[1:]:
-        total = total + b * b
-    mean = jnp.sum(total, axis=0, keepdims=True) * (1.0 / 256.0)
+def make_queries(
+    where, q0, q1, q2, q3, up_own, up_other, gain, cos_ref, low_ref, high_ref, out, latents
+):
+    y, c = where[2], where[3]
+    for j, part in enumerate((q0, q1, q2, q3)):
+        own, other = part[0].astype(F32), part[1].astype(F32)
+        rows = pl.ds(pl.multiple_of(lax.rem(y - j + NY, NY) * 64, 64), 64)
+        latents[rows, 0:128] = jnp.where(c == 0, own, other)
+        latents[rows, 128:256] = jnp.where(c == 0, other, own)
+    raw = latents[...]
+    mean = jnp.sum(raw * raw, axis=0, keepdims=True) * (1.0 / 256.0)
     inverse = lax.rsqrt(mean + EPS)
     gains = jnp.concatenate([column(gain[0:1, :]), column(gain[1:2, :])], axis=0)
     gains = jnp.concatenate([gains, gains], axis=1)
-    latent = jnp.concatenate(blocks, axis=0) * inverse * gains
+    latent = raw * inverse * gains
     latent = jnp.transpose(latent).astype(BF)
     lane = lanes((256, 128))
     for p, up in enumerate((up_own, up_other)):
@@ -243,7 +243,7 @@
     send_ref[...] = acc[pl.ds(pl.multiple_of((1 - c) * 128, 128), 128), :].astype(BF)
 
 
-def combine(where, keep, got, ml_own, ml_got, w_own, w_other, part_ref, lse_ref, f_own, f_got):
+def combine(where, keep, got, ml_own, ml_got, w_own, w_other, part_ref, lse_ref, f_own, f_got, scratch):
     c = where[3]
     own = ml_own[...]
     other = ml_got[...]
@@ -274,16 +274,20 @@
         theirs = got[:, 128 * (1 - p) : 128 * (2 - p)].astype(F32)
         attended = (mine * a + theirs * b).astype(BF)
         result = result + lax.dot_general(
-            attended, w[:, 32:64, :].reshape(1024, 128), (((1,), (1,)), ((), ())),
+            attended, w[...].reshape(1024, 128), (((1,), (1,)), ((), ())),
             preferred_element_type=F32,
         )
-    part_ref[...] = result.astype(BF).reshape(NY, 32, 1024)
-
-
-def finish(parts, gain, out):
-    summed = parts[0].astype(F32)
-    for y in range(1, NY):
-        summed = summed + parts[y].astype(F32)
+    scratch[...] = result
+    y = where[2]
+    for j in range(NY):
+        to = lax.rem(y + j, NY)
+        part_ref[j] = scratch[pl.ds(pl.multiple_of(to * 32, 32), 32), :].astype(BF)
+
+
+def finish(part, p1, p2, p3, gain, out):
+    summed = part[0].astype(F32)
+    for other in (p1, p2, p3):
+        summed = summed + other[...].astype(F32)
     wide = summed.astype(BF).astype(F32)
     mean = jnp.mean(wide * wide, axis=1, keepdims=True)
     out[...] = (wide * lax.rsqrt(mean + EPS) * gain[...]).astype(BF)
@@ -291,6 +295,10 @@
 
 def flat(z, x, y, c):
     return ((z * NX + x) * NY + y) * NC + c
+
+
+def ring(j):
+    return [(i, (i + j) % NY) for i in range(NY)]
 
 
 def shift_pairs(stage, j):
@@ -322,17 +330,16 @@
     )(here, down_query, down_key, down_rotary)
     gathered = lax.all_to_all(message, SP, 0, 0)
 
-    shifted = [
-        lax.ppermute(tokens, "y", [(i, (i + j) % NY) for i in range(NY)]) for j in range(1, NY)
-    ]
+    rows = [tokens] + [lax.ppermute(tokens, "y", ring(j)) for j in range(1, NY)]
 
     heads = up_query.reshape(8, 2, NOPE + ROPE)
     plain = heads[:, :, :NOPE].reshape(8, 128)
     turning = heads[:, :, NOPE:].reshape(8, 2, 2, 4, 4).transpose(0, 1, 3, 2, 4).reshape(8, 64)
     docs = doc_ids.astype(BF).reshape(8, 32)
     mixed_rows = jnp.concatenate([turning, docs, jnp.zeros((8, 32), BF)], axis=1)
-    later = jnp.concatenate([plain, up_key, up_value, mixed_rows, output_weight.T], axis=0)
-    later = jnp.broadcast_to(later[None], (NS, 64, 128))
+    later = jnp.concatenate([plain, up_key, up_value, mixed_rows], axis=0)
+    later = jnp.broadcast_to(later[None], (NS, 32, 128))
+    last = jnp.broadcast_to(output_weight.T[None], (NS, 32, 128))
 
     f32_base = (sp * 256).astype(F32)
     key_tok = lax.broadcasted_iota(jnp.int32, (8, 128), 1)
@@ -356,9 +363,9 @@
 
     q_part, k_part = call(
         project,
-        (jax.ShapeDtypeStruct((NY * NC, 64, 128), BF), jax.ShapeDtypeStruct((NZ, 72, 128), BF)),
+        (jax.ShapeDtypeStruct((64, 128), BF), jax.ShapeDtypeStruct((NZ, 72, 128), BF)),
         1, 7, scratch=[VMEM((128, 1024), BF)],
-    )(here, tokens, *shifted, gathered, key_cos, key_sin)
+    )(here, *rows, gathered, key_cos, key_sin)
 
     stage1 = lax.all_to_all(k_part, "z", 0, 0)
     stage2 = [lax.ppermute(stage1, AXES, shift_pairs(2, j)) for j in range(1, 4)]
@@ -367,10 +374,13 @@
 
     up_own = lax.all_to_all(later, SP, 0, 0)
     up_other = lax.ppermute(up_own, "c", swap)
-    q_all = lax.all_to_all(q_part, TP, 0, 0)
+    out_own = lax.all_to_all(last, SP, 0, 0)
+    q_pair = jnp.stack([q_part, lax.ppermute(q_part, "c", swap)])
+    q_all = [q_pair] + [lax.ppermute(q_pair, "y", ring(j)) for j in range(1, NY)]
     queries = call(
-        make_queries, jax.ShapeDtypeStruct((2, 512, 256), BF), 0, 7
-    )(q_all, up_own, up_other, query_gain.reshape(2, 128), cos, low_sin, high_sin)
+        make_queries, jax.ShapeDtypeStruct((2, 512, 256), BF), 1, 10,
+        scratch=[VMEM((256, 256), F32)],
+    )(here, *q_all, up_own, up_other, query_gain.reshape(2, 128), cos, low_sin, high_sin)
 
     all_docs = up_own[:, 24:32, 64:96].astype(F32)
     key_docs = lax.dynamic_index_in_dim(
@@ -408,14 +418,17 @@
 
     got = lax.ppermute(send, "c", swap)
     ml_got = lax.ppermute(ml, "c", swap)
+    out_other = lax.ppermute(out_own, "c", swap)
     part, log_sums = call(
         combine,
         (jax.ShapeDtypeStruct((NY, 32, 1024), BF), jax.ShapeDtypeStruct((256, 2), F32)),
-        1, 6, scratch=[VMEM((4, 256, 128), F32), VMEM((4, 256, 128), F32)],
-    )(here, keep, got, ml, ml_got, up_own, up_other)
-    parts = lax.all_to_all(part, "y", 0, 0)
-    mixed = call(finish, jax.ShapeDtypeStruct((32, 1024), BF), 0, 2)(
-        parts, out_gain.reshape(1, 1024)
+        1, 6, scratch=[VMEM((4, 256, 128), F32), VMEM((4, 256, 128), F32), VMEM((128, 1024), F32)],
+    )(here, keep, got, ml, ml_got, out_own, out_other)
+    parts = [
+        lax.ppermute(part[j], "y", ring(j)) for j in range(1, NY)
+    ]
+    mixed = call(finish, jax.ShapeDtypeStruct((32, 1024), BF), 0, 5)(
+        part, *parts, out_gain.reshape(1, 1024)
     )
     return mixed, log_sums
 

time: 124 us -> 129 us (1.040)
  the two profiles are of different devices: /device:TPU:1 before, /device:TPU:2 now
where the time goes in v1:
time: 129 us; the launch traced here: 128 us
  starting transfers between devices  51.9 us (40%)
  waiting for transfers between devices  37.7 us (29%)
  Pallas kernels  18.1 us (14%)
  local copies, waits for them, and re-layouts  11.7 us (9%)
  other arithmetic  5.52 us (4%)
  between operations  3.03 us (2%)
    all_to_all x1, starting transfers between devices, layer(): gathered = lax.all_to_all(message, SP, 0, 0)  11.7 us
    all_to_all x1, waiting for transfers between devices, layer(): gathered = lax.all_to_all(message, SP, 0, 0)  11.4 us
    ppermute x3, waiting for transfers between devices, layer(): lax.ppermute(q_pair, 'y', ring(j))  10.5 us
    pallas_call x1, Pallas kernels, layer(): call(attend, (jax.ShapeDtypeStruct((128, 256), F32), jax.ShapeDtypeStruct...  10.4 us
    all_to_all x1, waiting for transfers between devices, layer(): stage1 = lax.all_to_all(k_part, 'z', 0, 0)  7.94 us
    all_to_all x1, starting transfers between devices, layer(): out_own = lax.all_to_all(last, SP, 0, 0)  5.95 us
    ppermute x3, starting transfers between devices, layer(): rows = [tokens] + [lax.ppermute(tokens, 'y', ring(j)) for j in range(1, NY)]  5.9 us
    all_to_all x1, starting transfers between devices, layer(): up_own = lax.all_to_all(later, SP, 0, 0)  5.43 us
  transfers between devices with their start and end apart: 24, of which 9 were waited for; matrix products, arithmetic and copies ran while one was open for 10% of the time, Pallas kernels for 10%

profile of v1, /device:TPU:2, one launch (start us, length us, event | category | flops | bytes accessed | tf_op | source)
XLA Modules:
  0.0 127.8 jit_solution(11174557453818080715)
XLA Ops:
  0.6 1.7 %collective-permute-start = (bf16[32,1024]{1,0:T(8,128)(2,1)}, bf16[32,1024]{1,0:T(8,128)(2,1)S(1)}, u32[]{:S(2)}, u32[]{:S(2)}) collective-permute-start(bf16[32,1024]{1,0:T(8,128)(2,1)} %t0.1), channel_id=1, source_target_pairs={{0,2},{2,4},{4,6},{6,0},{1,3},{3,5},{5,7},{7,1},{8,10},{10,12},{12... | collective-permute-start | bytes 196616 | tf_op jit(solution)/shard_map/ppermute | solution.py:333
  2.3 2.9 %collective-permute-start.1 = (bf16[32,1024]{1,0:T(8,128)(2,1)}, bf16[32,1024]{1,0:T(8,128)(2,1)S(1)}, u32[]{:S(2)}, u32[]{:S(2)}) collective-permute-start(bf16[32,1024]{1,0:T(8,128)(2,1)} %t0.1), channel_id=1, source_target_pairs={{0,4},{2,6},{4,0},{6,2},{1,5},{3,7},{5,1},{7,3},{8,12},{10,14},{12... | collective-permute-start | bytes 196616 | tf_op jit(solution)/shard_map/ppermute | solution.py:333
  5.2 1.3 %collective-permute-start.2 = (bf16[32,1024]{1,0:T(8,128)(2,1)}, bf16[32,1024]{1,0:T(8,128)(2,1)S(1)}, u32[]{:S(2)}, u32[]{:S(2)}) collective-permute-start(bf16[32,1024]{1,0:T(8,128)(2,1)} %t0.1), channel_id=1, source_target_pairs={{0,6},{2,0},{4,2},{6,4},{1,7},{3,1},{5,3},{7,5},{8,14},{10,8},{12,... | collective-permute-start | bytes 196616 | tf_op jit(solution)/shard_map/ppermute | solution.py:333
  7.3 1.6 %shard_map.131 = bf16[32,40,128]{2,1,0:T(8,128)(2,1)} custom-call(s32[4]{0:T(128)S(1)} %pad_add_fusion.where, bf16[32,256]{1,0:T(8,128)(2,1)S(1)} %copy-done.3, bf16[32,256]{1,0:T(8,128)(2,1)S(1)} %copy-done.4, bf16[32,32]{1,0:T(8,128)(2,1)S(1)} %copy-done.7), custom_call_target="tpu_custom_call" | custom-call | tf_op jit(solution)/shard_map/pallas_call | solution.py:328
  8.9 11.7 %all-to-all-start.1 = ((bf16[32,40,128]{2,1,0:T(8,128)(2,1)}), bf16[32,40,128]{2,1,0:T(8,128)(2,1)S(1)}, u32[]{:S(2)}, u32[]{:S(2)}) async-start(bf16[32,40,128]{2,1,0:T(8,128)(2,1)} %shard_map.131), calls=%async_computation.1 | async-start | bytes 655360 | tf_op jit(solution)/shard_map/all_to_all | solution.py:331
  21.0 11.4 %all-to-all-done.1.gathered = bf16[32,40,128]{2,1,0:T(8,128)(2,1)S(1)} async-done(((bf16[32,40,128]{2,1,0:T(8,128)(2,1)}), bf16[32,40,128]{2,1,0:T(8,128)(2,1)S(1)}, u32[]{:S(2)}, u32[]{:S(2)}) %all-to-all-start.1) | async-done | bytes 327712 | tf_op jit(solution)/shard_map/all_to_all | solution.py:331
  32.5 1.5 %shard_map.132 = (bf16[64,128]{1,0:T(8,128)(2,1)S(1)}, bf16[8,72,128]{2,1,0:T(8,128)(2,1)}) custom-call(s32[4]{0:T(128)S(1)} %pad_add_fusion.where, bf16[32,1024]{1,0:T(8,128)(2,1)S(1)} %copy-done, bf16[32,1024]{1,0:T(8,128)(2,1)S(1)} %collective-permute-done.t1, bf16[32,1024]{1,0:T(8,128)(2,1)S(1)} %collective-permute-done.1.t2, ...), custom_call_target="tpu_custom_call" | custom-call | tf_op jit(solution)/shard_map/pallas_call | solution.py:364
  34.0 3.5 %all-to-all-start.2 = ((bf16[8,72,128]{2,1,0:T(8,128)(2,1)}), bf16[8,72,128]{2,1,0:T(8,128)(2,1)S(1)}, u32[]{:S(2)}, u32[]{:S(2)}) async-start(bf16[8,72,128]{2,1,0:T(8,128)(2,1)} %get-tuple-element.10), calls=%async_computation.2 | async-start | bytes 294912 | tf_op jit(solution)/shard_map/all_to_all | solution.py:370
  38.7 7.9 %all-to-all-done.2 = bf16[8,72,128]{2,1,0:T(8,128)(2,1)S(1)} async-done(((bf16[8,72,128]{2,1,0:T(8,128)(2,1)}), bf16[8,72,128]{2,1,0:T(8,128)(2,1)S(1)}, u32[]{:S(2)}, u32[]{:S(2)}) %all-to-all-start.2) | async-done | bytes 147488 | tf_op jit(solution)/shard_map/all_to_all | solution.py:370
  47.4 5.4 %all-to-all-start = ((bf16[32,32,128]{2,1,0:T(8,128)(2,1)}), bf16[32,32,128]{2,1,0:T(8,128)(2,1)S(1)}, u32[]{:S(2)}, u32[]{:S(2)}) async-start(bf16[32,32,128]{2,1,0:T(8,128)(2,1)} %broadcast_in_dim.30), calls=%async_computation | async-start | bytes 524288 | tf_op jit(solution)/shard_map/all_to_all | solution.py:375
  54.6 2.6 %collective-permute-start.9 = (bf16[8,72,128]{2,1,0:T(8,128)(2,1)S(1)}, bf16[8,72,128]{2,1,0:T(8,128)(2,1)S(1)}, u32[]{:S(2)}, u32[]{:S(2)}) collective-permute-start(bf16[8,72,128]{2,1,0:T(8,128)(2,1)S(1)} %all-to-all-done.2), channel_id=1, source_target_pairs={{0,16},{1,5},{2,18},{3,7},{4,20},{5,1},{6,22},{7,3},{8,24},{9,13},... | collective-permute-start | bytes 442376 | tf_op jit(solution)/shard_map/ppermute | solution.py:371
  57.2 1.8 %collective-permute-start.8 = (bf16[8,72,128]{2,1,0:T(8,128)(2,1)S(1)}, bf16[8,72,128]{2,1,0:T(8,128)(2,1)S(1)}, u32[]{:S(2)}, u32[]{:S(2)}) collective-permute-start(bf16[8,72,128]{2,1,0:T(8,128)(2,1)S(1)} %all-to-all-done.2), channel_id=1, source_target_pairs={{0,8},{1,3},{2,10},{3,5},{4,12},{5,7},{6,14},{7,1},{8,16},{9,11},{... | collective-permute-start | bytes 442376 | tf_op jit(solution)/shard_map/ppermute | solution.py:371
  59.7 3.0 %all-to-all-done.up_own = bf16[32,32,128]{2,1,0:T(8,128)(2,1)S(1)} async-done(((bf16[32,32,128]{2,1,0:T(8,128)(2,1)}), bf16[32,32,128]{2,1,0:T(8,128)(2,1)S(1)}, u32[]{:S(2)}, u32[]{:S(2)}) %all-to-all-start) | async-done | bytes 262176 | tf_op jit(solution)/shard_map/all_to_all | solution.py:375
  63.5 6.0 %all-to-all-start.3 = ((bf16[32,32,128]{2,1,0:T(8,128)(2,1)}), bf16[32,32,128]{2,1,0:T(8,128)(2,1)S(1)}, u32[]{:S(2)}, u32[]{:S(2)}) async-start(bf16[32,32,128]{2,1,0:T(8,128)(2,1)} %broadcast_in_dim.34), calls=%async_computation.3 | async-start | bytes 524288 | tf_op jit(solution)/shard_map/all_to_all | solution.py:377
  71.0 2.0 %collective-permute-start.13 = (bf16[4,8,72,128]{3,2,1,0:T(8,128)(2,1)S(1)}, bf16[4,8,72,128]{3,2,1,0:T(8,128)(2,1)S(1)}, u32[]{:S(2)}, u32[]{:S(2)}) collective-permute-start(bf16[4,8,72,128]{3,2,1,0:T(8,128)(2,1)S(1)} %pad_maximum_fusion.b0), channel_id=1, source_target_pairs={{0,6},{1,25},{2,0},{3,27},{4,2},{5,29},{6,4},{7,31},{8,14},{9,1},{... | collective-permute-start | bytes 1769480 | tf_op jit(solution)/shard_map/ppermute | solution.py:373
  74.3 2.1 %collective-permute-start.5 = (bf16[2,64,128]{2,1,0:T(8,128)(2,1)}, bf16[2,64,128]{2,1,0:T(8,128)(2,1)}, u32[]{:S(2)}, u32[]{:S(2)}) collective-permute-start(bf16[2,64,128]{2,1,0:T(8,128)(2,1)} %pad_maximum_fusion.1.q0), channel_id=1, source_target_pairs={{0,4},{2,6},{4,0},{6,2},{1,5},{3,7},{5,1},{7,3},{8,12},{10,14},{12... | collective-permute-start | bytes 98312 | tf_op jit(solution)/shard_map/ppermute | solution.py:379
  79.1 9.3 %collective-permute-done.4.q1 = bf16[2,64,128]{2,1,0:T(8,128)(2,1)S(1)} collective-permute-done((bf16[2,64,128]{2,1,0:T(8,128)(2,1)}, bf16[2,64,128]{2,1,0:T(8,128)(2,1)S(1)}, u32[]{:S(2)}, u32[]{:S(2)}) %collective-permute-start.4) | collective-permute-done | bytes 32800 | tf_op jit(solution)/shard_map/ppermute | solution.py:379
  89.1 2.4 %collective-permute-start.6 = (bf16[2,64,128]{2,1,0:T(8,128)(2,1)}, bf16[2,64,128]{2,1,0:T(8,128)(2,1)}, u32[]{:S(2)}, u32[]{:S(2)}) collective-permute-start(bf16[2,64,128]{2,1,0:T(8,128)(2,1)} %pad_maximum_fusion.1.q0), channel_id=1, source_target_pairs={{0,6},{2,0},{4,2},{6,4},{1,7},{3,1},{5,3},{7,5},{8,14},{10,8},{12,... | collective-permute-start | bytes 98312 | tf_op jit(solution)/shard_map/ppermute | solution.py:379
  93.3 1.6 %constant_dynamic-slice_fusion = f32[32,4,1,32]{3,2,1,0:T(1,128)} fusion(f32[32,4,2,32]{3,2,1,0:T(2,128)} %bitcast.40, s32[]{:T(128)S(6)} %select_n.91), kind=kLoop, calls=%fused_computation.91 | loop fusion | bytes 32772 | tf_op jit(solution)/shard_map/jit(dynamic_index_in_dim)/dynamic_slice | solution.py:386
  95.9 1.8 %fusion.26 = (s32[]{:T(128)}, s32[]{:T(128)}) fusion(f32[32,8,32]{2,1,0:T(8,128)} %slice_convert_fusion, f32[]{:T(128)} %bitcast.11, f32[]{:T(128)} %bitcast.9), kind=kLoop, calls=%fused_computation.56 | loop fusion | flops 190 | bytes 272 | tf_op jit(solution)/shard_map/reduce_sum | solution.py:393
  102.9 10.4 %shard_map.134 = (f32[128,256]{1,0:T(8,128)S(1)}, bf16[128,256]{1,0:T(8,128)(2,1)S(1)}, f32[256,128]{1,0:T(8,128)S(1)}) custom-call(s32[6]{0:T(128)S(1)} %copy-done.10, bf16[2,512,256]{2,1,0:T(8,128)(2,1)S(1)} %shard_map.133.q_ref, bf16[32,32,128]{2,1,0:T(8,128)(2,1)S(1)} %all-to-all-done.up_own, bf16[32,32,128]{2,1,0:T(8,128)(2,1)S(1)} %collective-permute-done.7.up_other, ...), custom_call_target="tpu_custom_call" | custom-call | tf_op jit(solution)/shard_map/pallas_call | solution.py:396
  115.2 2.5 %shard_map.135 = (bf16[4,32,1024]{2,1,0:T(8,128)(2,1)S(1)}, f32[256,2]{1,0:T(8,128)S(1)}) custom-call(s32[4]{0:T(128)S(1)} %copy-done.6, f32[128,256]{1,0:T(8,128)S(1)} %get-tuple-element.11.keep, bf16[128,256]{1,0:T(8,128)(2,1)S(1)} %collective-permute-done.14.got, f32[256,128]{1,0:T(8,128)S(1)} %get-tuple-element.13.ml_own, ...), custom_call_target="tpu_custom_call" | custom-call | tf_op jit(solution)/shard_map/pallas_call | solution.py:422
  117.8 5.0 %collective-permute-start.18 = (bf16[32,1024]{1,0:T(8,128)(2,1)S(1)}, bf16[32,1024]{1,0:T(8,128)(2,1)S(1)}, u32[]{:S(2)}, u32[]{:S(2)}) collective-permute-start(bf16[32,1024]{1,0:T(8,128)(2,1)S(1)} %get-tuple-element.27), channel_id=1, source_target_pairs={{0,4},{2,6},{4,0},{6,2},{1,5},{3,7},{5,1},{7,3},{8,12},{10,14},{12... | collective-permute-start | bytes 196616 | tf_op jit(solution)/shard_map/ppermute | solution.py:428
  123.7 2.6 %collective-permute-done.18.p2 = bf16[32,1024]{1,0:T(8,128)(2,1)S(1)} collective-permute-done((bf16[32,1024]{1,0:T(8,128)(2,1)S(1)}, bf16[32,1024]{1,0:T(8,128)(2,1)S(1)}, u32[]{:S(2)}, u32[]{:S(2)}) %collective-permute-start.18) | collective-permute-done | bytes 65568 | tf_op jit(solution)/shard_map/ppermute | solution.py:428
  (112 shorter events, 22.7 us)
Async XLA Ops:
  0.6 20.4 %collective-permute-start = (bf16[32,1024]{1,0:T(8,128)(2,1)}, bf16[32,1024]{1,0:T(8,128)(2,1)S(1)}, u32[]{:S(2)}, u32[]{:S(2)}) collective-permute-start(bf16[32,1024]{1,0:T(8,128)(2,1)} %t0.1), channel_id=1, source_target_pairs={{0,2},{2,4},{4,6},{6,0},{1,3},{3,5},{5,7},{7,1},{8,10},{10,12},{12... | collective-permute-start | bytes 196616 | tf_op jit(solution)/shard_map/ppermute | solution.py:333
  2.3 18.7 %collective-permute-start.1 = (bf16[32,1024]{1,0:T(8,128)(2,1)}, bf16[32,1024]{1,0:T(8,128)(2,1)S(1)}, u32[]{:S(2)}, u32[]{:S(2)}) collective-permute-start(bf16[32,1024]{1,0:T(8,128)(2,1)} %t0.1), channel_id=1, source_target_pairs={{0,4},{2,6},{4,0},{6,2},{1,5},{3,7},{5,1},{7,3},{8,12},{10,14},{12... | collective-permute-start | bytes 196616 | tf_op jit(solution)/shard_map/ppermute | solution.py:333
  5.2 15.8 %collective-permute-start.2 = (bf16[32,1024]{1,0:T(8,128)(2,1)}, bf16[32,1024]{1,0:T(8,128)(2,1)S(1)}, u32[]{:S(2)}, u32[]{:S(2)}) collective-permute-start(bf16[32,1024]{1,0:T(8,128)(2,1)} %t0.1), channel_id=1, source_target_pairs={{0,6},{2,0},{4,2},{6,4},{1,7},{3,1},{5,3},{7,5},{8,14},{10,8},{12,... | collective-permute-start | bytes 196616 | tf_op jit(solution)/shard_map/ppermute | solution.py:333
  8.9 23.5 %all-to-all-start.1 = ((bf16[32,40,128]{2,1,0:T(8,128)(2,1)}), bf16[32,40,128]{2,1,0:T(8,128)(2,1)S(1)}, u32[]{:S(2)}, u32[]{:S(2)}) async-start(bf16[32,40,128]{2,1,0:T(8,128)(2,1)} %shard_map.131), calls=%async_computation.1 | async-start | bytes 655360 | tf_op jit(solution)/shard_map/all_to_all | solution.py:331
  34.0 12.7 %all-to-all-start.2 = ((bf16[8,72,128]{2,1,0:T(8,128)(2,1)}), bf16[8,72,128]{2,1,0:T(8,128)(2,1)S(1)}, u32[]{:S(2)}, u32[]{:S(2)}) async-start(bf16[8,72,128]{2,1,0:T(8,128)(2,1)} %get-tuple-element.10), calls=%async_computation.2 | async-start | bytes 294912 | tf_op jit(solution)/shard_map/all_to_all | solution.py:370
  47.4 15.3 %all-to-all-start = ((bf16[32,32,128]{2,1,0:T(8,128)(2,1)}), bf16[32,32,128]{2,1,0:T(8,128)(2,1)S(1)}, u32[]{:S(2)}, u32[]{:S(2)}) async-start(bf16[32,32,128]{2,1,0:T(8,128)(2,1)} %broadcast_in_dim.30), calls=%async_computation | async-start | bytes 524288 | tf_op jit(solution)/shard_map/all_to_all | solution.py:375
  54.2 15.3 %collective-permute-start.10 = (bf16[8,72,128]{2,1,0:T(8,128)(2,1)S(1)}, bf16[8,72,128]{2,1,0:T(8,128)(2,1)S(1)}, u32[]{:S(2)}, u32[]{:S(2)}) collective-permute-start(bf16[8,72,128]{2,1,0:T(8,128)(2,1)S(1)} %all-to-all-done.2), channel_id=1, source_target_pairs={{0,24},{1,7},{2,26},{3,1},{4,28},{5,3},{6,30},{7,5},{8,0},{9,15},{... | collective-permute-start | bytes 442376 | tf_op jit(solution)/shard_map/ppermute | solution.py:371
  54.6 14.8 %collective-permute-start.9 = (bf16[8,72,128]{2,1,0:T(8,128)(2,1)S(1)}, bf16[8,72,128]{2,1,0:T(8,128)(2,1)S(1)}, u32[]{:S(2)}, u32[]{:S(2)}) collective-permute-start(bf16[8,72,128]{2,1,0:T(8,128)(2,1)S(1)} %all-to-all-done.2), channel_id=1, source_target_pairs={{0,16},{1,5},{2,18},{3,7},{4,20},{5,1},{6,22},{7,3},{8,24},{9,13},... | collective-permute-start | bytes 442376 | tf_op jit(solution)/shard_map/ppermute | solution.py:371
  57.2 12.3 %collective-permute-start.8 = (bf16[8,72,128]{2,1,0:T(8,128)(2,1)S(1)}, bf16[8,72,128]{2,1,0:T(8,128)(2,1)S(1)}, u32[]{:S(2)}, u32[]{:S(2)}) collective-permute-start(bf16[8,72,128]{2,1,0:T(8,128)(2,1)S(1)} %all-to-all-done.2), channel_id=1, source_target_pairs={{0,8},{1,3},{2,10},{3,5},{4,12},{5,7},{6,14},{7,1},{8,16},{9,11},{... | collective-permute-start | bytes 442376 | tf_op jit(solution)/shard_map/ppermute | solution.py:371
  59.6 13.5 %collective-permute-start.3 = (bf16[64,128]{1,0:T(8,128)(2,1)S(1)}, bf16[64,128]{1,0:T(8,128)(2,1)S(1)}, u32[]{:S(2)}, u32[]{:S(2)}) collective-permute-start(bf16[64,128]{1,0:T(8,128)(2,1)S(1)} %get-tuple-element.9), channel_id=1, source_target_pairs={{0,1},{1,0},{2,3},{3,2},{4,5},{5,4},{6,7},{7,6},{8,9},{9,8},{10,11... | collective-permute-start | bytes 49160 | tf_op jit(solution)/shard_map/ppermute | solution.py:378
  63.5 28.7 %all-to-all-start.3 = ((bf16[32,32,128]{2,1,0:T(8,128)(2,1)}), bf16[32,32,128]{2,1,0:T(8,128)(2,1)S(1)}, u32[]{:S(2)}, u32[]{:S(2)}) async-start(bf16[32,32,128]{2,1,0:T(8,128)(2,1)} %broadcast_in_dim.34), calls=%async_computation.3 | async-start | bytes 524288 | tf_op jit(solution)/shard_map/all_to_all | solution.py:377
  69.5 32.7 %collective-permute-start.11 = (bf16[4,8,72,128]{3,2,1,0:T(8,128)(2,1)S(1)}, bf16[4,8,72,128]{3,2,1,0:T(8,128)(2,1)S(1)}, u32[]{:S(2)}, u32[]{:S(2)}) collective-permute-start(bf16[4,8,72,128]{3,2,1,0:T(8,128)(2,1)S(1)} %pad_maximum_fusion.b0), channel_id=1, source_target_pairs={{0,2},{1,9},{2,4},{3,11},{4,6},{5,13},{6,0},{7,15},{8,10},{9,17},{... | collective-permute-start | bytes 1769480 | tf_op jit(solution)/shard_map/ppermute | solution.py:373
  70.3 32.0 %collective-permute-start.12 = (bf16[4,8,72,128]{3,2,1,0:T(8,128)(2,1)S(1)}, bf16[4,8,72,128]{3,2,1,0:T(8,128)(2,1)S(1)}, u32[]{:S(2)}, u32[]{:S(2)}) collective-permute-start(bf16[4,8,72,128]{3,2,1,0:T(8,128)(2,1)S(1)} %pad_maximum_fusion.b0), channel_id=1, source_target_pairs={{0,4},{1,17},{2,6},{3,19},{4,0},{5,21},{6,2},{7,23},{8,12},{9,25},... | collective-permute-start | bytes 1769480 | tf_op jit(solution)/shard_map/ppermute | solution.py:373
  71.0 31.3 %collective-permute-start.13 = (bf16[4,8,72,128]{3,2,1,0:T(8,128)(2,1)S(1)}, bf16[4,8,72,128]{3,2,1,0:T(8,128)(2,1)S(1)}, u32[]{:S(2)}, u32[]{:S(2)}) collective-permute-start(bf16[4,8,72,128]{3,2,1,0:T(8,128)(2,1)S(1)} %pad_maximum_fusion.b0), channel_id=1, source_target_pairs={{0,6},{1,25},{2,0},{3,27},{4,2},{5,29},{6,4},{7,31},{8,14},{9,1},{... | collective-permute-start | bytes 1769480 | tf_op jit(solution)/shard_map/ppermute | solution.py:373
  73.7 14.7 %collective-permute-start.4 = (bf16[2,64,128]{2,1,0:T(8,128)(2,1)}, bf16[2,64,128]{2,1,0:T(8,128)(2,1)S(1)}, u32[]{:S(2)}, u32[]{:S(2)}) collective-permute-start(bf16[2,64,128]{2,1,0:T(8,128)(2,1)} %pad_maximum_fusion.1.q0), channel_id=1, source_target_pairs={{0,2},{2,4},{4,6},{6,0},{1,3},{3,5},{5,7},{7,1},{8,10},{10,12},{12... | collective-permute-start | bytes 98312 | tf_op jit(solution)/shard_map/ppermute | solution.py:379
  74.3 14.7 %collective-permute-start.5 = (bf16[2,64,128]{2,1,0:T(8,128)(2,1)}, bf16[2,64,128]{2,1,0:T(8,128)(2,1)}, u32[]{:S(2)}, u32[]{:S(2)}) collective-permute-start(bf16[2,64,128]{2,1,0:T(8,128)(2,1)} %pad_maximum_fusion.1.q0), channel_id=1, source_target_pairs={{0,4},{2,6},{4,0},{6,2},{1,5},{3,7},{5,1},{7,3},{8,12},{10,14},{12... | collective-permute-start | bytes 98312 | tf_op jit(solution)/shard_map/ppermute | solution.py:379
  89.0 10.5 %collective-permute-start.7 = (bf16[32,32,128]{2,1,0:T(8,128)(2,1)S(1)}, bf16[32,32,128]{2,1,0:T(8,128)(2,1)S(1)}, u32[]{:S(2)}, u32[]{:S(2)}) collective-permute-start(bf16[32,32,128]{2,1,0:T(8,128)(2,1)S(1)} %all-to-all-done.up_own), channel_id=1, source_target_pairs={{0,1},{1,0},{2,3},{3,2},{4,5},{5,4},{6,7},{7,6},{8,9},{9,8},{10,11... | collective-permute-start | bytes 786440 | tf_op jit(solution)/shard_map/ppermute | solution.py:376
  89.1 4.3 %collective-permute-start.6 = (bf16[2,64,128]{2,1,0:T(8,128)(2,1)}, bf16[2,64,128]{2,1,0:T(8,128)(2,1)}, u32[]{:S(2)}, u32[]{:S(2)}) collective-permute-start(bf16[2,64,128]{2,1,0:T(8,128)(2,1)} %pad_maximum_fusion.1.q0), channel_id=1, source_target_pairs={{0,6},{2,0},{4,2},{6,4},{1,7},{3,1},{5,3},{7,5},{8,14},{10,8},{12,... | collective-permute-start | bytes 98312 | tf_op jit(solution)/shard_map/ppermute | solution.py:379
  93.3 20.7 %collective-permute-start.16 = (bf16[32,32,128]{2,1,0:T(8,128)(2,1)S(1)}, bf16[32,32,128]{2,1,0:T(8,128)(2,1)}, u32[]{:S(2)}, u32[]{:S(2)}) collective-permute-start(bf16[32,32,128]{2,1,0:T(8,128)(2,1)S(1)} %all-to-all-done.3.w_own), channel_id=1, source_target_pairs={{0,1},{1,0},{2,3},{3,2},{4,5},{5,4},{6,7},{7,6},{8,9},{9,8},{10,11... | collective-permute-start | bytes 786440 | tf_op jit(solution)/shard_map/ppermute | solution.py:421
  113.4 1.9 %collective-permute-start.15 = (f32[256,128]{1,0:T(8,128)S(1)}, f32[256,128]{1,0:T(8,128)S(1)}, u32[]{:S(2)}, u32[]{:S(2)}) collective-permute-start(f32[256,128]{1,0:T(8,128)S(1)} %get-tuple-element.13.ml_own), channel_id=1, source_target_pairs={{0,1},{1,0},{2,3},{3,2},{4,5},{5,4},{6,7},{7,6},{8,9},{9,8},{10,11... | collective-permute-start | bytes 393224 | tf_op jit(solution)/shard_map/ppermute | solution.py:420
  114.0 1.3 collective-permute-start.14
  117.7 6.0 %collective-permute-start.17 = (bf16[32,1024]{1,0:T(8,128)(2,1)S(1)}, bf16[32,1024]{1,0:T(8,128)(2,1)S(1)}, u32[]{:S(2)}, u32[]{:S(2)}) collective-permute-start(bf16[32,1024]{1,0:T(8,128)(2,1)S(1)} %get-tuple-element.28), channel_id=1, source_target_pairs={{0,2},{2,4},{4,6},{6,0},{1,3},{3,5},{5,7},{7,1},{8,10},{10,12},{12... | collective-permute-start | bytes 196616 | tf_op jit(solution)/shard_map/ppermute | solution.py:428
  117.8 8.5 %collective-permute-start.18 = (bf16[32,1024]{1,0:T(8,128)(2,1)S(1)}, bf16[32,1024]{1,0:T(8,128)(2,1)S(1)}, u32[]{:S(2)}, u32[]{:S(2)}) collective-permute-start(bf16[32,1024]{1,0:T(8,128)(2,1)S(1)} %get-tuple-element.27), channel_id=1, source_target_pairs={{0,4},{2,6},{4,0},{6,2},{1,5},{3,7},{5,1},{7,3},{8,12},{10,14},{12... | collective-permute-start | bytes 196616 | tf_op jit(solution)/shard_map/ppermute | solution.py:428
  122.8 4.3 %collective-permute-start.19 = (bf16[32,1024]{1,0:T(8,128)(2,1)S(1)}, bf16[32,1024]{1,0:T(8,128)(2,1)S(1)}, u32[]{:S(2)}, u32[]{:S(2)}) collective-permute-start(bf16[32,1024]{1,0:T(8,128)(2,1)S(1)} %get-tuple-element.26), channel_id=1, source_target_pairs={{0,6},{2,0},{4,2},{6,4},{1,7},{3,1},{5,3},{7,5},{8,14},{10,8},{12,... | collective-permute-start | bytes 196616 | tf_op jit(solution)/shard_map/ppermute | solution.py:428
  (18 other events, 80.0 us)

commit v2 on v1

--- a/solution.py
+++ b/solution.py
@@ -32,7 +32,7 @@
 ANY_SPEC = pl.BlockSpec(memory_space=pl.ANY)
 
 
-def call(body, outs, n_smem, n_in, scratch=(), any_from=None, cost=None):
+def call(body, outs, n_smem, n_in, scratch=(), any_from=None, cost=None, room=16):
     specs = [SMEM_SPEC] * n_smem
     for i in range(n_in):
         specs.append(ANY_SPEC if any_from is not None and i >= any_from else VMEM_SPEC)
@@ -43,7 +43,7 @@
         in_specs=specs,
         out_specs=VMEM_SPEC if single else tuple(VMEM_SPEC for _ in outs),
         scratch_shapes=list(scratch),
-        compiler_params=pltpu.CompilerParams(vmem_limit_bytes=50 * 1024 * 1024),
+        compiler_params=pltpu.CompilerParams(vmem_limit_bytes=room * 1024 * 1024),
         cost_estimate=cost,
     )
 
@@ -54,6 +54,14 @@
 
 def column(row):
     return jnp.transpose(jnp.broadcast_to(row, (128, 128)))
+
+
+def frequency(index):
+    value = jnp.ones(index.shape, F32)
+    for bit in range(4):
+        factor = THETA ** (-(1 << bit) / 16)
+        value = value * jnp.where((index // (1 << bit)) % 2 == 1, factor, 1.0)
+    return value
 
 
 def pack(where, dq, dk, dr, out, flipped):
@@ -76,7 +84,7 @@
         out[s, 32:40, :] = turned
 
 
-def project(where, t0, t1, t2, t3, gathered, cos_ref, sin_ref, q_ref, k_ref, tok):
+def project(where, t0, t1, t2, t3, gathered, q_ref, k_ref, tok):
     y = where[2]
     for j, part in enumerate((t0, t1, t2, t3)):
         at = lax.rem(y - j + NY, NY)
@@ -99,14 +107,19 @@
     rope = jnp.concatenate([rope, jnp.zeros_like(rope)], axis=0).astype(BF)
     raw = lax.dot_general(rope, rows, (((1,), (1,)), ((), ())), preferred_element_type=F32)
     raw = raw[0:8, :].astype(BF).astype(F32)
-    rotated = raw * cos_ref[...] + pltpu.roll(raw, 4, 0) * sin_ref[...]
+    at = lanes((8, 128))
+    row = lax.broadcasted_iota(jnp.int32, (8, 128), 0)
+    pos = where[4] + 64 * (at // 32) + 32 * where[3] + at % 32
+    angle = pos.astype(F32) * frequency(4 * y + row % 4)
+    sine = jnp.sin(angle)
+    rotated = raw * jnp.cos(angle) + pltpu.roll(raw, 4, 0) * jnp.where(row < 4, -sine, sine)
     rotated = rotated.astype(BF)
     for t in range(NZ):
         k_ref[t, 64:72, :] = rotated
 
 
 def make_queries(
-    where, q0, q1, q2, q3, up_own, up_other, gain, cos_ref, low_ref, high_ref, out, latents
+    where, q0, q1, q2, q3, up_own, up_other, gain, out, latents
 ):
     y, c = where[2], where[3]
     for j, part in enumerate((q0, q1, q2, q3)):
@@ -122,6 +135,15 @@
     latent = raw * inverse * gains
     latent = jnp.transpose(latent).astype(BF)
     lane = lanes((256, 128))
+    row = lax.broadcasted_iota(jnp.int32, (256, 128), 0)
+    pos = where[4] + 64 * ((row % 128) // 32) + 32 * (row // 128) + row % 32
+    angle = pos.astype(F32) * frequency(4 * ((lane % 32) // 8) + lane % 4)
+    used = lane < 64
+    is_low = (lane // 4) % 2 == 0
+    cos = jnp.where(used, jnp.cos(angle), 0.0)
+    sine = jnp.where(used, jnp.sin(angle), 0.0)
+    low_sin = jnp.where(is_low, -sine, 0.0)
+    high_sin = jnp.where(is_low, 0.0, sine)
     for p, up in enumerate((up_own, up_other)):
         wide = up[...].astype(F32)
         plain_w = wide[:, 0:8, :].reshape(256, 128).astype(BF)
@@ -129,9 +151,9 @@
         plain = jnp.dot(latent, plain_w, preferred_element_type=F32) * SCALE2
         raw = jnp.dot(latent, rope_w, preferred_element_type=F32) * SCALE2
         rope = (
-            raw * cos_ref[...]
-            + pltpu.roll(raw, 124, 1) * low_ref[...]
-            + pltpu.roll(raw, 4, 1) * high_ref[...]
+            raw * cos
+            + pltpu.roll(raw, 124, 1) * low_sin
+            + pltpu.roll(raw, 4, 1) * high_sin
         )
         for i in range(2):
             own = slice(256 * i, 256 * (i + 1))
@@ -140,10 +162,10 @@
 
 
 def attend(
-    where, q_ref, up_own, up_other, gain, key_docs, query_docs, b0, b1, b2, b3,
-    keep_ref, send_ref, ml_ref, kb, s_buf, v_buf, mx, total, acc, uk, uv, gains, docs_col, sems,
+    where, q_ref, up_own, up_other, gain, query_docs, b0, b1, b2, b3,
+    keep_ref, send_ref, ml_ref, kb, s_buf, v_buf, mx, total, acc, uk, uv, gains, docs_col, key_docs, sems,
 ):
-    x0, y0, c, low, high = where[1], where[2], where[3], where[4], where[5]
+    x0, y0, c = where[1], where[2], where[3]
     copies = [
         pltpu.make_async_copy(part, kb.at[j], sems.at[j]) for j, part in enumerate((b0, b1, b2, b3))
     ]
@@ -157,6 +179,19 @@
     for i in range(2):
         gains[128 * i : 128 * (i + 1), :] = column(gain[i : i + 1, :])
         docs_col[128 * i : 128 * (i + 1), :] = column(query_docs[i : i + 1, :])
+    docs = up_own[:, 24:32, :].astype(F32)
+    at = lanes((NS, 8, 128))
+    row = lax.broadcasted_iota(jnp.int32, (NS, 8, 128), 1)
+    before = (row == 7) & (at == 95) & (docs < where[5].astype(F32))
+    behind = (row == 0) & (at == 64) & (docs > where[6].astype(F32))
+    low = jnp.sum(before.astype(jnp.int32))
+    high = NS - 1 - jnp.sum(behind.astype(jnp.int32))
+    spread = jnp.zeros((NS, 128), F32)
+    at = lanes((NS, 128))
+    for y in range(NY):
+        piece = jnp.where(c == 0, docs[:, 2 * y, :], docs[:, 2 * y + 1, :])
+        spread = jnp.where(at // 32 == y, pltpu.roll(piece, (32 * y + 64) % 128, 1), spread)
+    key_docs[...] = spread
     mx[...] = jnp.full(mx.shape, NEG_BIG, F32)
     total[...] = jnp.zeros(total.shape, F32)
     acc[...] = jnp.zeros(acc.shape, F32)
@@ -243,7 +278,10 @@
     send_ref[...] = acc[pl.ds(pl.multiple_of((1 - c) * 128, 128), 128), :].astype(BF)
 
 
-def combine(where, keep, got, ml_own, ml_got, w_own, w_other, part_ref, lse_ref, f_own, f_got, scratch):
+def combine(
+    where, keep, got, ml_own, ml_got, w_own, w_other, part_ref, p1_ref, p2_ref, p3_ref, lse_ref,
+    f_own, f_got, scratch,
+):
     c = where[3]
     own = ml_own[...]
     other = ml_got[...]
@@ -274,18 +312,18 @@
         theirs = got[:, 128 * (1 - p) : 128 * (2 - p)].astype(F32)
         attended = (mine * a + theirs * b).astype(BF)
         result = result + lax.dot_general(
-            attended, w[...].reshape(1024, 128), (((1,), (1,)), ((), ())),
+            attended, w[:, 32:64, :].reshape(1024, 128), (((1,), (1,)), ((), ())),
             preferred_element_type=F32,
         )
     scratch[...] = result
     y = where[2]
-    for j in range(NY):
+    for j, out in enumerate((part_ref, p1_ref, p2_ref, p3_ref)):
         to = lax.rem(y + j, NY)
-        part_ref[j] = scratch[pl.ds(pl.multiple_of(to * 32, 32), 32), :].astype(BF)
+        out[...] = scratch[pl.ds(pl.multiple_of(to * 32, 32), 32), :].astype(BF)
 
 
 def finish(part, p1, p2, p3, gain, out):
-    summed = part[0].astype(F32)
+    summed = part[...].astype(F32)
     for other in (p1, p2, p3):
         summed = summed + other[...].astype(F32)
     wide = summed.astype(BF).astype(F32)
@@ -322,7 +360,7 @@
     y = lax.axis_index("y")
     c = lax.axis_index("c")
     sp = z * NX + x
-    here = jnp.stack([z, x, y, c]).astype(jnp.int32)
+    here = jnp.stack([z, x, y, c, sp * 256]).astype(jnp.int32)
     swap = [(0, 1), (1, 0)]
 
     message = call(
@@ -337,35 +375,14 @@
     turning = heads[:, :, NOPE:].reshape(8, 2, 2, 4, 4).transpose(0, 1, 3, 2, 4).reshape(8, 64)
     docs = doc_ids.astype(BF).reshape(8, 32)
     mixed_rows = jnp.concatenate([turning, docs, jnp.zeros((8, 32), BF)], axis=1)
-    later = jnp.concatenate([plain, up_key, up_value, mixed_rows], axis=0)
-    later = jnp.broadcast_to(later[None], (NS, 32, 128))
-    last = jnp.broadcast_to(output_weight.T[None], (NS, 32, 128))
-
-    f32_base = (sp * 256).astype(F32)
-    key_tok = lax.broadcasted_iota(jnp.int32, (8, 128), 1)
-    key_row = lax.broadcasted_iota(jnp.int32, (8, 128), 0)
-    key_pos = f32_base + (64 * (key_tok // 32) + 32 * c + key_tok % 32).astype(F32)
-    key_freq = THETA ** (-(4 * y + key_row % 4).astype(F32) / 16)
-    key_angle = key_pos * key_freq
-    key_cos = jnp.cos(key_angle)
-    key_sin = jnp.sin(key_angle) * jnp.where(key_row < 4, -1.0, 1.0)
-    tok = lax.broadcasted_iota(jnp.int32, (256, 128), 0)
-    lane = lax.broadcasted_iota(jnp.int32, (256, 128), 1)
-    pos = f32_base + (64 * ((tok % 128) // 32) + 32 * (tok // 128) + tok % 32).astype(F32)
-    freq = THETA ** (-(4 * ((lane % 32) // 8) + lane % 4).astype(F32) / 16)
-    angle = pos * freq
-    used = lane < 64
-    is_low = (lane // 4) % 2 == 0
-    cos = jnp.where(used, jnp.cos(angle), 0.0)
-    sine = jnp.sin(angle)
-    low_sin = jnp.where(used & is_low, -sine, 0.0)
-    high_sin = jnp.where(used & ~is_low, sine, 0.0)
+    later = jnp.concatenate([plain, up_key, up_value, mixed_rows, output_weight.T], axis=0)
+    later = jnp.broadcast_to(later[None], (NS, 64, 128))
 
     q_part, k_part = call(
         project,
         (jax.ShapeDtypeStruct((64, 128), BF), jax.ShapeDtypeStruct((NZ, 72, 128), BF)),
-        1, 7, scratch=[VMEM((128, 1024), BF)],
-    )(here, *rows, gathered, key_cos, key_sin)
+        1, 5, scratch=[VMEM((128, 1024), BF)],
+    )(here, *rows, gathered)
 
     stage1 = lax.all_to_all(k_part, "z", 0, 0)
     stage2 = [lax.ppermute(stage1, AXES, shift_pairs(2, j)) for j in range(1, 4)]
@@ -374,25 +391,15 @@
 
     up_own = lax.all_to_all(later, SP, 0, 0)
     up_other = lax.ppermute(up_own, "c", swap)
-    out_own = lax.all_to_all(last, SP, 0, 0)
     q_pair = jnp.stack([q_part, lax.ppermute(q_part, "c", swap)])
     q_all = [q_pair] + [lax.ppermute(q_pair, "y", ring(j)) for j in range(1, NY)]
     queries = call(
-        make_queries, jax.ShapeDtypeStruct((2, 512, 256), BF), 1, 10,
+        make_queries, jax.ShapeDtypeStruct((2, 512, 256), BF), 1, 7,
         scratch=[VMEM((256, 256), F32)],
-    )(here, *q_all, up_own, up_other, query_gain.reshape(2, 128), cos, low_sin, high_sin)
-
-    all_docs = up_own[:, 24:32, 64:96].astype(F32)
-    key_docs = lax.dynamic_index_in_dim(
-        all_docs.reshape(NS, 4, 2, 32), c, 2, keepdims=False
-    ).reshape(NS, 128)
+    )(here, *q_all, up_own, up_other, query_gain.reshape(2, 128))
+
+    there = jnp.concatenate([here, doc_ids[:1], doc_ids[255:]])
     query_docs = doc_ids.astype(F32).reshape(4, 2, 32).transpose(1, 0, 2).reshape(2, 128)
-    own_first = doc_ids[0].astype(F32)
-    own_last = doc_ids[255].astype(F32)
-    low = jnp.sum((all_docs[:, 7, 31] < own_first).astype(jnp.int32))
-    high = NS - 1 - jnp.sum((all_docs[:, 0, 0] > own_last).astype(jnp.int32))
-    where = jnp.stack([z, x, y, c, low, high]).astype(jnp.int32)
-
     keep, send, ml = call(
         attend,
         (
@@ -400,7 +407,7 @@
             jax.ShapeDtypeStruct((128, 256), BF),
             jax.ShapeDtypeStruct((256, 128), F32),
         ),
-        1, 10, any_from=6,
+        1, 9, any_from=5, room=34,
         scratch=[
             VMEM((4, 4, NZ, 72, 128), BF),
             VMEM((16, 4, 256, 256), F32),
@@ -412,23 +419,21 @@
             VMEM((256, 256), BF),
             VMEM((256, 128), F32),
             VMEM((256, 128), F32),
+            VMEM((NS, 128), F32),
             pltpu.SemaphoreType.DMA((4,)),
         ],
-    )(where, queries, up_own, up_other, key_gain.reshape(2, 128), key_docs, query_docs, held, *stage3)
+    )(there, queries, up_own, up_other, key_gain.reshape(2, 128), query_docs, held, *stage3)
 
     got = lax.ppermute(send, "c", swap)
     ml_got = lax.ppermute(ml, "c", swap)
-    out_other = lax.ppermute(out_own, "c", swap)
-    part, log_sums = call(
+    *parts, log_sums = call(
         combine,
-        (jax.ShapeDtypeStruct((NY, 32, 1024), BF), jax.ShapeDtypeStruct((256, 2), F32)),
+        (jax.ShapeDtypeStruct((32, 1024), BF),) * NY + (jax.ShapeDtypeStruct((256, 2), F32),),
         1, 6, scratch=[VMEM((4, 256, 128), F32), VMEM((4, 256, 128), F32), VMEM((128, 1024), F32)],
-    )(here, keep, got, ml, ml_got, out_own, out_other)
-    parts = [
-        lax.ppermute(part[j], "y", ring(j)) for j in range(1, NY)
-    ]
+    )(here, keep, got, ml, ml_got, up_own, up_other)
+    parts[1:] = [lax.ppermute(parts[j], "y", ring(j)) for j in range(1, NY)]
     mixed = call(finish, jax.ShapeDtypeStruct((32, 1024), BF), 0, 5)(
-        part, *parts, out_gain.reshape(1, 1024)
+        *parts, out_gain.reshape(1, 1024)
     )
     return mixed, log_sums
 

time: 129 us -> 123 us (0.953)
  the two profiles are of different devices: /device:TPU:2 before, /device:TPU:1 now
where the time goes in v2:
time: 123 us
  starting transfers between devices  59.4 us (48%)
  waiting for transfers between devices  36.9 us (30%)
  Pallas kernels  17.9 us (15%)
  local copies, waits for them, and re-layouts  7.53 us (6%)
    ppermute x1, starting transfers between devices, layer(): up_other = lax.ppermute(up_own, 'c', swap)  15.7 us
    ppermute x3, waiting for transfers between devices, layer(): lax.ppermute(q_pair, 'y', ring(j))  13.3 us
    all_to_all x1, starting transfers between devices, layer(): gathered = lax.all_to_all(message, SP, 0, 0)  12 us
    pallas_call x1, Pallas kernels, layer(): call(attend, (jax.ShapeDtypeStruct((128, 256), F32), jax.ShapeDtypeStruct...  10.5 us
    all_to_all x1, waiting for transfers between devices, layer(): stage1 = lax.all_to_all(k_part, 'z', 0, 0)  8.02 us
    ppermute x3, waiting for transfers between devices, layer(): lax.ppermute(stage1, AXES, shift_pairs(2, j))  6.33 us
    ppermute x3, starting transfers between devices, layer(): rows = [tokens] + [lax.ppermute(tokens, 'y', ring(j)) for j in range(1, NY)]  5.68 us
    all_to_all x1, waiting for transfers between devices, layer(): gathered = lax.all_to_all(message, SP, 0, 0)  4.44 us
  transfers between devices with their start and end apart: 22, of which 12 were waited for; matrix products, arithmetic and copies ran while one was open for 3% of the time, Pallas kernels for 1%

profile of v2, /device:TPU:1, one launch (start us, length us, event | category | flops | bytes accessed | tf_op | source)
XLA Modules:
  0.0 122.7 jit_solution(5530131095223148837)
XLA Ops:
  1.4 1.6 %shard_map.131 = bf16[32,40,128]{2,1,0:T(8,128)(2,1)} custom-call(s32[5]{0:T(128)S(1)} %stack.47.where, bf16[32,256]{1,0:T(8,128)(2,1)S(1)} %copy-done.1, bf16[32,256]{1,0:T(8,128)(2,1)S(1)} %copy-done.2, bf16[32,32]{1,0:T(8,128)(2,1)S(1)} %copy-done.3), custom_call_target="tpu_custom_call" | custom-call | tf_op jit(solution)/shard_map/pallas_call | solution.py:366
  3.0 12.0 %all-to-all-start = ((bf16[32,40,128]{2,1,0:T(8,128)(2,1)}), bf16[32,40,128]{2,1,0:T(8,128)(2,1)S(1)}, u32[]{:S(2)}, u32[]{:S(2)}) async-start(bf16[32,40,128]{2,1,0:T(8,128)(2,1)} %shard_map.131), calls=%async_computation | async-start | bytes 655360 | tf_op jit(solution)/shard_map/all_to_all | solution.py:369
  15.0 3.0 %collective-permute-start.1 = (bf16[32,1024]{1,0:T(8,128)(2,1)S(1)}, bf16[32,1024]{1,0:T(8,128)(2,1)S(1)}, u32[]{:S(2)}, u32[]{:S(2)}) collective-permute-start(bf16[32,1024]{1,0:T(8,128)(2,1)S(1)} %copy-done), channel_id=1, source_target_pairs={{0,4},{2,6},{4,0},{6,2},{1,5},{3,7},{5,1},{7,3},{8,12},{10,14},{12... | collective-permute-start | bytes 196616 | tf_op jit(solution)/shard_map/ppermute | solution.py:371
  18.4 2.3 %collective-permute-start.2 = (bf16[32,1024]{1,0:T(8,128)(2,1)S(1)}, bf16[32,1024]{1,0:T(8,128)(2,1)S(1)}, u32[]{:S(2)}, u32[]{:S(2)}) collective-permute-start(bf16[32,1024]{1,0:T(8,128)(2,1)S(1)} %copy-done), channel_id=1, source_target_pairs={{0,6},{2,0},{4,2},{6,4},{1,7},{3,1},{5,3},{7,5},{8,14},{10,8},{12,... | collective-permute-start | bytes 196616 | tf_op jit(solution)/shard_map/ppermute | solution.py:371
  23.2 4.4 %all-to-all-done.gathered = bf16[32,40,128]{2,1,0:T(8,128)(2,1)S(1)} async-done(((bf16[32,40,128]{2,1,0:T(8,128)(2,1)}), bf16[32,40,128]{2,1,0:T(8,128)(2,1)S(1)}, u32[]{:S(2)}, u32[]{:S(2)}) %all-to-all-start) | async-done | bytes 327712 | tf_op jit(solution)/shard_map/all_to_all | solution.py:369
  29.2 3.5 %all-to-all-start.2 = ((bf16[8,72,128]{2,1,0:T(8,128)(2,1)}), bf16[8,72,128]{2,1,0:T(8,128)(2,1)S(1)}, u32[]{:S(2)}, u32[]{:S(2)}) async-start(bf16[8,72,128]{2,1,0:T(8,128)(2,1)} %get-tuple-element.13), calls=%async_computation.2 | async-start | bytes 294912 | tf_op jit(solution)/shard_map/all_to_all | solution.py:387
  32.8 8.0 %all-to-all-done.2 = bf16[8,72,128]{2,1,0:T(8,128)(2,1)S(1)} async-done(((bf16[8,72,128]{2,1,0:T(8,128)(2,1)}), bf16[8,72,128]{2,1,0:T(8,128)(2,1)S(1)}, u32[]{:S(2)}, u32[]{:S(2)}) %all-to-all-start.2) | async-done | bytes 147488 | tf_op jit(solution)/shard_map/all_to_all | solution.py:387
  41.7 3.9 %all-to-all-start.1 = ((bf16[32,64,128]{2,1,0:T(8,128)(2,1)}), bf16[32,64,128]{2,1,0:T(8,128)(2,1)S(1)}, u32[]{:S(2)}, u32[]{:S(2)}) async-start(bf16[32,64,128]{2,1,0:T(8,128)(2,1)} %broadcast_in_dim.10), calls=%async_computation.1 | async-start | bytes 1048576 | tf_op jit(solution)/shard_map/all_to_all | solution.py:392
  45.6 2.8 %collective-permute-start.10 = (bf16[8,72,128]{2,1,0:T(8,128)(2,1)S(1)}, bf16[8,72,128]{2,1,0:T(8,128)(2,1)S(1)}, u32[]{:S(2)}, u32[]{:S(2)}) collective-permute-start(bf16[8,72,128]{2,1,0:T(8,128)(2,1)S(1)} %all-to-all-done.2), channel_id=1, source_target_pairs={{0,24},{1,7},{2,26},{3,1},{4,28},{5,3},{6,30},{7,5},{8,0},{9,15},{... | collective-permute-start | bytes 442376 | tf_op jit(solution)/shard_map/ppermute | solution.py:388
  49.5 2.6 %collective-permute-done.10 = bf16[8,72,128]{2,1,0:T(8,128)(2,1)S(1)} collective-permute-done((bf16[8,72,128]{2,1,0:T(8,128)(2,1)S(1)}, bf16[8,72,128]{2,1,0:T(8,128)(2,1)S(1)}, u32[]{:S(2)}, u32[]{:S(2)}) %collective-permute-start.10) | collective-permute-done | bytes 147488 | tf_op jit(solution)/shard_map/ppermute | solution.py:388
  52.1 1.9 %collective-permute-done.9 = bf16[8,72,128]{2,1,0:T(8,128)(2,1)S(1)} collective-permute-done((bf16[8,72,128]{2,1,0:T(8,128)(2,1)S(1)}, bf16[8,72,128]{2,1,0:T(8,128)(2,1)S(1)}, u32[]{:S(2)}, u32[]{:S(2)}) %collective-permute-start.9) | collective-permute-done | bytes 147488 | tf_op jit(solution)/shard_map/ppermute | solution.py:388
  54.0 1.8 %collective-permute-done.8 = bf16[8,72,128]{2,1,0:T(8,128)(2,1)S(1)} collective-permute-done((bf16[8,72,128]{2,1,0:T(8,128)(2,1)S(1)}, bf16[8,72,128]{2,1,0:T(8,128)(2,1)S(1)}, u32[]{:S(2)}, u32[]{:S(2)}) %collective-permute-start.8) | collective-permute-done | bytes 147488 | tf_op jit(solution)/shard_map/ppermute | solution.py:388
  55.9 2.4 %collective-permute-start.13 = (bf16[4,8,72,128]{3,2,1,0:T(8,128)(2,1)S(1)}, bf16[4,8,72,128]{3,2,1,0:T(8,128)(2,1)S(1)}, u32[]{:S(2)}, u32[]{:S(2)}) collective-permute-start(bf16[4,8,72,128]{3,2,1,0:T(8,128)(2,1)S(1)} %pad_maximum_fusion.b0), channel_id=1, source_target_pairs={{0,6},{1,25},{2,0},{3,27},{4,2},{5,29},{6,4},{7,31},{8,14},{9,1},{... | collective-permute-start | bytes 1769480 | tf_op jit(solution)/shard_map/ppermute | solution.py:390
  59.4 15.7 %collective-permute-start.7 = (bf16[32,64,128]{2,1,0:T(8,128)(2,1)S(1)}, bf16[32,64,128]{2,1,0:T(8,128)(2,1)S(1)}, u32[]{:S(2)}, u32[]{:S(2)}) collective-permute-start(bf16[32,64,128]{2,1,0:T(8,128)(2,1)S(1)} %all-to-all-done.1.up_own.w_own), channel_id=1, source_target_pairs={{0,1},{1,0},{2,3},{3,2},{4,5},{5,4},{6,7},{7,6},{8,9},{9,8},{10,11... | collective-permute-start | bytes 1572872 | tf_op jit(solution)/shard_map/ppermute | solution.py:393
  75.2 1.6 %collective-permute-done.3 = bf16[64,128]{1,0:T(8,128)(2,1)S(1)} collective-permute-done((bf16[64,128]{1,0:T(8,128)(2,1)S(1)}, bf16[64,128]{1,0:T(8,128)(2,1)S(1)}, u32[]{:S(2)}, u32[]{:S(2)}) %collective-permute-start.3) | collective-permute-done | bytes 16416 | tf_op jit(solution)/shard_map/ppermute | solution.py:394
  76.7 1.9 %collective-permute-start.6 = (bf16[2,64,128]{2,1,0:T(8,128)(2,1)S(1)}, bf16[2,64,128]{2,1,0:T(8,128)(2,1)S(1)}, u32[]{:S(2)}, u32[]{:S(2)}) collective-permute-start(bf16[2,64,128]{2,1,0:T(8,128)(2,1)S(1)} %pad_maximum_fusion.1.q0), channel_id=1, source_target_pairs={{0,6},{2,0},{4,2},{6,4},{1,7},{3,1},{5,3},{7,5},{8,14},{10,8},{12,... | collective-permute-start | bytes 98312 | tf_op jit(solution)/shard_map/ppermute | solution.py:395
  78.6 7.1 %collective-permute-done.6.q3 = bf16[2,64,128]{2,1,0:T(8,128)(2,1)S(1)} collective-permute-done((bf16[2,64,128]{2,1,0:T(8,128)(2,1)S(1)}, bf16[2,64,128]{2,1,0:T(8,128)(2,1)S(1)}, u32[]{:S(2)}, u32[]{:S(2)}) %collective-permute-start.6) | collective-permute-done | bytes 32800 | tf_op jit(solution)/shard_map/ppermute | solution.py:395
  85.7 4.6 %collective-permute-done.5.q2 = bf16[2,64,128]{2,1,0:T(8,128)(2,1)S(1)} collective-permute-done((bf16[2,64,128]{2,1,0:T(8,128)(2,1)S(1)}, bf16[2,64,128]{2,1,0:T(8,128)(2,1)S(1)}, u32[]{:S(2)}, u32[]{:S(2)}) %collective-permute-start.5) | collective-permute-done | bytes 32800 | tf_op jit(solution)/shard_map/ppermute | solution.py:395
  93.2 1.6 %collective-permute-done.4.q1 = bf16[2,64,128]{2,1,0:T(8,128)(2,1)S(1)} collective-permute-done((bf16[2,64,128]{2,1,0:T(8,128)(2,1)S(1)}, bf16[2,64,128]{2,1,0:T(8,128)(2,1)S(1)}, u32[]{:S(2)}, u32[]{:S(2)}) %collective-permute-start.4) | collective-permute-done | bytes 32800 | tf_op jit(solution)/shard_map/ppermute | solution.py:395
  97.0 10.5 %shard_map.134 = (f32[128,256]{1,0:T(8,128)S(1)}, bf16[128,256]{1,0:T(8,128)(2,1)S(1)}, f32[256,128]{1,0:T(8,128)S(1)}) custom-call(s32[7]{0:T(128)S(1)} %concatenate.10.where, bf16[2,512,256]{2,1,0:T(8,128)(2,1)S(1)} %shard_map.133.q_ref, bf16[32,64,128]{2,1,0:T(8,128)(2,1)S(1)} %all-to-all-done.1.up_own.w_own, ...), custom_call_target="tpu_custom_call" | custom-call | tf_op jit(solution)/shard_map/pallas_call | solution.py:403
  107.5 4.2 %collective-permute-start.15 = (f32[256,128]{1,0:T(8,128)S(1)}, f32[256,128]{1,0:T(8,128)S(1)}, u32[]{:S(2)}, u32[]{:S(2)}) collective-permute-start(f32[256,128]{1,0:T(8,128)S(1)} %get-tuple-element.16.ml_own), channel_id=1, source_target_pairs={{0,1},{1,0},{2,3},{3,2},{4,5},{5,4},{6,7},{7,6},{8,9},{9,8},{10,11... | collective-permute-start | bytes 393224 | tf_op jit(solution)/shard_map/ppermute | solution.py:428
  112.9 2.0 %shard_map.135 = (bf16[32,1024]{1,0:T(8,128)(2,1)S(1)}, bf16[32,1024]{1,0:T(8,128)(2,1)S(1)}, bf16[32,1024]{1,0:T(8,128)(2,1)S(1)}, bf16[32,1024]{1,0:T(8,128)(2,1)S(1)}, f32[256,2]{1,0:T(8,128)S(1)}) custom-call(s32[5]{0:T(128)S(1)} %stack.47.where, f32[128,256]{1,0:T(8,128)S(1)} %get-tuple-element.14.keep, ...), custom_call_target="tpu_custom_call" | custom-call | tf_op jit(solution)/shard_map/pallas_call | solution.py:429
  115.1 2.9 %collective-permute-start.17 = (bf16[32,1024]{1,0:T(8,128)(2,1)S(1)}, bf16[32,1024]{1,0:T(8,128)(2,1)S(1)}, u32[]{:S(2)}, u32[]{:S(2)}) collective-permute-start(bf16[32,1024]{1,0:T(8,128)(2,1)S(1)} %get-tuple-element.19), channel_id=1, source_target_pairs={{0,4},{2,6},{4,0},{6,2},{1,5},{3,7},{5,1},{7,3},{8,12},{10,14},{12... | collective-permute-start | bytes 196616 | tf_op jit(solution)/shard_map/ppermute | solution.py:434
  119.8 1.5 %collective-permute-done.17.p2 = bf16[32,1024]{1,0:T(8,128)(2,1)S(1)} collective-permute-done((bf16[32,1024]{1,0:T(8,128)(2,1)S(1)}, bf16[32,1024]{1,0:T(8,128)(2,1)S(1)}, u32[]{:S(2)}, u32[]{:S(2)}) %collective-permute-start.17) | collective-permute-done | bytes 65568 | tf_op jit(solution)/shard_map/ppermute | solution.py:434
  (75 shorter events, 17.9 us)
Async XLA Ops:
  3.0 12.0 %copy-start = (bf16[32,1024]{1,0:T(8,128)(2,1)S(1)}, bf16[32,1024]{1,0:T(8,128)(2,1)}, u32[]{:S(2)}) copy-start(bf16[32,1024]{1,0:T(8,128)(2,1)} %t0.1) | copy-start | bytes 196612
  3.0 17.7 %copy-start.9 = (bf16[8,192]{1,0:T(8,128)(2,1)S(1)}, bf16[8,192]{1,0:T(8,128)(2,1)}, u32[]{:S(2)}) copy-start(bf16[8,192]{1,0:T(8,128)(2,1)} %param.19) | copy-start | bytes 9220
  3.0 24.7 %all-to-all-start = ((bf16[32,40,128]{2,1,0:T(8,128)(2,1)}), bf16[32,40,128]{2,1,0:T(8,128)(2,1)S(1)}, u32[]{:S(2)}, u32[]{:S(2)}) async-start(bf16[32,40,128]{2,1,0:T(8,128)(2,1)} %shard_map.131), calls=%async_computation | async-start | bytes 655360 | tf_op jit(solution)/shard_map/all_to_all | solution.py:369
  15.0 8.2 %collective-permute-start.1 = (bf16[32,1024]{1,0:T(8,128)(2,1)S(1)}, bf16[32,1024]{1,0:T(8,128)(2,1)S(1)}, u32[]{:S(2)}, u32[]{:S(2)}) collective-permute-start(bf16[32,1024]{1,0:T(8,128)(2,1)S(1)} %copy-done), channel_id=1, source_target_pairs={{0,4},{2,6},{4,0},{6,2},{1,5},{3,7},{5,1},{7,3},{8,12},{10,14},{12... | collective-permute-start | bytes 196616 | tf_op jit(solution)/shard_map/ppermute | solution.py:371
  18.0 5.2 %collective-permute-start = (bf16[32,1024]{1,0:T(8,128)(2,1)S(1)}, bf16[32,1024]{1,0:T(8,128)(2,1)S(1)}, u32[]{:S(2)}, u32[]{:S(2)}) collective-permute-start(bf16[32,1024]{1,0:T(8,128)(2,1)S(1)} %copy-done), channel_id=1, source_target_pairs={{0,2},{2,4},{4,6},{6,0},{1,3},{3,5},{5,7},{7,1},{8,10},{10,12},{12... | collective-permute-start | bytes 196616 | tf_op jit(solution)/shard_map/ppermute | solution.py:371
  18.4 4.8 %collective-permute-start.2 = (bf16[32,1024]{1,0:T(8,128)(2,1)S(1)}, bf16[32,1024]{1,0:T(8,128)(2,1)S(1)}, u32[]{:S(2)}, u32[]{:S(2)}) collective-permute-start(bf16[32,1024]{1,0:T(8,128)(2,1)S(1)} %copy-done), channel_id=1, source_target_pairs={{0,6},{2,0},{4,2},{6,4},{1,7},{3,1},{5,3},{7,5},{8,14},{10,8},{12,... | collective-permute-start | bytes 196616 | tf_op jit(solution)/shard_map/ppermute | solution.py:371
  29.2 11.6 %all-to-all-start.2 = ((bf16[8,72,128]{2,1,0:T(8,128)(2,1)}), bf16[8,72,128]{2,1,0:T(8,128)(2,1)S(1)}, u32[]{:S(2)}, u32[]{:S(2)}) async-start(bf16[8,72,128]{2,1,0:T(8,128)(2,1)} %get-tuple-element.13), calls=%async_computation.2 | async-start | bytes 294912 | tf_op jit(solution)/shard_map/all_to_all | solution.py:387
  41.7 17.7 %all-to-all-start.1 = ((bf16[32,64,128]{2,1,0:T(8,128)(2,1)}), bf16[32,64,128]{2,1,0:T(8,128)(2,1)S(1)}, u32[]{:S(2)}, u32[]{:S(2)}) async-start(bf16[32,64,128]{2,1,0:T(8,128)(2,1)} %broadcast_in_dim.10), calls=%async_computation.1 | async-start | bytes 1048576 | tf_op jit(solution)/shard_map/all_to_all | solution.py:392
  45.6 6.5 %collective-permute-start.10 = (bf16[8,72,128]{2,1,0:T(8,128)(2,1)S(1)}, bf16[8,72,128]{2,1,0:T(8,128)(2,1)S(1)}, u32[]{:S(2)}, u32[]{:S(2)}) collective-permute-start(bf16[8,72,128]{2,1,0:T(8,128)(2,1)S(1)} %all-to-all-done.2), channel_id=1, source_target_pairs={{0,24},{1,7},{2,26},{3,1},{4,28},{5,3},{6,30},{7,5},{8,0},{9,15},{... | collective-permute-start | bytes 442376 | tf_op jit(solution)/shard_map/ppermute | solution.py:388
  48.4 5.6 %collective-permute-start.9 = (bf16[8,72,128]{2,1,0:T(8,128)(2,1)S(1)}, bf16[8,72,128]{2,1,0:T(8,128)(2,1)S(1)}, u32[]{:S(2)}, u32[]{:S(2)}) collective-permute-start(bf16[8,72,128]{2,1,0:T(8,128)(2,1)S(1)} %all-to-all-done.2), channel_id=1, source_target_pairs={{0,16},{1,5},{2,18},{3,7},{4,20},{5,1},{6,22},{7,3},{8,24},{9,13},... | collective-permute-start | bytes 442376 | tf_op jit(solution)/shard_map/ppermute | solution.py:388
  48.8 7.0 %collective-permute-start.8 = (bf16[8,72,128]{2,1,0:T(8,128)(2,1)S(1)}, bf16[8,72,128]{2,1,0:T(8,128)(2,1)S(1)}, u32[]{:S(2)}, u32[]{:S(2)}) collective-permute-start(bf16[8,72,128]{2,1,0:T(8,128)(2,1)S(1)} %all-to-all-done.2), channel_id=1, source_target_pairs={{0,8},{1,3},{2,10},{3,5},{4,12},{5,7},{6,14},{7,1},{8,16},{9,11},{... | collective-permute-start | bytes 442376 | tf_op jit(solution)/shard_map/ppermute | solution.py:388
  55.9 40.5 %collective-permute-start.13 = (bf16[4,8,72,128]{3,2,1,0:T(8,128)(2,1)S(1)}, bf16[4,8,72,128]{3,2,1,0:T(8,128)(2,1)S(1)}, u32[]{:S(2)}, u32[]{:S(2)}) collective-permute-start(bf16[4,8,72,128]{3,2,1,0:T(8,128)(2,1)S(1)} %pad_maximum_fusion.b0), channel_id=1, source_target_pairs={{0,6},{1,25},{2,0},{3,27},{4,2},{5,29},{6,4},{7,31},{8,14},{9,1},{... | collective-permute-start | bytes 1769480 | tf_op jit(solution)/shard_map/ppermute | solution.py:390
  58.3 38.0 %collective-permute-start.12 = (bf16[4,8,72,128]{3,2,1,0:T(8,128)(2,1)S(1)}, bf16[4,8,72,128]{3,2,1,0:T(8,128)(2,1)S(1)}, u32[]{:S(2)}, u32[]{:S(2)}) collective-permute-start(bf16[4,8,72,128]{3,2,1,0:T(8,128)(2,1)S(1)} %pad_maximum_fusion.b0), channel_id=1, source_target_pairs={{0,4},{1,17},{2,6},{3,19},{4,0},{5,21},{6,2},{7,23},{8,12},{9,25},... | collective-permute-start | bytes 1769480 | tf_op jit(solution)/shard_map/ppermute | solution.py:390
  58.9 37.5 %collective-permute-start.11 = (bf16[4,8,72,128]{3,2,1,0:T(8,128)(2,1)S(1)}, bf16[4,8,72,128]{3,2,1,0:T(8,128)(2,1)S(1)}, u32[]{:S(2)}, u32[]{:S(2)}) collective-permute-start(bf16[4,8,72,128]{3,2,1,0:T(8,128)(2,1)S(1)} %pad_maximum_fusion.b0), channel_id=1, source_target_pairs={{0,2},{1,9},{2,4},{3,11},{4,6},{5,13},{6,0},{7,15},{8,10},{9,17},{... | collective-permute-start | bytes 1769480 | tf_op jit(solution)/shard_map/ppermute | solution.py:390
  59.4 35.4 %collective-permute-start.7 = (bf16[32,64,128]{2,1,0:T(8,128)(2,1)S(1)}, bf16[32,64,128]{2,1,0:T(8,128)(2,1)S(1)}, u32[]{:S(2)}, u32[]{:S(2)}) collective-permute-start(bf16[32,64,128]{2,1,0:T(8,128)(2,1)S(1)} %all-to-all-done.1.up_own.w_own), channel_id=1, source_target_pairs={{0,1},{1,0},{2,3},{3,2},{4,5},{5,4},{6,7},{7,6},{8,9},{9,8},{10,11... | collective-permute-start | bytes 1572872 | tf_op jit(solution)/shard_map/ppermute | solution.py:393
  75.2 1.6 %collective-permute-start.3 = (bf16[64,128]{1,0:T(8,128)(2,1)S(1)}, bf16[64,128]{1,0:T(8,128)(2,1)S(1)}, u32[]{:S(2)}, u32[]{:S(2)}) collective-permute-start(bf16[64,128]{1,0:T(8,128)(2,1)S(1)} %get-tuple-element.12), channel_id=1, source_target_pairs={{0,1},{1,0},{2,3},{3,2},{4,5},{5,4},{6,7},{7,6},{8,9},{9,8},{10,11... | collective-permute-start | bytes 49160 | tf_op jit(solution)/shard_map/ppermute | solution.py:394
  76.7 9.0 %collective-permute-start.6 = (bf16[2,64,128]{2,1,0:T(8,128)(2,1)S(1)}, bf16[2,64,128]{2,1,0:T(8,128)(2,1)S(1)}, u32[]{:S(2)}, u32[]{:S(2)}) collective-permute-start(bf16[2,64,128]{2,1,0:T(8,128)(2,1)S(1)} %pad_maximum_fusion.1.q0), channel_id=1, source_target_pairs={{0,6},{2,0},{4,2},{6,4},{1,7},{3,1},{5,3},{7,5},{8,14},{10,8},{12,... | collective-permute-start | bytes 98312 | tf_op jit(solution)/shard_map/ppermute | solution.py:395
  85.7 4.6 %collective-permute-start.5 = (bf16[2,64,128]{2,1,0:T(8,128)(2,1)S(1)}, bf16[2,64,128]{2,1,0:T(8,128)(2,1)S(1)}, u32[]{:S(2)}, u32[]{:S(2)}) collective-permute-start(bf16[2,64,128]{2,1,0:T(8,128)(2,1)S(1)} %pad_maximum_fusion.1.q0), channel_id=1, source_target_pairs={{0,4},{2,6},{4,0},{6,2},{1,5},{3,7},{5,1},{7,3},{8,12},{10,14},{12... | collective-permute-start | bytes 98312 | tf_op jit(solution)/shard_map/ppermute | solution.py:395
  90.3 4.5 %collective-permute-start.4 = (bf16[2,64,128]{2,1,0:T(8,128)(2,1)S(1)}, bf16[2,64,128]{2,1,0:T(8,128)(2,1)S(1)}, u32[]{:S(2)}, u32[]{:S(2)}) collective-permute-start(bf16[2,64,128]{2,1,0:T(8,128)(2,1)S(1)} %pad_maximum_fusion.1.q0), channel_id=1, source_target_pairs={{0,2},{2,4},{4,6},{6,0},{1,3},{3,5},{5,7},{7,1},{8,10},{10,12},{12... | collective-permute-start | bytes 98312 | tf_op jit(solution)/shard_map/ppermute | solution.py:395
  107.5 5.4 %collective-permute-start.15 = (f32[256,128]{1,0:T(8,128)S(1)}, f32[256,128]{1,0:T(8,128)S(1)}, u32[]{:S(2)}, u32[]{:S(2)}) collective-permute-start(f32[256,128]{1,0:T(8,128)S(1)} %get-tuple-element.16.ml_own), channel_id=1, source_target_pairs={{0,1},{1,0},{2,3},{3,2},{4,5},{5,4},{6,7},{7,6},{8,9},{9,8},{10,11... | collective-permute-start | bytes 393224 | tf_op jit(solution)/shard_map/ppermute | solution.py:428
  111.7 1.3 %collective-permute-start.14 = (bf16[128,256]{1,0:T(8,128)(2,1)S(1)}, bf16[128,256]{1,0:T(8,128)(2,1)S(1)}, u32[]{:S(2)}, u32[]{:S(2)}) collective-permute-start(bf16[128,256]{1,0:T(8,128)(2,1)S(1)} %get-tuple-element.15), channel_id=1, source_target_pairs={{0,1},{1,0},{2,3},{3,2},{4,5},{5,4},{6,7},{7,6},{8,9},{9,8},{10,11... | collective-permute-start | bytes 196616 | tf_op jit(solution)/shard_map/ppermute | solution.py:427
  115.0 4.9 %collective-permute-start.16 = (bf16[32,1024]{1,0:T(8,128)(2,1)S(1)}, bf16[32,1024]{1,0:T(8,128)(2,1)S(1)}, u32[]{:S(2)}, u32[]{:S(2)}) collective-permute-start(bf16[32,1024]{1,0:T(8,128)(2,1)S(1)} %get-tuple-element.18), channel_id=1, source_target_pairs={{0,2},{2,4},{4,6},{6,0},{1,3},{3,5},{5,7},{7,1},{8,10},{10,12},{12... | collective-permute-start | bytes 196616 | tf_op jit(solution)/shard_map/ppermute | solution.py:434
  115.1 6.3 %collective-permute-start.17 = (bf16[32,1024]{1,0:T(8,128)(2,1)S(1)}, bf16[32,1024]{1,0:T(8,128)(2,1)S(1)}, u32[]{:S(2)}, u32[]{:S(2)}) collective-permute-start(bf16[32,1024]{1,0:T(8,128)(2,1)S(1)} %get-tuple-element.19), channel_id=1, source_target_pairs={{0,4},{2,6},{4,0},{6,2},{1,5},{3,7},{5,1},{7,3},{8,12},{10,14},{12... | collective-permute-start | bytes 196616 | tf_op jit(solution)/shard_map/ppermute | solution.py:434
  118.0 3.9 %collective-permute-start.18 = (bf16[32,1024]{1,0:T(8,128)(2,1)S(1)}, bf16[32,1024]{1,0:T(8,128)(2,1)S(1)}, u32[]{:S(2)}, u32[]{:S(2)}) collective-permute-start(bf16[32,1024]{1,0:T(8,128)(2,1)S(1)} %get-tuple-element.20), channel_id=1, source_target_pairs={{0,6},{2,0},{4,2},{6,4},{1,7},{3,1},{5,3},{7,5},{8,14},{10,8},{12,... | collective-permute-start | bytes 196616 | tf_op jit(solution)/shard_map/ppermute | solution.py:434
  (10 other events, 12.8 us)

commit v3 on v2

--- a/solution.py
+++ b/solution.py
@@ -119,7 +119,7 @@
 
 
 def make_queries(
-    where, q0, q1, q2, q3, up_own, up_other, gain, out, latents
+    where, q0, q1, q2, q3, up_own, up_other, gain, out, uk_ref, uv_ref, docs_ref, latents
 ):
     y, c = where[2], where[3]
     for j, part in enumerate((q0, q1, q2, q3)):
@@ -132,77 +132,72 @@
     inverse = lax.rsqrt(mean + EPS)
     gains = jnp.concatenate([column(gain[0:1, :]), column(gain[1:2, :])], axis=0)
     gains = jnp.concatenate([gains, gains], axis=1)
-    latent = raw * inverse * gains
-    latent = jnp.transpose(latent).astype(BF)
-    lane = lanes((256, 128))
-    row = lax.broadcasted_iota(jnp.int32, (256, 128), 0)
-    pos = where[4] + 64 * ((row % 128) // 32) + 32 * (row // 128) + row % 32
-    angle = pos.astype(F32) * frequency(4 * ((lane % 32) // 8) + lane % 4)
-    used = lane < 64
-    is_low = (lane // 4) % 2 == 0
-    cos = jnp.where(used, jnp.cos(angle), 0.0)
-    sine = jnp.where(used, jnp.sin(angle), 0.0)
+    latent = (raw * inverse * gains).astype(BF)
+    tok = lanes((64, 256))
+    row = lax.broadcasted_iota(jnp.int32, (64, 256), 0)
+    pos = where[4] + 64 * ((tok % 128) // 32) + 32 * (tok // 128) + tok % 32
+    angle = pos.astype(F32) * frequency(4 * ((row % 32) // 8) + row % 4)
+    is_low = (row // 4) % 2 == 0
+    cos = jnp.cos(angle)
+    sine = jnp.sin(angle)
     low_sin = jnp.where(is_low, -sine, 0.0)
     high_sin = jnp.where(is_low, 0.0, sine)
     for p, up in enumerate((up_own, up_other)):
-        wide = up[...].astype(F32)
-        plain_w = wide[:, 0:8, :].reshape(256, 128).astype(BF)
-        rope_w = wide[:, 24:32, :].reshape(256, 128).astype(BF)
-        plain = jnp.dot(latent, plain_w, preferred_element_type=F32) * SCALE2
-        raw = jnp.dot(latent, rope_w, preferred_element_type=F32) * SCALE2
-        rope = (
-            raw * cos
-            + pltpu.roll(raw, 124, 1) * low_sin
-            + pltpu.roll(raw, 4, 1) * high_sin
-        )
+        wide = up[:, 0:32, :].astype(F32)
+        own = slice(128 * p, 128 * (p + 1))
+        plain_w = jnp.transpose(wide[:, 0:8, :].reshape(256, 128)).astype(BF)
+        rope_w = jnp.transpose(wide[:, 24:32, :].reshape(256, 128))[0:64, :].astype(BF)
+        uk_ref[:, own] = wide[:, 8:16, :].reshape(256, 128).astype(BF)
+        uv_ref[own, :] = jnp.transpose(wide[:, 16:24, :].reshape(256, 128)).astype(BF)
+        plain = (jnp.dot(plain_w, latent, preferred_element_type=F32) * SCALE2).astype(BF)
+        raw = jnp.dot(rope_w, latent, preferred_element_type=F32) * SCALE2
+        rope = raw * cos + pltpu.roll(raw, 60, 0) * low_sin + pltpu.roll(raw, 4, 0) * high_sin
+        rope = rope.astype(BF)
         for i in range(2):
-            own = slice(256 * i, 256 * (i + 1))
-            out[p, own, 0:128] = jnp.where(lane // 64 == i, plain, 0.0).astype(BF)
-            out[p, own, 128:256] = jnp.where(lane // 32 == i, rope, 0.0).astype(BF)
+            h = 2 * p + i
+            out[h] = jnp.zeros((256, 256), BF)
+            out[h, 64 * i : 64 * (i + 1), :] = plain[64 * i : 64 * (i + 1), :]
+            out[h, 128:160, :] = rope[32 * i : 32 * (i + 1), :]
+    docs = up_own[:, 24:32, :].astype(F32)
+    at = lanes((NS, 128))
+    spread = jnp.zeros((NS, 128), F32)
+    for k in range(NY):
+        piece = jnp.where(c == 0, docs[:, 2 * k, :], docs[:, 2 * k + 1, :])
+        spread = jnp.where(at // 32 == k, pltpu.roll(piece, (32 * k + 64) % 128, 1), spread)
+    docs_ref[...] = spread
 
 
 def attend(
-    where, q_ref, up_own, up_other, gain, query_docs, b0, b1, b2, b3,
-    keep_ref, send_ref, ml_ref, kb, s_buf, v_buf, mx, total, acc, uk, uv, gains, docs_col, key_docs, sems,
+    where, q_ref, uk, uv, key_docs, gain, query_docs, b0, b1, b2, b3,
+    keep_ref, send_ref, ml_ref, kb, s_buf, v_buf, mx, total, acc, gains,
 ):
     x0, y0, c = where[1], where[2], where[3]
-    copies = [
-        pltpu.make_async_copy(part, kb.at[j], sems.at[j]) for j, part in enumerate((b0, b1, b2, b3))
-    ]
-    for copy in copies:
-        copy.start()
-    for p, up in enumerate((up_own, up_other)):
-        wide = up[...].astype(F32)
-        own = slice(128 * p, 128 * (p + 1))
-        uk[own, :] = jnp.transpose(wide[:, 8:16, :].reshape(256, 128)).astype(BF)
-        uv[own, :] = jnp.transpose(wide[:, 16:24, :].reshape(256, 128)).astype(BF)
+    docs = key_docs[...]
+    at = lanes((NS, 128))
+    before = (at == 127) & (docs < where[5].astype(F32))
+    behind = (at == 0) & (docs > where[6].astype(F32))
+    low = jnp.sum(before.astype(jnp.int32))
+    high = NS - 1 - jnp.sum(behind.astype(jnp.int32))
+    first = low // 2
+    last = jnp.maximum(high // 2, first) + 1
+
+    def fetch(z, carry):
+        for j, part in enumerate((b0, b1, b2, b3)):
+            for k in range(4):
+                kb[j, k, z] = part[k, z]
+        return carry
+
+    lax.fori_loop(first // 2, (last + 1) // 2, fetch, 0)
     for i in range(2):
         gains[128 * i : 128 * (i + 1), :] = column(gain[i : i + 1, :])
-        docs_col[128 * i : 128 * (i + 1), :] = column(query_docs[i : i + 1, :])
-    docs = up_own[:, 24:32, :].astype(F32)
-    at = lanes((NS, 8, 128))
-    row = lax.broadcasted_iota(jnp.int32, (NS, 8, 128), 1)
-    before = (row == 7) & (at == 95) & (docs < where[5].astype(F32))
-    behind = (row == 0) & (at == 64) & (docs > where[6].astype(F32))
-    low = jnp.sum(before.astype(jnp.int32))
-    high = NS - 1 - jnp.sum(behind.astype(jnp.int32))
-    spread = jnp.zeros((NS, 128), F32)
-    at = lanes((NS, 128))
-    for y in range(NY):
-        piece = jnp.where(c == 0, docs[:, 2 * y, :], docs[:, 2 * y + 1, :])
-        spread = jnp.where(at // 32 == y, pltpu.roll(piece, (32 * y + 64) % 128, 1), spread)
-    key_docs[...] = spread
     mx[...] = jnp.full(mx.shape, NEG_BIG, F32)
     total[...] = jnp.zeros(total.shape, F32)
     acc[...] = jnp.zeros(acc.shape, F32)
-    for copy in copies:
-        copy.wait()
-    first = low // 2
-    last = high // 2 + 1
+    wanted = jnp.concatenate([query_docs[0:1, :], query_docs[1:2, :]], axis=1)
 
     def scores(tile, carry):
         z = tile // 2
-        latents, ropes = [], []
+        latents, ropes, same = [], [], []
         for half in range(2):
             x = 2 * lax.rem(tile, 2) + half
             jx = lax.rem(x0 - x + NX, NX)
@@ -219,98 +214,85 @@
                 squares = squares + part * part
             mean = jnp.sum(squares, axis=0, keepdims=True) * (1.0 / 256.0)
             inverse = lax.rsqrt(mean + EPS)
-            latent = jnp.concatenate(parts, axis=0) * inverse * gains[...]
-            latents.append(latent.astype(BF))
-            ropes.append(jnp.concatenate(turned, axis=0).astype(BF))
+            latents.append(jnp.concatenate(parts, axis=0) * inverse * gains[...])
+            ropes.append(jnp.concatenate(turned, axis=0))
+            docs_col = column(key_docs[pl.ds(2 * tile + half, 1), :])
+            same.append(jnp.concatenate([docs_col, docs_col], axis=1) == wanted)
         latent = jnp.concatenate(latents, axis=1)
+        v_buf[tile] = jnp.dot(uv[...], latent.astype(BF), preferred_element_type=F32).astype(BF)
+        turned = jnp.transpose(latent).astype(BF)
         rope = jnp.concatenate(ropes, axis=1)
-        keys = jnp.dot(uk[...], latent, preferred_element_type=F32).astype(BF)
-        values = jnp.dot(uv[...], latent, preferred_element_type=F32)
-        v_buf[tile] = jnp.transpose(values).astype(BF)
-        blank = jnp.zeros((64, 256), BF)
-        same = []
-        for half in range(2):
-            docs_row = key_docs[pl.ds(2 * tile + half, 1), :]
-            same.append(docs_col[...] == docs_row)
-        for p in range(2):
-            stack = jnp.concatenate([keys[128 * p : 128 * (p + 1), :], rope, rope, blank], axis=0)
-            for i in range(2):
-                own = slice(256 * i, 256 * (i + 1))
-                got = jnp.dot(q_ref[p, own, :], stack, preferred_element_type=F32)
-                lhs = jnp.where(same[0], got[:, 0:128], NEG_BIG)
-                rhs = jnp.where(same[1], got[:, 128:256], NEG_BIG)
-                s_buf[tile, 2 * p + i, :, 0:128] = lhs
-                s_buf[tile, 2 * p + i, :, 128:256] = rhs
-                mx[2 * p + i] = jnp.maximum(mx[2 * p + i], jnp.maximum(lhs, rhs))
+        rope = jnp.concatenate([rope, jnp.zeros((96, 256), F32)], axis=0)
+        rope = jnp.transpose(rope).astype(BF)
+        keys = jnp.dot(turned, uk[...], preferred_element_type=F32).astype(BF)
+        for h in range(4):
+            p = h // 2
+            stack = jnp.concatenate([keys[:, 128 * p : 128 * (p + 1)], rope], axis=1)
+            got = jnp.dot(stack, q_ref[h], preferred_element_type=F32)
+            got = jnp.concatenate(
+                [
+                    jnp.where(same[0], got[0:128, :], NEG_BIG),
+                    jnp.where(same[1], got[128:256, :], NEG_BIG),
+                ],
+                axis=0,
+            )
+            s_buf[tile, h] = got
+            mx[h] = jnp.maximum(mx[h], jnp.max(got.reshape(32, 8, 256), axis=0))
         return carry
 
     lax.fori_loop(first, last, scores, 0)
     tops = []
     for h in range(4):
-        top = jnp.max(mx[h], axis=1, keepdims=True)
-        top = jnp.maximum(top, FLOOR)
-        mx[h] = jnp.broadcast_to(top, (256, 128))
+        top = jnp.maximum(jnp.max(mx[h], axis=0, keepdims=True), FLOOR)
+        mx[h] = jnp.broadcast_to(top, (8, 256))
         tops.append(top)
 
     def weigh(tile, carry):
-        v = v_buf[tile]
-        lane = lanes((256, 256)) // 64
-        result = acc[...]
         for h in range(4):
-            top = mx[h]
-            lhs = jnp.exp2(s_buf[tile, h, :, 0:128] - top)
-            rhs = jnp.exp2(s_buf[tile, h, :, 128:256] - top)
-            total[h] = total[h] + lhs + rhs
-            weights = jnp.concatenate([lhs.astype(BF), rhs.astype(BF)], axis=1)
-            own = jnp.where(lane == h, v, jnp.zeros_like(v))
-            result = result + jnp.dot(weights, own, preferred_element_type=F32)
-        acc[...] = result
+            own = slice(64 * h, 64 * (h + 1))
+            weights = jnp.exp2(s_buf[tile, h].reshape(32, 8, 256) - mx[h][None])
+            total[h] = total[h] + jnp.sum(weights, axis=0)
+            weights = weights.reshape(256, 256).astype(BF)
+            acc[own, :] = acc[own, :] + jnp.dot(
+                v_buf[tile, own, :], weights, preferred_element_type=F32
+            )
         return carry
 
     lax.fori_loop(first, last, weigh, 0)
-    lane = lanes((256, 128))
-    packed = jnp.zeros((256, 128), F32)
     for h in range(4):
-        packed = jnp.where(lane == h, tops[h], packed)
-        packed = jnp.where(lane == 4 + h, jnp.sum(total[h], axis=1, keepdims=True), packed)
-    ml_ref[...] = packed
-    keep_ref[...] = acc[pl.ds(pl.multiple_of(c * 128, 128), 128), :]
-    send_ref[...] = acc[pl.ds(pl.multiple_of((1 - c) * 128, 128), 128), :].astype(BF)
+        ml_ref[h : h + 1, :] = tops[h]
+        ml_ref[4 + h : 5 + h, :] = jnp.sum(total[h], axis=0, keepdims=True)
+    left, right = acc[:, 0:128], acc[:, 128:256]
+    keep_ref[...] = jnp.where(c == 0, left, right)
+    send_ref[...] = jnp.where(c == 0, right, left).astype(BF)
 
 
 def combine(
     where, keep, got, ml_own, ml_got, w_own, w_other, part_ref, p1_ref, p2_ref, p3_ref, lse_ref,
-    f_own, f_got, scratch,
+    scratch,
 ):
     c = where[3]
-    own = ml_own[...]
-    other = ml_got[...]
-    for h in range(4):
-        k = (h + 2) % 4
-        m0, l0 = own[:, h : h + 1], own[:, 4 + h : 5 + h]
-        m1, l1 = other[:, k : k + 1], other[:, 4 + k : 5 + k]
-        top = jnp.maximum(m0, m1)
-        e0 = jnp.exp2(m0 - top)
-        e1 = jnp.exp2(m1 - top)
-        weight_sum = l0 * e0 + l1 * e1
-        if h < 2:
-            lse = (top + jnp.log2(weight_sum)) * LN2
-            for half in range(2):
-                for y in range(NY):
-                    lse_ref[64 * y + 32 * half : 64 * y + 32 * half + 32, h : h + 1] = lse[
-                        128 * half + 32 * y : 128 * half + 32 * y + 32, :
-                    ]
-        f_own[h] = jnp.broadcast_to(e0 / weight_sum, (256, 128))
-        f_got[h] = jnp.broadcast_to(e1 / weight_sum, (256, 128))
-    rows = pl.ds(pl.multiple_of(c * 128, 128), 128)
-    lane = lanes((128, 128)) // 64
+    m0, l0 = ml_own[0:4, :], ml_own[4:8, :]
+    m1 = jnp.concatenate([ml_got[2:4, :], ml_got[0:2, :]], axis=0)
+    l1 = jnp.concatenate([ml_got[6:8, :], ml_got[4:6, :]], axis=0)
+    top = jnp.maximum(m0, m1)
+    e0 = jnp.exp2(m0 - top)
+    e1 = jnp.exp2(m1 - top)
+    weight_sum = l0 * e0 + l1 * e1
+    lse_ref[...] = ((top + jnp.log2(weight_sum)) * LN2)[0:2, :]
+    f0 = e0 / weight_sum
+    f1 = e1 / weight_sum
+    f0 = jnp.where(c == 0, f0[:, 0:128], f0[:, 128:256])
+    f1 = jnp.where(c == 0, f1[:, 0:128], f1[:, 128:256])
     result = jnp.zeros((128, 1024), F32)
     for p, w in enumerate((w_own, w_other)):
-        a = jnp.where(lane == 0, f_own[2 * p, rows, :], f_own[2 * p + 1, rows, :])
-        b = jnp.where(lane == 0, f_got[2 * p, rows, :], f_got[2 * p + 1, rows, :])
-        mine = keep[:, 128 * p : 128 * (p + 1)]
-        theirs = got[:, 128 * (1 - p) : 128 * (2 - p)].astype(F32)
-        attended = (mine * a + theirs * b).astype(BF)
+        pieces = []
+        for i in range(2):
+            h, k = 2 * p + i, (2 * p + i + 2) % 4
+            mine = keep[64 * h : 64 * (h + 1), :]
+            theirs = got[64 * k : 64 * (k + 1), :].astype(F32)
+            pieces.append(mine * f0[h : h + 1, :] + theirs * f1[h : h + 1, :])
+        attended = jnp.transpose(jnp.concatenate(pieces, axis=0)).astype(BF)
         result = result + lax.dot_general(
             attended, w[:, 32:64, :].reshape(1024, 128), (((1,), (1,)), ((), ())),
             preferred_element_type=F32,
@@ -393,9 +375,15 @@
     up_other = lax.ppermute(up_own, "c", swap)
     q_pair = jnp.stack([q_part, lax.ppermute(q_part, "c", swap)])
     q_all = [q_pair] + [lax.ppermute(q_pair, "y", ring(j)) for j in range(1, NY)]
-    queries = call(
-        make_queries, jax.ShapeDtypeStruct((2, 512, 256), BF), 1, 7,
-        scratch=[VMEM((256, 256), F32)],
+    queries, uk, uv, key_docs = call(
+        make_queries,
+        (
+            jax.ShapeDtypeStruct((4, 256, 256), BF),
+            jax.ShapeDtypeStruct((256, 256), BF),
+            jax.ShapeDtypeStruct((256, 256), BF),
+            jax.ShapeDtypeStruct((NS, 128), F32),
+        ),
+        1, 7, scratch=[VMEM((256, 256), F32)],
     )(here, *q_all, up_own, up_other, query_gain.reshape(2, 128))
 
     there = jnp.concatenate([here, doc_ids[:1], doc_ids[255:]])
@@ -403,38 +391,34 @@
     keep, send, ml = call(
         attend,
         (
-            jax.ShapeDtypeStruct((128, 256), F32),
-            jax.ShapeDtypeStruct((128, 256), BF),
             jax.ShapeDtypeStruct((256, 128), F32),
+            jax.ShapeDtypeStruct((256, 128), BF),
+            jax.ShapeDtypeStruct((8, 256), F32),
         ),
-        1, 9, any_from=5, room=34,
+        1, 10, room=34,
         scratch=[
             VMEM((4, 4, NZ, 72, 128), BF),
             VMEM((16, 4, 256, 256), F32),
             VMEM((16, 256, 256), BF),
-            VMEM((4, 256, 128), F32),
-            VMEM((4, 256, 128), F32),
+            VMEM((4, 8, 256), F32),
+            VMEM((4, 8, 256), F32),
             VMEM((256, 256), F32),
-            VMEM((256, 256), BF),
-            VMEM((256, 256), BF),
             VMEM((256, 128), F32),
-            VMEM((256, 128), F32),
-            VMEM((NS, 128), F32),
-            pltpu.SemaphoreType.DMA((4,)),
         ],
-    )(there, queries, up_own, up_other, key_gain.reshape(2, 128), query_docs, held, *stage3)
+    )(there, queries, uk, uv, key_docs, key_gain.reshape(2, 128), query_docs, held, *stage3)
 
     got = lax.ppermute(send, "c", swap)
     ml_got = lax.ppermute(ml, "c", swap)
     *parts, log_sums = call(
         combine,
-        (jax.ShapeDtypeStruct((32, 1024), BF),) * NY + (jax.ShapeDtypeStruct((256, 2), F32),),
-        1, 6, scratch=[VMEM((4, 256, 128), F32), VMEM((4, 256, 128), F32), VMEM((128, 1024), F32)],
+        (jax.ShapeDtypeStruct((32, 1024), BF),) * NY + (jax.ShapeDtypeStruct((2, 256), F32),),
+        1, 6, scratch=[VMEM((128, 1024), F32)],
     )(here, keep, got, ml, ml_got, up_own, up_other)
     parts[1:] = [lax.ppermute(parts[j], "y", ring(j)) for j in range(1, NY)]
     mixed = call(finish, jax.ShapeDtypeStruct((32, 1024), BF), 0, 5)(
         *parts, out_gain.reshape(1, 1024)
     )
+    log_sums = log_sums.reshape(2, 2, 4, 32).transpose(2, 1, 3, 0).reshape(256, 2)
     return mixed, log_sums
 
 

time: 123 us -> 121 us (0.984)
  Pallas kernels: 17.9 us -> 15.3 us
    ppermute x1, starting transfers between devices: 0.1 us -> 4.2 us  [layer(): got = lax.ppermute(send, 'c', swap)]
    ppermute x1, starting transfers between devices: 4.16 us -> 0.1 us  [layer(): ml_got = lax.ppermute(ml, 'c', swap)]
    pallas_call x2, Pallas kernels: 12 us -> 10.5 us  [the longest x1 9.29 us: layer(): call(attend, (jax.ShapeDtypeStruct((256, 128), F32), jax.ShapeDtypeStruct...]
    unnamed x29 -> x28, local copies, waits for them, and re-layouts: 4.12 us -> 3.49 us
where the time goes in v3:
time: 121 us; the launch traced here: 120 us
  starting transfers between devices  59.4 us (49%)
  waiting for transfers between devices  36.7 us (30%)
  Pallas kernels  15.3 us (13%)
  local copies, waits for them, and re-layouts  7.63 us (6%)
    ppermute x1, starting transfers between devices, layer(): up_other = lax.ppermute(up_own, 'c', swap)  15.7 us
    ppermute x3, waiting for transfers between devices, layer(): lax.ppermute(q_pair, 'y', ring(j))  13.3 us
    all_to_all x1, starting transfers between devices, layer(): gathered = lax.all_to_all(message, SP, 0, 0)  12 us
    pallas_call x1, Pallas kernels, layer(): call(attend, (jax.ShapeDtypeStruct((256, 128), F32), jax.ShapeDtypeStruct...  9.29 us
    all_to_all x1, waiting for transfers between devices, layer(): stage1 = lax.all_to_all(k_part, 'z', 0, 0)  8.02 us
    ppermute x3, waiting for transfers between devices, layer(): lax.ppermute(stage1, AXES, shift_pairs(2, j))  6.33 us
    ppermute x3, starting transfers between devices, layer(): rows = [tokens] + [lax.ppermute(tokens, 'y', ring(j)) for j in range(1, NY)]  5.68 us
    all_to_all x1, waiting for transfers between devices, layer(): gathered = lax.all_to_all(message, SP, 0, 0)  4.44 us
  transfers between devices with their start and end apart: 22, of which 12 were waited for; matrix products, arithmetic and copies ran while one was open for 3% of the time, Pallas kernels for 1%

profile of v3, /device:TPU:1, one launch (start us, length us, event | category | flops | bytes accessed | tf_op | source)
XLA Modules:
  0.0 120.0 jit_solution(6249432404657264178)
XLA Ops:
  1.4 1.6 %shard_map.131 = bf16[32,40,128]{2,1,0:T(8,128)(2,1)} custom-call(s32[5]{0:T(128)S(1)} %stack.47.where, bf16[32,256]{1,0:T(8,128)(2,1)S(1)} %copy-done.1, bf16[32,256]{1,0:T(8,128)(2,1)S(1)} %copy-done.2, bf16[32,32]{1,0:T(8,128)(2,1)S(1)} %copy-done.3), custom_call_target="tpu_custom_call" | custom-call | tf_op jit(solution)/shard_map/pallas_call | solution.py:348
  3.0 12.0 %all-to-all-start = ((bf16[32,40,128]{2,1,0:T(8,128)(2,1)}), bf16[32,40,128]{2,1,0:T(8,128)(2,1)S(1)}, u32[]{:S(2)}, u32[]{:S(2)}) async-start(bf16[32,40,128]{2,1,0:T(8,128)(2,1)} %shard_map.131), calls=%async_computation | async-start | bytes 655360 | tf_op jit(solution)/shard_map/all_to_all | solution.py:351
  15.0 3.0 %collective-permute-start.1 = (bf16[32,1024]{1,0:T(8,128)(2,1)S(1)}, bf16[32,1024]{1,0:T(8,128)(2,1)S(1)}, u32[]{:S(2)}, u32[]{:S(2)}) collective-permute-start(bf16[32,1024]{1,0:T(8,128)(2,1)S(1)} %copy-done), channel_id=1, source_target_pairs={{0,4},{2,6},{4,0},{6,2},{1,5},{3,7},{5,1},{7,3},{8,12},{10,14},{12... | collective-permute-start | bytes 196616 | tf_op jit(solution)/shard_map/ppermute | solution.py:353
  18.4 2.3 %collective-permute-start.2 = (bf16[32,1024]{1,0:T(8,128)(2,1)S(1)}, bf16[32,1024]{1,0:T(8,128)(2,1)S(1)}, u32[]{:S(2)}, u32[]{:S(2)}) collective-permute-start(bf16[32,1024]{1,0:T(8,128)(2,1)S(1)} %copy-done), channel_id=1, source_target_pairs={{0,6},{2,0},{4,2},{6,4},{1,7},{3,1},{5,3},{7,5},{8,14},{10,8},{12,... | collective-permute-start | bytes 196616 | tf_op jit(solution)/shard_map/ppermute | solution.py:353
  23.2 4.4 %all-to-all-done.gathered = bf16[32,40,128]{2,1,0:T(8,128)(2,1)S(1)} async-done(((bf16[32,40,128]{2,1,0:T(8,128)(2,1)}), bf16[32,40,128]{2,1,0:T(8,128)(2,1)S(1)}, u32[]{:S(2)}, u32[]{:S(2)}) %all-to-all-start) | async-done | bytes 327712 | tf_op jit(solution)/shard_map/all_to_all | solution.py:351
  27.7 1.5 %shard_map.132 = (bf16[64,128]{1,0:T(8,128)(2,1)S(1)}, bf16[8,72,128]{2,1,0:T(8,128)(2,1)}) custom-call(s32[5]{0:T(128)S(1)} %stack.47.where, bf16[32,1024]{1,0:T(8,128)(2,1)S(1)} %copy-done, bf16[32,1024]{1,0:T(8,128)(2,1)S(1)} %collective-permute-done.t1, bf16[32,1024]{1,0:T(8,128)(2,1)S(1)} %collective-permute-done.1.t2, ...), custom_call_target="tpu_custom_call" | custom-call | tf_op jit(solution)/shard_map/pallas_call | solution.py:363
  29.2 3.5 %all-to-all-start.2 = ((bf16[8,72,128]{2,1,0:T(8,128)(2,1)}), bf16[8,72,128]{2,1,0:T(8,128)(2,1)S(1)}, u32[]{:S(2)}, u32[]{:S(2)}) async-start(bf16[8,72,128]{2,1,0:T(8,128)(2,1)} %get-tuple-element.21), calls=%async_computation.2 | async-start | bytes 294912 | tf_op jit(solution)/shard_map/all_to_all | solution.py:369
  32.8 8.0 %all-to-all-done.2 = bf16[8,72,128]{2,1,0:T(8,128)(2,1)S(1)} async-done(((bf16[8,72,128]{2,1,0:T(8,128)(2,1)}), bf16[8,72,128]{2,1,0:T(8,128)(2,1)S(1)}, u32[]{:S(2)}, u32[]{:S(2)}) %all-to-all-start.2) | async-done | bytes 147488 | tf_op jit(solution)/shard_map/all_to_all | solution.py:369
  41.7 3.9 %all-to-all-start.1 = ((bf16[32,64,128]{2,1,0:T(8,128)(2,1)}), bf16[32,64,128]{2,1,0:T(8,128)(2,1)S(1)}, u32[]{:S(2)}, u32[]{:S(2)}) async-start(bf16[32,64,128]{2,1,0:T(8,128)(2,1)} %broadcast_in_dim.10), calls=%async_computation.1 | async-start | bytes 1048576 | tf_op jit(solution)/shard_map/all_to_all | solution.py:374
  45.6 2.8 %collective-permute-start.10 = (bf16[8,72,128]{2,1,0:T(8,128)(2,1)S(1)}, bf16[8,72,128]{2,1,0:T(8,128)(2,1)S(1)}, u32[]{:S(2)}, u32[]{:S(2)}) collective-permute-start(bf16[8,72,128]{2,1,0:T(8,128)(2,1)S(1)} %all-to-all-done.2), channel_id=1, source_target_pairs={{0,24},{1,7},{2,26},{3,1},{4,28},{5,3},{6,30},{7,5},{8,0},{9,15},{... | collective-permute-start | bytes 442376 | tf_op jit(solution)/shard_map/ppermute | solution.py:370
  49.5 2.6 %collective-permute-done.10 = bf16[8,72,128]{2,1,0:T(8,128)(2,1)S(1)} collective-permute-done((bf16[8,72,128]{2,1,0:T(8,128)(2,1)S(1)}, bf16[8,72,128]{2,1,0:T(8,128)(2,1)S(1)}, u32[]{:S(2)}, u32[]{:S(2)}) %collective-permute-start.10) | collective-permute-done | bytes 147488 | tf_op jit(solution)/shard_map/ppermute | solution.py:370
  52.1 1.9 %collective-permute-done.9 = bf16[8,72,128]{2,1,0:T(8,128)(2,1)S(1)} collective-permute-done((bf16[8,72,128]{2,1,0:T(8,128)(2,1)S(1)}, bf16[8,72,128]{2,1,0:T(8,128)(2,1)S(1)}, u32[]{:S(2)}, u32[]{:S(2)}) %collective-permute-start.9) | collective-permute-done | bytes 147488 | tf_op jit(solution)/shard_map/ppermute | solution.py:370
  54.0 1.8 %collective-permute-done.8 = bf16[8,72,128]{2,1,0:T(8,128)(2,1)S(1)} collective-permute-done((bf16[8,72,128]{2,1,0:T(8,128)(2,1)S(1)}, bf16[8,72,128]{2,1,0:T(8,128)(2,1)S(1)}, u32[]{:S(2)}, u32[]{:S(2)}) %collective-permute-start.8) | collective-permute-done | bytes 147488 | tf_op jit(solution)/shard_map/ppermute | solution.py:370
  55.9 2.4 %collective-permute-start.13 = (bf16[4,8,72,128]{3,2,1,0:T(8,128)(2,1)S(1)}, bf16[4,8,72,128]{3,2,1,0:T(8,128)(2,1)S(1)}, u32[]{:S(2)}, u32[]{:S(2)}) collective-permute-start(bf16[4,8,72,128]{3,2,1,0:T(8,128)(2,1)S(1)} %pad_maximum_fusion.b0), channel_id=1, source_target_pairs={{0,6},{1,25},{2,0},{3,27},{4,2},{5,29},{6,4},{7,31},{8,14},{9,1},{... | collective-permute-start | bytes 1769480 | tf_op jit(solution)/shard_map/ppermute | solution.py:372
  59.5 15.7 %collective-permute-start.7 = (bf16[32,64,128]{2,1,0:T(8,128)(2,1)S(1)}, bf16[32,64,128]{2,1,0:T(8,128)(2,1)S(1)}, u32[]{:S(2)}, u32[]{:S(2)}) collective-permute-start(bf16[32,64,128]{2,1,0:T(8,128)(2,1)S(1)} %all-to-all-done.1.up_own.w_own), channel_id=1, source_target_pairs={{0,1},{1,0},{2,3},{3,2},{4,5},{5,4},{6,7},{7,6},{8,9},{9,8},{10,11... | collective-permute-start | bytes 1572872 | tf_op jit(solution)/shard_map/ppermute | solution.py:375
  75.2 1.6 %collective-permute-done.3 = bf16[64,128]{1,0:T(8,128)(2,1)S(1)} collective-permute-done((bf16[64,128]{1,0:T(8,128)(2,1)S(1)}, bf16[64,128]{1,0:T(8,128)(2,1)S(1)}, u32[]{:S(2)}, u32[]{:S(2)}) %collective-permute-start.3) | collective-permute-done | bytes 16416 | tf_op jit(solution)/shard_map/ppermute | solution.py:376
  76.7 1.9 %collective-permute-start.6 = (bf16[2,64,128]{2,1,0:T(8,128)(2,1)S(1)}, bf16[2,64,128]{2,1,0:T(8,128)(2,1)S(1)}, u32[]{:S(2)}, u32[]{:S(2)}) collective-permute-start(bf16[2,64,128]{2,1,0:T(8,128)(2,1)S(1)} %pad_maximum_fusion.1.q0), channel_id=1, source_target_pairs={{0,6},{2,0},{4,2},{6,4},{1,7},{3,1},{5,3},{7,5},{8,14},{10,8},{12,... | collective-permute-start | bytes 98312 | tf_op jit(solution)/shard_map/ppermute | solution.py:377
  78.6 7.1 %collective-permute-done.6.q3 = bf16[2,64,128]{2,1,0:T(8,128)(2,1)S(1)} collective-permute-done((bf16[2,64,128]{2,1,0:T(8,128)(2,1)S(1)}, bf16[2,64,128]{2,1,0:T(8,128)(2,1)S(1)}, u32[]{:S(2)}, u32[]{:S(2)}) %collective-permute-start.6) | collective-permute-done | bytes 32800 | tf_op jit(solution)/shard_map/ppermute | solution.py:377
  85.7 4.6 %collective-permute-done.5.q2 = bf16[2,64,128]{2,1,0:T(8,128)(2,1)S(1)} collective-permute-done((bf16[2,64,128]{2,1,0:T(8,128)(2,1)S(1)}, bf16[2,64,128]{2,1,0:T(8,128)(2,1)S(1)}, u32[]{:S(2)}, u32[]{:S(2)}) %collective-permute-start.5) | collective-permute-done | bytes 32800 | tf_op jit(solution)/shard_map/ppermute | solution.py:377
  93.2 1.6 %collective-permute-done.4.q1 = bf16[2,64,128]{2,1,0:T(8,128)(2,1)S(1)} collective-permute-done((bf16[2,64,128]{2,1,0:T(8,128)(2,1)S(1)}, bf16[2,64,128]{2,1,0:T(8,128)(2,1)S(1)}, u32[]{:S(2)}, u32[]{:S(2)}) %collective-permute-start.4) | collective-permute-done | bytes 32800 | tf_op jit(solution)/shard_map/ppermute | solution.py:377
  96.7 9.3 %shard_map.134 = (f32[256,128]{1,0:T(8,128)S(1)}, bf16[256,128]{1,0:T(8,128)(2,1)S(1)}, f32[8,256]{1,0:T(8,128)S(1)}) custom-call(s32[7]{0:T(128)S(1)} %concatenate.10.where, bf16[4,256,256]{2,1,0:T(8,128)(2,1)S(1)} %get-tuple-element.17.q_ref, bf16[256,256]{1,0:T(8,128)(2,1)S(1)} %get-tuple-element.18.uk, bf16[256,256]{1,0:T(8,128)(2,1)S(1)} %get-tuple-element.19.uv, ...), custom_call_target="tpu_custom_call" | custom-call | tf_op jit(solution)/shard_map/pallas_call | solution.py:391
  106.0 4.2 %collective-permute-start.14 = (bf16[256,128]{1,0:T(8,128)(2,1)S(1)}, bf16[256,128]{1,0:T(8,128)(2,1)S(1)}, u32[]{:S(2)}, u32[]{:S(2)}) collective-permute-start(bf16[256,128]{1,0:T(8,128)(2,1)S(1)} %get-tuple-element.23), channel_id=1, source_target_pairs={{0,1},{1,0},{2,3},{3,2},{4,5},{5,4},{6,7},{7,6},{8,9},{9,8},{10,11... | collective-permute-start | bytes 196616 | tf_op jit(solution)/shard_map/ppermute | solution.py:410
  112.4 2.9 %collective-permute-start.17 = (bf16[32,1024]{1,0:T(8,128)(2,1)S(1)}, bf16[32,1024]{1,0:T(8,128)(2,1)S(1)}, u32[]{:S(2)}, u32[]{:S(2)}) collective-permute-start(bf16[32,1024]{1,0:T(8,128)(2,1)S(1)} %get-tuple-element.27), channel_id=1, source_target_pairs={{0,4},{2,6},{4,0},{6,2},{1,5},{3,7},{5,1},{7,3},{8,12},{10,14},{12... | collective-permute-start | bytes 196616 | tf_op jit(solution)/shard_map/ppermute | solution.py:417
  117.3 1.5 %collective-permute-done.17.p2 = bf16[32,1024]{1,0:T(8,128)(2,1)S(1)} collective-permute-done((bf16[32,1024]{1,0:T(8,128)(2,1)S(1)}, bf16[32,1024]{1,0:T(8,128)(2,1)S(1)}, u32[]{:S(2)}, u32[]{:S(2)}) %collective-permute-start.17) | collective-permute-done | bytes 65568 | tf_op jit(solution)/shard_map/ppermute | solution.py:417
  (77 shorter events, 17.0 us)
Async XLA Ops:
  3.0 12.0 %copy-start = (bf16[32,1024]{1,0:T(8,128)(2,1)S(1)}, bf16[32,1024]{1,0:T(8,128)(2,1)}, u32[]{:S(2)}) copy-start(bf16[32,1024]{1,0:T(8,128)(2,1)} %t0.1) | copy-start | bytes 196612
  3.0 17.7 %copy-start.9 = (bf16[8,192]{1,0:T(8,128)(2,1)S(1)}, bf16[8,192]{1,0:T(8,128)(2,1)}, u32[]{:S(2)}) copy-start(bf16[8,192]{1,0:T(8,128)(2,1)} %param.19) | copy-start | bytes 9220
  3.0 24.7 %all-to-all-start = ((bf16[32,40,128]{2,1,0:T(8,128)(2,1)}), bf16[32,40,128]{2,1,0:T(8,128)(2,1)S(1)}, u32[]{:S(2)}, u32[]{:S(2)}) async-start(bf16[32,40,128]{2,1,0:T(8,128)(2,1)} %shard_map.131), calls=%async_computation | async-start | bytes 655360 | tf_op jit(solution)/shard_map/all_to_all | solution.py:351
  15.0 8.2 %collective-permute-start.1 = (bf16[32,1024]{1,0:T(8,128)(2,1)S(1)}, bf16[32,1024]{1,0:T(8,128)(2,1)S(1)}, u32[]{:S(2)}, u32[]{:S(2)}) collective-permute-start(bf16[32,1024]{1,0:T(8,128)(2,1)S(1)} %copy-done), channel_id=1, source_target_pairs={{0,4},{2,6},{4,0},{6,2},{1,5},{3,7},{5,1},{7,3},{8,12},{10,14},{12... | collective-permute-start | bytes 196616 | tf_op jit(solution)/shard_map/ppermute | solution.py:353
  18.0 5.2 %collective-permute-start = (bf16[32,1024]{1,0:T(8,128)(2,1)S(1)}, bf16[32,1024]{1,0:T(8,128)(2,1)S(1)}, u32[]{:S(2)}, u32[]{:S(2)}) collective-permute-start(bf16[32,1024]{1,0:T(8,128)(2,1)S(1)} %copy-done), channel_id=1, source_target_pairs={{0,2},{2,4},{4,6},{6,0},{1,3},{3,5},{5,7},{7,1},{8,10},{10,12},{12... | collective-permute-start | bytes 196616 | tf_op jit(solution)/shard_map/ppermute | solution.py:353
  18.4 4.8 %collective-permute-start.2 = (bf16[32,1024]{1,0:T(8,128)(2,1)S(1)}, bf16[32,1024]{1,0:T(8,128)(2,1)S(1)}, u32[]{:S(2)}, u32[]{:S(2)}) collective-permute-start(bf16[32,1024]{1,0:T(8,128)(2,1)S(1)} %copy-done), channel_id=1, source_target_pairs={{0,6},{2,0},{4,2},{6,4},{1,7},{3,1},{5,3},{7,5},{8,14},{10,8},{12,... | collective-permute-start | bytes 196616 | tf_op jit(solution)/shard_map/ppermute | solution.py:353
  29.2 11.6 %all-to-all-start.2 = ((bf16[8,72,128]{2,1,0:T(8,128)(2,1)}), bf16[8,72,128]{2,1,0:T(8,128)(2,1)S(1)}, u32[]{:S(2)}, u32[]{:S(2)}) async-start(bf16[8,72,128]{2,1,0:T(8,128)(2,1)} %get-tuple-element.21), calls=%async_computation.2 | async-start | bytes 294912 | tf_op jit(solution)/shard_map/all_to_all | solution.py:369
  41.7 17.7 %all-to-all-start.1 = ((bf16[32,64,128]{2,1,0:T(8,128)(2,1)}), bf16[32,64,128]{2,1,0:T(8,128)(2,1)S(1)}, u32[]{:S(2)}, u32[]{:S(2)}) async-start(bf16[32,64,128]{2,1,0:T(8,128)(2,1)} %broadcast_in_dim.10), calls=%async_computation.1 | async-start | bytes 1048576 | tf_op jit(solution)/shard_map/all_to_all | solution.py:374
  45.6 6.5 %collective-permute-start.10 = (bf16[8,72,128]{2,1,0:T(8,128)(2,1)S(1)}, bf16[8,72,128]{2,1,0:T(8,128)(2,1)S(1)}, u32[]{:S(2)}, u32[]{:S(2)}) collective-permute-start(bf16[8,72,128]{2,1,0:T(8,128)(2,1)S(1)} %all-to-all-done.2), channel_id=1, source_target_pairs={{0,24},{1,7},{2,26},{3,1},{4,28},{5,3},{6,30},{7,5},{8,0},{9,15},{... | collective-permute-start | bytes 442376 | tf_op jit(solution)/shard_map/ppermute | solution.py:370
  48.4 5.6 %collective-permute-start.9 = (bf16[8,72,128]{2,1,0:T(8,128)(2,1)S(1)}, bf16[8,72,128]{2,1,0:T(8,128)(2,1)S(1)}, u32[]{:S(2)}, u32[]{:S(2)}) collective-permute-start(bf16[8,72,128]{2,1,0:T(8,128)(2,1)S(1)} %all-to-all-done.2), channel_id=1, source_target_pairs={{0,16},{1,5},{2,18},{3,7},{4,20},{5,1},{6,22},{7,3},{8,24},{9,13},... | collective-permute-start | bytes 442376 | tf_op jit(solution)/shard_map/ppermute | solution.py:370
  48.8 7.0 %collective-permute-start.8 = (bf16[8,72,128]{2,1,0:T(8,128)(2,1)S(1)}, bf16[8,72,128]{2,1,0:T(8,128)(2,1)S(1)}, u32[]{:S(2)}, u32[]{:S(2)}) collective-permute-start(bf16[8,72,128]{2,1,0:T(8,128)(2,1)S(1)} %all-to-all-done.2), channel_id=1, source_target_pairs={{0,8},{1,3},{2,10},{3,5},{4,12},{5,7},{6,14},{7,1},{8,16},{9,11},{... | collective-permute-start | bytes 442376 | tf_op jit(solution)/shard_map/ppermute | solution.py:370
  55.9 40.1 %collective-permute-start.13 = (bf16[4,8,72,128]{3,2,1,0:T(8,128)(2,1)S(1)}, bf16[4,8,72,128]{3,2,1,0:T(8,128)(2,1)S(1)}, u32[]{:S(2)}, u32[]{:S(2)}) collective-permute-start(bf16[4,8,72,128]{3,2,1,0:T(8,128)(2,1)S(1)} %pad_maximum_fusion.b0), channel_id=1, source_target_pairs={{0,6},{1,25},{2,0},{3,27},{4,2},{5,29},{6,4},{7,31},{8,14},{9,1},{... | collective-permute-start | bytes 1769480 | tf_op jit(solution)/shard_map/ppermute | solution.py:372
  58.3 37.7 %collective-permute-start.12 = (bf16[4,8,72,128]{3,2,1,0:T(8,128)(2,1)S(1)}, bf16[4,8,72,128]{3,2,1,0:T(8,128)(2,1)S(1)}, u32[]{:S(2)}, u32[]{:S(2)}) collective-permute-start(bf16[4,8,72,128]{3,2,1,0:T(8,128)(2,1)S(1)} %pad_maximum_fusion.b0), channel_id=1, source_target_pairs={{0,4},{1,17},{2,6},{3,19},{4,0},{5,21},{6,2},{7,23},{8,12},{9,25},... | collective-permute-start | bytes 1769480 | tf_op jit(solution)/shard_map/ppermute | solution.py:372
  58.9 37.2 %collective-permute-start.11 = (bf16[4,8,72,128]{3,2,1,0:T(8,128)(2,1)S(1)}, bf16[4,8,72,128]{3,2,1,0:T(8,128)(2,1)S(1)}, u32[]{:S(2)}, u32[]{:S(2)}) collective-permute-start(bf16[4,8,72,128]{3,2,1,0:T(8,128)(2,1)S(1)} %pad_maximum_fusion.b0), channel_id=1, source_target_pairs={{0,2},{1,9},{2,4},{3,11},{4,6},{5,13},{6,0},{7,15},{8,10},{9,17},{... | collective-permute-start | bytes 1769480 | tf_op jit(solution)/shard_map/ppermute | solution.py:372
  59.5 35.4 %collective-permute-start.7 = (bf16[32,64,128]{2,1,0:T(8,128)(2,1)S(1)}, bf16[32,64,128]{2,1,0:T(8,128)(2,1)S(1)}, u32[]{:S(2)}, u32[]{:S(2)}) collective-permute-start(bf16[32,64,128]{2,1,0:T(8,128)(2,1)S(1)} %all-to-all-done.1.up_own.w_own), channel_id=1, source_target_pairs={{0,1},{1,0},{2,3},{3,2},{4,5},{5,4},{6,7},{7,6},{8,9},{9,8},{10,11... | collective-permute-start | bytes 1572872 | tf_op jit(solution)/shard_map/ppermute | solution.py:375
  75.2 1.6 %collective-permute-start.3 = (bf16[64,128]{1,0:T(8,128)(2,1)S(1)}, bf16[64,128]{1,0:T(8,128)(2,1)S(1)}, u32[]{:S(2)}, u32[]{:S(2)}) collective-permute-start(bf16[64,128]{1,0:T(8,128)(2,1)S(1)} %get-tuple-element.16), channel_id=1, source_target_pairs={{0,1},{1,0},{2,3},{3,2},{4,5},{5,4},{6,7},{7,6},{8,9},{9,8},{10,11... | collective-permute-start | bytes 49160 | tf_op jit(solution)/shard_map/ppermute | solution.py:376
  76.7 8.9 %collective-permute-start.6 = (bf16[2,64,128]{2,1,0:T(8,128)(2,1)S(1)}, bf16[2,64,128]{2,1,0:T(8,128)(2,1)S(1)}, u32[]{:S(2)}, u32[]{:S(2)}) collective-permute-start(bf16[2,64,128]{2,1,0:T(8,128)(2,1)S(1)} %pad_maximum_fusion.1.q0), channel_id=1, source_target_pairs={{0,6},{2,0},{4,2},{6,4},{1,7},{3,1},{5,3},{7,5},{8,14},{10,8},{12,... | collective-permute-start | bytes 98312 | tf_op jit(solution)/shard_map/ppermute | solution.py:377
  85.7 4.6 %collective-permute-start.5 = (bf16[2,64,128]{2,1,0:T(8,128)(2,1)S(1)}, bf16[2,64,128]{2,1,0:T(8,128)(2,1)S(1)}, u32[]{:S(2)}, u32[]{:S(2)}) collective-permute-start(bf16[2,64,128]{2,1,0:T(8,128)(2,1)S(1)} %pad_maximum_fusion.1.q0), channel_id=1, source_target_pairs={{0,4},{2,6},{4,0},{6,2},{1,5},{3,7},{5,1},{7,3},{8,12},{10,14},{12... | collective-permute-start | bytes 98312 | tf_op jit(solution)/shard_map/ppermute | solution.py:377
  90.3 4.5 %collective-permute-start.4 = (bf16[2,64,128]{2,1,0:T(8,128)(2,1)S(1)}, bf16[2,64,128]{2,1,0:T(8,128)(2,1)S(1)}, u32[]{:S(2)}, u32[]{:S(2)}) collective-permute-start(bf16[2,64,128]{2,1,0:T(8,128)(2,1)S(1)} %pad_maximum_fusion.1.q0), channel_id=1, source_target_pairs={{0,2},{2,4},{4,6},{6,0},{1,3},{3,5},{5,7},{7,1},{8,10},{10,12},{12... | collective-permute-start | bytes 98312 | tf_op jit(solution)/shard_map/ppermute | solution.py:377
  106.0 5.4 %collective-permute-start.14 = (bf16[256,128]{1,0:T(8,128)(2,1)S(1)}, bf16[256,128]{1,0:T(8,128)(2,1)S(1)}, u32[]{:S(2)}, u32[]{:S(2)}) collective-permute-start(bf16[256,128]{1,0:T(8,128)(2,1)S(1)} %get-tuple-element.23), channel_id=1, source_target_pairs={{0,1},{1,0},{2,3},{3,2},{4,5},{5,4},{6,7},{7,6},{8,9},{9,8},{10,11... | collective-permute-start | bytes 196616 | tf_op jit(solution)/shard_map/ppermute | solution.py:410
  110.2 1.2 collective-permute-start.15
  112.4 4.9 %collective-permute-start.16 = (bf16[32,1024]{1,0:T(8,128)(2,1)S(1)}, bf16[32,1024]{1,0:T(8,128)(2,1)S(1)}, u32[]{:S(2)}, u32[]{:S(2)}) collective-permute-start(bf16[32,1024]{1,0:T(8,128)(2,1)S(1)} %get-tuple-element.26), channel_id=1, source_target_pairs={{0,2},{2,4},{4,6},{6,0},{1,3},{3,5},{5,7},{7,1},{8,10},{10,12},{12... | collective-permute-start | bytes 196616 | tf_op jit(solution)/shard_map/ppermute | solution.py:417
  112.4 6.3 %collective-permute-start.17 = (bf16[32,1024]{1,0:T(8,128)(2,1)S(1)}, bf16[32,1024]{1,0:T(8,128)(2,1)S(1)}, u32[]{:S(2)}, u32[]{:S(2)}) collective-permute-start(bf16[32,1024]{1,0:T(8,128)(2,1)S(1)} %get-tuple-element.27), channel_id=1, source_target_pairs={{0,4},{2,6},{4,0},{6,2},{1,5},{3,7},{5,1},{7,3},{8,12},{10,14},{12... | collective-permute-start | bytes 196616 | tf_op jit(solution)/shard_map/ppermute | solution.py:417
  115.4 3.9 %collective-permute-start.18 = (bf16[32,1024]{1,0:T(8,128)(2,1)S(1)}, bf16[32,1024]{1,0:T(8,128)(2,1)S(1)}, u32[]{:S(2)}, u32[]{:S(2)}) collective-permute-start(bf16[32,1024]{1,0:T(8,128)(2,1)S(1)} %get-tuple-element.28), channel_id=1, source_target_pairs={{0,6},{2,0},{4,2},{6,4},{1,7},{3,1},{5,3},{7,5},{8,14},{10,8},{12,... | collective-permute-start | bytes 196616 | tf_op jit(solution)/shard_map/ppermute | solution.py:417
  (10 other events, 12.8 us)

commit v4 on v3

--- a/solution.py
+++ b/solution.py
@@ -79,18 +79,47 @@
     flipped[...] = jnp.transpose(jnp.concatenate([rope] * 4, axis=0))
     turned = jnp.concatenate([flipped[pl.ds(4 * y, 4), :], flipped[pl.ds(16 + 4 * y, 4), :]], axis=0)
     turned = turned.astype(BF)
-    for s in range(NS):
-        out[s, 0:32, :] = block
-        out[s, 32:40, :] = turned
-
-
-def project(where, t0, t1, t2, t3, gathered, q_ref, k_ref, tok):
+    for z in range(NZ):
+        out[z, 0:32, :] = block
+        out[z, 32:40, :] = turned
+
+
+def pack_later(up_query, up_key, up_value, docs_ref, out_t, out):
+    src = lax.broadcasted_iota(jnp.int32, (192, 256), 0)
+    lane = lanes((192, 256))
+    plain = 96 * (lane // 64) + lane % 64
+    turn = lane - 128
+    rope = 64 + 96 * (turn // 32) + 16 * ((turn // 4) % 2) + 4 * ((turn % 32) // 8) + turn % 4
+    chosen = jnp.where(lane < 128, plain, jnp.where(lane < 192, rope, -1))
+    pick = jnp.where(src == chosen, 1.0, 0.0).astype(BF)
+    sorted_query = jnp.dot(up_query[...], pick, preferred_element_type=F32)
+    out[0:8, :] = sorted_query[:, 0:128].astype(BF)
+    out[8:16, :] = up_key[...]
+    out[16:24, :] = up_value[...]
+    mixed = sorted_query[:, 128:256]
+    docs = docs_ref[...].astype(F32)
+    row = lax.broadcasted_iota(jnp.int32, (8, 128), 0)
+    at = lanes((8, 128))
+    for r in range(8):
+        line = docs[r // 4 : r // 4 + 1, :]
+        moved = pltpu.roll(jnp.broadcast_to(line, (8, 128)), (64 - 32 * (r % 4)) % 128, 1)
+        mixed = jnp.where((row == r) & (at // 32 == 2), moved, mixed)
+    out[24:32, :] = mixed.astype(BF)
+    out[32:64, :] = out_t[...]
+
+
+def project(where, t0, t1, t2, t3, g0, g1, g2, g3, q_ref, k_ref, tok, gathered):
+    x = where[1]
     y = where[2]
     for j, part in enumerate((t0, t1, t2, t3)):
         at = lax.rem(y - j + NY, NY)
         tok[pl.ds(pl.multiple_of(at * 32, 32), 32), :] = part[...]
+    for j, part in enumerate((g0, g1, g2, g3)):
+        gathered[lax.rem(x - j + NX, NX)] = part[...]
     rows = tok[...]
-    weights = gathered[:, 0:32, :].reshape(NS * 32, 128)
+    weights = jnp.concatenate(
+        [gathered[k, z, 0:32, :] for z in range(NZ) for k in range(NX)], axis=0
+    )
     both = jnp.dot(rows, weights, preferred_element_type=F32)
     turned = jnp.transpose(both).astype(BF)
     q_ref[...] = turned[0:64, :]
@@ -99,9 +128,9 @@
     group = lanes((8, 128)) // 32
     pieces = []
     for z in range(NZ):
-        piece = gathered[4 * z, 32:40, :].astype(F32)
+        piece = gathered[0, z, 32:40, :].astype(F32)
         for g in range(1, 4):
-            piece = jnp.where(group == g, gathered[4 * z + g, 32:40, :].astype(F32), piece)
+            piece = jnp.where(group == g, gathered[g, z, 32:40, :].astype(F32), piece)
         pieces.append(piece)
     rope = jnp.concatenate(pieces, axis=1)
     rope = jnp.concatenate([rope, jnp.zeros_like(rope)], axis=0).astype(BF)
@@ -119,9 +148,9 @@
 
 
 def make_queries(
-    where, q0, q1, q2, q3, up_own, up_other, gain, out, uk_ref, uv_ref, docs_ref, latents
+    where, q0, q1, q2, q3, up_own, up_other, gain, out, uk_ref, uv_ref, docs_ref, latents, ups
 ):
-    y, c = where[2], where[3]
+    x, y, c = where[1], where[2], where[3]
     for j, part in enumerate((q0, q1, q2, q3)):
         own, other = part[0].astype(F32), part[1].astype(F32)
         rows = pl.ds(pl.multiple_of(lax.rem(y - j + NY, NY) * 64, 64), 64)
@@ -143,7 +172,9 @@
     low_sin = jnp.where(is_low, -sine, 0.0)
     high_sin = jnp.where(is_low, 0.0, sine)
     for p, up in enumerate((up_own, up_other)):
-        wide = up[:, 0:32, :].astype(F32)
+        for j in range(NX):
+            ups[p, :, lax.rem(x - j + NX, NX)] = up[:, j, 0:32, :]
+        wide = ups[p].reshape(NS, 32, 128).astype(F32)
         own = slice(128 * p, 128 * (p + 1))
         plain_w = jnp.transpose(wide[:, 0:8, :].reshape(256, 128)).astype(BF)
         rope_w = jnp.transpose(wide[:, 24:32, :].reshape(256, 128))[0:64, :].astype(BF)
@@ -158,7 +189,7 @@
             out[h] = jnp.zeros((256, 256), BF)
             out[h, 64 * i : 64 * (i + 1), :] = plain[64 * i : 64 * (i + 1), :]
             out[h, 128:160, :] = rope[32 * i : 32 * (i + 1), :]
-    docs = up_own[:, 24:32, :].astype(F32)
+    docs = ups[0].reshape(NS, 32, 128)[:, 24:32, :].astype(F32)
     at = lanes((NS, 128))
     spread = jnp.zeros((NS, 128), F32)
     for k in range(NY):
@@ -168,14 +199,14 @@
 
 
 def attend(
-    where, q_ref, uk, uv, key_docs, gain, query_docs, b0, b1, b2, b3,
+    where, ids, q_ref, uk, uv, key_docs, gain, query_docs, b0, b1, b2, b3,
     keep_ref, send_ref, ml_ref, kb, s_buf, v_buf, mx, total, acc, gains,
 ):
     x0, y0, c = where[1], where[2], where[3]
     docs = key_docs[...]
     at = lanes((NS, 128))
-    before = (at == 127) & (docs < where[5].astype(F32))
-    behind = (at == 0) & (docs > where[6].astype(F32))
+    before = (at == 127) & (docs < ids[0].astype(F32))
+    behind = (at == 0) & (docs > ids[255].astype(F32))
     low = jnp.sum(before.astype(jnp.int32))
     high = NS - 1 - jnp.sum(behind.astype(jnp.int32))
     first = low // 2
@@ -269,9 +300,9 @@
 
 def combine(
     where, keep, got, ml_own, ml_got, w_own, w_other, part_ref, p1_ref, p2_ref, p3_ref, lse_ref,
-    scratch,
+    scratch, outs,
 ):
-    c = where[3]
+    x, c = where[1], where[3]
     m0, l0 = ml_own[0:4, :], ml_own[4:8, :]
     m1 = jnp.concatenate([ml_got[2:4, :], ml_got[0:2, :]], axis=0)
     l1 = jnp.concatenate([ml_got[6:8, :], ml_got[4:6, :]], axis=0)
@@ -293,8 +324,10 @@
             theirs = got[64 * k : 64 * (k + 1), :].astype(F32)
             pieces.append(mine * f0[h : h + 1, :] + theirs * f1[h : h + 1, :])
         attended = jnp.transpose(jnp.concatenate(pieces, axis=0)).astype(BF)
+        for j in range(NX):
+            outs[p, :, lax.rem(x - j + NX, NX)] = w[:, j, 32:64, :]
         result = result + lax.dot_general(
-            attended, w[:, 32:64, :].reshape(1024, 128), (((1,), (1,)), ((), ())),
+            attended, outs[p].reshape(1024, 128), (((1,), (1,)), ((), ())),
             preferred_element_type=F32,
         )
     scratch[...] = result
@@ -346,32 +379,31 @@
     swap = [(0, 1), (1, 0)]
 
     message = call(
-        pack, jax.ShapeDtypeStruct((NS, 40, 128), BF), 1, 3, scratch=[VMEM((128, 128), F32)]
+        pack, jax.ShapeDtypeStruct((NZ, 40, 128), BF), 1, 3, scratch=[VMEM((128, 128), F32)]
     )(here, down_query, down_key, down_rotary)
-    gathered = lax.all_to_all(message, SP, 0, 0)
+    gathered = lax.all_to_all(message, "z", 0, 0)
+    gathered = [gathered] + [lax.ppermute(gathered, "x", ring(j)) for j in range(1, NX)]
 
     rows = [tokens] + [lax.ppermute(tokens, "y", ring(j)) for j in range(1, NY)]
 
-    heads = up_query.reshape(8, 2, NOPE + ROPE)
-    plain = heads[:, :, :NOPE].reshape(8, 128)
-    turning = heads[:, :, NOPE:].reshape(8, 2, 2, 4, 4).transpose(0, 1, 3, 2, 4).reshape(8, 64)
-    docs = doc_ids.astype(BF).reshape(8, 32)
-    mixed_rows = jnp.concatenate([turning, docs, jnp.zeros((8, 32), BF)], axis=1)
-    later = jnp.concatenate([plain, up_key, up_value, mixed_rows, output_weight.T], axis=0)
-    later = jnp.broadcast_to(later[None], (NS, 64, 128))
+    later = call(pack_later, jax.ShapeDtypeStruct((64, 128), BF), 0, 5)(
+        up_query, up_key, up_value, doc_ids.reshape(2, 128), output_weight.T
+    )
+    later = [later] + [lax.ppermute(later, "x", ring(j)) for j in range(1, NX)]
+    later = jnp.broadcast_to(jnp.stack(later)[None], (NZ, NX, 64, 128))
 
     q_part, k_part = call(
         project,
         (jax.ShapeDtypeStruct((64, 128), BF), jax.ShapeDtypeStruct((NZ, 72, 128), BF)),
-        1, 5, scratch=[VMEM((128, 1024), BF)],
-    )(here, *rows, gathered)
+        1, 8, scratch=[VMEM((128, 1024), BF), VMEM((NX, NZ, 40, 128), BF)],
+    )(here, *rows, *gathered)
 
     stage1 = lax.all_to_all(k_part, "z", 0, 0)
     stage2 = [lax.ppermute(stage1, AXES, shift_pairs(2, j)) for j in range(1, 4)]
     held = jnp.stack([stage1] + stage2)
     stage3 = [lax.ppermute(held, AXES, shift_pairs(3, j)) for j in range(1, 4)]
 
-    up_own = lax.all_to_all(later, SP, 0, 0)
+    up_own = lax.all_to_all(later, "z", 0, 0)
     up_other = lax.ppermute(up_own, "c", swap)
     q_pair = jnp.stack([q_part, lax.ppermute(q_part, "c", swap)])
     q_all = [q_pair] + [lax.ppermute(q_pair, "y", ring(j)) for j in range(1, NY)]
@@ -383,10 +415,9 @@
             jax.ShapeDtypeStruct((256, 256), BF),
             jax.ShapeDtypeStruct((NS, 128), F32),
         ),
-        1, 7, scratch=[VMEM((256, 256), F32)],
+        1, 7, scratch=[VMEM((256, 256), F32), VMEM((2, NZ, NX, 32, 128), BF)],
     )(here, *q_all, up_own, up_other, query_gain.reshape(2, 128))
 
-    there = jnp.concatenate([here, doc_ids[:1], doc_ids[255:]])
     query_docs = doc_ids.astype(F32).reshape(4, 2, 32).transpose(1, 0, 2).reshape(2, 128)
     keep, send, ml = call(
         attend,
@@ -395,7 +426,7 @@
             jax.ShapeDtypeStruct((256, 128), BF),
             jax.ShapeDtypeStruct((8, 256), F32),
         ),
-        1, 10, room=34,
+        2, 10, room=34,
         scratch=[
             VMEM((4, 4, NZ, 72, 128), BF),
             VMEM((16, 4, 256, 256), F32),
@@ -405,14 +436,14 @@
             VMEM((256, 256), F32),
             VMEM((256, 128), F32),
         ],
-    )(there, queries, uk, uv, key_docs, key_gain.reshape(2, 128), query_docs, held, *stage3)
+    )(here, doc_ids, queries, uk, uv, key_docs, key_gain.reshape(2, 128), query_docs, held, *stage3)
 
     got = lax.ppermute(send, "c", swap)
     ml_got = lax.ppermute(ml, "c", swap)
     *parts, log_sums = call(
         combine,
         (jax.ShapeDtypeStruct((32, 1024), BF),) * NY + (jax.ShapeDtypeStruct((2, 256), F32),),
-        1, 6, scratch=[VMEM((128, 1024), F32)],
+        1, 6, scratch=[VMEM((128, 1024), F32), VMEM((2, NZ, NX, 32, 128), BF)],
     )(here, keep, got, ml, ml_got, up_own, up_other)
     parts[1:] = [lax.ppermute(parts[j], "y", ring(j)) for j in range(1, NY)]
     mixed = call(finish, jax.ShapeDtypeStruct((32, 1024), BF), 0, 5)(

time: 121 us -> 121 us (level)
  local copies, waits for them, and re-layouts: 7.63 us -> 3.92 us
  starting transfers between devices: 59.4 us -> 62.5 us
    all_to_all x1, waiting for transfers between devices: 8.02 us -> 0.01 us  [layer(): stage1 = lax.all_to_all(k_part, 'z', 0, 0)]
    ppermute x0 -> x6, starting transfers between devices: none -> 7.17 us  [the longest x3 3.6 us: layer(): lax.ppermute(gathered, 'x', ring(j))]
    ppermute x0 -> x6, waiting for transfers between devices: none -> 3.92 us  [the longest x3 3.8 us: layer(): later = [later] + [lax.ppermute(later, 'x', ring(j)) for j in range(1, NX)]]
    ppermute x3, waiting for transfers between devices: 13.3 us -> 15.3 us  [layer(): lax.ppermute(q_pair, 'y', ring(j))]
    ppermute x3, waiting for transfers between devices: 0.01 us -> 1.68 us  [layer(): rows = [tokens] + [lax.ppermute(tokens, 'y', ring(j)) for j in range(1, NY)]]
    ppermute x3, starting transfers between devices: 3.57 us -> 2.05 us  [layer(): stage3 = [lax.ppermute(held, AXES, shift_pairs(3, j)) for j in range(1, 4)]]
    unnamed x28 -> x24, local copies, waits for them, and re-layouts: 3.49 us -> 1.98 us
    concatenate x3 -> x0, local copies, waits for them, and re-layouts: 1.38 us -> none  [the longest x1 1.29 us: layer(): there = jnp.concatenate([here, doc_ids[:1], doc_ids[255:]])]
  transfers between devices with their start and end apart: 22 -> 28, of which waited for: 12 -> 17; matrix products, arithmetic and copies ran while one was open for 3% -> 1% of each run, Pallas kernels for 1% -> 1%
where the time goes in v4:
time: 121 us
  starting transfers between devices  62.5 us (52%)
  waiting for transfers between devices  37.7 us (31%)
  Pallas kernels  15.6 us (13%)
  local copies, waits for them, and re-layouts  3.92 us (3%)
    ppermute x3, waiting for transfers between devices, layer(): lax.ppermute(q_pair, 'y', ring(j))  15.3 us
    ppermute x1, starting transfers between devices, layer(): up_other = lax.ppermute(up_own, 'c', swap)  14.6 us
    pallas_call x1, Pallas kernels, layer(): call(attend, (jax.ShapeDtypeStruct((256, 128), F32), jax.ShapeDtypeStruct...  9.34 us
    all_to_all x1, starting transfers between devices, layer(): gathered = lax.all_to_all(message, 'z', 0, 0)  9.13 us
    all_to_all x1, starting transfers between devices, layer(): up_own = lax.all_to_all(later, 'z', 0, 0)  6.56 us
    ppermute x3, waiting for transfers between devices, layer(): lax.ppermute(stage1, AXES, shift_pairs(2, j))  5.95 us
    ppermute x3, starting transfers between devices, layer(): rows = [tokens] + [lax.ppermute(tokens, 'y', ring(j)) for j in range(1, NY)]  5.74 us
    all_to_all x1, waiting for transfers between devices, layer(): gathered = lax.all_to_all(message, 'z', 0, 0)  4.5 us
  transfers between devices with their start and end apart: 28, of which 17 were waited for; matrix products, arithmetic and copies ran while one was open for 1% of the time, Pallas kernels for 1%

profile of v4, /device:TPU:1, one launch (start us, length us, event | category | flops | bytes accessed | tf_op | source)
XLA Modules:
  0.0 120.6 jit_solution(3060122126453484829)
XLA Ops:
  2.8 9.1 %all-to-all-start = ((bf16[8,40,128]{2,1,0:T(8,128)(2,1)}), bf16[8,40,128]{2,1,0:T(8,128)(2,1)S(1)}, u32[]{:S(2)}, u32[]{:S(2)}) async-start(bf16[8,40,128]{2,1,0:T(8,128)(2,1)} %shard_map.131), calls=%async_computation | async-start | bytes 163840 | tf_op jit(solution)/shard_map/all_to_all | solution.py:384
  12.0 3.0 %collective-permute-start.1 = (bf16[32,1024]{1,0:T(8,128)(2,1)S(1)}, bf16[32,1024]{1,0:T(8,128)(2,1)S(1)}, u32[]{:S(2)}, u32[]{:S(2)}) collective-permute-start(bf16[32,1024]{1,0:T(8,128)(2,1)S(1)} %copy-done), channel_id=1, source_target_pairs={{0,4},{2,6},{4,0},{6,2},{1,5},{3,7},{5,1},{7,3},{8,12},{10,14},{12... | collective-permute-start | bytes 196616 | tf_op jit(solution)/shard_map/ppermute | solution.py:387
  15.0 4.5 %all-to-all-done.g0 = bf16[8,40,128]{2,1,0:T(8,128)(2,1)S(1)} async-done(((bf16[8,40,128]{2,1,0:T(8,128)(2,1)}), bf16[8,40,128]{2,1,0:T(8,128)(2,1)S(1)}, u32[]{:S(2)}, u32[]{:S(2)}) %all-to-all-start) | async-done | bytes 81952 | tf_op jit(solution)/shard_map/all_to_all | solution.py:384
  19.5 2.5 %collective-permute-start.5 = (bf16[8,40,128]{2,1,0:T(8,128)(2,1)S(1)}, bf16[8,40,128]{2,1,0:T(8,128)(2,1)S(1)}, u32[]{:S(2)}, u32[]{:S(2)}) collective-permute-start(bf16[8,40,128]{2,1,0:T(8,128)(2,1)S(1)} %all-to-all-done.g0), channel_id=1, source_target_pairs={{0,24},{8,0},{16,8},{24,16},{1,25},{9,1},{17,9},{25,17},{2,26},{10... | collective-permute-start | bytes 245768 | tf_op jit(solution)/shard_map/ppermute | solution.py:385
  25.8 1.6 %collective-permute-done.t1 = bf16[32,1024]{1,0:T(8,128)(2,1)S(1)} collective-permute-done((bf16[32,1024]{1,0:T(8,128)(2,1)S(1)}, bf16[32,1024]{1,0:T(8,128)(2,1)S(1)}, u32[]{:S(2)}, u32[]{:S(2)}) %collective-permute-start) | collective-permute-done | bytes 65568 | tf_op jit(solution)/shard_map/ppermute | solution.py:387
  27.6 1.6 %shard_map.132 = (bf16[64,128]{1,0:T(8,128)(2,1)S(1)}, bf16[8,72,128]{2,1,0:T(8,128)(2,1)}) custom-call(s32[5]{0:T(128)S(1)} %stack.62.where, bf16[32,1024]{1,0:T(8,128)(2,1)S(1)} %copy-done, bf16[32,1024]{1,0:T(8,128)(2,1)S(1)} %collective-permute-done.t1, bf16[32,1024]{1,0:T(8,128)(2,1)S(1)} %collective-permute-done.1.t2, ...), custom_call_target="tpu_custom_call" | custom-call | tf_op jit(solution)/shard_map/pallas_call | solution.py:395
  29.2 3.5 %all-to-all-start.2 = ((bf16[8,72,128]{2,1,0:T(8,128)(2,1)}), bf16[8,72,128]{2,1,0:T(8,128)(2,1)S(1)}, u32[]{:S(2)}, u32[]{:S(2)}) async-start(bf16[8,72,128]{2,1,0:T(8,128)(2,1)} %get-tuple-element.21), calls=%async_computation.2 | async-start | bytes 294912 | tf_op jit(solution)/shard_map/all_to_all | solution.py:401
  33.6 2.3 %collective-permute-start.12 = (bf16[64,128]{1,0:T(8,128)(2,1)S(1)}, bf16[64,128]{1,0:T(8,128)(2,1)S(1)}, u32[]{:S(2)}, u32[]{:S(2)}) collective-permute-start(bf16[64,128]{1,0:T(8,128)(2,1)S(1)} %shard_map.133), channel_id=1, source_target_pairs={{0,24},{8,0},{16,8},{24,16},{1,25},{9,1},{17,9},{25,17},{2,26},{10... | collective-permute-start | bytes 49160 | tf_op jit(solution)/shard_map/ppermute | solution.py:392
  37.2 2.8 %collective-permute-done.11 = bf16[64,128]{1,0:T(8,128)(2,1)S(1)} collective-permute-done((bf16[64,128]{1,0:T(8,128)(2,1)S(1)}, bf16[64,128]{1,0:T(8,128)(2,1)S(1)}, u32[]{:S(2)}, u32[]{:S(2)}) %collective-permute-start.11) | collective-permute-done | bytes 16416 | tf_op jit(solution)/shard_map/ppermute | solution.py:392
  41.9 6.6 %all-to-all-start.1 = ((bf16[8,4,64,128]{3,2,1,0:T(8,128)(2,1)}), bf16[8,4,64,128]{3,2,1,0:T(8,128)(2,1)S(1)}, u32[]{:S(2)}, u32[]{:S(2)}) async-start(bf16[8,4,64,128]{3,2,1,0:T(8,128)(2,1)} %broadcast_in_dim.2), calls=%async_computation.1 | async-start | bytes 1048576 | tf_op jit(solution)/shard_map/all_to_all | solution.py:406
  48.5 2.4 %collective-permute-start.16 = (bf16[8,72,128]{2,1,0:T(8,128)(2,1)S(1)}, bf16[8,72,128]{2,1,0:T(8,128)(2,1)S(1)}, u32[]{:S(2)}, u32[]{:S(2)}) collective-permute-start(bf16[8,72,128]{2,1,0:T(8,128)(2,1)S(1)} %all-to-all-done.2), channel_id=1, source_target_pairs={{0,24},{1,7},{2,26},{3,1},{4,28},{5,3},{6,30},{7,5},{8,0},{9,15},{... | collective-permute-start | bytes 442376 | tf_op jit(solution)/shard_map/ppermute | solution.py:402
  51.9 2.5 %collective-permute-done.16 = bf16[8,72,128]{2,1,0:T(8,128)(2,1)S(1)} collective-permute-done((bf16[8,72,128]{2,1,0:T(8,128)(2,1)S(1)}, bf16[8,72,128]{2,1,0:T(8,128)(2,1)S(1)}, u32[]{:S(2)}, u32[]{:S(2)}) %collective-permute-start.16) | collective-permute-done | bytes 147488 | tf_op jit(solution)/shard_map/ppermute | solution.py:402
  54.5 1.9 %collective-permute-done.15 = bf16[8,72,128]{2,1,0:T(8,128)(2,1)S(1)} collective-permute-done((bf16[8,72,128]{2,1,0:T(8,128)(2,1)S(1)}, bf16[8,72,128]{2,1,0:T(8,128)(2,1)S(1)}, u32[]{:S(2)}, u32[]{:S(2)}) %collective-permute-start.15) | collective-permute-done | bytes 147488 | tf_op jit(solution)/shard_map/ppermute | solution.py:402
  56.4 1.5 %collective-permute-done.14 = bf16[8,72,128]{2,1,0:T(8,128)(2,1)S(1)} collective-permute-done((bf16[8,72,128]{2,1,0:T(8,128)(2,1)S(1)}, bf16[8,72,128]{2,1,0:T(8,128)(2,1)S(1)}, u32[]{:S(2)}, u32[]{:S(2)}) %collective-permute-start.14) | collective-permute-done | bytes 147488 | tf_op jit(solution)/shard_map/ppermute | solution.py:402
  60.7 14.6 %collective-permute-start.13 = (bf16[8,4,64,128]{3,2,1,0:T(8,128)(2,1)S(1)}, bf16[8,4,64,128]{3,2,1,0:T(8,128)(2,1)S(1)}, u32[]{:S(2)}, u32[]{:S(2)}) collective-permute-start(bf16[8,4,64,128]{3,2,1,0:T(8,128)(2,1)S(1)} %all-to-all-done.1.up_own.w_own), channel_id=1, source_target_pairs={{0,1},{1,0},{2,3},{3,2},{4,5},{5,4},{6,7},{7,6},{8,9},{9,8},{10,11... | collective-permute-start | bytes 1572872 | tf_op jit(solution)/shard_map/ppermute | solution.py:407
  75.4 1.6 %collective-permute-done.6 = bf16[64,128]{1,0:T(8,128)(2,1)S(1)} collective-permute-done((bf16[64,128]{1,0:T(8,128)(2,1)S(1)}, bf16[64,128]{1,0:T(8,128)(2,1)S(1)}, u32[]{:S(2)}, u32[]{:S(2)}) %collective-permute-start.6) | collective-permute-done | bytes 16416 | tf_op jit(solution)/shard_map/ppermute | solution.py:408
  76.9 2.3 %collective-permute-start.9 = (bf16[2,64,128]{2,1,0:T(8,128)(2,1)S(1)}, bf16[2,64,128]{2,1,0:T(8,128)(2,1)S(1)}, u32[]{:S(2)}, u32[]{:S(2)}) collective-permute-start(bf16[2,64,128]{2,1,0:T(8,128)(2,1)S(1)} %pad_maximum_fusion.2.q0), channel_id=1, source_target_pairs={{0,6},{2,0},{4,2},{6,4},{1,7},{3,1},{5,3},{7,5},{8,14},{10,8},{12,... | collective-permute-start | bytes 98312 | tf_op jit(solution)/shard_map/ppermute | solution.py:409
  79.2 7.2 %collective-permute-done.9.q3 = bf16[2,64,128]{2,1,0:T(8,128)(2,1)S(1)} collective-permute-done((bf16[2,64,128]{2,1,0:T(8,128)(2,1)S(1)}, bf16[2,64,128]{2,1,0:T(8,128)(2,1)S(1)}, u32[]{:S(2)}, u32[]{:S(2)}) %collective-permute-start.9) | collective-permute-done | bytes 32800 | tf_op jit(solution)/shard_map/ppermute | solution.py:409
  86.4 4.6 %collective-permute-done.8.q2 = bf16[2,64,128]{2,1,0:T(8,128)(2,1)S(1)} collective-permute-done((bf16[2,64,128]{2,1,0:T(8,128)(2,1)S(1)}, bf16[2,64,128]{2,1,0:T(8,128)(2,1)S(1)}, u32[]{:S(2)}, u32[]{:S(2)}) %collective-permute-start.8) | collective-permute-done | bytes 32800 | tf_op jit(solution)/shard_map/ppermute | solution.py:409
  92.0 3.5 %collective-permute-done.7.q1 = bf16[2,64,128]{2,1,0:T(8,128)(2,1)S(1)} collective-permute-done((bf16[2,64,128]{2,1,0:T(8,128)(2,1)S(1)}, bf16[2,64,128]{2,1,0:T(8,128)(2,1)S(1)}, u32[]{:S(2)}, u32[]{:S(2)}) %collective-permute-start.7) | collective-permute-done | bytes 32800 | tf_op jit(solution)/shard_map/ppermute | solution.py:409
  97.5 9.3 %shard_map.135 = (f32[256,128]{1,0:T(8,128)S(1)}, bf16[256,128]{1,0:T(8,128)(2,1)S(1)}, f32[8,256]{1,0:T(8,128)S(1)}) custom-call(s32[5]{0:T(128)S(1)} %stack.62.where, s32[256]{0:T(256)S(1)} %copy-done.3, bf16[4,256,256]{2,1,0:T(8,128)(2,1)S(1)} %get-tuple-element.17.q_ref, bf16[256,256]{1,0:T(8,128)(2,1)S(1)} %get-tuple-element.18.uk, ...), custom_call_target="tpu_custom_call" | custom-call | tf_op jit(solution)/shard_map/pallas_call | solution.py:422
  106.9 4.0 %collective-permute-start.20 = (bf16[256,128]{1,0:T(8,128)(2,1)S(1)}, bf16[256,128]{1,0:T(8,128)(2,1)S(1)}, u32[]{:S(2)}, u32[]{:S(2)}) collective-permute-start(bf16[256,128]{1,0:T(8,128)(2,1)S(1)} %get-tuple-element.23), channel_id=1, source_target_pairs={{0,1},{1,0},{2,3},{3,2},{4,5},{5,4},{6,7},{7,6},{8,9},{9,8},{10,11... | collective-permute-start | bytes 196616 | tf_op jit(solution)/shard_map/ppermute | solution.py:441
  113.1 2.9 %collective-permute-start.23 = (bf16[32,1024]{1,0:T(8,128)(2,1)S(1)}, bf16[32,1024]{1,0:T(8,128)(2,1)S(1)}, u32[]{:S(2)}, u32[]{:S(2)}) collective-permute-start(bf16[32,1024]{1,0:T(8,128)(2,1)S(1)} %get-tuple-element.27), channel_id=1, source_target_pairs={{0,4},{2,6},{4,0},{6,2},{1,5},{3,7},{5,1},{7,3},{8,12},{10,14},{12... | collective-permute-start | bytes 196616 | tf_op jit(solution)/shard_map/ppermute | solution.py:448
  117.8 1.7 %collective-permute-done.23.p2 = bf16[32,1024]{1,0:T(8,128)(2,1)S(1)} collective-permute-done((bf16[32,1024]{1,0:T(8,128)(2,1)S(1)}, bf16[32,1024]{1,0:T(8,128)(2,1)S(1)}, u32[]{:S(2)}, u32[]{:S(2)}) %collective-permute-start.23) | collective-permute-done | bytes 65568 | tf_op jit(solution)/shard_map/ppermute | solution.py:448
  (75 shorter events, 22.3 us)
Async XLA Ops:
  2.8 16.6 %all-to-all-start = ((bf16[8,40,128]{2,1,0:T(8,128)(2,1)}), bf16[8,40,128]{2,1,0:T(8,128)(2,1)S(1)}, u32[]{:S(2)}, u32[]{:S(2)}) async-start(bf16[8,40,128]{2,1,0:T(8,128)(2,1)} %shard_map.131), calls=%async_computation | async-start | bytes 163840 | tf_op jit(solution)/shard_map/all_to_all | solution.py:384
  12.0 12.4 %collective-permute-start.1 = (bf16[32,1024]{1,0:T(8,128)(2,1)S(1)}, bf16[32,1024]{1,0:T(8,128)(2,1)S(1)}, u32[]{:S(2)}, u32[]{:S(2)}) collective-permute-start(bf16[32,1024]{1,0:T(8,128)(2,1)S(1)} %copy-done), channel_id=1, source_target_pairs={{0,4},{2,6},{4,0},{6,2},{1,5},{3,7},{5,1},{7,3},{8,12},{10,14},{12... | collective-permute-start | bytes 196616 | tf_op jit(solution)/shard_map/ppermute | solution.py:387
  19.5 8.0 %collective-permute-start.5 = (bf16[8,40,128]{2,1,0:T(8,128)(2,1)S(1)}, bf16[8,40,128]{2,1,0:T(8,128)(2,1)S(1)}, u32[]{:S(2)}, u32[]{:S(2)}) collective-permute-start(bf16[8,40,128]{2,1,0:T(8,128)(2,1)S(1)} %all-to-all-done.g0), channel_id=1, source_target_pairs={{0,24},{8,0},{16,8},{24,16},{1,25},{9,1},{17,9},{25,17},{2,26},{10... | collective-permute-start | bytes 245768 | tf_op jit(solution)/shard_map/ppermute | solution.py:385
  21.9 5.5 %collective-permute-start.4 = (bf16[8,40,128]{2,1,0:T(8,128)(2,1)S(1)}, bf16[8,40,128]{2,1,0:T(8,128)(2,1)S(1)}, u32[]{:S(2)}, u32[]{:S(2)}) collective-permute-start(bf16[8,40,128]{2,1,0:T(8,128)(2,1)S(1)} %all-to-all-done.g0), channel_id=1, source_target_pairs={{0,16},{8,24},{16,0},{24,8},{1,17},{9,25},{17,1},{25,9},{2,18},{10... | collective-permute-start | bytes 245768 | tf_op jit(solution)/shard_map/ppermute | solution.py:385
  22.5 5.2 %collective-permute-start.3 = (bf16[8,40,128]{2,1,0:T(8,128)(2,1)S(1)}, bf16[8,40,128]{2,1,0:T(8,128)(2,1)S(1)}, u32[]{:S(2)}, u32[]{:S(2)}) collective-permute-start(bf16[8,40,128]{2,1,0:T(8,128)(2,1)S(1)} %all-to-all-done.g0), channel_id=1, source_target_pairs={{0,8},{8,16},{16,24},{24,0},{1,9},{9,17},{17,25},{25,1},{2,10},{10... | collective-permute-start | bytes 245768 | tf_op jit(solution)/shard_map/ppermute | solution.py:385
  23.1 4.4 %collective-permute-start = (bf16[32,1024]{1,0:T(8,128)(2,1)S(1)}, bf16[32,1024]{1,0:T(8,128)(2,1)S(1)}, u32[]{:S(2)}, u32[]{:S(2)}) collective-permute-start(bf16[32,1024]{1,0:T(8,128)(2,1)S(1)} %copy-done), channel_id=1, source_target_pairs={{0,2},{2,4},{4,6},{6,0},{1,3},{3,5},{5,7},{7,1},{8,10},{10,12},{12... | collective-permute-start | bytes 196616 | tf_op jit(solution)/shard_map/ppermute | solution.py:387
  29.2 11.8 %all-to-all-start.2 = ((bf16[8,72,128]{2,1,0:T(8,128)(2,1)}), bf16[8,72,128]{2,1,0:T(8,128)(2,1)S(1)}, u32[]{:S(2)}, u32[]{:S(2)}) async-start(bf16[8,72,128]{2,1,0:T(8,128)(2,1)} %get-tuple-element.21), calls=%async_computation.2 | async-start | bytes 294912 | tf_op jit(solution)/shard_map/all_to_all | solution.py:401
  35.9 4.1 %collective-permute-start.11 = (bf16[64,128]{1,0:T(8,128)(2,1)S(1)}, bf16[64,128]{1,0:T(8,128)(2,1)S(1)}, u32[]{:S(2)}, u32[]{:S(2)}) collective-permute-start(bf16[64,128]{1,0:T(8,128)(2,1)S(1)} %shard_map.133), channel_id=1, source_target_pairs={{0,16},{8,24},{16,0},{24,8},{1,17},{9,25},{17,1},{25,9},{2,18},{10... | collective-permute-start | bytes 49160 | tf_op jit(solution)/shard_map/ppermute | solution.py:392
  37.2 3.8 %collective-permute-start.10 = (bf16[64,128]{1,0:T(8,128)(2,1)S(1)}, bf16[64,128]{1,0:T(8,128)(2,1)S(1)}, u32[]{:S(2)}, u32[]{:S(2)}) collective-permute-start(bf16[64,128]{1,0:T(8,128)(2,1)S(1)} %shard_map.133), channel_id=1, source_target_pairs={{0,8},{8,16},{16,24},{24,0},{1,9},{9,17},{17,25},{25,1},{2,10},{10... | collective-permute-start | bytes 49160 | tf_op jit(solution)/shard_map/ppermute | solution.py:392
  41.9 18.8 %all-to-all-start.1 = ((bf16[8,4,64,128]{3,2,1,0:T(8,128)(2,1)}), bf16[8,4,64,128]{3,2,1,0:T(8,128)(2,1)S(1)}, u32[]{:S(2)}, u32[]{:S(2)}) async-start(bf16[8,4,64,128]{3,2,1,0:T(8,128)(2,1)} %broadcast_in_dim.2), calls=%async_computation.1 | async-start | bytes 1048576 | tf_op jit(solution)/shard_map/all_to_all | solution.py:406
  48.5 6.0 %collective-permute-start.16 = (bf16[8,72,128]{2,1,0:T(8,128)(2,1)S(1)}, bf16[8,72,128]{2,1,0:T(8,128)(2,1)S(1)}, u32[]{:S(2)}, u32[]{:S(2)}) collective-permute-start(bf16[8,72,128]{2,1,0:T(8,128)(2,1)S(1)} %all-to-all-done.2), channel_id=1, source_target_pairs={{0,24},{1,7},{2,26},{3,1},{4,28},{5,3},{6,30},{7,5},{8,0},{9,15},{... | collective-permute-start | bytes 442376 | tf_op jit(solution)/shard_map/ppermute | solution.py:402
  50.8 5.6 %collective-permute-start.15 = (bf16[8,72,128]{2,1,0:T(8,128)(2,1)S(1)}, bf16[8,72,128]{2,1,0:T(8,128)(2,1)S(1)}, u32[]{:S(2)}, u32[]{:S(2)}) collective-permute-start(bf16[8,72,128]{2,1,0:T(8,128)(2,1)S(1)} %all-to-all-done.2), channel_id=1, source_target_pairs={{0,16},{1,5},{2,18},{3,7},{4,20},{5,1},{6,22},{7,3},{8,24},{9,13},... | collective-permute-start | bytes 442376 | tf_op jit(solution)/shard_map/ppermute | solution.py:402
  51.5 6.3 %collective-permute-start.14 = (bf16[8,72,128]{2,1,0:T(8,128)(2,1)S(1)}, bf16[8,72,128]{2,1,0:T(8,128)(2,1)S(1)}, u32[]{:S(2)}, u32[]{:S(2)}) collective-permute-start(bf16[8,72,128]{2,1,0:T(8,128)(2,1)S(1)} %all-to-all-done.2), channel_id=1, source_target_pairs={{0,8},{1,3},{2,10},{3,5},{4,12},{5,7},{6,14},{7,1},{8,16},{9,11},{... | collective-permute-start | bytes 442376 | tf_op jit(solution)/shard_map/ppermute | solution.py:402
  58.0 38.8 %collective-permute-start.19 = (bf16[4,8,72,128]{3,2,1,0:T(8,128)(2,1)S(1)}, bf16[4,8,72,128]{3,2,1,0:T(8,128)(2,1)S(1)}, u32[]{:S(2)}, u32[]{:S(2)}) collective-permute-start(bf16[4,8,72,128]{3,2,1,0:T(8,128)(2,1)S(1)} %pad_maximum_fusion.b0), channel_id=1, source_target_pairs={{0,6},{1,25},{2,0},{3,27},{4,2},{5,29},{6,4},{7,31},{8,14},{9,1},{... | collective-permute-start | bytes 1769480 | tf_op jit(solution)/shard_map/ppermute | solution.py:404
  58.2 38.7 %collective-permute-start.18 = (bf16[4,8,72,128]{3,2,1,0:T(8,128)(2,1)S(1)}, bf16[4,8,72,128]{3,2,1,0:T(8,128)(2,1)S(1)}, u32[]{:S(2)}, u32[]{:S(2)}) collective-permute-start(bf16[4,8,72,128]{3,2,1,0:T(8,128)(2,1)S(1)} %pad_maximum_fusion.b0), channel_id=1, source_target_pairs={{0,4},{1,17},{2,6},{3,19},{4,0},{5,21},{6,2},{7,23},{8,12},{9,25},... | collective-permute-start | bytes 1769480 | tf_op jit(solution)/shard_map/ppermute | solution.py:404
  59.3 37.6 %collective-permute-start.17 = (bf16[4,8,72,128]{3,2,1,0:T(8,128)(2,1)S(1)}, bf16[4,8,72,128]{3,2,1,0:T(8,128)(2,1)S(1)}, u32[]{:S(2)}, u32[]{:S(2)}) collective-permute-start(bf16[4,8,72,128]{3,2,1,0:T(8,128)(2,1)S(1)} %pad_maximum_fusion.b0), channel_id=1, source_target_pairs={{0,2},{1,9},{2,4},{3,11},{4,6},{5,13},{6,0},{7,15},{8,10},{9,17},{... | collective-permute-start | bytes 1769480 | tf_op jit(solution)/shard_map/ppermute | solution.py:404
  60.7 34.8 %collective-permute-start.13 = (bf16[8,4,64,128]{3,2,1,0:T(8,128)(2,1)S(1)}, bf16[8,4,64,128]{3,2,1,0:T(8,128)(2,1)S(1)}, u32[]{:S(2)}, u32[]{:S(2)}) collective-permute-start(bf16[8,4,64,128]{3,2,1,0:T(8,128)(2,1)S(1)} %all-to-all-done.1.up_own.w_own), channel_id=1, source_target_pairs={{0,1},{1,0},{2,3},{3,2},{4,5},{5,4},{6,7},{7,6},{8,9},{9,8},{10,11... | collective-permute-start | bytes 1572872 | tf_op jit(solution)/shard_map/ppermute | solution.py:407
  76.9 9.4 %collective-permute-start.9 = (bf16[2,64,128]{2,1,0:T(8,128)(2,1)S(1)}, bf16[2,64,128]{2,1,0:T(8,128)(2,1)S(1)}, u32[]{:S(2)}, u32[]{:S(2)}) collective-permute-start(bf16[2,64,128]{2,1,0:T(8,128)(2,1)S(1)} %pad_maximum_fusion.2.q0), channel_id=1, source_target_pairs={{0,6},{2,0},{4,2},{6,4},{1,7},{3,1},{5,3},{7,5},{8,14},{10,8},{12,... | collective-permute-start | bytes 98312 | tf_op jit(solution)/shard_map/ppermute | solution.py:409
  86.4 4.6 %collective-permute-start.8 = (bf16[2,64,128]{2,1,0:T(8,128)(2,1)S(1)}, bf16[2,64,128]{2,1,0:T(8,128)(2,1)S(1)}, u32[]{:S(2)}, u32[]{:S(2)}) collective-permute-start(bf16[2,64,128]{2,1,0:T(8,128)(2,1)S(1)} %pad_maximum_fusion.2.q0), channel_id=1, source_target_pairs={{0,4},{2,6},{4,0},{6,2},{1,5},{3,7},{5,1},{7,3},{8,12},{10,14},{12... | collective-permute-start | bytes 98312 | tf_op jit(solution)/shard_map/ppermute | solution.py:409
  91.0 4.5 %collective-permute-start.7 = (bf16[2,64,128]{2,1,0:T(8,128)(2,1)S(1)}, bf16[2,64,128]{2,1,0:T(8,128)(2,1)S(1)}, u32[]{:S(2)}, u32[]{:S(2)}) collective-permute-start(bf16[2,64,128]{2,1,0:T(8,128)(2,1)S(1)} %pad_maximum_fusion.2.q0), channel_id=1, source_target_pairs={{0,2},{2,4},{4,6},{6,0},{1,3},{3,5},{5,7},{7,1},{8,10},{10,12},{12... | collective-permute-start | bytes 98312 | tf_op jit(solution)/shard_map/ppermute | solution.py:409
  106.9 5.1 %collective-permute-start.20 = (bf16[256,128]{1,0:T(8,128)(2,1)S(1)}, bf16[256,128]{1,0:T(8,128)(2,1)S(1)}, u32[]{:S(2)}, u32[]{:S(2)}) collective-permute-start(bf16[256,128]{1,0:T(8,128)(2,1)S(1)} %get-tuple-element.23), channel_id=1, source_target_pairs={{0,1},{1,0},{2,3},{3,2},{4,5},{5,4},{6,7},{7,6},{8,9},{9,8},{10,11... | collective-permute-start | bytes 196616 | tf_op jit(solution)/shard_map/ppermute | solution.py:441
  113.0 4.8 %collective-permute-start.22 = (bf16[32,1024]{1,0:T(8,128)(2,1)S(1)}, bf16[32,1024]{1,0:T(8,128)(2,1)S(1)}, u32[]{:S(2)}, u32[]{:S(2)}) collective-permute-start(bf16[32,1024]{1,0:T(8,128)(2,1)S(1)} %get-tuple-element.26), channel_id=1, source_target_pairs={{0,2},{2,4},{4,6},{6,0},{1,3},{3,5},{5,7},{7,1},{8,10},{10,12},{12... | collective-permute-start | bytes 196616 | tf_op jit(solution)/shard_map/ppermute | solution.py:448
  113.1 6.3 %collective-permute-start.23 = (bf16[32,1024]{1,0:T(8,128)(2,1)S(1)}, bf16[32,1024]{1,0:T(8,128)(2,1)S(1)}, u32[]{:S(2)}, u32[]{:S(2)}) collective-permute-start(bf16[32,1024]{1,0:T(8,128)(2,1)S(1)} %get-tuple-element.27), channel_id=1, source_target_pairs={{0,4},{2,6},{4,0},{6,2},{1,5},{3,7},{5,1},{7,3},{8,12},{10,14},{12... | collective-permute-start | bytes 196616 | tf_op jit(solution)/shard_map/ppermute | solution.py:448
  116.0 3.9 %collective-permute-start.24 = (bf16[32,1024]{1,0:T(8,128)(2,1)S(1)}, bf16[32,1024]{1,0:T(8,128)(2,1)S(1)}, u32[]{:S(2)}, u32[]{:S(2)}) collective-permute-start(bf16[32,1024]{1,0:T(8,128)(2,1)S(1)} %get-tuple-element.28), channel_id=1, source_target_pairs={{0,6},{2,0},{4,2},{6,4},{1,7},{3,1},{5,3},{7,5},{8,14},{10,8},{12,... | collective-permute-start | bytes 196616 | tf_op jit(solution)/shard_map/ppermute | solution.py:448
  (16 other events, 40.7 us)

commit v5 on v4

--- a/solution.py
+++ b/solution.py
@@ -2,6 +2,7 @@
 
 import jax
 import jax.numpy as jnp
+import numpy as np
 from jax import lax
 from jax.experimental import pallas as pl
 from jax.experimental.pallas import tpu as pltpu
@@ -29,7 +30,7 @@
 VMEM = pltpu.VMEM
 SMEM_SPEC = pl.BlockSpec(memory_space=pltpu.SMEM)
 VMEM_SPEC = pl.BlockSpec(memory_space=pltpu.VMEM)
-ANY_SPEC = pl.BlockSpec(memory_space=pl.ANY)
+ANY_SPEC = pl.BlockSpec(memory_space=pltpu.HBM)
 
 
 def call(body, outs, n_smem, n_in, scratch=(), any_from=None, cost=None, room=16):
@@ -64,7 +65,29 @@
     return value
 
 
-def pack(where, dq, dk, dr, out, flipped):
+def picks():
+    pick = np.zeros((192, 256), np.float32)
+    for lane in range(192):
+        if lane < 128:
+            src = 96 * (lane // 64) + lane % 64
+        else:
+            turn = lane - 128
+            src = 64 + 96 * (turn // 32) + 16 * ((turn // 4) % 2) + 4 * ((turn % 32) // 8) + turn % 4
+        pick[src, lane] = 1.0
+    return pick
+
+
+def pack(where, *refs):
+    inputs, out, flipped, places, sems = refs[:9], refs[9], refs[10], refs[11:20], refs[20]
+    copies = [
+        pltpu.make_async_copy(source, place, sems.at[i])
+        for i, (source, place) in enumerate(zip(inputs, places))
+    ]
+    for copy in copies:
+        copy.start()
+    for copy in copies:
+        copy.wait()
+    dq, dk, dr, up_query, pick, up_key, up_value, docs_ref, out_t = places
     y = where[2]
 
     def chosen(ref):
@@ -79,23 +102,8 @@
     flipped[...] = jnp.transpose(jnp.concatenate([rope] * 4, axis=0))
     turned = jnp.concatenate([flipped[pl.ds(4 * y, 4), :], flipped[pl.ds(16 + 4 * y, 4), :]], axis=0)
     turned = turned.astype(BF)
-    for z in range(NZ):
-        out[z, 0:32, :] = block
-        out[z, 32:40, :] = turned
-
-
-def pack_later(up_query, up_key, up_value, docs_ref, out_t, out):
-    src = lax.broadcasted_iota(jnp.int32, (192, 256), 0)
-    lane = lanes((192, 256))
-    plain = 96 * (lane // 64) + lane % 64
-    turn = lane - 128
-    rope = 64 + 96 * (turn // 32) + 16 * ((turn // 4) % 2) + 4 * ((turn % 32) // 8) + turn % 4
-    chosen = jnp.where(lane < 128, plain, jnp.where(lane < 192, rope, -1))
-    pick = jnp.where(src == chosen, 1.0, 0.0).astype(BF)
-    sorted_query = jnp.dot(up_query[...], pick, preferred_element_type=F32)
-    out[0:8, :] = sorted_query[:, 0:128].astype(BF)
-    out[8:16, :] = up_key[...]
-    out[16:24, :] = up_value[...]
+    sorted_query = jnp.dot(up_query[...], pick[...], preferred_element_type=F32)
+    plain = sorted_query[:, 0:128].astype(BF)
     mixed = sorted_query[:, 128:256]
     docs = docs_ref[...].astype(F32)
     row = lax.broadcasted_iota(jnp.int32, (8, 128), 0)
@@ -104,8 +112,15 @@
         line = docs[r // 4 : r // 4 + 1, :]
         moved = pltpu.roll(jnp.broadcast_to(line, (8, 128)), (64 - 32 * (r % 4)) % 128, 1)
         mixed = jnp.where((row == r) & (at // 32 == 2), moved, mixed)
-    out[24:32, :] = mixed.astype(BF)
-    out[32:64, :] = out_t[...]
+    mixed = mixed.astype(BF)
+    for z in range(NZ):
+        out[z, 0:32, :] = block
+        out[z, 32:40, :] = turned
+        out[z, 40:48, :] = plain
+        out[z, 48:56, :] = up_key[...]
+        out[z, 56:64, :] = up_value[...]
+        out[z, 64:72, :] = mixed
+        out[z, 72:104, :] = out_t[...]
 
 
 def project(where, t0, t1, t2, t3, g0, g1, g2, g3, q_ref, k_ref, tok, gathered):
@@ -115,7 +130,7 @@
         at = lax.rem(y - j + NY, NY)
         tok[pl.ds(pl.multiple_of(at * 32, 32), 32), :] = part[...]
     for j, part in enumerate((g0, g1, g2, g3)):
-        gathered[lax.rem(x - j + NX, NX)] = part[...]
+        gathered[lax.rem(x - j + NX, NX)] = part[:, 0:40, :]
     rows = tok[...]
     weights = jnp.concatenate(
         [gathered[k, z, 0:32, :] for z in range(NZ) for k in range(NX)], axis=0
@@ -148,7 +163,8 @@
 
 
 def make_queries(
-    where, q0, q1, q2, q3, up_own, up_other, gain, out, uk_ref, uv_ref, docs_ref, latents, ups
+    where, q0, q1, q2, q3, up_own, up_other, gain, key_gain, out, uk_ref, uv_ref, docs_ref, col_ref,
+    latents, ups,
 ):
     x, y, c = where[1], where[2], where[3]
     for j, part in enumerate((q0, q1, q2, q3)):
@@ -161,6 +177,8 @@
     inverse = lax.rsqrt(mean + EPS)
     gains = jnp.concatenate([column(gain[0:1, :]), column(gain[1:2, :])], axis=0)
     gains = jnp.concatenate([gains, gains], axis=1)
+    for i in range(2):
+        col_ref[128 * i : 128 * (i + 1), :] = column(key_gain[i : i + 1, :])
     latent = (raw * inverse * gains).astype(BF)
     tok = lanes((64, 256))
     row = lax.broadcasted_iota(jnp.int32, (64, 256), 0)
@@ -173,7 +191,7 @@
     high_sin = jnp.where(is_low, 0.0, sine)
     for p, up in enumerate((up_own, up_other)):
         for j in range(NX):
-            ups[p, :, lax.rem(x - j + NX, NX)] = up[:, j, 0:32, :]
+            ups[p, :, lax.rem(x - j + NX, NX)] = up[j, :, 0:32, :]
         wide = ups[p].reshape(NS, 32, 128).astype(F32)
         own = slice(128 * p, 128 * (p + 1))
         plain_w = jnp.transpose(wide[:, 0:8, :].reshape(256, 128)).astype(BF)
@@ -199,8 +217,8 @@
 
 
 def attend(
-    where, ids, q_ref, uk, uv, key_docs, gain, query_docs, b0, b1, b2, b3,
-    keep_ref, send_ref, ml_ref, kb, s_buf, v_buf, mx, total, acc, gains,
+    where, ids, q_ref, uk, uv, key_docs, gains, query_docs, b0, b1, b2, b3,
+    keep_ref, send_ref, ml_ref, kb, s_buf, v_buf, mx, total, acc,
 ):
     x0, y0, c = where[1], where[2], where[3]
     docs = key_docs[...]
@@ -219,8 +237,6 @@
         return carry
 
     lax.fori_loop(first // 2, (last + 1) // 2, fetch, 0)
-    for i in range(2):
-        gains[128 * i : 128 * (i + 1), :] = column(gain[i : i + 1, :])
     mx[...] = jnp.full(mx.shape, NEG_BIG, F32)
     total[...] = jnp.zeros(total.shape, F32)
     acc[...] = jnp.zeros(acc.shape, F32)
@@ -325,7 +341,7 @@
             pieces.append(mine * f0[h : h + 1, :] + theirs * f1[h : h + 1, :])
         attended = jnp.transpose(jnp.concatenate(pieces, axis=0)).astype(BF)
         for j in range(NX):
-            outs[p, :, lax.rem(x - j + NX, NX)] = w[:, j, 32:64, :]
+            outs[p, :, lax.rem(x - j + NX, NX)] = w[j, :, 32:64, :]
         result = result + lax.dot_general(
             attended, outs[p].reshape(1024, 128), (((1,), (1,)), ((), ())),
             preferred_element_type=F32,
@@ -378,19 +394,21 @@
     here = jnp.stack([z, x, y, c, sp * 256]).astype(jnp.int32)
     swap = [(0, 1), (1, 0)]
 
+    sources = (
+        down_query, down_key, down_rotary, up_query, jnp.asarray(picks(), BF), up_key,
+        up_value, doc_ids.reshape(2, 128), output_weight.T,
+    )
     message = call(
-        pack, jax.ShapeDtypeStruct((NZ, 40, 128), BF), 1, 3, scratch=[VMEM((128, 128), F32)]
-    )(here, down_query, down_key, down_rotary)
-    gathered = lax.all_to_all(message, "z", 0, 0)
-    gathered = [gathered] + [lax.ppermute(gathered, "x", ring(j)) for j in range(1, NX)]
+        pack, jax.ShapeDtypeStruct((NZ, 104, 128), BF), 1, 9, any_from=0,
+        scratch=[VMEM((128, 128), F32)]
+        + [VMEM(a.shape, a.dtype) for a in sources]
+        + [pltpu.SemaphoreType.DMA((9,))],
+    )(here, *(pltpu.with_memory_space_constraint(a, pltpu.HBM) for a in sources))
+    arrived = lax.all_to_all(message, "z", 0, 0)
+    sent = arrived[:, 0:40, :]
+    gathered = [arrived] + [lax.ppermute(sent, "x", ring(j)) for j in range(1, NX)]
 
     rows = [tokens] + [lax.ppermute(tokens, "y", ring(j)) for j in range(1, NY)]
-
-    later = call(pack_later, jax.ShapeDtypeStruct((64, 128), BF), 0, 5)(
-        up_query, up_key, up_value, doc_ids.reshape(2, 128), output_weight.T
-    )
-    later = [later] + [lax.ppermute(later, "x", ring(j)) for j in range(1, NX)]
-    later = jnp.broadcast_to(jnp.stack(later)[None], (NZ, NX, 64, 128))
 
     q_part, k_part = call(
         project,
@@ -403,20 +421,23 @@
     held = jnp.stack([stage1] + stage2)
     stage3 = [lax.ppermute(held, AXES, shift_pairs(3, j)) for j in range(1, 4)]
 
-    up_own = lax.all_to_all(later, "z", 0, 0)
+    later = arrived[:, 40:104, :]
+    later = [later] + [lax.ppermute(later, "x", ring(j)) for j in range(1, NX)]
+    up_own = jnp.stack(later)
     up_other = lax.ppermute(up_own, "c", swap)
     q_pair = jnp.stack([q_part, lax.ppermute(q_part, "c", swap)])
     q_all = [q_pair] + [lax.ppermute(q_pair, "y", ring(j)) for j in range(1, NY)]
-    queries, uk, uv, key_docs = call(
+    queries, uk, uv, key_docs, gains = call(
         make_queries,
         (
             jax.ShapeDtypeStruct((4, 256, 256), BF),
             jax.ShapeDtypeStruct((256, 256), BF),
             jax.ShapeDtypeStruct((256, 256), BF),
             jax.ShapeDtypeStruct((NS, 128), F32),
+            jax.ShapeDtypeStruct((256, 128), F32),
         ),
-        1, 7, scratch=[VMEM((256, 256), F32), VMEM((2, NZ, NX, 32, 128), BF)],
-    )(here, *q_all, up_own, up_other, query_gain.reshape(2, 128))
+        1, 8, scratch=[VMEM((256, 256), F32), VMEM((2, NZ, NX, 32, 128), BF)],
+    )(here, *q_all, up_own, up_other, query_gain.reshape(2, 128), key_gain.reshape(2, 128))
 
     query_docs = doc_ids.astype(F32).reshape(4, 2, 32).transpose(1, 0, 2).reshape(2, 128)
     keep, send, ml = call(
@@ -434,9 +455,8 @@
             VMEM((4, 8, 256), F32),
             VMEM((4, 8, 256), F32),
             VMEM((256, 256), F32),
-            VMEM((256, 128), F32),
         ],
-    )(here, doc_ids, queries, uk, uv, key_docs, key_gain.reshape(2, 128), query_docs, held, *stage3)
+    )(here, doc_ids, queries, uk, uv, key_docs, gains, query_docs, held, *stage3)
 
     got = lax.ppermute(send, "c", swap)
     ml_got = lax.ppermute(ml, "c", swap)

time: 121 us -> 115 us (0.950)
  the two profiles are of different devices: /device:TPU:1 before, /device:TPU:4 now
where the time goes in v5:
time: 115 us
  starting transfers between devices  54.6 us (47%)
  waiting for transfers between devices  27.5 us (24%)
  Pallas kernels  15.8 us (14%)
  blocking collectives  11.6 us (10%)
  local copies, waits for them, and re-layouts  3.71 us (3%)
    ppermute x3, starting transfers between devices, layer(): stage3 = [lax.ppermute(held, AXES, shift_pairs(3, j)) for j in range(1, 4)]  13.1 us
    ppermute x3, waiting for transfers between devices, layer(): lax.ppermute(q_pair, 'y', ring(j))  13 us
    all_to_all x1, blocking collectives, layer(): stage1 = lax.all_to_all(k_part, 'z', 0, 0)  11.6 us
    pallas_call x1, Pallas kernels, layer(): call(attend, (jax.ShapeDtypeStruct((256, 128), F32), jax.ShapeDtypeStruct...  9.34 us
    all_to_all x1, starting transfers between devices, layer(): arrived = lax.all_to_all(message, 'z', 0, 0)  8.61 us
    all_to_all x1, waiting for transfers between devices, layer(): arrived = lax.all_to_all(message, 'z', 0, 0)  7.54 us
    ppermute x3, starting transfers between devices, layer(): rows = [tokens] + [lax.ppermute(tokens, 'y', ring(j)) for j in range(1, NY)]  6.52 us
    ppermute x3, starting transfers between devices, layer(): later = [later] + [lax.ppermute(later, 'x', ring(j)) for j in range(1, NX)]  6.34 us
  transfers between devices with their start and end apart: 26, of which 11 were waited for; matrix products, arithmetic and copies ran while one was open for 3% of the time, Pallas kernels for 1%

profile of v5, /device:TPU:4, one launch (start us, length us, event | category | flops | bytes accessed | tf_op | source)
XLA Modules:
  0.0 114.8 jit_solution(8916353965580798778)
XLA Ops:
  0.7 2.5 %shard_map.140 = bf16[8,104,128]{2,1,0:T(8,128)(2,1)} custom-call(s32[5]{0:T(128)S(1)} %stack.62.where, bf16[32,256]{1,0:T(8,128)(2,1)} %refs_0_.1, bf16[32,256]{1,0:T(8,128)(2,1)} %refs_1_.1, bf16[32,32]{1,0:T(8,128)(2,1)} %refs_2_.1, bf16[8,192]{1,0:T(8,128)(2,1)} %refs_3_.1, bf16[192,256]{1,0:T(8,128)(2,1)} %constant.22.clone.refs_4_, ...), custom_call_target="tpu_custom_call" | custom-call | tf_op jit(solution)/shard_map/pallas_call | solution.py:401
  3.3 8.6 %all-to-all-start = ((bf16[8,104,128]{2,1,0:T(8,128)(2,1)}), bf16[8,104,128]{2,1,0:T(8,128)(2,1)S(1)}, u32[]{:S(2)}, u32[]{:S(2)}) async-start(bf16[8,104,128]{2,1,0:T(8,128)(2,1)} %shard_map.140), calls=%async_computation | async-start | bytes 425984 | tf_op jit(solution)/shard_map/all_to_all | solution.py:407
  11.9 3.3 %collective-permute-start.1 = (bf16[32,1024]{1,0:T(8,128)(2,1)S(1)}, bf16[32,1024]{1,0:T(8,128)(2,1)S(1)}, u32[]{:S(2)}, u32[]{:S(2)}) collective-permute-start(bf16[32,1024]{1,0:T(8,128)(2,1)S(1)} %copy-done), channel_id=1, source_target_pairs={{0,4},{2,6},{4,0},{6,2},{1,5},{3,7},{5,1},{7,3},{8,12},{10,14},{12... | collective-permute-start | bytes 196616 | tf_op jit(solution)/shard_map/ppermute | solution.py:411
  15.2 7.5 %all-to-all-done.g0 = bf16[8,104,128]{2,1,0:T(8,128)(2,1)S(1)} async-done(((bf16[8,104,128]{2,1,0:T(8,128)(2,1)}), bf16[8,104,128]{2,1,0:T(8,128)(2,1)S(1)}, u32[]{:S(2)}, u32[]{:S(2)}) %all-to-all-start) | async-done | bytes 213024 | tf_op jit(solution)/shard_map/all_to_all | solution.py:407
  23.3 2.7 %collective-permute-start.4 = (bf16[8,40,128]{2,1,0:T(8,128)(2,1)S(1)}, bf16[8,40,128]{2,1,0:T(8,128)(2,1)S(1)}, u32[]{:S(2)}, u32[]{:S(2)}) collective-permute-start(bf16[8,40,128]{2,1,0:T(8,128)(2,1)S(1)} %slice.8), channel_id=1, source_target_pairs={{0,16},{8,24},{16,0},{24,8},{1,17},{9,25},{17,1},{25,9},{2,18},{10... | collective-permute-start | bytes 245768 | tf_op jit(solution)/shard_map/ppermute | solution.py:409
  26.1 1.6 %collective-permute-start = (bf16[32,1024]{1,0:T(8,128)(2,1)S(1)}, bf16[32,1024]{1,0:T(8,128)(2,1)S(1)}, u32[]{:S(2)}, u32[]{:S(2)}) collective-permute-start(bf16[32,1024]{1,0:T(8,128)(2,1)S(1)} %copy-done), channel_id=1, source_target_pairs={{0,2},{2,4},{4,6},{6,0},{1,3},{3,5},{5,7},{7,1},{8,10},{10,12},{12... | collective-permute-start | bytes 196616 | tf_op jit(solution)/shard_map/ppermute | solution.py:411
  27.7 1.7 %collective-permute-start.2 = (bf16[32,1024]{1,0:T(8,128)(2,1)S(1)}, bf16[32,1024]{1,0:T(8,128)(2,1)S(1)}, u32[]{:S(2)}, u32[]{:S(2)}) collective-permute-start(bf16[32,1024]{1,0:T(8,128)(2,1)S(1)} %copy-done), channel_id=1, source_target_pairs={{0,6},{2,0},{4,2},{6,4},{1,7},{3,1},{5,3},{7,5},{8,14},{10,8},{12,... | collective-permute-start | bytes 196616 | tf_op jit(solution)/shard_map/ppermute | solution.py:411
  29.3 2.2 %collective-permute-done.t1 = bf16[32,1024]{1,0:T(8,128)(2,1)S(1)} collective-permute-done((bf16[32,1024]{1,0:T(8,128)(2,1)S(1)}, bf16[32,1024]{1,0:T(8,128)(2,1)S(1)}, u32[]{:S(2)}, u32[]{:S(2)}) %collective-permute-start) | collective-permute-done | bytes 65568 | tf_op jit(solution)/shard_map/ppermute | solution.py:411
  32.9 11.6 %all_to_all.10 = bf16[8,72,128]{2,1,0:T(8,128)(2,1)S(1)} all-to-all(bf16[8,72,128]{2,1,0:T(8,128)(2,1)S(1)} %get-tuple-element.23), channel_id=1, replica_groups=mesh['z'=8,'x'=4,'y'=4,'c'=2] {'z'}, dimensions={0} | all-to-all | bytes 294912 | tf_op jit(solution)/shard_map/all_to_all | solution.py:419
  44.5 2.0 %collective-permute-start.16 = (bf16[8,72,128]{2,1,0:T(8,128)(2,1)S(1)}, bf16[8,72,128]{2,1,0:T(8,128)(2,1)S(1)}, u32[]{:S(2)}, u32[]{:S(2)}) collective-permute-start(bf16[8,72,128]{2,1,0:T(8,128)(2,1)S(1)} %all_to_all.10), channel_id=1, source_target_pairs={{0,24},{1,7},{2,26},{3,1},{4,28},{5,3},{6,30},{7,5},{8,0},{9,15},{... | collective-permute-start | bytes 442376 | tf_op jit(solution)/shard_map/ppermute | solution.py:420
  46.5 2.0 %collective-permute-start.15 = (bf16[8,72,128]{2,1,0:T(8,128)(2,1)S(1)}, bf16[8,72,128]{2,1,0:T(8,128)(2,1)S(1)}, u32[]{:S(2)}, u32[]{:S(2)}) collective-permute-start(bf16[8,72,128]{2,1,0:T(8,128)(2,1)S(1)} %all_to_all.10), channel_id=1, source_target_pairs={{0,16},{1,5},{2,18},{3,7},{4,20},{5,1},{6,22},{7,3},{8,24},{9,13},... | collective-permute-start | bytes 442376 | tf_op jit(solution)/shard_map/ppermute | solution.py:420
  48.9 1.3 %collective-permute-start.11 = (bf16[8,64,128]{2,1,0:T(8,128)(2,1)S(1)}, bf16[8,64,128]{2,1,0:T(8,128)(2,1)S(1)}, u32[]{:S(2)}, u32[]{:S(2)}) collective-permute-start(bf16[8,64,128]{2,1,0:T(8,128)(2,1)S(1)} %get-tuple-element.33), channel_id=1, source_target_pairs={{0,16},{8,24},{16,0},{24,8},{1,17},{9,25},{17,1},{25,9},{2,18},{10... | collective-permute-start | bytes 393224 | tf_op jit(solution)/shard_map/ppermute | solution.py:425
  50.2 2.6 %collective-permute-start.10 = (bf16[8,64,128]{2,1,0:T(8,128)(2,1)S(1)}, bf16[8,64,128]{2,1,0:T(8,128)(2,1)S(1)}, u32[]{:S(2)}, u32[]{:S(2)}) collective-permute-start(bf16[8,64,128]{2,1,0:T(8,128)(2,1)S(1)} %get-tuple-element.33), channel_id=1, source_target_pairs={{0,8},{8,16},{16,24},{24,0},{1,9},{9,17},{17,25},{25,1},{2,10},{10... | collective-permute-start | bytes 393224 | tf_op jit(solution)/shard_map/ppermute | solution.py:425
  52.8 2.4 %collective-permute-start.12 = (bf16[8,64,128]{2,1,0:T(8,128)(2,1)S(1)}, bf16[8,64,128]{2,1,0:T(8,128)(2,1)S(1)}, u32[]{:S(2)}, u32[]{:S(2)}) collective-permute-start(bf16[8,64,128]{2,1,0:T(8,128)(2,1)S(1)} %get-tuple-element.33), channel_id=1, source_target_pairs={{0,24},{8,0},{16,8},{24,16},{1,25},{9,1},{17,9},{25,17},{2,26},{10... | collective-permute-start | bytes 393224 | tf_op jit(solution)/shard_map/ppermute | solution.py:425
  55.3 11.7 %collective-permute-start.19 = (bf16[4,8,72,128]{3,2,1,0:T(8,128)(2,1)S(1)}, bf16[4,8,72,128]{3,2,1,0:T(8,128)(2,1)S(1)}, u32[]{:S(2)}, u32[]{:S(2)}) collective-permute-start(bf16[4,8,72,128]{3,2,1,0:T(8,128)(2,1)S(1)} %pad_maximum_fusion.b0), channel_id=1, source_target_pairs={{0,6},{1,25},{2,0},{3,27},{4,2},{5,29},{6,4},{7,31},{8,14},{9,1},{... | collective-permute-start | bytes 1769480 | tf_op jit(solution)/shard_map/ppermute | solution.py:422
  69.1 1.4 %collective-permute-done.6 = bf16[64,128]{1,0:T(8,128)(2,1)S(1)} collective-permute-done((bf16[64,128]{1,0:T(8,128)(2,1)S(1)}, bf16[64,128]{1,0:T(8,128)(2,1)S(1)}, u32[]{:S(2)}, u32[]{:S(2)}) %collective-permute-start.6) | collective-permute-done | bytes 16416 | tf_op jit(solution)/shard_map/ppermute | solution.py:428
  70.6 2.6 %collective-permute-start.9 = (bf16[2,64,128]{2,1,0:T(8,128)(2,1)S(1)}, bf16[2,64,128]{2,1,0:T(8,128)(2,1)S(1)}, u32[]{:S(2)}, u32[]{:S(2)}) collective-permute-start(bf16[2,64,128]{2,1,0:T(8,128)(2,1)S(1)} %pad_maximum_fusion.2.q0), channel_id=1, source_target_pairs={{0,6},{2,0},{4,2},{6,4},{1,7},{3,1},{5,3},{7,5},{8,14},{10,8},{12,... | collective-permute-start | bytes 98312 | tf_op jit(solution)/shard_map/ppermute | solution.py:429
  73.2 8.2 %collective-permute-done.9.q3 = bf16[2,64,128]{2,1,0:T(8,128)(2,1)S(1)} collective-permute-done((bf16[2,64,128]{2,1,0:T(8,128)(2,1)S(1)}, bf16[2,64,128]{2,1,0:T(8,128)(2,1)S(1)}, u32[]{:S(2)}, u32[]{:S(2)}) %collective-permute-start.9) | collective-permute-done | bytes 32800 | tf_op jit(solution)/shard_map/ppermute | solution.py:429
  81.4 2.5 %collective-permute-start.8 = (bf16[2,64,128]{2,1,0:T(8,128)(2,1)S(1)}, bf16[2,64,128]{2,1,0:T(8,128)(2,1)S(1)}, u32[]{:S(2)}, u32[]{:S(2)}) collective-permute-start(bf16[2,64,128]{2,1,0:T(8,128)(2,1)S(1)} %pad_maximum_fusion.2.q0), channel_id=1, source_target_pairs={{0,4},{2,6},{4,0},{6,2},{1,5},{3,7},{5,1},{7,3},{8,12},{10,14},{12... | collective-permute-start | bytes 98312 | tf_op jit(solution)/shard_map/ppermute | solution.py:429
  83.9 2.9 %collective-permute-done.8.q2 = bf16[2,64,128]{2,1,0:T(8,128)(2,1)S(1)} collective-permute-done((bf16[2,64,128]{2,1,0:T(8,128)(2,1)S(1)}, bf16[2,64,128]{2,1,0:T(8,128)(2,1)S(1)}, u32[]{:S(2)}, u32[]{:S(2)}) %collective-permute-start.8) | collective-permute-done | bytes 32800 | tf_op jit(solution)/shard_map/ppermute | solution.py:429
  90.5 1.9 %collective-permute-done.7.q1 = bf16[2,64,128]{2,1,0:T(8,128)(2,1)S(1)} collective-permute-done((bf16[2,64,128]{2,1,0:T(8,128)(2,1)S(1)}, bf16[2,64,128]{2,1,0:T(8,128)(2,1)S(1)}, u32[]{:S(2)}, u32[]{:S(2)}) %collective-permute-start.7) | collective-permute-done | bytes 32800 | tf_op jit(solution)/shard_map/ppermute | solution.py:429
  94.4 9.3 %shard_map.143 = (f32[256,128]{1,0:T(8,128)S(1)}, bf16[256,128]{1,0:T(8,128)(2,1)S(1)}, f32[8,256]{1,0:T(8,128)S(1)}) custom-call(s32[5]{0:T(128)S(1)} %stack.62.where, s32[256]{0:T(256)S(1)} %copy-done.1, bf16[4,256,256]{2,1,0:T(8,128)(2,1)S(1)} %get-tuple-element.18.q_ref, bf16[256,256]{1,0:T(8,128)(2,1)S(1)} %get-tuple-element.19.uk, ...), custom_call_target="tpu_custom_call" | custom-call | tf_op jit(solution)/shard_map/pallas_call | solution.py:443
  106.3 3.5 %collective-permute-start.23 = (bf16[32,1024]{1,0:T(8,128)(2,1)S(1)}, bf16[32,1024]{1,0:T(8,128)(2,1)S(1)}, u32[]{:S(2)}, u32[]{:S(2)}) collective-permute-start(bf16[32,1024]{1,0:T(8,128)(2,1)S(1)} %get-tuple-element.29), channel_id=1, source_target_pairs={{0,4},{2,6},{4,0},{6,2},{1,5},{3,7},{5,1},{7,3},{8,12},{10,14},{12... | collective-permute-start | bytes 196616 | tf_op jit(solution)/shard_map/ppermute | solution.py:468
  109.8 1.4 %collective-permute-start.24 = (bf16[32,1024]{1,0:T(8,128)(2,1)S(1)}, bf16[32,1024]{1,0:T(8,128)(2,1)S(1)}, u32[]{:S(2)}, u32[]{:S(2)}) collective-permute-start(bf16[32,1024]{1,0:T(8,128)(2,1)S(1)} %get-tuple-element.30), channel_id=1, source_target_pairs={{0,6},{2,0},{4,2},{6,4},{1,7},{3,1},{5,3},{7,5},{8,14},{10,8},{12,... | collective-permute-start | bytes 196616 | tf_op jit(solution)/shard_map/ppermute | solution.py:468
  (58 shorter events, 16.4 us)
Async XLA Ops:
  3.3 19.4 %all-to-all-start = ((bf16[8,104,128]{2,1,0:T(8,128)(2,1)}), bf16[8,104,128]{2,1,0:T(8,128)(2,1)S(1)}, u32[]{:S(2)}, u32[]{:S(2)}) async-start(bf16[8,104,128]{2,1,0:T(8,128)(2,1)} %shard_map.140), calls=%async_computation | async-start | bytes 425984 | tf_op jit(solution)/shard_map/all_to_all | solution.py:407
  11.9 15.8 %collective-permute-start.1 = (bf16[32,1024]{1,0:T(8,128)(2,1)S(1)}, bf16[32,1024]{1,0:T(8,128)(2,1)S(1)}, u32[]{:S(2)}, u32[]{:S(2)}) collective-permute-start(bf16[32,1024]{1,0:T(8,128)(2,1)S(1)} %copy-done), channel_id=1, source_target_pairs={{0,4},{2,6},{4,0},{6,2},{1,5},{3,7},{5,1},{7,3},{8,12},{10,14},{12... | collective-permute-start | bytes 196616 | tf_op jit(solution)/shard_map/ppermute | solution.py:411
  22.7 9.2 %collective-permute-start.5 = (bf16[8,40,128]{2,1,0:T(8,128)(2,1)S(1)}, bf16[8,40,128]{2,1,0:T(8,128)(2,1)S(1)}, u32[]{:S(2)}, u32[]{:S(2)}) collective-permute-start(bf16[8,40,128]{2,1,0:T(8,128)(2,1)S(1)} %slice.8), channel_id=1, source_target_pairs={{0,24},{8,0},{16,8},{24,16},{1,25},{9,1},{17,9},{25,17},{2,26},{10... | collective-permute-start | bytes 245768 | tf_op jit(solution)/shard_map/ppermute | solution.py:409
  23.3 8.6 %collective-permute-start.4 = (bf16[8,40,128]{2,1,0:T(8,128)(2,1)S(1)}, bf16[8,40,128]{2,1,0:T(8,128)(2,1)S(1)}, u32[]{:S(2)}, u32[]{:S(2)}) collective-permute-start(bf16[8,40,128]{2,1,0:T(8,128)(2,1)S(1)} %slice.8), channel_id=1, source_target_pairs={{0,16},{8,24},{16,0},{24,8},{1,17},{9,25},{17,1},{25,9},{2,18},{10... | collective-permute-start | bytes 245768 | tf_op jit(solution)/shard_map/ppermute | solution.py:409
  26.1 5.9 %collective-permute-start.3 = (bf16[8,40,128]{2,1,0:T(8,128)(2,1)S(1)}, bf16[8,40,128]{2,1,0:T(8,128)(2,1)S(1)}, u32[]{:S(2)}, u32[]{:S(2)}) collective-permute-start(bf16[8,40,128]{2,1,0:T(8,128)(2,1)S(1)} %slice.8), channel_id=1, source_target_pairs={{0,8},{8,16},{16,24},{24,0},{1,9},{9,17},{17,25},{25,1},{2,10},{10... | collective-permute-start | bytes 245768 | tf_op jit(solution)/shard_map/ppermute | solution.py:409
  26.1 5.5 %collective-permute-start = (bf16[32,1024]{1,0:T(8,128)(2,1)S(1)}, bf16[32,1024]{1,0:T(8,128)(2,1)S(1)}, u32[]{:S(2)}, u32[]{:S(2)}) collective-permute-start(bf16[32,1024]{1,0:T(8,128)(2,1)S(1)} %copy-done), channel_id=1, source_target_pairs={{0,2},{2,4},{4,6},{6,0},{1,3},{3,5},{5,7},{7,1},{8,10},{10,12},{12... | collective-permute-start | bytes 196616 | tf_op jit(solution)/shard_map/ppermute | solution.py:411
  27.7 4.3 %collective-permute-start.2 = (bf16[32,1024]{1,0:T(8,128)(2,1)S(1)}, bf16[32,1024]{1,0:T(8,128)(2,1)S(1)}, u32[]{:S(2)}, u32[]{:S(2)}) collective-permute-start(bf16[32,1024]{1,0:T(8,128)(2,1)S(1)} %copy-done), channel_id=1, source_target_pairs={{0,6},{2,0},{4,2},{6,4},{1,7},{3,1},{5,3},{7,5},{8,14},{10,8},{12,... | collective-permute-start | bytes 196616 | tf_op jit(solution)/shard_map/ppermute | solution.py:411
  44.5 8.3 %collective-permute-start.16 = (bf16[8,72,128]{2,1,0:T(8,128)(2,1)S(1)}, bf16[8,72,128]{2,1,0:T(8,128)(2,1)S(1)}, u32[]{:S(2)}, u32[]{:S(2)}) collective-permute-start(bf16[8,72,128]{2,1,0:T(8,128)(2,1)S(1)} %all_to_all.10), channel_id=1, source_target_pairs={{0,24},{1,7},{2,26},{3,1},{4,28},{5,3},{6,30},{7,5},{8,0},{9,15},{... | collective-permute-start | bytes 442376 | tf_op jit(solution)/shard_map/ppermute | solution.py:420
  46.5 8.7 %collective-permute-start.15 = (bf16[8,72,128]{2,1,0:T(8,128)(2,1)S(1)}, bf16[8,72,128]{2,1,0:T(8,128)(2,1)S(1)}, u32[]{:S(2)}, u32[]{:S(2)}) collective-permute-start(bf16[8,72,128]{2,1,0:T(8,128)(2,1)S(1)} %all_to_all.10), channel_id=1, source_target_pairs={{0,16},{1,5},{2,18},{3,7},{4,20},{5,1},{6,22},{7,3},{8,24},{9,13},... | collective-permute-start | bytes 442376 | tf_op jit(solution)/shard_map/ppermute | solution.py:420
  48.5 6.7 %collective-permute-start.14 = (bf16[8,72,128]{2,1,0:T(8,128)(2,1)S(1)}, bf16[8,72,128]{2,1,0:T(8,128)(2,1)S(1)}, u32[]{:S(2)}, u32[]{:S(2)}) collective-permute-start(bf16[8,72,128]{2,1,0:T(8,128)(2,1)S(1)} %all_to_all.10), channel_id=1, source_target_pairs={{0,8},{1,3},{2,10},{3,5},{4,12},{5,7},{6,14},{7,1},{8,16},{9,11},{... | collective-permute-start | bytes 442376 | tf_op jit(solution)/shard_map/ppermute | solution.py:420
  48.9 18.9 %collective-permute-start.11 = (bf16[8,64,128]{2,1,0:T(8,128)(2,1)S(1)}, bf16[8,64,128]{2,1,0:T(8,128)(2,1)S(1)}, u32[]{:S(2)}, u32[]{:S(2)}) collective-permute-start(bf16[8,64,128]{2,1,0:T(8,128)(2,1)S(1)} %get-tuple-element.33), channel_id=1, source_target_pairs={{0,16},{8,24},{16,0},{24,8},{1,17},{9,25},{17,1},{25,9},{2,18},{10... | collective-permute-start | bytes 393224 | tf_op jit(solution)/shard_map/ppermute | solution.py:425
  50.2 18.2 %collective-permute-start.10 = (bf16[8,64,128]{2,1,0:T(8,128)(2,1)S(1)}, bf16[8,64,128]{2,1,0:T(8,128)(2,1)S(1)}, u32[]{:S(2)}, u32[]{:S(2)}) collective-permute-start(bf16[8,64,128]{2,1,0:T(8,128)(2,1)S(1)} %get-tuple-element.33), channel_id=1, source_target_pairs={{0,8},{8,16},{16,24},{24,0},{1,9},{9,17},{17,25},{25,1},{2,10},{10... | collective-permute-start | bytes 393224 | tf_op jit(solution)/shard_map/ppermute | solution.py:425
  52.8 15.7 %collective-permute-start.12 = (bf16[8,64,128]{2,1,0:T(8,128)(2,1)S(1)}, bf16[8,64,128]{2,1,0:T(8,128)(2,1)S(1)}, u32[]{:S(2)}, u32[]{:S(2)}) collective-permute-start(bf16[8,64,128]{2,1,0:T(8,128)(2,1)S(1)} %get-tuple-element.33), channel_id=1, source_target_pairs={{0,24},{8,0},{16,8},{24,16},{1,25},{9,1},{17,9},{25,17},{2,26},{10... | collective-permute-start | bytes 393224 | tf_op jit(solution)/shard_map/ppermute | solution.py:425
  55.3 39.1 %collective-permute-start.19 = (bf16[4,8,72,128]{3,2,1,0:T(8,128)(2,1)S(1)}, bf16[4,8,72,128]{3,2,1,0:T(8,128)(2,1)S(1)}, u32[]{:S(2)}, u32[]{:S(2)}) collective-permute-start(bf16[4,8,72,128]{3,2,1,0:T(8,128)(2,1)S(1)} %pad_maximum_fusion.b0), channel_id=1, source_target_pairs={{0,6},{1,25},{2,0},{3,27},{4,2},{5,29},{6,4},{7,31},{8,14},{9,1},{... | collective-permute-start | bytes 1769480 | tf_op jit(solution)/shard_map/ppermute | solution.py:422
  67.0 27.4 %collective-permute-start.18 = (bf16[4,8,72,128]{3,2,1,0:T(8,128)(2,1)S(1)}, bf16[4,8,72,128]{3,2,1,0:T(8,128)(2,1)S(1)}, u32[]{:S(2)}, u32[]{:S(2)}) collective-permute-start(bf16[4,8,72,128]{3,2,1,0:T(8,128)(2,1)S(1)} %pad_maximum_fusion.b0), channel_id=1, source_target_pairs={{0,4},{1,17},{2,6},{3,19},{4,0},{5,21},{6,2},{7,23},{8,12},{9,25},... | collective-permute-start | bytes 1769480 | tf_op jit(solution)/shard_map/ppermute | solution.py:422
  67.8 26.7 %collective-permute-start.17 = (bf16[4,8,72,128]{3,2,1,0:T(8,128)(2,1)S(1)}, bf16[4,8,72,128]{3,2,1,0:T(8,128)(2,1)S(1)}, u32[]{:S(2)}, u32[]{:S(2)}) collective-permute-start(bf16[4,8,72,128]{3,2,1,0:T(8,128)(2,1)S(1)} %pad_maximum_fusion.b0), channel_id=1, source_target_pairs={{0,2},{1,9},{2,4},{3,11},{4,6},{5,13},{6,0},{7,15},{8,10},{9,17},{... | collective-permute-start | bytes 1769480 | tf_op jit(solution)/shard_map/ppermute | solution.py:422
  68.5 23.9 %collective-permute-start.13 = (bf16[4,8,64,128]{3,2,1,0:T(8,128)(2,1)S(1)}, bf16[4,8,64,128]{3,2,1,0:T(8,128)(2,1)S(1)}, u32[]{:S(2)}, u32[]{:S(2)}) collective-permute-start(bf16[4,8,64,128]{3,2,1,0:T(8,128)(2,1)S(1)} %pad_maximum_fusion.1.up_own.w_own), channel_id=1, source_target_pairs={{0,1},{1,0},{2,3},{3,2},{4,5},{5,4},{6,7},{7,6},{8,9},{9,8},{10,11... | collective-permute-start | bytes 1572872 | tf_op jit(solution)/shard_map/ppermute | solution.py:427
  68.6 1.9 %collective-permute-start.6 = (bf16[64,128]{1,0:T(8,128)(2,1)S(1)}, bf16[64,128]{1,0:T(8,128)(2,1)S(1)}, u32[]{:S(2)}, u32[]{:S(2)}) collective-permute-start(bf16[64,128]{1,0:T(8,128)(2,1)S(1)} %get-tuple-element.17), channel_id=1, source_target_pairs={{0,1},{1,0},{2,3},{3,2},{4,5},{5,4},{6,7},{7,6},{8,9},{9,8},{10,11... | collective-permute-start | bytes 49160 | tf_op jit(solution)/shard_map/ppermute | solution.py:428
  70.6 10.9 %collective-permute-start.9 = (bf16[2,64,128]{2,1,0:T(8,128)(2,1)S(1)}, bf16[2,64,128]{2,1,0:T(8,128)(2,1)S(1)}, u32[]{:S(2)}, u32[]{:S(2)}) collective-permute-start(bf16[2,64,128]{2,1,0:T(8,128)(2,1)S(1)} %pad_maximum_fusion.2.q0), channel_id=1, source_target_pairs={{0,6},{2,0},{4,2},{6,4},{1,7},{3,1},{5,3},{7,5},{8,14},{10,8},{12,... | collective-permute-start | bytes 98312 | tf_op jit(solution)/shard_map/ppermute | solution.py:429
  81.4 5.4 %collective-permute-start.8 = (bf16[2,64,128]{2,1,0:T(8,128)(2,1)S(1)}, bf16[2,64,128]{2,1,0:T(8,128)(2,1)S(1)}, u32[]{:S(2)}, u32[]{:S(2)}) collective-permute-start(bf16[2,64,128]{2,1,0:T(8,128)(2,1)S(1)} %pad_maximum_fusion.2.q0), channel_id=1, source_target_pairs={{0,4},{2,6},{4,0},{6,2},{1,5},{3,7},{5,1},{7,3},{8,12},{10,14},{12... | collective-permute-start | bytes 98312 | tf_op jit(solution)/shard_map/ppermute | solution.py:429
  86.8 5.6 %collective-permute-start.7 = (bf16[2,64,128]{2,1,0:T(8,128)(2,1)S(1)}, bf16[2,64,128]{2,1,0:T(8,128)(2,1)S(1)}, u32[]{:S(2)}, u32[]{:S(2)}) collective-permute-start(bf16[2,64,128]{2,1,0:T(8,128)(2,1)S(1)} %pad_maximum_fusion.2.q0), channel_id=1, source_target_pairs={{0,2},{2,4},{4,6},{6,0},{1,3},{3,5},{5,7},{7,1},{8,10},{10,12},{12... | collective-permute-start | bytes 98312 | tf_op jit(solution)/shard_map/ppermute | solution.py:429
  106.2 6.0 %collective-permute-start.22 = (bf16[32,1024]{1,0:T(8,128)(2,1)S(1)}, bf16[32,1024]{1,0:T(8,128)(2,1)S(1)}, u32[]{:S(2)}, u32[]{:S(2)}) collective-permute-start(bf16[32,1024]{1,0:T(8,128)(2,1)S(1)} %get-tuple-element.28), channel_id=1, source_target_pairs={{0,2},{2,4},{4,6},{6,0},{1,3},{3,5},{5,7},{7,1},{8,10},{10,12},{12... | collective-permute-start | bytes 196616 | tf_op jit(solution)/shard_map/ppermute | solution.py:468
  106.3 7.2 %collective-permute-start.23 = (bf16[32,1024]{1,0:T(8,128)(2,1)S(1)}, bf16[32,1024]{1,0:T(8,128)(2,1)S(1)}, u32[]{:S(2)}, u32[]{:S(2)}) collective-permute-start(bf16[32,1024]{1,0:T(8,128)(2,1)S(1)} %get-tuple-element.29), channel_id=1, source_target_pairs={{0,4},{2,6},{4,0},{6,2},{1,5},{3,7},{5,1},{7,3},{8,12},{10,14},{12... | collective-permute-start | bytes 196616 | tf_op jit(solution)/shard_map/ppermute | solution.py:468
  109.8 4.3 %collective-permute-start.24 = (bf16[32,1024]{1,0:T(8,128)(2,1)S(1)}, bf16[32,1024]{1,0:T(8,128)(2,1)S(1)}, u32[]{:S(2)}, u32[]{:S(2)}) collective-permute-start(bf16[32,1024]{1,0:T(8,128)(2,1)S(1)} %get-tuple-element.30), channel_id=1, source_target_pairs={{0,6},{2,0},{4,2},{6,4},{1,7},{3,1},{5,3},{7,5},{8,14},{10,8},{12,... | collective-permute-start | bytes 196616 | tf_op jit(solution)/shard_map/ppermute | solution.py:468
  (7 other events, 54.0 us)

commit v6 on v4

--- a/solution.py
+++ b/solution.py
@@ -29,7 +29,7 @@
 VMEM = pltpu.VMEM
 SMEM_SPEC = pl.BlockSpec(memory_space=pltpu.SMEM)
 VMEM_SPEC = pl.BlockSpec(memory_space=pltpu.VMEM)
-ANY_SPEC = pl.BlockSpec(memory_space=pl.ANY)
+ANY_SPEC = pl.BlockSpec(memory_space=pltpu.HBM)
 
 
 def call(body, outs, n_smem, n_in, scratch=(), any_from=None, cost=None, room=16):
@@ -64,7 +64,15 @@
     return value
 
 
-def pack(where, dq, dk, dr, out, flipped):
+def pack(where, dq_in, dk_in, dr_in, out, flipped, dq, dk, dr, sems):
+    copies = [
+        pltpu.make_async_copy(source, place, sems.at[i])
+        for i, (source, place) in enumerate(((dq_in, dq), (dk_in, dk), (dr_in, dr)))
+    ]
+    for copy in copies:
+        copy.start()
+    for copy in copies:
+        copy.wait()
     y = where[2]
 
     def chosen(ref):
@@ -148,11 +156,12 @@
 
 
 def make_queries(
-    where, q0, q1, q2, q3, up_own, up_other, gain, out, uk_ref, uv_ref, docs_ref, latents, ups
+    where, q0, q1, q2, q3, q_other, up_own, up_other, gain, key_gain, docs_in,
+    out, uk_ref, uv_ref, docs_ref, col_ref, row_ref, latents, ups,
 ):
     x, y, c = where[1], where[2], where[3]
     for j, part in enumerate((q0, q1, q2, q3)):
-        own, other = part[0].astype(F32), part[1].astype(F32)
+        own, other = part[...].astype(F32), q_other[j].astype(F32)
         rows = pl.ds(pl.multiple_of(lax.rem(y - j + NY, NY) * 64, 64), 64)
         latents[rows, 0:128] = jnp.where(c == 0, own, other)
         latents[rows, 128:256] = jnp.where(c == 0, other, own)
@@ -161,6 +170,16 @@
     inverse = lax.rsqrt(mean + EPS)
     gains = jnp.concatenate([column(gain[0:1, :]), column(gain[1:2, :])], axis=0)
     gains = jnp.concatenate([gains, gains], axis=1)
+    tokens_docs = docs_in[...].astype(F32)
+    at = lanes((1, 128))
+    for i in range(2):
+        col_ref[128 * i : 128 * (i + 1), :] = column(key_gain[i : i + 1, :])
+        ordered = jnp.zeros((1, 128), F32)
+        for k in range(NY):
+            line = tokens_docs[k // 2 : k // 2 + 1, :]
+            moved = pltpu.roll(line, (32 * k - 64 * (k % 2) - 32 * i) % 128, 1)
+            ordered = jnp.where(at // 32 == k, moved, ordered)
+        row_ref[i : i + 1, :] = ordered
     latent = (raw * inverse * gains).astype(BF)
     tok = lanes((64, 256))
     row = lax.broadcasted_iota(jnp.int32, (64, 256), 0)
@@ -199,8 +218,8 @@
 
 
 def attend(
-    where, ids, q_ref, uk, uv, key_docs, gain, query_docs, b0, b1, b2, b3,
-    keep_ref, send_ref, ml_ref, kb, s_buf, v_buf, mx, total, acc, gains,
+    where, ids, q_ref, uk, uv, key_docs, gains, query_docs, b0, b1, b2, b3,
+    keep_ref, send_ref, ml_ref, kb, s_buf, v_buf, mx, total, acc,
 ):
     x0, y0, c = where[1], where[2], where[3]
     docs = key_docs[...]
@@ -219,8 +238,6 @@
         return carry
 
     lax.fori_loop(first // 2, (last + 1) // 2, fetch, 0)
-    for i in range(2):
-        gains[128 * i : 128 * (i + 1), :] = column(gain[i : i + 1, :])
     mx[...] = jnp.full(mx.shape, NEG_BIG, F32)
     total[...] = jnp.zeros(total.shape, F32)
     acc[...] = jnp.zeros(acc.shape, F32)
@@ -378,9 +395,13 @@
     here = jnp.stack([z, x, y, c, sp * 256]).astype(jnp.int32)
     swap = [(0, 1), (1, 0)]
 
+    sources = (down_query, down_key, down_rotary)
     message = call(
-        pack, jax.ShapeDtypeStruct((NZ, 40, 128), BF), 1, 3, scratch=[VMEM((128, 128), F32)]
-    )(here, down_query, down_key, down_rotary)
+        pack, jax.ShapeDtypeStruct((NZ, 40, 128), BF), 1, 3, any_from=0,
+        scratch=[VMEM((128, 128), F32)]
+        + [VMEM(a.shape, a.dtype) for a in sources]
+        + [pltpu.SemaphoreType.DMA((3,))],
+    )(here, *(pltpu.with_memory_space_constraint(a, pltpu.HBM) for a in sources))
     gathered = lax.all_to_all(message, "z", 0, 0)
     gathered = [gathered] + [lax.ppermute(gathered, "x", ring(j)) for j in range(1, NX)]
 
@@ -405,20 +426,24 @@
 
     up_own = lax.all_to_all(later, "z", 0, 0)
     up_other = lax.ppermute(up_own, "c", swap)
-    q_pair = jnp.stack([q_part, lax.ppermute(q_part, "c", swap)])
-    q_all = [q_pair] + [lax.ppermute(q_pair, "y", ring(j)) for j in range(1, NY)]
-    queries, uk, uv, key_docs = call(
+    q_all = [q_part] + [lax.ppermute(q_part, "y", ring(j)) for j in range(1, NY)]
+    q_other = lax.ppermute(jnp.stack(q_all), "c", swap)
+    queries, uk, uv, key_docs, gains, query_docs = call(
         make_queries,
         (
             jax.ShapeDtypeStruct((4, 256, 256), BF),
             jax.ShapeDtypeStruct((256, 256), BF),
             jax.ShapeDtypeStruct((256, 256), BF),
             jax.ShapeDtypeStruct((NS, 128), F32),
+            jax.ShapeDtypeStruct((256, 128), F32),
+            jax.ShapeDtypeStruct((2, 128), F32),
         ),
-        1, 7, scratch=[VMEM((256, 256), F32), VMEM((2, NZ, NX, 32, 128), BF)],
-    )(here, *q_all, up_own, up_other, query_gain.reshape(2, 128))
-
-    query_docs = doc_ids.astype(F32).reshape(4, 2, 32).transpose(1, 0, 2).reshape(2, 128)
+        1, 10, scratch=[VMEM((256, 256), F32), VMEM((2, NZ, NX, 32, 128), BF)],
+    )(
+        here, *q_all, q_other, up_own, up_other, query_gain.reshape(2, 128),
+        key_gain.reshape(2, 128), doc_ids.reshape(2, 128),
+    )
+
     keep, send, ml = call(
         attend,
         (
@@ -434,9 +459,8 @@
             VMEM((4, 8, 256), F32),
             VMEM((4, 8, 256), F32),
             VMEM((256, 256), F32),
-            VMEM((256, 128), F32),
         ],
-    )(here, doc_ids, queries, uk, uv, key_docs, key_gain.reshape(2, 128), query_docs, held, *stage3)
+    )(here, doc_ids, queries, uk, uv, key_docs, gains, query_docs, held, *stage3)
 
     got = lax.ppermute(send, "c", swap)
     ml_got = lax.ppermute(ml, "c", swap)

time: 121 us -> 122 us (level)
  starting transfers between devices: 62.5 us -> 72.2 us
  waiting for transfers between devices: 37.7 us -> 29 us
    ppermute x4, starting transfers between devices: 3.12 us -> 16.3 us  [the longest x1 10.8 us: layer(): q_other = lax.ppermute(jnp.stack(q_all), 'c', swap)]
    ppermute x4, waiting for transfers between devices: 16.8 us -> 8.18 us  [the longest x3 7.27 us: layer(): lax.ppermute(q_part, 'y', ring(j))]
    ppermute x1, starting transfers between devices: 3.96 us -> 0.44 us  [layer(): got = lax.ppermute(send, 'c', swap)]
where the time goes in v6:
time: 122 us
  starting transfers between devices  72.2 us (59%)
  waiting for transfers between devices  29 us (24%)
  Pallas kernels  16.3 us (13%)
  local copies, waits for them, and re-layouts  3.09 us (3%)
    ppermute x1, starting transfers between devices, layer(): up_other = lax.ppermute(up_own, 'c', swap)  14.6 us
    ppermute x1, starting transfers between devices, layer(): q_other = lax.ppermute(jnp.stack(q_all), 'c', swap)  10.8 us
    pallas_call x1, Pallas kernels, layer(): call(attend, (jax.ShapeDtypeStruct((256, 128), F32), jax.ShapeDtypeStruct...  9.31 us
    all_to_all x1, starting transfers between devices, layer(): gathered = lax.all_to_all(message, 'z', 0, 0)  9.15 us
    ppermute x3, waiting for transfers between devices, layer(): lax.ppermute(q_part, 'y', ring(j))  7.27 us
    all_to_all x1, starting transfers between devices, layer(): up_own = lax.all_to_all(later, 'z', 0, 0)  6.56 us
    ppermute x3, waiting for transfers between devices, layer(): lax.ppermute(stage1, AXES, shift_pairs(2, j))  5.95 us
    ppermute x3, starting transfers between devices, layer(): rows = [tokens] + [lax.ppermute(tokens, 'y', ring(j)) for j in range(1, NY)]  5.74 us
  transfers between devices with their start and end apart: 28, of which 17 were waited for; matrix products, arithmetic and copies ran while one was open for 1% of the time, Pallas kernels for 1%

profile of v6, /device:TPU:1, one launch (start us, length us, event | category | flops | bytes accessed | tf_op | source)
XLA Modules:
  0.0 121.5 jit_solution(10404092316954313064)
XLA Ops:
  0.7 2.2 %shard_map.131 = bf16[8,40,128]{2,1,0:T(8,128)(2,1)} custom-call(s32[5]{0:T(128)S(1)} %stack.68.where, bf16[32,256]{1,0:T(8,128)(2,1)} %dq_in.1, bf16[32,256]{1,0:T(8,128)(2,1)} %dk_in.1, bf16[32,32]{1,0:T(8,128)(2,1)} %dr_in.1), custom_call_target="tpu_custom_call" | custom-call | tf_op jit(solution)/shard_map/pallas_call | solution.py:399
  3.0 9.1 %all-to-all-start = ((bf16[8,40,128]{2,1,0:T(8,128)(2,1)}), bf16[8,40,128]{2,1,0:T(8,128)(2,1)S(1)}, u32[]{:S(2)}, u32[]{:S(2)}) async-start(bf16[8,40,128]{2,1,0:T(8,128)(2,1)} %shard_map.131), calls=%async_computation | async-start | bytes 163840 | tf_op jit(solution)/shard_map/all_to_all | solution.py:405
  12.1 3.0 %collective-permute-start.1 = (bf16[32,1024]{1,0:T(8,128)(2,1)S(1)}, bf16[32,1024]{1,0:T(8,128)(2,1)S(1)}, u32[]{:S(2)}, u32[]{:S(2)}) collective-permute-start(bf16[32,1024]{1,0:T(8,128)(2,1)S(1)} %copy-done), channel_id=1, source_target_pairs={{0,4},{2,6},{4,0},{6,2},{1,5},{3,7},{5,1},{7,3},{8,12},{10,14},{12... | collective-permute-start | bytes 196616 | tf_op jit(solution)/shard_map/ppermute | solution.py:408
  15.1 4.5 %all-to-all-done.g0 = bf16[8,40,128]{2,1,0:T(8,128)(2,1)S(1)} async-done(((bf16[8,40,128]{2,1,0:T(8,128)(2,1)}), bf16[8,40,128]{2,1,0:T(8,128)(2,1)S(1)}, u32[]{:S(2)}, u32[]{:S(2)}) %all-to-all-start) | async-done | bytes 81952 | tf_op jit(solution)/shard_map/all_to_all | solution.py:405
  19.6 2.5 %collective-permute-start.5 = (bf16[8,40,128]{2,1,0:T(8,128)(2,1)S(1)}, bf16[8,40,128]{2,1,0:T(8,128)(2,1)S(1)}, u32[]{:S(2)}, u32[]{:S(2)}) collective-permute-start(bf16[8,40,128]{2,1,0:T(8,128)(2,1)S(1)} %all-to-all-done.g0), channel_id=1, source_target_pairs={{0,24},{8,0},{16,8},{24,16},{1,25},{9,1},{17,9},{25,17},{2,26},{10... | collective-permute-start | bytes 245768 | tf_op jit(solution)/shard_map/ppermute | solution.py:406
  26.0 1.6 %collective-permute-done.t1 = bf16[32,1024]{1,0:T(8,128)(2,1)S(1)} collective-permute-done((bf16[32,1024]{1,0:T(8,128)(2,1)S(1)}, bf16[32,1024]{1,0:T(8,128)(2,1)S(1)}, u32[]{:S(2)}, u32[]{:S(2)}) %collective-permute-start) | collective-permute-done | bytes 65568 | tf_op jit(solution)/shard_map/ppermute | solution.py:408
  27.8 1.6 %shard_map.132 = (bf16[64,128]{1,0:T(8,128)(2,1)S(1)}, bf16[8,72,128]{2,1,0:T(8,128)(2,1)}) custom-call(s32[5]{0:T(128)S(1)} %stack.68.where, bf16[32,1024]{1,0:T(8,128)(2,1)S(1)} %copy-done, bf16[32,1024]{1,0:T(8,128)(2,1)S(1)} %collective-permute-done.t1, bf16[32,1024]{1,0:T(8,128)(2,1)S(1)} %collective-permute-done.1.t2, ...), custom_call_target="tpu_custom_call" | custom-call | tf_op jit(solution)/shard_map/pallas_call | solution.py:416
  29.3 3.5 %all-to-all-start.2 = ((bf16[8,72,128]{2,1,0:T(8,128)(2,1)}), bf16[8,72,128]{2,1,0:T(8,128)(2,1)S(1)}, u32[]{:S(2)}, u32[]{:S(2)}) async-start(bf16[8,72,128]{2,1,0:T(8,128)(2,1)} %get-tuple-element.25), calls=%async_computation.2 | async-start | bytes 294912 | tf_op jit(solution)/shard_map/all_to_all | solution.py:422
  33.7 2.3 %collective-permute-start.12 = (bf16[64,128]{1,0:T(8,128)(2,1)S(1)}, bf16[64,128]{1,0:T(8,128)(2,1)S(1)}, u32[]{:S(2)}, u32[]{:S(2)}) collective-permute-start(bf16[64,128]{1,0:T(8,128)(2,1)S(1)} %shard_map.133), channel_id=1, source_target_pairs={{0,24},{8,0},{16,8},{24,16},{1,25},{9,1},{17,9},{25,17},{2,26},{10... | collective-permute-start | bytes 49160 | tf_op jit(solution)/shard_map/ppermute | solution.py:413
  37.3 2.8 %collective-permute-done.11 = bf16[64,128]{1,0:T(8,128)(2,1)S(1)} collective-permute-done((bf16[64,128]{1,0:T(8,128)(2,1)S(1)}, bf16[64,128]{1,0:T(8,128)(2,1)S(1)}, u32[]{:S(2)}, u32[]{:S(2)}) %collective-permute-start.11) | collective-permute-done | bytes 16416 | tf_op jit(solution)/shard_map/ppermute | solution.py:413
  42.0 6.6 %all-to-all-start.1 = ((bf16[8,4,64,128]{3,2,1,0:T(8,128)(2,1)}), bf16[8,4,64,128]{3,2,1,0:T(8,128)(2,1)S(1)}, u32[]{:S(2)}, u32[]{:S(2)}) async-start(bf16[8,4,64,128]{3,2,1,0:T(8,128)(2,1)} %broadcast_in_dim.2), calls=%async_computation.1 | async-start | bytes 1048576 | tf_op jit(solution)/shard_map/all_to_all | solution.py:427
  48.6 2.4 %collective-permute-start.16 = (bf16[8,72,128]{2,1,0:T(8,128)(2,1)S(1)}, bf16[8,72,128]{2,1,0:T(8,128)(2,1)S(1)}, u32[]{:S(2)}, u32[]{:S(2)}) collective-permute-start(bf16[8,72,128]{2,1,0:T(8,128)(2,1)S(1)} %all-to-all-done.2), channel_id=1, source_target_pairs={{0,24},{1,7},{2,26},{3,1},{4,28},{5,3},{6,30},{7,5},{8,0},{9,15},{... | collective-permute-start | bytes 442376 | tf_op jit(solution)/shard_map/ppermute | solution.py:423
  52.1 2.5 %collective-permute-done.16 = bf16[8,72,128]{2,1,0:T(8,128)(2,1)S(1)} collective-permute-done((bf16[8,72,128]{2,1,0:T(8,128)(2,1)S(1)}, bf16[8,72,128]{2,1,0:T(8,128)(2,1)S(1)}, u32[]{:S(2)}, u32[]{:S(2)}) %collective-permute-start.16) | collective-permute-done | bytes 147488 | tf_op jit(solution)/shard_map/ppermute | solution.py:423
  54.6 1.9 %collective-permute-done.15 = bf16[8,72,128]{2,1,0:T(8,128)(2,1)S(1)} collective-permute-done((bf16[8,72,128]{2,1,0:T(8,128)(2,1)S(1)}, bf16[8,72,128]{2,1,0:T(8,128)(2,1)S(1)}, u32[]{:S(2)}, u32[]{:S(2)}) %collective-permute-start.15) | collective-permute-done | bytes 147488 | tf_op jit(solution)/shard_map/ppermute | solution.py:423
  56.5 1.5 %collective-permute-done.14 = bf16[8,72,128]{2,1,0:T(8,128)(2,1)S(1)} collective-permute-done((bf16[8,72,128]{2,1,0:T(8,128)(2,1)S(1)}, bf16[8,72,128]{2,1,0:T(8,128)(2,1)S(1)}, u32[]{:S(2)}, u32[]{:S(2)}) %collective-permute-start.14) | collective-permute-done | bytes 147488 | tf_op jit(solution)/shard_map/ppermute | solution.py:423
  60.8 14.6 %collective-permute-start.13 = (bf16[8,4,64,128]{3,2,1,0:T(8,128)(2,1)S(1)}, bf16[8,4,64,128]{3,2,1,0:T(8,128)(2,1)S(1)}, u32[]{:S(2)}, u32[]{:S(2)}) collective-permute-start(bf16[8,4,64,128]{3,2,1,0:T(8,128)(2,1)S(1)} %all-to-all-done.1.up_own.w_own), channel_id=1, source_target_pairs={{0,1},{1,0},{2,3},{3,2},{4,5},{5,4},{6,7},{7,6},{8,9},{9,8},{10,11... | collective-permute-start | bytes 1572872 | tf_op jit(solution)/shard_map/ppermute | solution.py:428
  75.5 2.3 %collective-permute-start.8 = (bf16[64,128]{1,0:T(8,128)(2,1)S(1)}, bf16[64,128]{1,0:T(8,128)(2,1)S(1)}, u32[]{:S(2)}, u32[]{:S(2)}) collective-permute-start(bf16[64,128]{1,0:T(8,128)(2,1)S(1)} %get-tuple-element.18.q0), channel_id=1, source_target_pairs={{0,6},{2,0},{4,2},{6,4},{1,7},{3,1},{5,3},{7,5},{8,14},{10,8},{12,... | collective-permute-start | bytes 49160 | tf_op jit(solution)/shard_map/ppermute | solution.py:429
  78.9 1.7 %collective-permute-start.7 = (bf16[64,128]{1,0:T(8,128)(2,1)S(1)}, bf16[64,128]{1,0:T(8,128)(2,1)S(1)}, u32[]{:S(2)}, u32[]{:S(2)}) collective-permute-start(bf16[64,128]{1,0:T(8,128)(2,1)S(1)} %get-tuple-element.18.q0), channel_id=1, source_target_pairs={{0,4},{2,6},{4,0},{6,2},{1,5},{3,7},{5,1},{7,3},{8,12},{10,14},{12... | collective-permute-start | bytes 49160 | tf_op jit(solution)/shard_map/ppermute | solution.py:429
  80.5 2.9 %collective-permute-done.7.q2 = bf16[64,128]{1,0:T(8,128)(2,1)S(1)} collective-permute-done((bf16[64,128]{1,0:T(8,128)(2,1)S(1)}, bf16[64,128]{1,0:T(8,128)(2,1)S(1)}, u32[]{:S(2)}, u32[]{:S(2)}) %collective-permute-start.7) | collective-permute-done | bytes 16416 | tf_op jit(solution)/shard_map/ppermute | solution.py:429
  84.9 3.3 %collective-permute-done.6.q1 = bf16[64,128]{1,0:T(8,128)(2,1)S(1)} collective-permute-done((bf16[64,128]{1,0:T(8,128)(2,1)S(1)}, bf16[64,128]{1,0:T(8,128)(2,1)S(1)}, u32[]{:S(2)}, u32[]{:S(2)}) %collective-permute-start.6) | collective-permute-done | bytes 16416 | tf_op jit(solution)/shard_map/ppermute | solution.py:429
  88.2 10.8 %collective-permute-start.9 = (bf16[4,64,128]{2,1,0:T(8,128)(2,1)S(1)}, bf16[4,64,128]{2,1,0:T(8,128)(2,1)S(1)}, u32[]{:S(2)}, u32[]{:S(2)}) collective-permute-start(bf16[4,64,128]{2,1,0:T(8,128)(2,1)S(1)} %pad_maximum_fusion.1), channel_id=1, source_target_pairs={{0,1},{1,0},{2,3},{3,2},{4,5},{5,4},{6,7},{7,6},{8,9},{9,8},{10,11... | collective-permute-start | bytes 196616 | tf_op jit(solution)/shard_map/ppermute | solution.py:430
  102.0 9.3 %shard_map.135 = (f32[256,128]{1,0:T(8,128)S(1)}, bf16[256,128]{1,0:T(8,128)(2,1)S(1)}, f32[8,256]{1,0:T(8,128)S(1)}) custom-call(s32[5]{0:T(128)S(1)} %stack.68.where, s32[256]{0:T(256)S(1)} %copy-done.1, bf16[4,256,256]{2,1,0:T(8,128)(2,1)S(1)} %get-tuple-element.19.q_ref, bf16[256,256]{1,0:T(8,128)(2,1)S(1)} %get-tuple-element.20.uk, ...), custom_call_target="tpu_custom_call" | custom-call | tf_op jit(solution)/shard_map/pallas_call | solution.py:447
  114.0 2.9 %collective-permute-start.23 = (bf16[32,1024]{1,0:T(8,128)(2,1)S(1)}, bf16[32,1024]{1,0:T(8,128)(2,1)S(1)}, u32[]{:S(2)}, u32[]{:S(2)}) collective-permute-start(bf16[32,1024]{1,0:T(8,128)(2,1)S(1)} %get-tuple-element.31), channel_id=1, source_target_pairs={{0,4},{2,6},{4,0},{6,2},{1,5},{3,7},{5,1},{7,3},{8,12},{10,14},{12... | collective-permute-start | bytes 196616 | tf_op jit(solution)/shard_map/ppermute | solution.py:472
  118.7 1.7 %collective-permute-done.23.p2 = bf16[32,1024]{1,0:T(8,128)(2,1)S(1)} collective-permute-done((bf16[32,1024]{1,0:T(8,128)(2,1)S(1)}, bf16[32,1024]{1,0:T(8,128)(2,1)S(1)}, u32[]{:S(2)}, u32[]{:S(2)}) %collective-permute-start.23) | collective-permute-done | bytes 65568 | tf_op jit(solution)/shard_map/ppermute | solution.py:472
  (65 shorter events, 23.1 us)
Async XLA Ops:
  3.0 16.7 %all-to-all-start = ((bf16[8,40,128]{2,1,0:T(8,128)(2,1)}), bf16[8,40,128]{2,1,0:T(8,128)(2,1)S(1)}, u32[]{:S(2)}, u32[]{:S(2)}) async-start(bf16[8,40,128]{2,1,0:T(8,128)(2,1)} %shard_map.131), calls=%async_computation | async-start | bytes 163840 | tf_op jit(solution)/shard_map/all_to_all | solution.py:405
  12.1 12.4 %collective-permute-start.1 = (bf16[32,1024]{1,0:T(8,128)(2,1)S(1)}, bf16[32,1024]{1,0:T(8,128)(2,1)S(1)}, u32[]{:S(2)}, u32[]{:S(2)}) collective-permute-start(bf16[32,1024]{1,0:T(8,128)(2,1)S(1)} %copy-done), channel_id=1, source_target_pairs={{0,4},{2,6},{4,0},{6,2},{1,5},{3,7},{5,1},{7,3},{8,12},{10,14},{12... | collective-permute-start | bytes 196616 | tf_op jit(solution)/shard_map/ppermute | solution.py:408
  19.6 8.0 %collective-permute-start.5 = (bf16[8,40,128]{2,1,0:T(8,128)(2,1)S(1)}, bf16[8,40,128]{2,1,0:T(8,128)(2,1)S(1)}, u32[]{:S(2)}, u32[]{:S(2)}) collective-permute-start(bf16[8,40,128]{2,1,0:T(8,128)(2,1)S(1)} %all-to-all-done.g0), channel_id=1, source_target_pairs={{0,24},{8,0},{16,8},{24,16},{1,25},{9,1},{17,9},{25,17},{2,26},{10... | collective-permute-start | bytes 245768 | tf_op jit(solution)/shard_map/ppermute | solution.py:406
  22.1 5.5 %collective-permute-start.4 = (bf16[8,40,128]{2,1,0:T(8,128)(2,1)S(1)}, bf16[8,40,128]{2,1,0:T(8,128)(2,1)S(1)}, u32[]{:S(2)}, u32[]{:S(2)}) collective-permute-start(bf16[8,40,128]{2,1,0:T(8,128)(2,1)S(1)} %all-to-all-done.g0), channel_id=1, source_target_pairs={{0,16},{8,24},{16,0},{24,8},{1,17},{9,25},{17,1},{25,9},{2,18},{10... | collective-permute-start | bytes 245768 | tf_op jit(solution)/shard_map/ppermute | solution.py:406
  22.6 5.2 %collective-permute-start.3 = (bf16[8,40,128]{2,1,0:T(8,128)(2,1)S(1)}, bf16[8,40,128]{2,1,0:T(8,128)(2,1)S(1)}, u32[]{:S(2)}, u32[]{:S(2)}) collective-permute-start(bf16[8,40,128]{2,1,0:T(8,128)(2,1)S(1)} %all-to-all-done.g0), channel_id=1, source_target_pairs={{0,8},{8,16},{16,24},{24,0},{1,9},{9,17},{17,25},{25,1},{2,10},{10... | collective-permute-start | bytes 245768 | tf_op jit(solution)/shard_map/ppermute | solution.py:406
  23.2 4.4 %collective-permute-start = (bf16[32,1024]{1,0:T(8,128)(2,1)S(1)}, bf16[32,1024]{1,0:T(8,128)(2,1)S(1)}, u32[]{:S(2)}, u32[]{:S(2)}) collective-permute-start(bf16[32,1024]{1,0:T(8,128)(2,1)S(1)} %copy-done), channel_id=1, source_target_pairs={{0,2},{2,4},{4,6},{6,0},{1,3},{3,5},{5,7},{7,1},{8,10},{10,12},{12... | collective-permute-start | bytes 196616 | tf_op jit(solution)/shard_map/ppermute | solution.py:408
  29.3 11.8 %all-to-all-start.2 = ((bf16[8,72,128]{2,1,0:T(8,128)(2,1)}), bf16[8,72,128]{2,1,0:T(8,128)(2,1)S(1)}, u32[]{:S(2)}, u32[]{:S(2)}) async-start(bf16[8,72,128]{2,1,0:T(8,128)(2,1)} %get-tuple-element.25), calls=%async_computation.2 | async-start | bytes 294912 | tf_op jit(solution)/shard_map/all_to_all | solution.py:422
  33.7 3.6 %collective-permute-start.12 = (bf16[64,128]{1,0:T(8,128)(2,1)S(1)}, bf16[64,128]{1,0:T(8,128)(2,1)S(1)}, u32[]{:S(2)}, u32[]{:S(2)}) collective-permute-start(bf16[64,128]{1,0:T(8,128)(2,1)S(1)} %shard_map.133), channel_id=1, source_target_pairs={{0,24},{8,0},{16,8},{24,16},{1,25},{9,1},{17,9},{25,17},{2,26},{10... | collective-permute-start | bytes 49160 | tf_op jit(solution)/shard_map/ppermute | solution.py:413
  36.1 4.1 %collective-permute-start.11 = (bf16[64,128]{1,0:T(8,128)(2,1)S(1)}, bf16[64,128]{1,0:T(8,128)(2,1)S(1)}, u32[]{:S(2)}, u32[]{:S(2)}) collective-permute-start(bf16[64,128]{1,0:T(8,128)(2,1)S(1)} %shard_map.133), channel_id=1, source_target_pairs={{0,16},{8,24},{16,0},{24,8},{1,17},{9,25},{17,1},{25,9},{2,18},{10... | collective-permute-start | bytes 49160 | tf_op jit(solution)/shard_map/ppermute | solution.py:413
  37.3 3.8 %collective-permute-start.10 = (bf16[64,128]{1,0:T(8,128)(2,1)S(1)}, bf16[64,128]{1,0:T(8,128)(2,1)S(1)}, u32[]{:S(2)}, u32[]{:S(2)}) collective-permute-start(bf16[64,128]{1,0:T(8,128)(2,1)S(1)} %shard_map.133), channel_id=1, source_target_pairs={{0,8},{8,16},{16,24},{24,0},{1,9},{9,17},{17,25},{25,1},{2,10},{10... | collective-permute-start | bytes 49160 | tf_op jit(solution)/shard_map/ppermute | solution.py:413
  42.0 18.8 %all-to-all-start.1 = ((bf16[8,4,64,128]{3,2,1,0:T(8,128)(2,1)}), bf16[8,4,64,128]{3,2,1,0:T(8,128)(2,1)S(1)}, u32[]{:S(2)}, u32[]{:S(2)}) async-start(bf16[8,4,64,128]{3,2,1,0:T(8,128)(2,1)} %broadcast_in_dim.2), calls=%async_computation.1 | async-start | bytes 1048576 | tf_op jit(solution)/shard_map/all_to_all | solution.py:427
  48.6 6.0 %collective-permute-start.16 = (bf16[8,72,128]{2,1,0:T(8,128)(2,1)S(1)}, bf16[8,72,128]{2,1,0:T(8,128)(2,1)S(1)}, u32[]{:S(2)}, u32[]{:S(2)}) collective-permute-start(bf16[8,72,128]{2,1,0:T(8,128)(2,1)S(1)} %all-to-all-done.2), channel_id=1, source_target_pairs={{0,24},{1,7},{2,26},{3,1},{4,28},{5,3},{6,30},{7,5},{8,0},{9,15},{... | collective-permute-start | bytes 442376 | tf_op jit(solution)/shard_map/ppermute | solution.py:423
  50.9 5.6 %collective-permute-start.15 = (bf16[8,72,128]{2,1,0:T(8,128)(2,1)S(1)}, bf16[8,72,128]{2,1,0:T(8,128)(2,1)S(1)}, u32[]{:S(2)}, u32[]{:S(2)}) collective-permute-start(bf16[8,72,128]{2,1,0:T(8,128)(2,1)S(1)} %all-to-all-done.2), channel_id=1, source_target_pairs={{0,16},{1,5},{2,18},{3,7},{4,20},{5,1},{6,22},{7,3},{8,24},{9,13},... | collective-permute-start | bytes 442376 | tf_op jit(solution)/shard_map/ppermute | solution.py:423
  51.7 6.3 %collective-permute-start.14 = (bf16[8,72,128]{2,1,0:T(8,128)(2,1)S(1)}, bf16[8,72,128]{2,1,0:T(8,128)(2,1)S(1)}, u32[]{:S(2)}, u32[]{:S(2)}) collective-permute-start(bf16[8,72,128]{2,1,0:T(8,128)(2,1)S(1)} %all-to-all-done.2), channel_id=1, source_target_pairs={{0,8},{1,3},{2,10},{3,5},{4,12},{5,7},{6,14},{7,1},{8,16},{9,11},{... | collective-permute-start | bytes 442376 | tf_op jit(solution)/shard_map/ppermute | solution.py:423
  58.1 43.9 %collective-permute-start.19 = (bf16[4,8,72,128]{3,2,1,0:T(8,128)(2,1)S(1)}, bf16[4,8,72,128]{3,2,1,0:T(8,128)(2,1)S(1)}, u32[]{:S(2)}, u32[]{:S(2)}) collective-permute-start(bf16[4,8,72,128]{3,2,1,0:T(8,128)(2,1)S(1)} %pad_maximum_fusion.b0), channel_id=1, source_target_pairs={{0,6},{1,25},{2,0},{3,27},{4,2},{5,29},{6,4},{7,31},{8,14},{9,1},{... | collective-permute-start | bytes 1769480 | tf_op jit(solution)/shard_map/ppermute | solution.py:425
  58.3 43.7 %collective-permute-start.18 = (bf16[4,8,72,128]{3,2,1,0:T(8,128)(2,1)S(1)}, bf16[4,8,72,128]{3,2,1,0:T(8,128)(2,1)S(1)}, u32[]{:S(2)}, u32[]{:S(2)}) collective-permute-start(bf16[4,8,72,128]{3,2,1,0:T(8,128)(2,1)S(1)} %pad_maximum_fusion.b0), channel_id=1, source_target_pairs={{0,4},{1,17},{2,6},{3,19},{4,0},{5,21},{6,2},{7,23},{8,12},{9,25},... | collective-permute-start | bytes 1769480 | tf_op jit(solution)/shard_map/ppermute | solution.py:425
  59.4 42.6 %collective-permute-start.17 = (bf16[4,8,72,128]{3,2,1,0:T(8,128)(2,1)S(1)}, bf16[4,8,72,128]{3,2,1,0:T(8,128)(2,1)S(1)}, u32[]{:S(2)}, u32[]{:S(2)}) collective-permute-start(bf16[4,8,72,128]{3,2,1,0:T(8,128)(2,1)S(1)} %pad_maximum_fusion.b0), channel_id=1, source_target_pairs={{0,2},{1,9},{2,4},{3,11},{4,6},{5,13},{6,0},{7,15},{8,10},{9,17},{... | collective-permute-start | bytes 1769480 | tf_op jit(solution)/shard_map/ppermute | solution.py:425
  60.8 39.1 %collective-permute-start.13 = (bf16[8,4,64,128]{3,2,1,0:T(8,128)(2,1)S(1)}, bf16[8,4,64,128]{3,2,1,0:T(8,128)(2,1)S(1)}, u32[]{:S(2)}, u32[]{:S(2)}) collective-permute-start(bf16[8,4,64,128]{3,2,1,0:T(8,128)(2,1)S(1)} %all-to-all-done.1.up_own.w_own), channel_id=1, source_target_pairs={{0,1},{1,0},{2,3},{3,2},{4,5},{5,4},{6,7},{7,6},{8,9},{9,8},{10,11... | collective-permute-start | bytes 1572872 | tf_op jit(solution)/shard_map/ppermute | solution.py:428
  78.9 4.6 %collective-permute-start.7 = (bf16[64,128]{1,0:T(8,128)(2,1)S(1)}, bf16[64,128]{1,0:T(8,128)(2,1)S(1)}, u32[]{:S(2)}, u32[]{:S(2)}) collective-permute-start(bf16[64,128]{1,0:T(8,128)(2,1)S(1)} %get-tuple-element.18.q0), channel_id=1, source_target_pairs={{0,4},{2,6},{4,0},{6,2},{1,5},{3,7},{5,1},{7,3},{8,12},{10,14},{12... | collective-permute-start | bytes 49160 | tf_op jit(solution)/shard_map/ppermute | solution.py:429
  83.4 4.8 %collective-permute-start.6 = (bf16[64,128]{1,0:T(8,128)(2,1)S(1)}, bf16[64,128]{1,0:T(8,128)(2,1)S(1)}, u32[]{:S(2)}, u32[]{:S(2)}) collective-permute-start(bf16[64,128]{1,0:T(8,128)(2,1)S(1)} %get-tuple-element.18.q0), channel_id=1, source_target_pairs={{0,2},{2,4},{4,6},{6,0},{1,3},{3,5},{5,7},{7,1},{8,10},{10,12},{12... | collective-permute-start | bytes 49160 | tf_op jit(solution)/shard_map/ppermute | solution.py:429
  88.2 11.7 %collective-permute-start.9 = (bf16[4,64,128]{2,1,0:T(8,128)(2,1)S(1)}, bf16[4,64,128]{2,1,0:T(8,128)(2,1)S(1)}, u32[]{:S(2)}, u32[]{:S(2)}) collective-permute-start(bf16[4,64,128]{2,1,0:T(8,128)(2,1)S(1)} %pad_maximum_fusion.1), channel_id=1, source_target_pairs={{0,1},{1,0},{2,3},{3,2},{4,5},{5,4},{6,7},{7,6},{8,9},{9,8},{10,11... | collective-permute-start | bytes 196616 | tf_op jit(solution)/shard_map/ppermute | solution.py:430
  113.9 4.8 %collective-permute-start.22 = (bf16[32,1024]{1,0:T(8,128)(2,1)S(1)}, bf16[32,1024]{1,0:T(8,128)(2,1)S(1)}, u32[]{:S(2)}, u32[]{:S(2)}) collective-permute-start(bf16[32,1024]{1,0:T(8,128)(2,1)S(1)} %get-tuple-element.30), channel_id=1, source_target_pairs={{0,2},{2,4},{4,6},{6,0},{1,3},{3,5},{5,7},{7,1},{8,10},{10,12},{12... | collective-permute-start | bytes 196616 | tf_op jit(solution)/shard_map/ppermute | solution.py:472
  114.0 6.3 %collective-permute-start.23 = (bf16[32,1024]{1,0:T(8,128)(2,1)S(1)}, bf16[32,1024]{1,0:T(8,128)(2,1)S(1)}, u32[]{:S(2)}, u32[]{:S(2)}) collective-permute-start(bf16[32,1024]{1,0:T(8,128)(2,1)S(1)} %get-tuple-element.31), channel_id=1, source_target_pairs={{0,4},{2,6},{4,0},{6,2},{1,5},{3,7},{5,1},{7,3},{8,12},{10,14},{12... | collective-permute-start | bytes 196616 | tf_op jit(solution)/shard_map/ppermute | solution.py:472
  116.9 3.9 %collective-permute-start.24 = (bf16[32,1024]{1,0:T(8,128)(2,1)S(1)}, bf16[32,1024]{1,0:T(8,128)(2,1)S(1)}, u32[]{:S(2)}, u32[]{:S(2)}) collective-permute-start(bf16[32,1024]{1,0:T(8,128)(2,1)S(1)} %get-tuple-element.32), channel_id=1, source_target_pairs={{0,6},{2,0},{4,2},{6,4},{1,7},{3,1},{5,3},{7,5},{8,14},{10,8},{12,... | collective-permute-start | bytes 196616 | tf_op jit(solution)/shard_map/ppermute | solution.py:472
  (13 other events, 46.7 us)

commit v7 on v6

--- a/solution.py
+++ b/solution.py
@@ -228,8 +228,8 @@
     behind = (at == 0) & (docs > ids[255].astype(F32))
     low = jnp.sum(before.astype(jnp.int32))
     high = NS - 1 - jnp.sum(behind.astype(jnp.int32))
-    first = low // 2
-    last = jnp.maximum(high // 2, first) + 1
+    count = (high - low) // 2 + 1
+    begin = jnp.minimum(low, NS - 2 * count)
 
     def fetch(z, carry):
         for j, part in enumerate((b0, b1, b2, b3)):
@@ -237,17 +237,17 @@
                 kb[j, k, z] = part[k, z]
         return carry
 
-    lax.fori_loop(first // 2, (last + 1) // 2, fetch, 0)
+    lax.fori_loop(begin // 4, (begin + 2 * count - 1) // 4 + 1, fetch, 0)
     mx[...] = jnp.full(mx.shape, NEG_BIG, F32)
     total[...] = jnp.zeros(total.shape, F32)
     acc[...] = jnp.zeros(acc.shape, F32)
     wanted = jnp.concatenate([query_docs[0:1, :], query_docs[1:2, :]], axis=1)
 
     def scores(tile, carry):
-        z = tile // 2
         latents, ropes, same = [], [], []
         for half in range(2):
-            x = 2 * lax.rem(tile, 2) + half
+            block = begin + 2 * tile + half
+            z, x = block // NX, lax.rem(block, NX)
             jx = lax.rem(x0 - x + NX, NX)
             parts, turned = [], []
             for y in range(NY):
@@ -264,7 +264,7 @@
             inverse = lax.rsqrt(mean + EPS)
             latents.append(jnp.concatenate(parts, axis=0) * inverse * gains[...])
             ropes.append(jnp.concatenate(turned, axis=0))
-            docs_col = column(key_docs[pl.ds(2 * tile + half, 1), :])
+            docs_col = column(key_docs[pl.ds(block, 1), :])
             same.append(jnp.concatenate([docs_col, docs_col], axis=1) == wanted)
         latent = jnp.concatenate(latents, axis=1)
         v_buf[tile] = jnp.dot(uv[...], latent.astype(BF), preferred_element_type=F32).astype(BF)
@@ -288,7 +288,7 @@
             mx[h] = jnp.maximum(mx[h], jnp.max(got.reshape(32, 8, 256), axis=0))
         return carry
 
-    lax.fori_loop(first, last, scores, 0)
+    lax.fori_loop(0, count, scores, 0)
     tops = []
     for h in range(4):
         top = jnp.maximum(jnp.max(mx[h], axis=0, keepdims=True), FLOOR)
@@ -306,7 +306,7 @@
             )
         return carry
 
-    lax.fori_loop(first, last, weigh, 0)
+    lax.fori_loop(0, count, weigh, 0)
     for h in range(4):
         ml_ref[h : h + 1, :] = tops[h]
         ml_ref[4 + h : 5 + h, :] = jnp.sum(total[h], axis=0, keepdims=True)

time: 122 us -> 122 us (level)
  no operation moved by 1% of the time
where the time goes in v7:
time: 122 us
  starting transfers between devices  72.3 us (59%)
  waiting for transfers between devices  29 us (24%)
  Pallas kernels  16.3 us (13%)
  local copies, waits for them, and re-layouts  3.09 us (3%)
    ppermute x1, starting transfers between devices, layer(): up_other = lax.ppermute(up_own, 'c', swap)  14.6 us
    ppermute x1, starting transfers between devices, layer(): q_other = lax.ppermute(jnp.stack(q_all), 'c', swap)  10.8 us
    pallas_call x1, Pallas kernels, layer(): call(attend, (jax.ShapeDtypeStruct((256, 128), F32), jax.ShapeDtypeStruct...  9.3 us
    all_to_all x1, starting transfers between devices, layer(): gathered = lax.all_to_all(message, 'z', 0, 0)  9.15 us
    ppermute x3, waiting for transfers between devices, layer(): lax.ppermute(q_part, 'y', ring(j))  7.27 us
    all_to_all x1, starting transfers between devices, layer(): up_own = lax.all_to_all(later, 'z', 0, 0)  6.56 us
    ppermute x3, waiting for transfers between devices, layer(): lax.ppermute(stage1, AXES, shift_pairs(2, j))  5.95 us
    ppermute x3, starting transfers between devices, layer(): rows = [tokens] + [lax.ppermute(tokens, 'y', ring(j)) for j in range(1, NY)]  5.74 us
  transfers between devices with their start and end apart: 28, of which 17 were waited for; matrix products, arithmetic and copies ran while one was open for 1% of the time, Pallas kernels for 1%

profile of v7, /device:TPU:1, one launch (start us, length us, event | category | flops | bytes accessed | tf_op | source)
XLA Modules:
  0.0 121.5 jit_solution(11476582278018405495)
XLA Ops:
  0.7 2.2 %shard_map.131 = bf16[8,40,128]{2,1,0:T(8,128)(2,1)} custom-call(s32[5]{0:T(128)S(1)} %stack.68.where, bf16[32,256]{1,0:T(8,128)(2,1)} %dq_in.1, bf16[32,256]{1,0:T(8,128)(2,1)} %dk_in.1, bf16[32,32]{1,0:T(8,128)(2,1)} %dr_in.1), custom_call_target="tpu_custom_call" | custom-call | tf_op jit(solution)/shard_map/pallas_call | solution.py:399
  3.0 9.1 %all-to-all-start = ((bf16[8,40,128]{2,1,0:T(8,128)(2,1)}), bf16[8,40,128]{2,1,0:T(8,128)(2,1)S(1)}, u32[]{:S(2)}, u32[]{:S(2)}) async-start(bf16[8,40,128]{2,1,0:T(8,128)(2,1)} %shard_map.131), calls=%async_computation | async-start | bytes 163840 | tf_op jit(solution)/shard_map/all_to_all | solution.py:405
  12.1 3.0 %collective-permute-start.1 = (bf16[32,1024]{1,0:T(8,128)(2,1)S(1)}, bf16[32,1024]{1,0:T(8,128)(2,1)S(1)}, u32[]{:S(2)}, u32[]{:S(2)}) collective-permute-start(bf16[32,1024]{1,0:T(8,128)(2,1)S(1)} %copy-done), channel_id=1, source_target_pairs={{0,4},{2,6},{4,0},{6,2},{1,5},{3,7},{5,1},{7,3},{8,12},{10,14},{12... | collective-permute-start | bytes 196616 | tf_op jit(solution)/shard_map/ppermute | solution.py:408
  15.1 4.5 %all-to-all-done.g0 = bf16[8,40,128]{2,1,0:T(8,128)(2,1)S(1)} async-done(((bf16[8,40,128]{2,1,0:T(8,128)(2,1)}), bf16[8,40,128]{2,1,0:T(8,128)(2,1)S(1)}, u32[]{:S(2)}, u32[]{:S(2)}) %all-to-all-start) | async-done | bytes 81952 | tf_op jit(solution)/shard_map/all_to_all | solution.py:405
  19.6 2.5 %collective-permute-start.5 = (bf16[8,40,128]{2,1,0:T(8,128)(2,1)S(1)}, bf16[8,40,128]{2,1,0:T(8,128)(2,1)S(1)}, u32[]{:S(2)}, u32[]{:S(2)}) collective-permute-start(bf16[8,40,128]{2,1,0:T(8,128)(2,1)S(1)} %all-to-all-done.g0), channel_id=1, source_target_pairs={{0,24},{8,0},{16,8},{24,16},{1,25},{9,1},{17,9},{25,17},{2,26},{10... | collective-permute-start | bytes 245768 | tf_op jit(solution)/shard_map/ppermute | solution.py:406
  26.0 1.6 %collective-permute-done.t1 = bf16[32,1024]{1,0:T(8,128)(2,1)S(1)} collective-permute-done((bf16[32,1024]{1,0:T(8,128)(2,1)S(1)}, bf16[32,1024]{1,0:T(8,128)(2,1)S(1)}, u32[]{:S(2)}, u32[]{:S(2)}) %collective-permute-start) | collective-permute-done | bytes 65568 | tf_op jit(solution)/shard_map/ppermute | solution.py:408
  27.8 1.6 %shard_map.132 = (bf16[64,128]{1,0:T(8,128)(2,1)S(1)}, bf16[8,72,128]{2,1,0:T(8,128)(2,1)}) custom-call(s32[5]{0:T(128)S(1)} %stack.68.where, bf16[32,1024]{1,0:T(8,128)(2,1)S(1)} %copy-done, bf16[32,1024]{1,0:T(8,128)(2,1)S(1)} %collective-permute-done.t1, bf16[32,1024]{1,0:T(8,128)(2,1)S(1)} %collective-permute-done.1.t2, ...), custom_call_target="tpu_custom_call" | custom-call | tf_op jit(solution)/shard_map/pallas_call | solution.py:416
  29.3 3.5 %all-to-all-start.2 = ((bf16[8,72,128]{2,1,0:T(8,128)(2,1)}), bf16[8,72,128]{2,1,0:T(8,128)(2,1)S(1)}, u32[]{:S(2)}, u32[]{:S(2)}) async-start(bf16[8,72,128]{2,1,0:T(8,128)(2,1)} %get-tuple-element.25), calls=%async_computation.2 | async-start | bytes 294912 | tf_op jit(solution)/shard_map/all_to_all | solution.py:422
  33.7 2.3 %collective-permute-start.12 = (bf16[64,128]{1,0:T(8,128)(2,1)S(1)}, bf16[64,128]{1,0:T(8,128)(2,1)S(1)}, u32[]{:S(2)}, u32[]{:S(2)}) collective-permute-start(bf16[64,128]{1,0:T(8,128)(2,1)S(1)} %shard_map.133), channel_id=1, source_target_pairs={{0,24},{8,0},{16,8},{24,16},{1,25},{9,1},{17,9},{25,17},{2,26},{10... | collective-permute-start | bytes 49160 | tf_op jit(solution)/shard_map/ppermute | solution.py:413
  37.3 2.8 %collective-permute-done.11 = bf16[64,128]{1,0:T(8,128)(2,1)S(1)} collective-permute-done((bf16[64,128]{1,0:T(8,128)(2,1)S(1)}, bf16[64,128]{1,0:T(8,128)(2,1)S(1)}, u32[]{:S(2)}, u32[]{:S(2)}) %collective-permute-start.11) | collective-permute-done | bytes 16416 | tf_op jit(solution)/shard_map/ppermute | solution.py:413
  42.0 6.6 %all-to-all-start.1 = ((bf16[8,4,64,128]{3,2,1,0:T(8,128)(2,1)}), bf16[8,4,64,128]{3,2,1,0:T(8,128)(2,1)S(1)}, u32[]{:S(2)}, u32[]{:S(2)}) async-start(bf16[8,4,64,128]{3,2,1,0:T(8,128)(2,1)} %broadcast_in_dim.2), calls=%async_computation.1 | async-start | bytes 1048576 | tf_op jit(solution)/shard_map/all_to_all | solution.py:427
  48.6 2.4 %collective-permute-start.16 = (bf16[8,72,128]{2,1,0:T(8,128)(2,1)S(1)}, bf16[8,72,128]{2,1,0:T(8,128)(2,1)S(1)}, u32[]{:S(2)}, u32[]{:S(2)}) collective-permute-start(bf16[8,72,128]{2,1,0:T(8,128)(2,1)S(1)} %all-to-all-done.2), channel_id=1, source_target_pairs={{0,24},{1,7},{2,26},{3,1},{4,28},{5,3},{6,30},{7,5},{8,0},{9,15},{... | collective-permute-start | bytes 442376 | tf_op jit(solution)/shard_map/ppermute | solution.py:423
  52.1 2.5 %collective-permute-done.16 = bf16[8,72,128]{2,1,0:T(8,128)(2,1)S(1)} collective-permute-done((bf16[8,72,128]{2,1,0:T(8,128)(2,1)S(1)}, bf16[8,72,128]{2,1,0:T(8,128)(2,1)S(1)}, u32[]{:S(2)}, u32[]{:S(2)}) %collective-permute-start.16) | collective-permute-done | bytes 147488 | tf_op jit(solution)/shard_map/ppermute | solution.py:423
  54.6 1.9 %collective-permute-done.15 = bf16[8,72,128]{2,1,0:T(8,128)(2,1)S(1)} collective-permute-done((bf16[8,72,128]{2,1,0:T(8,128)(2,1)S(1)}, bf16[8,72,128]{2,1,0:T(8,128)(2,1)S(1)}, u32[]{:S(2)}, u32[]{:S(2)}) %collective-permute-start.15) | collective-permute-done | bytes 147488 | tf_op jit(solution)/shard_map/ppermute | solution.py:423
  56.5 1.5 %collective-permute-done.14 = bf16[8,72,128]{2,1,0:T(8,128)(2,1)S(1)} collective-permute-done((bf16[8,72,128]{2,1,0:T(8,128)(2,1)S(1)}, bf16[8,72,128]{2,1,0:T(8,128)(2,1)S(1)}, u32[]{:S(2)}, u32[]{:S(2)}) %collective-permute-start.14) | collective-permute-done | bytes 147488 | tf_op jit(solution)/shard_map/ppermute | solution.py:423
  60.8 14.6 %collective-permute-start.13 = (bf16[8,4,64,128]{3,2,1,0:T(8,128)(2,1)S(1)}, bf16[8,4,64,128]{3,2,1,0:T(8,128)(2,1)S(1)}, u32[]{:S(2)}, u32[]{:S(2)}) collective-permute-start(bf16[8,4,64,128]{3,2,1,0:T(8,128)(2,1)S(1)} %all-to-all-done.1.up_own.w_own), channel_id=1, source_target_pairs={{0,1},{1,0},{2,3},{3,2},{4,5},{5,4},{6,7},{7,6},{8,9},{9,8},{10,11... | collective-permute-start | bytes 1572872 | tf_op jit(solution)/shard_map/ppermute | solution.py:428
  75.5 2.3 %collective-permute-start.8 = (bf16[64,128]{1,0:T(8,128)(2,1)S(1)}, bf16[64,128]{1,0:T(8,128)(2,1)S(1)}, u32[]{:S(2)}, u32[]{:S(2)}) collective-permute-start(bf16[64,128]{1,0:T(8,128)(2,1)S(1)} %get-tuple-element.18.q0), channel_id=1, source_target_pairs={{0,6},{2,0},{4,2},{6,4},{1,7},{3,1},{5,3},{7,5},{8,14},{10,8},{12,... | collective-permute-start | bytes 49160 | tf_op jit(solution)/shard_map/ppermute | solution.py:429
  78.9 1.7 %collective-permute-start.7 = (bf16[64,128]{1,0:T(8,128)(2,1)S(1)}, bf16[64,128]{1,0:T(8,128)(2,1)S(1)}, u32[]{:S(2)}, u32[]{:S(2)}) collective-permute-start(bf16[64,128]{1,0:T(8,128)(2,1)S(1)} %get-tuple-element.18.q0), channel_id=1, source_target_pairs={{0,4},{2,6},{4,0},{6,2},{1,5},{3,7},{5,1},{7,3},{8,12},{10,14},{12... | collective-permute-start | bytes 49160 | tf_op jit(solution)/shard_map/ppermute | solution.py:429
  80.5 2.9 %collective-permute-done.7.q2 = bf16[64,128]{1,0:T(8,128)(2,1)S(1)} collective-permute-done((bf16[64,128]{1,0:T(8,128)(2,1)S(1)}, bf16[64,128]{1,0:T(8,128)(2,1)S(1)}, u32[]{:S(2)}, u32[]{:S(2)}) %collective-permute-start.7) | collective-permute-done | bytes 16416 | tf_op jit(solution)/shard_map/ppermute | solution.py:429
  84.9 3.3 %collective-permute-done.6.q1 = bf16[64,128]{1,0:T(8,128)(2,1)S(1)} collective-permute-done((bf16[64,128]{1,0:T(8,128)(2,1)S(1)}, bf16[64,128]{1,0:T(8,128)(2,1)S(1)}, u32[]{:S(2)}, u32[]{:S(2)}) %collective-permute-start.6) | collective-permute-done | bytes 16416 | tf_op jit(solution)/shard_map/ppermute | solution.py:429
  88.2 10.8 %collective-permute-start.9 = (bf16[4,64,128]{2,1,0:T(8,128)(2,1)S(1)}, bf16[4,64,128]{2,1,0:T(8,128)(2,1)S(1)}, u32[]{:S(2)}, u32[]{:S(2)}) collective-permute-start(bf16[4,64,128]{2,1,0:T(8,128)(2,1)S(1)} %pad_maximum_fusion.1), channel_id=1, source_target_pairs={{0,1},{1,0},{2,3},{3,2},{4,5},{5,4},{6,7},{7,6},{8,9},{9,8},{10,11... | collective-permute-start | bytes 196616 | tf_op jit(solution)/shard_map/ppermute | solution.py:430
  102.0 9.3 %shard_map.135 = (f32[256,128]{1,0:T(8,128)S(1)}, bf16[256,128]{1,0:T(8,128)(2,1)S(1)}, f32[8,256]{1,0:T(8,128)S(1)}) custom-call(s32[5]{0:T(128)S(1)} %stack.68.where, s32[256]{0:T(256)S(1)} %copy-done.1, bf16[4,256,256]{2,1,0:T(8,128)(2,1)S(1)} %get-tuple-element.19.q_ref, bf16[256,256]{1,0:T(8,128)(2,1)S(1)} %get-tuple-element.20.uk, ...), custom_call_target="tpu_custom_call" | custom-call | tf_op jit(solution)/shard_map/pallas_call | solution.py:447
  114.0 2.9 %collective-permute-start.23 = (bf16[32,1024]{1,0:T(8,128)(2,1)S(1)}, bf16[32,1024]{1,0:T(8,128)(2,1)S(1)}, u32[]{:S(2)}, u32[]{:S(2)}) collective-permute-start(bf16[32,1024]{1,0:T(8,128)(2,1)S(1)} %get-tuple-element.31), channel_id=1, source_target_pairs={{0,4},{2,6},{4,0},{6,2},{1,5},{3,7},{5,1},{7,3},{8,12},{10,14},{12... | collective-permute-start | bytes 196616 | tf_op jit(solution)/shard_map/ppermute | solution.py:472
  118.7 1.6 %collective-permute-done.23.p2 = bf16[32,1024]{1,0:T(8,128)(2,1)S(1)} collective-permute-done((bf16[32,1024]{1,0:T(8,128)(2,1)S(1)}, bf16[32,1024]{1,0:T(8,128)(2,1)S(1)}, u32[]{:S(2)}, u32[]{:S(2)}) %collective-permute-start.23) | collective-permute-done | bytes 65568 | tf_op jit(solution)/shard_map/ppermute | solution.py:472
  (65 shorter events, 23.3 us)
Async XLA Ops:
  3.0 16.7 %all-to-all-start = ((bf16[8,40,128]{2,1,0:T(8,128)(2,1)}), bf16[8,40,128]{2,1,0:T(8,128)(2,1)S(1)}, u32[]{:S(2)}, u32[]{:S(2)}) async-start(bf16[8,40,128]{2,1,0:T(8,128)(2,1)} %shard_map.131), calls=%async_computation | async-start | bytes 163840 | tf_op jit(solution)/shard_map/all_to_all | solution.py:405
  12.1 12.4 %collective-permute-start.1 = (bf16[32,1024]{1,0:T(8,128)(2,1)S(1)}, bf16[32,1024]{1,0:T(8,128)(2,1)S(1)}, u32[]{:S(2)}, u32[]{:S(2)}) collective-permute-start(bf16[32,1024]{1,0:T(8,128)(2,1)S(1)} %copy-done), channel_id=1, source_target_pairs={{0,4},{2,6},{4,0},{6,2},{1,5},{3,7},{5,1},{7,3},{8,12},{10,14},{12... | collective-permute-start | bytes 196616 | tf_op jit(solution)/shard_map/ppermute | solution.py:408
  19.6 8.0 %collective-permute-start.5 = (bf16[8,40,128]{2,1,0:T(8,128)(2,1)S(1)}, bf16[8,40,128]{2,1,0:T(8,128)(2,1)S(1)}, u32[]{:S(2)}, u32[]{:S(2)}) collective-permute-start(bf16[8,40,128]{2,1,0:T(8,128)(2,1)S(1)} %all-to-all-done.g0), channel_id=1, source_target_pairs={{0,24},{8,0},{16,8},{24,16},{1,25},{9,1},{17,9},{25,17},{2,26},{10... | collective-permute-start | bytes 245768 | tf_op jit(solution)/shard_map/ppermute | solution.py:406
  22.1 5.5 %collective-permute-start.4 = (bf16[8,40,128]{2,1,0:T(8,128)(2,1)S(1)}, bf16[8,40,128]{2,1,0:T(8,128)(2,1)S(1)}, u32[]{:S(2)}, u32[]{:S(2)}) collective-permute-start(bf16[8,40,128]{2,1,0:T(8,128)(2,1)S(1)} %all-to-all-done.g0), channel_id=1, source_target_pairs={{0,16},{8,24},{16,0},{24,8},{1,17},{9,25},{17,1},{25,9},{2,18},{10... | collective-permute-start | bytes 245768 | tf_op jit(solution)/shard_map/ppermute | solution.py:406
  22.6 5.2 %collective-permute-start.3 = (bf16[8,40,128]{2,1,0:T(8,128)(2,1)S(1)}, bf16[8,40,128]{2,1,0:T(8,128)(2,1)S(1)}, u32[]{:S(2)}, u32[]{:S(2)}) collective-permute-start(bf16[8,40,128]{2,1,0:T(8,128)(2,1)S(1)} %all-to-all-done.g0), channel_id=1, source_target_pairs={{0,8},{8,16},{16,24},{24,0},{1,9},{9,17},{17,25},{25,1},{2,10},{10... | collective-permute-start | bytes 245768 | tf_op jit(solution)/shard_map/ppermute | solution.py:406
  23.2 4.4 %collective-permute-start = (bf16[32,1024]{1,0:T(8,128)(2,1)S(1)}, bf16[32,1024]{1,0:T(8,128)(2,1)S(1)}, u32[]{:S(2)}, u32[]{:S(2)}) collective-permute-start(bf16[32,1024]{1,0:T(8,128)(2,1)S(1)} %copy-done), channel_id=1, source_target_pairs={{0,2},{2,4},{4,6},{6,0},{1,3},{3,5},{5,7},{7,1},{8,10},{10,12},{12... | collective-permute-start | bytes 196616 | tf_op jit(solution)/shard_map/ppermute | solution.py:408
  29.3 11.8 %all-to-all-start.2 = ((bf16[8,72,128]{2,1,0:T(8,128)(2,1)}), bf16[8,72,128]{2,1,0:T(8,128)(2,1)S(1)}, u32[]{:S(2)}, u32[]{:S(2)}) async-start(bf16[8,72,128]{2,1,0:T(8,128)(2,1)} %get-tuple-element.25), calls=%async_computation.2 | async-start | bytes 294912 | tf_op jit(solution)/shard_map/all_to_all | solution.py:422
  33.7 3.6 %collective-permute-start.12 = (bf16[64,128]{1,0:T(8,128)(2,1)S(1)}, bf16[64,128]{1,0:T(8,128)(2,1)S(1)}, u32[]{:S(2)}, u32[]{:S(2)}) collective-permute-start(bf16[64,128]{1,0:T(8,128)(2,1)S(1)} %shard_map.133), channel_id=1, source_target_pairs={{0,24},{8,0},{16,8},{24,16},{1,25},{9,1},{17,9},{25,17},{2,26},{10... | collective-permute-start | bytes 49160 | tf_op jit(solution)/shard_map/ppermute | solution.py:413
  36.1 4.1 %collective-permute-start.11 = (bf16[64,128]{1,0:T(8,128)(2,1)S(1)}, bf16[64,128]{1,0:T(8,128)(2,1)S(1)}, u32[]{:S(2)}, u32[]{:S(2)}) collective-permute-start(bf16[64,128]{1,0:T(8,128)(2,1)S(1)} %shard_map.133), channel_id=1, source_target_pairs={{0,16},{8,24},{16,0},{24,8},{1,17},{9,25},{17,1},{25,9},{2,18},{10... | collective-permute-start | bytes 49160 | tf_op jit(solution)/shard_map/ppermute | solution.py:413
  37.3 3.8 %collective-permute-start.10 = (bf16[64,128]{1,0:T(8,128)(2,1)S(1)}, bf16[64,128]{1,0:T(8,128)(2,1)S(1)}, u32[]{:S(2)}, u32[]{:S(2)}) collective-permute-start(bf16[64,128]{1,0:T(8,128)(2,1)S(1)} %shard_map.133), channel_id=1, source_target_pairs={{0,8},{8,16},{16,24},{24,0},{1,9},{9,17},{17,25},{25,1},{2,10},{10... | collective-permute-start | bytes 49160 | tf_op jit(solution)/shard_map/ppermute | solution.py:413
  42.0 18.8 %all-to-all-start.1 = ((bf16[8,4,64,128]{3,2,1,0:T(8,128)(2,1)}), bf16[8,4,64,128]{3,2,1,0:T(8,128)(2,1)S(1)}, u32[]{:S(2)}, u32[]{:S(2)}) async-start(bf16[8,4,64,128]{3,2,1,0:T(8,128)(2,1)} %broadcast_in_dim.2), calls=%async_computation.1 | async-start | bytes 1048576 | tf_op jit(solution)/shard_map/all_to_all | solution.py:427
  48.6 6.0 %collective-permute-start.16 = (bf16[8,72,128]{2,1,0:T(8,128)(2,1)S(1)}, bf16[8,72,128]{2,1,0:T(8,128)(2,1)S(1)}, u32[]{:S(2)}, u32[]{:S(2)}) collective-permute-start(bf16[8,72,128]{2,1,0:T(8,128)(2,1)S(1)} %all-to-all-done.2), channel_id=1, source_target_pairs={{0,24},{1,7},{2,26},{3,1},{4,28},{5,3},{6,30},{7,5},{8,0},{9,15},{... | collective-permute-start | bytes 442376 | tf_op jit(solution)/shard_map/ppermute | solution.py:423
  50.9 5.6 %collective-permute-start.15 = (bf16[8,72,128]{2,1,0:T(8,128)(2,1)S(1)}, bf16[8,72,128]{2,1,0:T(8,128)(2,1)S(1)}, u32[]{:S(2)}, u32[]{:S(2)}) collective-permute-start(bf16[8,72,128]{2,1,0:T(8,128)(2,1)S(1)} %all-to-all-done.2), channel_id=1, source_target_pairs={{0,16},{1,5},{2,18},{3,7},{4,20},{5,1},{6,22},{7,3},{8,24},{9,13},... | collective-permute-start | bytes 442376 | tf_op jit(solution)/shard_map/ppermute | solution.py:423
  51.7 6.3 %collective-permute-start.14 = (bf16[8,72,128]{2,1,0:T(8,128)(2,1)S(1)}, bf16[8,72,128]{2,1,0:T(8,128)(2,1)S(1)}, u32[]{:S(2)}, u32[]{:S(2)}) collective-permute-start(bf16[8,72,128]{2,1,0:T(8,128)(2,1)S(1)} %all-to-all-done.2), channel_id=1, source_target_pairs={{0,8},{1,3},{2,10},{3,5},{4,12},{5,7},{6,14},{7,1},{8,16},{9,11},{... | collective-permute-start | bytes 442376 | tf_op jit(solution)/shard_map/ppermute | solution.py:423
  58.1 43.9 %collective-permute-start.19 = (bf16[4,8,72,128]{3,2,1,0:T(8,128)(2,1)S(1)}, bf16[4,8,72,128]{3,2,1,0:T(8,128)(2,1)S(1)}, u32[]{:S(2)}, u32[]{:S(2)}) collective-permute-start(bf16[4,8,72,128]{3,2,1,0:T(8,128)(2,1)S(1)} %pad_maximum_fusion.b0), channel_id=1, source_target_pairs={{0,6},{1,25},{2,0},{3,27},{4,2},{5,29},{6,4},{7,31},{8,14},{9,1},{... | collective-permute-start | bytes 1769480 | tf_op jit(solution)/shard_map/ppermute | solution.py:425
  58.3 43.7 %collective-permute-start.18 = (bf16[4,8,72,128]{3,2,1,0:T(8,128)(2,1)S(1)}, bf16[4,8,72,128]{3,2,1,0:T(8,128)(2,1)S(1)}, u32[]{:S(2)}, u32[]{:S(2)}) collective-permute-start(bf16[4,8,72,128]{3,2,1,0:T(8,128)(2,1)S(1)} %pad_maximum_fusion.b0), channel_id=1, source_target_pairs={{0,4},{1,17},{2,6},{3,19},{4,0},{5,21},{6,2},{7,23},{8,12},{9,25},... | collective-permute-start | bytes 1769480 | tf_op jit(solution)/shard_map/ppermute | solution.py:425
  59.4 42.6 %collective-permute-start.17 = (bf16[4,8,72,128]{3,2,1,0:T(8,128)(2,1)S(1)}, bf16[4,8,72,128]{3,2,1,0:T(8,128)(2,1)S(1)}, u32[]{:S(2)}, u32[]{:S(2)}) collective-permute-start(bf16[4,8,72,128]{3,2,1,0:T(8,128)(2,1)S(1)} %pad_maximum_fusion.b0), channel_id=1, source_target_pairs={{0,2},{1,9},{2,4},{3,11},{4,6},{5,13},{6,0},{7,15},{8,10},{9,17},{... | collective-permute-start | bytes 1769480 | tf_op jit(solution)/shard_map/ppermute | solution.py:425
  60.8 39.1 %collective-permute-start.13 = (bf16[8,4,64,128]{3,2,1,0:T(8,128)(2,1)S(1)}, bf16[8,4,64,128]{3,2,1,0:T(8,128)(2,1)S(1)}, u32[]{:S(2)}, u32[]{:S(2)}) collective-permute-start(bf16[8,4,64,128]{3,2,1,0:T(8,128)(2,1)S(1)} %all-to-all-done.1.up_own.w_own), channel_id=1, source_target_pairs={{0,1},{1,0},{2,3},{3,2},{4,5},{5,4},{6,7},{7,6},{8,9},{9,8},{10,11... | collective-permute-start | bytes 1572872 | tf_op jit(solution)/shard_map/ppermute | solution.py:428
  78.9 4.6 %collective-permute-start.7 = (bf16[64,128]{1,0:T(8,128)(2,1)S(1)}, bf16[64,128]{1,0:T(8,128)(2,1)S(1)}, u32[]{:S(2)}, u32[]{:S(2)}) collective-permute-start(bf16[64,128]{1,0:T(8,128)(2,1)S(1)} %get-tuple-element.18.q0), channel_id=1, source_target_pairs={{0,4},{2,6},{4,0},{6,2},{1,5},{3,7},{5,1},{7,3},{8,12},{10,14},{12... | collective-permute-start | bytes 49160 | tf_op jit(solution)/shard_map/ppermute | solution.py:429
  83.4 4.8 %collective-permute-start.6 = (bf16[64,128]{1,0:T(8,128)(2,1)S(1)}, bf16[64,128]{1,0:T(8,128)(2,1)S(1)}, u32[]{:S(2)}, u32[]{:S(2)}) collective-permute-start(bf16[64,128]{1,0:T(8,128)(2,1)S(1)} %get-tuple-element.18.q0), channel_id=1, source_target_pairs={{0,2},{2,4},{4,6},{6,0},{1,3},{3,5},{5,7},{7,1},{8,10},{10,12},{12... | collective-permute-start | bytes 49160 | tf_op jit(solution)/shard_map/ppermute | solution.py:429
  88.2 11.7 %collective-permute-start.9 = (bf16[4,64,128]{2,1,0:T(8,128)(2,1)S(1)}, bf16[4,64,128]{2,1,0:T(8,128)(2,1)S(1)}, u32[]{:S(2)}, u32[]{:S(2)}) collective-permute-start(bf16[4,64,128]{2,1,0:T(8,128)(2,1)S(1)} %pad_maximum_fusion.1), channel_id=1, source_target_pairs={{0,1},{1,0},{2,3},{3,2},{4,5},{5,4},{6,7},{7,6},{8,9},{9,8},{10,11... | collective-permute-start | bytes 196616 | tf_op jit(solution)/shard_map/ppermute | solution.py:430
  113.9 4.8 %collective-permute-start.22 = (bf16[32,1024]{1,0:T(8,128)(2,1)S(1)}, bf16[32,1024]{1,0:T(8,128)(2,1)S(1)}, u32[]{:S(2)}, u32[]{:S(2)}) collective-permute-start(bf16[32,1024]{1,0:T(8,128)(2,1)S(1)} %get-tuple-element.30), channel_id=1, source_target_pairs={{0,2},{2,4},{4,6},{6,0},{1,3},{3,5},{5,7},{7,1},{8,10},{10,12},{12... | collective-permute-start | bytes 196616 | tf_op jit(solution)/shard_map/ppermute | solution.py:472
  114.0 6.2 %collective-permute-start.23 = (bf16[32,1024]{1,0:T(8,128)(2,1)S(1)}, bf16[32,1024]{1,0:T(8,128)(2,1)S(1)}, u32[]{:S(2)}, u32[]{:S(2)}) collective-permute-start(bf16[32,1024]{1,0:T(8,128)(2,1)S(1)} %get-tuple-element.31), channel_id=1, source_target_pairs={{0,4},{2,6},{4,0},{6,2},{1,5},{3,7},{5,1},{7,3},{8,12},{10,14},{12... | collective-permute-start | bytes 196616 | tf_op jit(solution)/shard_map/ppermute | solution.py:472
  116.8 3.9 %collective-permute-start.24 = (bf16[32,1024]{1,0:T(8,128)(2,1)S(1)}, bf16[32,1024]{1,0:T(8,128)(2,1)S(1)}, u32[]{:S(2)}, u32[]{:S(2)}) collective-permute-start(bf16[32,1024]{1,0:T(8,128)(2,1)S(1)} %get-tuple-element.32), channel_id=1, source_target_pairs={{0,6},{2,0},{4,2},{6,4},{1,7},{3,1},{5,3},{7,5},{8,14},{10,8},{12,... | collective-permute-start | bytes 196616 | tf_op jit(solution)/shard_map/ppermute | solution.py:472
  (13 other events, 46.7 us)

commit v8 on v7

--- a/solution.py
+++ b/solution.py
@@ -156,12 +156,12 @@
 
 
 def make_queries(
-    where, q0, q1, q2, q3, q_other, up_own, up_other, gain, key_gain, docs_in,
+    where, q0, q1, q2, q3, up_own, up_other, gain, key_gain, docs_in,
     out, uk_ref, uv_ref, docs_ref, col_ref, row_ref, latents, ups,
 ):
     x, y, c = where[1], where[2], where[3]
     for j, part in enumerate((q0, q1, q2, q3)):
-        own, other = part[...].astype(F32), q_other[j].astype(F32)
+        own, other = part[0].astype(F32), part[1].astype(F32)
         rows = pl.ds(pl.multiple_of(lax.rem(y - j + NY, NY) * 64, 64), 64)
         latents[rows, 0:128] = jnp.where(c == 0, own, other)
         latents[rows, 128:256] = jnp.where(c == 0, other, own)
@@ -426,8 +426,8 @@
 
     up_own = lax.all_to_all(later, "z", 0, 0)
     up_other = lax.ppermute(up_own, "c", swap)
-    q_all = [q_part] + [lax.ppermute(q_part, "y", ring(j)) for j in range(1, NY)]
-    q_other = lax.ppermute(jnp.stack(q_all), "c", swap)
+    q_pair = jnp.stack([q_part, lax.ppermute(q_part, "c", swap)])
+    q_all = [q_pair] + [lax.ppermute(q_pair, "y", ring(j)) for j in range(1, NY)]
     queries, uk, uv, key_docs, gains, query_docs = call(
         make_queries,
         (
@@ -438,9 +438,9 @@
             jax.ShapeDtypeStruct((256, 128), F32),
             jax.ShapeDtypeStruct((2, 128), F32),
         ),
-        1, 10, scratch=[VMEM((256, 256), F32), VMEM((2, NZ, NX, 32, 128), BF)],
+        1, 9, scratch=[VMEM((256, 256), F32), VMEM((2, NZ, NX, 32, 128), BF)],
     )(
-        here, *q_all, q_other, up_own, up_other, query_gain.reshape(2, 128),
+        here, *q_all, up_own, up_other, query_gain.reshape(2, 128),
         key_gain.reshape(2, 128), doc_ids.reshape(2, 128),
     )
 

time: 122 us -> 121 us (level)
  starting transfers between devices: 72.3 us -> 62.6 us
  waiting for transfers between devices: 29 us -> 37.9 us
    ppermute x4, starting transfers between devices: 16.3 us -> 3.12 us  [the longest x3 3.12 us: layer(): lax.ppermute(q_pair, 'y', ring(j))]
    ppermute x4, waiting for transfers between devices: 8.18 us -> 17 us  [the longest x3 15.4 us: layer(): lax.ppermute(q_pair, 'y', ring(j))]
    ppermute x1, starting transfers between devices: 0.45 us -> 4.01 us  [layer(): got = lax.ppermute(send, 'c', swap)]
where the time goes in v8:
time: 121 us
  starting transfers between devices  62.6 us (52%)
  waiting for transfers between devices  37.9 us (31%)
  Pallas kernels  16.2 us (13%)
  local copies, waits for them, and re-layouts  3.09 us (3%)
    ppermute x3, waiting for transfers between devices, layer(): lax.ppermute(q_pair, 'y', ring(j))  15.4 us
    ppermute x1, starting transfers between devices, layer(): up_other = lax.ppermute(up_own, 'c', swap)  14.6 us
    pallas_call x1, Pallas kernels, layer(): call(attend, (jax.ShapeDtypeStruct((256, 128), F32), jax.ShapeDtypeStruct...  9.26 us
    all_to_all x1, starting transfers between devices, layer(): gathered = lax.all_to_all(message, 'z', 0, 0)  9.15 us
    all_to_all x1, starting transfers between devices, layer(): up_own = lax.all_to_all(later, 'z', 0, 0)  6.56 us
    ppermute x3, waiting for transfers between devices, layer(): lax.ppermute(stage1, AXES, shift_pairs(2, j))  5.95 us
    ppermute x3, starting transfers between devices, layer(): rows = [tokens] + [lax.ppermute(tokens, 'y', ring(j)) for j in range(1, NY)]  5.74 us
    all_to_all x1, waiting for transfers between devices, layer(): gathered = lax.all_to_all(message, 'z', 0, 0)  4.5 us
  transfers between devices with their start and end apart: 28, of which 17 were waited for; matrix products, arithmetic and copies ran while one was open for 1% of the time, Pallas kernels for 1%

profile of v8, /device:TPU:1, one launch (start us, length us, event | category | flops | bytes accessed | tf_op | source)
XLA Modules:
  0.0 120.7 jit_solution(8324912762629346390)
XLA Ops:
  0.7 2.2 %shard_map.131 = bf16[8,40,128]{2,1,0:T(8,128)(2,1)} custom-call(s32[5]{0:T(128)S(1)} %stack.62.where, bf16[32,256]{1,0:T(8,128)(2,1)} %dq_in.1, bf16[32,256]{1,0:T(8,128)(2,1)} %dk_in.1, bf16[32,32]{1,0:T(8,128)(2,1)} %dr_in.1), custom_call_target="tpu_custom_call" | custom-call | tf_op jit(solution)/shard_map/pallas_call | solution.py:399
  3.0 9.1 %all-to-all-start = ((bf16[8,40,128]{2,1,0:T(8,128)(2,1)}), bf16[8,40,128]{2,1,0:T(8,128)(2,1)S(1)}, u32[]{:S(2)}, u32[]{:S(2)}) async-start(bf16[8,40,128]{2,1,0:T(8,128)(2,1)} %shard_map.131), calls=%async_computation | async-start | bytes 163840 | tf_op jit(solution)/shard_map/all_to_all | solution.py:405
  12.1 3.0 %collective-permute-start.1 = (bf16[32,1024]{1,0:T(8,128)(2,1)S(1)}, bf16[32,1024]{1,0:T(8,128)(2,1)S(1)}, u32[]{:S(2)}, u32[]{:S(2)}) collective-permute-start(bf16[32,1024]{1,0:T(8,128)(2,1)S(1)} %copy-done), channel_id=1, source_target_pairs={{0,4},{2,6},{4,0},{6,2},{1,5},{3,7},{5,1},{7,3},{8,12},{10,14},{12... | collective-permute-start | bytes 196616 | tf_op jit(solution)/shard_map/ppermute | solution.py:408
  15.1 4.5 %all-to-all-done.g0 = bf16[8,40,128]{2,1,0:T(8,128)(2,1)S(1)} async-done(((bf16[8,40,128]{2,1,0:T(8,128)(2,1)}), bf16[8,40,128]{2,1,0:T(8,128)(2,1)S(1)}, u32[]{:S(2)}, u32[]{:S(2)}) %all-to-all-start) | async-done | bytes 81952 | tf_op jit(solution)/shard_map/all_to_all | solution.py:405
  19.6 2.5 %collective-permute-start.5 = (bf16[8,40,128]{2,1,0:T(8,128)(2,1)S(1)}, bf16[8,40,128]{2,1,0:T(8,128)(2,1)S(1)}, u32[]{:S(2)}, u32[]{:S(2)}) collective-permute-start(bf16[8,40,128]{2,1,0:T(8,128)(2,1)S(1)} %all-to-all-done.g0), channel_id=1, source_target_pairs={{0,24},{8,0},{16,8},{24,16},{1,25},{9,1},{17,9},{25,17},{2,26},{10... | collective-permute-start | bytes 245768 | tf_op jit(solution)/shard_map/ppermute | solution.py:406
  26.0 1.6 %collective-permute-done.t1 = bf16[32,1024]{1,0:T(8,128)(2,1)S(1)} collective-permute-done((bf16[32,1024]{1,0:T(8,128)(2,1)S(1)}, bf16[32,1024]{1,0:T(8,128)(2,1)S(1)}, u32[]{:S(2)}, u32[]{:S(2)}) %collective-permute-start) | collective-permute-done | bytes 65568 | tf_op jit(solution)/shard_map/ppermute | solution.py:408
  27.8 1.6 %shard_map.132 = (bf16[64,128]{1,0:T(8,128)(2,1)S(1)}, bf16[8,72,128]{2,1,0:T(8,128)(2,1)}) custom-call(s32[5]{0:T(128)S(1)} %stack.62.where, bf16[32,1024]{1,0:T(8,128)(2,1)S(1)} %copy-done, bf16[32,1024]{1,0:T(8,128)(2,1)S(1)} %collective-permute-done.t1, bf16[32,1024]{1,0:T(8,128)(2,1)S(1)} %collective-permute-done.1.t2, ...), custom_call_target="tpu_custom_call" | custom-call | tf_op jit(solution)/shard_map/pallas_call | solution.py:416
  29.3 3.5 %all-to-all-start.2 = ((bf16[8,72,128]{2,1,0:T(8,128)(2,1)}), bf16[8,72,128]{2,1,0:T(8,128)(2,1)S(1)}, u32[]{:S(2)}, u32[]{:S(2)}) async-start(bf16[8,72,128]{2,1,0:T(8,128)(2,1)} %get-tuple-element.25), calls=%async_computation.2 | async-start | bytes 294912 | tf_op jit(solution)/shard_map/all_to_all | solution.py:422
  33.7 2.3 %collective-permute-start.12 = (bf16[64,128]{1,0:T(8,128)(2,1)S(1)}, bf16[64,128]{1,0:T(8,128)(2,1)S(1)}, u32[]{:S(2)}, u32[]{:S(2)}) collective-permute-start(bf16[64,128]{1,0:T(8,128)(2,1)S(1)} %shard_map.133), channel_id=1, source_target_pairs={{0,24},{8,0},{16,8},{24,16},{1,25},{9,1},{17,9},{25,17},{2,26},{10... | collective-permute-start | bytes 49160 | tf_op jit(solution)/shard_map/ppermute | solution.py:413
  37.3 2.8 %collective-permute-done.11 = bf16[64,128]{1,0:T(8,128)(2,1)S(1)} collective-permute-done((bf16[64,128]{1,0:T(8,128)(2,1)S(1)}, bf16[64,128]{1,0:T(8,128)(2,1)S(1)}, u32[]{:S(2)}, u32[]{:S(2)}) %collective-permute-start.11) | collective-permute-done | bytes 16416 | tf_op jit(solution)/shard_map/ppermute | solution.py:413
  42.0 6.6 %all-to-all-start.1 = ((bf16[8,4,64,128]{3,2,1,0:T(8,128)(2,1)}), bf16[8,4,64,128]{3,2,1,0:T(8,128)(2,1)S(1)}, u32[]{:S(2)}, u32[]{:S(2)}) async-start(bf16[8,4,64,128]{3,2,1,0:T(8,128)(2,1)} %broadcast_in_dim.2), calls=%async_computation.1 | async-start | bytes 1048576 | tf_op jit(solution)/shard_map/all_to_all | solution.py:427
  48.6 2.4 %collective-permute-start.16 = (bf16[8,72,128]{2,1,0:T(8,128)(2,1)S(1)}, bf16[8,72,128]{2,1,0:T(8,128)(2,1)S(1)}, u32[]{:S(2)}, u32[]{:S(2)}) collective-permute-start(bf16[8,72,128]{2,1,0:T(8,128)(2,1)S(1)} %all-to-all-done.2), channel_id=1, source_target_pairs={{0,24},{1,7},{2,26},{3,1},{4,28},{5,3},{6,30},{7,5},{8,0},{9,15},{... | collective-permute-start | bytes 442376 | tf_op jit(solution)/shard_map/ppermute | solution.py:423
  52.1 2.5 %collective-permute-done.16 = bf16[8,72,128]{2,1,0:T(8,128)(2,1)S(1)} collective-permute-done((bf16[8,72,128]{2,1,0:T(8,128)(2,1)S(1)}, bf16[8,72,128]{2,1,0:T(8,128)(2,1)S(1)}, u32[]{:S(2)}, u32[]{:S(2)}) %collective-permute-start.16) | collective-permute-done | bytes 147488 | tf_op jit(solution)/shard_map/ppermute | solution.py:423
  54.6 1.9 %collective-permute-done.15 = bf16[8,72,128]{2,1,0:T(8,128)(2,1)S(1)} collective-permute-done((bf16[8,72,128]{2,1,0:T(8,128)(2,1)S(1)}, bf16[8,72,128]{2,1,0:T(8,128)(2,1)S(1)}, u32[]{:S(2)}, u32[]{:S(2)}) %collective-permute-start.15) | collective-permute-done | bytes 147488 | tf_op jit(solution)/shard_map/ppermute | solution.py:423
  60.8 14.6 %collective-permute-start.13 = (bf16[8,4,64,128]{3,2,1,0:T(8,128)(2,1)S(1)}, bf16[8,4,64,128]{3,2,1,0:T(8,128)(2,1)S(1)}, u32[]{:S(2)}, u32[]{:S(2)}) collective-permute-start(bf16[8,4,64,128]{3,2,1,0:T(8,128)(2,1)S(1)} %all-to-all-done.1.up_own.w_own), channel_id=1, source_target_pairs={{0,1},{1,0},{2,3},{3,2},{4,5},{5,4},{6,7},{7,6},{8,9},{9,8},{10,11... | collective-permute-start | bytes 1572872 | tf_op jit(solution)/shard_map/ppermute | solution.py:428
  75.5 1.6 %collective-permute-done.6 = bf16[64,128]{1,0:T(8,128)(2,1)S(1)} collective-permute-done((bf16[64,128]{1,0:T(8,128)(2,1)S(1)}, bf16[64,128]{1,0:T(8,128)(2,1)S(1)}, u32[]{:S(2)}, u32[]{:S(2)}) %collective-permute-start.6) | collective-permute-done | bytes 16416 | tf_op jit(solution)/shard_map/ppermute | solution.py:429
  77.0 2.3 %collective-permute-start.9 = (bf16[2,64,128]{2,1,0:T(8,128)(2,1)S(1)}, bf16[2,64,128]{2,1,0:T(8,128)(2,1)S(1)}, u32[]{:S(2)}, u32[]{:S(2)}) collective-permute-start(bf16[2,64,128]{2,1,0:T(8,128)(2,1)S(1)} %pad_maximum_fusion.2.q0), channel_id=1, source_target_pairs={{0,6},{2,0},{4,2},{6,4},{1,7},{3,1},{5,3},{7,5},{8,14},{10,8},{12,... | collective-permute-start | bytes 98312 | tf_op jit(solution)/shard_map/ppermute | solution.py:430
  79.3 7.1 %collective-permute-done.9.q3 = bf16[2,64,128]{2,1,0:T(8,128)(2,1)S(1)} collective-permute-done((bf16[2,64,128]{2,1,0:T(8,128)(2,1)S(1)}, bf16[2,64,128]{2,1,0:T(8,128)(2,1)S(1)}, u32[]{:S(2)}, u32[]{:S(2)}) %collective-permute-start.9) | collective-permute-done | bytes 32800 | tf_op jit(solution)/shard_map/ppermute | solution.py:430
  86.5 4.6 %collective-permute-done.8.q2 = bf16[2,64,128]{2,1,0:T(8,128)(2,1)S(1)} collective-permute-done((bf16[2,64,128]{2,1,0:T(8,128)(2,1)S(1)}, bf16[2,64,128]{2,1,0:T(8,128)(2,1)S(1)}, u32[]{:S(2)}, u32[]{:S(2)}) %collective-permute-start.8) | collective-permute-done | bytes 32800 | tf_op jit(solution)/shard_map/ppermute | solution.py:430
  91.9 3.7 %collective-permute-done.7.q1 = bf16[2,64,128]{2,1,0:T(8,128)(2,1)S(1)} collective-permute-done((bf16[2,64,128]{2,1,0:T(8,128)(2,1)S(1)}, bf16[2,64,128]{2,1,0:T(8,128)(2,1)S(1)}, u32[]{:S(2)}, u32[]{:S(2)}) %collective-permute-start.7) | collective-permute-done | bytes 32800 | tf_op jit(solution)/shard_map/ppermute | solution.py:430
  97.6 9.3 %shard_map.135 = (f32[256,128]{1,0:T(8,128)S(1)}, bf16[256,128]{1,0:T(8,128)(2,1)S(1)}, f32[8,256]{1,0:T(8,128)S(1)}) custom-call(s32[5]{0:T(128)S(1)} %stack.62.where, s32[256]{0:T(256)S(1)} %copy-done.1, bf16[4,256,256]{2,1,0:T(8,128)(2,1)S(1)} %get-tuple-element.19.q_ref, bf16[256,256]{1,0:T(8,128)(2,1)S(1)} %get-tuple-element.20.uk, ...), custom_call_target="tpu_custom_call" | custom-call | tf_op jit(solution)/shard_map/pallas_call | solution.py:447
  106.9 4.0 %collective-permute-start.20 = (bf16[256,128]{1,0:T(8,128)(2,1)S(1)}, bf16[256,128]{1,0:T(8,128)(2,1)S(1)}, u32[]{:S(2)}, u32[]{:S(2)}) collective-permute-start(bf16[256,128]{1,0:T(8,128)(2,1)S(1)} %get-tuple-element.27), channel_id=1, source_target_pairs={{0,1},{1,0},{2,3},{3,2},{4,5},{5,4},{6,7},{7,6},{8,9},{9,8},{10,11... | collective-permute-start | bytes 196616 | tf_op jit(solution)/shard_map/ppermute | solution.py:465
  113.1 2.9 %collective-permute-start.23 = (bf16[32,1024]{1,0:T(8,128)(2,1)S(1)}, bf16[32,1024]{1,0:T(8,128)(2,1)S(1)}, u32[]{:S(2)}, u32[]{:S(2)}) collective-permute-start(bf16[32,1024]{1,0:T(8,128)(2,1)S(1)} %get-tuple-element.31), channel_id=1, source_target_pairs={{0,4},{2,6},{4,0},{6,2},{1,5},{3,7},{5,1},{7,3},{8,12},{10,14},{12... | collective-permute-start | bytes 196616 | tf_op jit(solution)/shard_map/ppermute | solution.py:472
  117.8 1.7 %collective-permute-done.23.p2 = bf16[32,1024]{1,0:T(8,128)(2,1)S(1)} collective-permute-done((bf16[32,1024]{1,0:T(8,128)(2,1)S(1)}, bf16[32,1024]{1,0:T(8,128)(2,1)S(1)}, u32[]{:S(2)}, u32[]{:S(2)}) %collective-permute-start.23) | collective-permute-done | bytes 65568 | tf_op jit(solution)/shard_map/ppermute | solution.py:472
  (65 shorter events, 21.5 us)
Async XLA Ops:
  3.0 16.7 %all-to-all-start = ((bf16[8,40,128]{2,1,0:T(8,128)(2,1)}), bf16[8,40,128]{2,1,0:T(8,128)(2,1)S(1)}, u32[]{:S(2)}, u32[]{:S(2)}) async-start(bf16[8,40,128]{2,1,0:T(8,128)(2,1)} %shard_map.131), calls=%async_computation | async-start | bytes 163840 | tf_op jit(solution)/shard_map/all_to_all | solution.py:405
  12.1 12.4 %collective-permute-start.1 = (bf16[32,1024]{1,0:T(8,128)(2,1)S(1)}, bf16[32,1024]{1,0:T(8,128)(2,1)S(1)}, u32[]{:S(2)}, u32[]{:S(2)}) collective-permute-start(bf16[32,1024]{1,0:T(8,128)(2,1)S(1)} %copy-done), channel_id=1, source_target_pairs={{0,4},{2,6},{4,0},{6,2},{1,5},{3,7},{5,1},{7,3},{8,12},{10,14},{12... | collective-permute-start | bytes 196616 | tf_op jit(solution)/shard_map/ppermute | solution.py:408
  19.6 8.0 %collective-permute-start.5 = (bf16[8,40,128]{2,1,0:T(8,128)(2,1)S(1)}, bf16[8,40,128]{2,1,0:T(8,128)(2,1)S(1)}, u32[]{:S(2)}, u32[]{:S(2)}) collective-permute-start(bf16[8,40,128]{2,1,0:T(8,128)(2,1)S(1)} %all-to-all-done.g0), channel_id=1, source_target_pairs={{0,24},{8,0},{16,8},{24,16},{1,25},{9,1},{17,9},{25,17},{2,26},{10... | collective-permute-start | bytes 245768 | tf_op jit(solution)/shard_map/ppermute | solution.py:406
  22.1 5.5 %collective-permute-start.4 = (bf16[8,40,128]{2,1,0:T(8,128)(2,1)S(1)}, bf16[8,40,128]{2,1,0:T(8,128)(2,1)S(1)}, u32[]{:S(2)}, u32[]{:S(2)}) collective-permute-start(bf16[8,40,128]{2,1,0:T(8,128)(2,1)S(1)} %all-to-all-done.g0), channel_id=1, source_target_pairs={{0,16},{8,24},{16,0},{24,8},{1,17},{9,25},{17,1},{25,9},{2,18},{10... | collective-permute-start | bytes 245768 | tf_op jit(solution)/shard_map/ppermute | solution.py:406
  22.6 5.2 %collective-permute-start.3 = (bf16[8,40,128]{2,1,0:T(8,128)(2,1)S(1)}, bf16[8,40,128]{2,1,0:T(8,128)(2,1)S(1)}, u32[]{:S(2)}, u32[]{:S(2)}) collective-permute-start(bf16[8,40,128]{2,1,0:T(8,128)(2,1)S(1)} %all-to-all-done.g0), channel_id=1, source_target_pairs={{0,8},{8,16},{16,24},{24,0},{1,9},{9,17},{17,25},{25,1},{2,10},{10... | collective-permute-start | bytes 245768 | tf_op jit(solution)/shard_map/ppermute | solution.py:406
  23.2 4.4 %collective-permute-start = (bf16[32,1024]{1,0:T(8,128)(2,1)S(1)}, bf16[32,1024]{1,0:T(8,128)(2,1)S(1)}, u32[]{:S(2)}, u32[]{:S(2)}) collective-permute-start(bf16[32,1024]{1,0:T(8,128)(2,1)S(1)} %copy-done), channel_id=1, source_target_pairs={{0,2},{2,4},{4,6},{6,0},{1,3},{3,5},{5,7},{7,1},{8,10},{10,12},{12... | collective-permute-start | bytes 196616 | tf_op jit(solution)/shard_map/ppermute | solution.py:408
  29.3 11.8 %all-to-all-start.2 = ((bf16[8,72,128]{2,1,0:T(8,128)(2,1)}), bf16[8,72,128]{2,1,0:T(8,128)(2,1)S(1)}, u32[]{:S(2)}, u32[]{:S(2)}) async-start(bf16[8,72,128]{2,1,0:T(8,128)(2,1)} %get-tuple-element.25), calls=%async_computation.2 | async-start | bytes 294912 | tf_op jit(solution)/shard_map/all_to_all | solution.py:422
  36.1 4.1 %collective-permute-start.11 = (bf16[64,128]{1,0:T(8,128)(2,1)S(1)}, bf16[64,128]{1,0:T(8,128)(2,1)S(1)}, u32[]{:S(2)}, u32[]{:S(2)}) collective-permute-start(bf16[64,128]{1,0:T(8,128)(2,1)S(1)} %shard_map.133), channel_id=1, source_target_pairs={{0,16},{8,24},{16,0},{24,8},{1,17},{9,25},{17,1},{25,9},{2,18},{10... | collective-permute-start | bytes 49160 | tf_op jit(solution)/shard_map/ppermute | solution.py:413
  37.3 3.8 %collective-permute-start.10 = (bf16[64,128]{1,0:T(8,128)(2,1)S(1)}, bf16[64,128]{1,0:T(8,128)(2,1)S(1)}, u32[]{:S(2)}, u32[]{:S(2)}) collective-permute-start(bf16[64,128]{1,0:T(8,128)(2,1)S(1)} %shard_map.133), channel_id=1, source_target_pairs={{0,8},{8,16},{16,24},{24,0},{1,9},{9,17},{17,25},{25,1},{2,10},{10... | collective-permute-start | bytes 49160 | tf_op jit(solution)/shard_map/ppermute | solution.py:413
  42.0 18.8 %all-to-all-start.1 = ((bf16[8,4,64,128]{3,2,1,0:T(8,128)(2,1)}), bf16[8,4,64,128]{3,2,1,0:T(8,128)(2,1)S(1)}, u32[]{:S(2)}, u32[]{:S(2)}) async-start(bf16[8,4,64,128]{3,2,1,0:T(8,128)(2,1)} %broadcast_in_dim.2), calls=%async_computation.1 | async-start | bytes 1048576 | tf_op jit(solution)/shard_map/all_to_all | solution.py:427
  48.6 6.0 %collective-permute-start.16 = (bf16[8,72,128]{2,1,0:T(8,128)(2,1)S(1)}, bf16[8,72,128]{2,1,0:T(8,128)(2,1)S(1)}, u32[]{:S(2)}, u32[]{:S(2)}) collective-permute-start(bf16[8,72,128]{2,1,0:T(8,128)(2,1)S(1)} %all-to-all-done.2), channel_id=1, source_target_pairs={{0,24},{1,7},{2,26},{3,1},{4,28},{5,3},{6,30},{7,5},{8,0},{9,15},{... | collective-permute-start | bytes 442376 | tf_op jit(solution)/shard_map/ppermute | solution.py:423
  50.9 5.6 %collective-permute-start.15 = (bf16[8,72,128]{2,1,0:T(8,128)(2,1)S(1)}, bf16[8,72,128]{2,1,0:T(8,128)(2,1)S(1)}, u32[]{:S(2)}, u32[]{:S(2)}) collective-permute-start(bf16[8,72,128]{2,1,0:T(8,128)(2,1)S(1)} %all-to-all-done.2), channel_id=1, source_target_pairs={{0,16},{1,5},{2,18},{3,7},{4,20},{5,1},{6,22},{7,3},{8,24},{9,13},... | collective-permute-start | bytes 442376 | tf_op jit(solution)/shard_map/ppermute | solution.py:423
  51.7 6.3 %collective-permute-start.14 = (bf16[8,72,128]{2,1,0:T(8,128)(2,1)S(1)}, bf16[8,72,128]{2,1,0:T(8,128)(2,1)S(1)}, u32[]{:S(2)}, u32[]{:S(2)}) collective-permute-start(bf16[8,72,128]{2,1,0:T(8,128)(2,1)S(1)} %all-to-all-done.2), channel_id=1, source_target_pairs={{0,8},{1,3},{2,10},{3,5},{4,12},{5,7},{6,14},{7,1},{8,16},{9,11},{... | collective-permute-start | bytes 442376 | tf_op jit(solution)/shard_map/ppermute | solution.py:423
  58.1 39.5 %collective-permute-start.19 = (bf16[4,8,72,128]{3,2,1,0:T(8,128)(2,1)S(1)}, bf16[4,8,72,128]{3,2,1,0:T(8,128)(2,1)S(1)}, u32[]{:S(2)}, u32[]{:S(2)}) collective-permute-start(bf16[4,8,72,128]{3,2,1,0:T(8,128)(2,1)S(1)} %pad_maximum_fusion.b0), channel_id=1, source_target_pairs={{0,6},{1,25},{2,0},{3,27},{4,2},{5,29},{6,4},{7,31},{8,14},{9,1},{... | collective-permute-start | bytes 1769480 | tf_op jit(solution)/shard_map/ppermute | solution.py:425
  58.3 39.3 %collective-permute-start.18 = (bf16[4,8,72,128]{3,2,1,0:T(8,128)(2,1)S(1)}, bf16[4,8,72,128]{3,2,1,0:T(8,128)(2,1)S(1)}, u32[]{:S(2)}, u32[]{:S(2)}) collective-permute-start(bf16[4,8,72,128]{3,2,1,0:T(8,128)(2,1)S(1)} %pad_maximum_fusion.b0), channel_id=1, source_target_pairs={{0,4},{1,17},{2,6},{3,19},{4,0},{5,21},{6,2},{7,23},{8,12},{9,25},... | collective-permute-start | bytes 1769480 | tf_op jit(solution)/shard_map/ppermute | solution.py:425
  59.4 38.2 %collective-permute-start.17 = (bf16[4,8,72,128]{3,2,1,0:T(8,128)(2,1)S(1)}, bf16[4,8,72,128]{3,2,1,0:T(8,128)(2,1)S(1)}, u32[]{:S(2)}, u32[]{:S(2)}) collective-permute-start(bf16[4,8,72,128]{3,2,1,0:T(8,128)(2,1)S(1)} %pad_maximum_fusion.b0), channel_id=1, source_target_pairs={{0,2},{1,9},{2,4},{3,11},{4,6},{5,13},{6,0},{7,15},{8,10},{9,17},{... | collective-permute-start | bytes 1769480 | tf_op jit(solution)/shard_map/ppermute | solution.py:425
  60.8 34.8 %collective-permute-start.13 = (bf16[8,4,64,128]{3,2,1,0:T(8,128)(2,1)S(1)}, bf16[8,4,64,128]{3,2,1,0:T(8,128)(2,1)S(1)}, u32[]{:S(2)}, u32[]{:S(2)}) collective-permute-start(bf16[8,4,64,128]{3,2,1,0:T(8,128)(2,1)S(1)} %all-to-all-done.1.up_own.w_own), channel_id=1, source_target_pairs={{0,1},{1,0},{2,3},{3,2},{4,5},{5,4},{6,7},{7,6},{8,9},{9,8},{10,11... | collective-permute-start | bytes 1572872 | tf_op jit(solution)/shard_map/ppermute | solution.py:428
  77.0 9.4 %collective-permute-start.9 = (bf16[2,64,128]{2,1,0:T(8,128)(2,1)S(1)}, bf16[2,64,128]{2,1,0:T(8,128)(2,1)S(1)}, u32[]{:S(2)}, u32[]{:S(2)}) collective-permute-start(bf16[2,64,128]{2,1,0:T(8,128)(2,1)S(1)} %pad_maximum_fusion.2.q0), channel_id=1, source_target_pairs={{0,6},{2,0},{4,2},{6,4},{1,7},{3,1},{5,3},{7,5},{8,14},{10,8},{12,... | collective-permute-start | bytes 98312 | tf_op jit(solution)/shard_map/ppermute | solution.py:430
  86.5 4.6 %collective-permute-start.8 = (bf16[2,64,128]{2,1,0:T(8,128)(2,1)S(1)}, bf16[2,64,128]{2,1,0:T(8,128)(2,1)S(1)}, u32[]{:S(2)}, u32[]{:S(2)}) collective-permute-start(bf16[2,64,128]{2,1,0:T(8,128)(2,1)S(1)} %pad_maximum_fusion.2.q0), channel_id=1, source_target_pairs={{0,4},{2,6},{4,0},{6,2},{1,5},{3,7},{5,1},{7,3},{8,12},{10,14},{12... | collective-permute-start | bytes 98312 | tf_op jit(solution)/shard_map/ppermute | solution.py:430
  91.1 4.5 %collective-permute-start.7 = (bf16[2,64,128]{2,1,0:T(8,128)(2,1)S(1)}, bf16[2,64,128]{2,1,0:T(8,128)(2,1)S(1)}, u32[]{:S(2)}, u32[]{:S(2)}) collective-permute-start(bf16[2,64,128]{2,1,0:T(8,128)(2,1)S(1)} %pad_maximum_fusion.2.q0), channel_id=1, source_target_pairs={{0,2},{2,4},{4,6},{6,0},{1,3},{3,5},{5,7},{7,1},{8,10},{10,12},{12... | collective-permute-start | bytes 98312 | tf_op jit(solution)/shard_map/ppermute | solution.py:430
  106.9 5.2 %collective-permute-start.20 = (bf16[256,128]{1,0:T(8,128)(2,1)S(1)}, bf16[256,128]{1,0:T(8,128)(2,1)S(1)}, u32[]{:S(2)}, u32[]{:S(2)}) collective-permute-start(bf16[256,128]{1,0:T(8,128)(2,1)S(1)} %get-tuple-element.27), channel_id=1, source_target_pairs={{0,1},{1,0},{2,3},{3,2},{4,5},{5,4},{6,7},{7,6},{8,9},{9,8},{10,11... | collective-permute-start | bytes 196616 | tf_op jit(solution)/shard_map/ppermute | solution.py:465
  113.1 4.8 %collective-permute-start.22 = (bf16[32,1024]{1,0:T(8,128)(2,1)S(1)}, bf16[32,1024]{1,0:T(8,128)(2,1)S(1)}, u32[]{:S(2)}, u32[]{:S(2)}) collective-permute-start(bf16[32,1024]{1,0:T(8,128)(2,1)S(1)} %get-tuple-element.30), channel_id=1, source_target_pairs={{0,2},{2,4},{4,6},{6,0},{1,3},{3,5},{5,7},{7,1},{8,10},{10,12},{12... | collective-permute-start | bytes 196616 | tf_op jit(solution)/shard_map/ppermute | solution.py:472
  113.1 6.3 %collective-permute-start.23 = (bf16[32,1024]{1,0:T(8,128)(2,1)S(1)}, bf16[32,1024]{1,0:T(8,128)(2,1)S(1)}, u32[]{:S(2)}, u32[]{:S(2)}) collective-permute-start(bf16[32,1024]{1,0:T(8,128)(2,1)S(1)} %get-tuple-element.31), channel_id=1, source_target_pairs={{0,4},{2,6},{4,0},{6,2},{1,5},{3,7},{5,1},{7,3},{8,12},{10,14},{12... | collective-permute-start | bytes 196616 | tf_op jit(solution)/shard_map/ppermute | solution.py:472
  116.1 3.9 %collective-permute-start.24 = (bf16[32,1024]{1,0:T(8,128)(2,1)S(1)}, bf16[32,1024]{1,0:T(8,128)(2,1)S(1)}, u32[]{:S(2)}, u32[]{:S(2)}) collective-permute-start(bf16[32,1024]{1,0:T(8,128)(2,1)S(1)} %get-tuple-element.32), channel_id=1, source_target_pairs={{0,6},{2,0},{4,2},{6,4},{1,7},{3,1},{5,3},{7,5},{8,14},{10,8},{12,... | collective-permute-start | bytes 196616 | tf_op jit(solution)/shard_map/ppermute | solution.py:472
  (13 other events, 53.7 us)

commit v9 on v8

--- a/solution.py
+++ b/solution.py
@@ -92,7 +92,20 @@
         out[z, 32:40, :] = turned
 
 
-def pack_later(up_query, up_key, up_value, docs_ref, out_t, out):
+def pack_later(*refs):
+    inputs, out, table, places, sems = refs[:7], refs[7], refs[8], refs[9:16], refs[16]
+    copies = [
+        pltpu.make_async_copy(source, place, sems.at[i])
+        for i, (source, place) in enumerate(zip(inputs, places))
+    ]
+    for copy in copies:
+        copy.start()
+    for copy in copies:
+        copy.wait()
+    up_query, up_key, up_value, docs_ref, out_t, query_gain, key_gain = places
+    table[0:2, :] = query_gain[...]
+    table[2:4, :] = key_gain[...]
+    table[4:6, :] = docs_ref[...].astype(F32)
     src = lax.broadcasted_iota(jnp.int32, (192, 256), 0)
     lane = lanes((192, 256))
     plain = 96 * (lane // 64) + lane % 64
@@ -156,7 +169,7 @@
 
 
 def make_queries(
-    where, q0, q1, q2, q3, up_own, up_other, gain, key_gain, docs_in,
+    where, q0, q1, q2, q3, up_own, up_other, table,
     out, uk_ref, uv_ref, docs_ref, col_ref, row_ref, latents, ups,
 ):
     x, y, c = where[1], where[2], where[3]
@@ -168,12 +181,12 @@
     raw = latents[...]
     mean = jnp.sum(raw * raw, axis=0, keepdims=True) * (1.0 / 256.0)
     inverse = lax.rsqrt(mean + EPS)
-    gains = jnp.concatenate([column(gain[0:1, :]), column(gain[1:2, :])], axis=0)
+    gains = jnp.concatenate([column(table[0:1, :]), column(table[1:2, :])], axis=0)
     gains = jnp.concatenate([gains, gains], axis=1)
-    tokens_docs = docs_in[...].astype(F32)
+    tokens_docs = table[4:6, :]
     at = lanes((1, 128))
     for i in range(2):
-        col_ref[128 * i : 128 * (i + 1), :] = column(key_gain[i : i + 1, :])
+        col_ref[128 * i : 128 * (i + 1), :] = column(table[2 + i : 3 + i, :])
         ordered = jnp.zeros((1, 128), F32)
         for k in range(NY):
             line = tokens_docs[k // 2 : k // 2 + 1, :]
@@ -407,9 +420,15 @@
 
     rows = [tokens] + [lax.ppermute(tokens, "y", ring(j)) for j in range(1, NY)]
 
-    later = call(pack_later, jax.ShapeDtypeStruct((64, 128), BF), 0, 5)(
-        up_query, up_key, up_value, doc_ids.reshape(2, 128), output_weight.T
+    sources = (
+        up_query, up_key, up_value, doc_ids.reshape(2, 128), output_weight.T,
+        query_gain.reshape(2, 128), key_gain.reshape(2, 128),
     )
+    later, table = call(
+        pack_later, (jax.ShapeDtypeStruct((64, 128), BF), jax.ShapeDtypeStruct((6, 128), F32)),
+        0, 7, any_from=0,
+        scratch=[VMEM(a.shape, a.dtype) for a in sources] + [pltpu.SemaphoreType.DMA((7,))],
+    )(*(pltpu.with_memory_space_constraint(a, pltpu.HBM) for a in sources))
     later = [later] + [lax.ppermute(later, "x", ring(j)) for j in range(1, NX)]
     later = jnp.broadcast_to(jnp.stack(later)[None], (NZ, NX, 64, 128))
 
@@ -438,10 +457,9 @@
             jax.ShapeDtypeStruct((256, 128), F32),
             jax.ShapeDtypeStruct((2, 128), F32),
         ),
-        1, 9, scratch=[VMEM((256, 256), F32), VMEM((2, NZ, NX, 32, 128), BF)],
+        1, 7, scratch=[VMEM((256, 256), F32), VMEM((2, NZ, NX, 32, 128), BF)],
     )(
-        here, *q_all, up_own, up_other, query_gain.reshape(2, 128),
-        key_gain.reshape(2, 128), doc_ids.reshape(2, 128),
+        here, *q_all, up_own, up_other, table
     )
 
     keep, send, ml = call(

time: 121 us -> 121 us (level)
  transfers between devices with their start and end apart: 28 -> 28, of which waited for: 17 -> 17; matrix products, arithmetic and copies ran while one was open for 1% -> 1% of each run, Pallas kernels for 1% -> 2%
where the time goes in v9:
time: 121 us
  starting transfers between devices  62.4 us (52%)
  waiting for transfers between devices  37.9 us (31%)
  Pallas kernels  17.1 us (14%)
  local copies, waits for them, and re-layouts  2.44 us (2%)
    ppermute x3, waiting for transfers between devices, layer(): lax.ppermute(q_pair, 'y', ring(j))  15.5 us
    ppermute x1, starting transfers between devices, layer(): up_other = lax.ppermute(up_own, 'c', swap)  14.6 us
    pallas_call x1, Pallas kernels, layer(): call(attend, (jax.ShapeDtypeStruct((256, 128), F32), jax.ShapeDtypeStruct...  9.3 us
    all_to_all x1, starting transfers between devices, layer(): gathered = lax.all_to_all(message, 'z', 0, 0)  9.15 us
    all_to_all x1, starting transfers between devices, layer(): up_own = lax.all_to_all(later, 'z', 0, 0)  6.56 us
    ppermute x3, waiting for transfers between devices, layer(): lax.ppermute(stage1, AXES, shift_pairs(2, j))  5.95 us
    ppermute x3, starting transfers between devices, layer(): rows = [tokens] + [lax.ppermute(tokens, 'y', ring(j)) for j in range(1, NY)]  5.74 us
    all_to_all x1, waiting for transfers between devices, layer(): gathered = lax.all_to_all(message, 'z', 0, 0)  4.5 us
  transfers between devices with their start and end apart: 28, of which 17 were waited for; matrix products, arithmetic and copies ran while one was open for 1% of the time, Pallas kernels for 2%

profile of v9, /device:TPU:1, one launch (start us, length us, event | category | flops | bytes accessed | tf_op | source)
XLA Modules:
  0.0 120.7 jit_solution(11267294634300138038)
XLA Ops:
  0.7 2.2 %shard_map.131 = bf16[8,40,128]{2,1,0:T(8,128)(2,1)} custom-call(s32[5]{0:T(128)S(1)} %stack.62.where, bf16[32,256]{1,0:T(8,128)(2,1)} %dq_in.1, bf16[32,256]{1,0:T(8,128)(2,1)} %dk_in.1, bf16[32,32]{1,0:T(8,128)(2,1)} %dr_in.1), custom_call_target="tpu_custom_call" | custom-call | tf_op jit(solution)/shard_map/pallas_call | solution.py:412
  3.0 9.1 %all-to-all-start = ((bf16[8,40,128]{2,1,0:T(8,128)(2,1)}), bf16[8,40,128]{2,1,0:T(8,128)(2,1)S(1)}, u32[]{:S(2)}, u32[]{:S(2)}) async-start(bf16[8,40,128]{2,1,0:T(8,128)(2,1)} %shard_map.131), calls=%async_computation | async-start | bytes 163840 | tf_op jit(solution)/shard_map/all_to_all | solution.py:418
  12.1 3.0 %collective-permute-start.1 = (bf16[32,1024]{1,0:T(8,128)(2,1)S(1)}, bf16[32,1024]{1,0:T(8,128)(2,1)S(1)}, u32[]{:S(2)}, u32[]{:S(2)}) collective-permute-start(bf16[32,1024]{1,0:T(8,128)(2,1)S(1)} %copy-done), channel_id=1, source_target_pairs={{0,4},{2,6},{4,0},{6,2},{1,5},{3,7},{5,1},{7,3},{8,12},{10,14},{12... | collective-permute-start | bytes 196616 | tf_op jit(solution)/shard_map/ppermute | solution.py:421
  15.1 4.5 %all-to-all-done.g0 = bf16[8,40,128]{2,1,0:T(8,128)(2,1)S(1)} async-done(((bf16[8,40,128]{2,1,0:T(8,128)(2,1)}), bf16[8,40,128]{2,1,0:T(8,128)(2,1)S(1)}, u32[]{:S(2)}, u32[]{:S(2)}) %all-to-all-start) | async-done | bytes 81952 | tf_op jit(solution)/shard_map/all_to_all | solution.py:418
  19.6 2.5 %collective-permute-start.5 = (bf16[8,40,128]{2,1,0:T(8,128)(2,1)S(1)}, bf16[8,40,128]{2,1,0:T(8,128)(2,1)S(1)}, u32[]{:S(2)}, u32[]{:S(2)}) collective-permute-start(bf16[8,40,128]{2,1,0:T(8,128)(2,1)S(1)} %all-to-all-done.g0), channel_id=1, source_target_pairs={{0,24},{8,0},{16,8},{24,16},{1,25},{9,1},{17,9},{25,17},{2,26},{10... | collective-permute-start | bytes 245768 | tf_op jit(solution)/shard_map/ppermute | solution.py:419
  26.0 1.6 %collective-permute-done.t1 = bf16[32,1024]{1,0:T(8,128)(2,1)S(1)} collective-permute-done((bf16[32,1024]{1,0:T(8,128)(2,1)S(1)}, bf16[32,1024]{1,0:T(8,128)(2,1)S(1)}, u32[]{:S(2)}, u32[]{:S(2)}) %collective-permute-start) | collective-permute-done | bytes 65568 | tf_op jit(solution)/shard_map/ppermute | solution.py:421
  27.8 1.6 %shard_map.132 = (bf16[64,128]{1,0:T(8,128)(2,1)S(1)}, bf16[8,72,128]{2,1,0:T(8,128)(2,1)}) custom-call(s32[5]{0:T(128)S(1)} %stack.62.where, bf16[32,1024]{1,0:T(8,128)(2,1)S(1)} %copy-done, bf16[32,1024]{1,0:T(8,128)(2,1)S(1)} %collective-permute-done.t1, bf16[32,1024]{1,0:T(8,128)(2,1)S(1)} %collective-permute-done.1.t2, ...), custom_call_target="tpu_custom_call" | custom-call | tf_op jit(solution)/shard_map/pallas_call | solution.py:435
  29.3 3.4 %all-to-all-start.2 = ((bf16[8,72,128]{2,1,0:T(8,128)(2,1)}), bf16[8,72,128]{2,1,0:T(8,128)(2,1)S(1)}, u32[]{:S(2)}, u32[]{:S(2)}) async-start(bf16[8,72,128]{2,1,0:T(8,128)(2,1)} %get-tuple-element.29), calls=%async_computation.2 | async-start | bytes 294912 | tf_op jit(solution)/shard_map/all_to_all | solution.py:441
  33.7 2.3 %collective-permute-start.12 = (bf16[64,128]{1,0:T(8,128)(2,1)S(1)}, bf16[64,128]{1,0:T(8,128)(2,1)S(1)}, u32[]{:S(2)}, u32[]{:S(2)}) collective-permute-start(bf16[64,128]{1,0:T(8,128)(2,1)S(1)} %get-tuple-element.21), channel_id=1, source_target_pairs={{0,24},{8,0},{16,8},{24,16},{1,25},{9,1},{17,9},{25,17},{2,26},{10... | collective-permute-start | bytes 49160 | tf_op jit(solution)/shard_map/ppermute | solution.py:432
  37.3 2.8 %collective-permute-done.11 = bf16[64,128]{1,0:T(8,128)(2,1)S(1)} collective-permute-done((bf16[64,128]{1,0:T(8,128)(2,1)S(1)}, bf16[64,128]{1,0:T(8,128)(2,1)S(1)}, u32[]{:S(2)}, u32[]{:S(2)}) %collective-permute-start.11) | collective-permute-done | bytes 16416 | tf_op jit(solution)/shard_map/ppermute | solution.py:432
  42.0 6.6 %all-to-all-start.1 = ((bf16[8,4,64,128]{3,2,1,0:T(8,128)(2,1)}), bf16[8,4,64,128]{3,2,1,0:T(8,128)(2,1)S(1)}, u32[]{:S(2)}, u32[]{:S(2)}) async-start(bf16[8,4,64,128]{3,2,1,0:T(8,128)(2,1)} %broadcast_in_dim.2), calls=%async_computation.1 | async-start | bytes 1048576 | tf_op jit(solution)/shard_map/all_to_all | solution.py:446
  48.6 2.4 %collective-permute-start.16 = (bf16[8,72,128]{2,1,0:T(8,128)(2,1)S(1)}, bf16[8,72,128]{2,1,0:T(8,128)(2,1)S(1)}, u32[]{:S(2)}, u32[]{:S(2)}) collective-permute-start(bf16[8,72,128]{2,1,0:T(8,128)(2,1)S(1)} %all-to-all-done.2), channel_id=1, source_target_pairs={{0,24},{1,7},{2,26},{3,1},{4,28},{5,3},{6,30},{7,5},{8,0},{9,15},{... | collective-permute-start | bytes 442376 | tf_op jit(solution)/shard_map/ppermute | solution.py:442
  52.1 2.5 %collective-permute-done.16 = bf16[8,72,128]{2,1,0:T(8,128)(2,1)S(1)} collective-permute-done((bf16[8,72,128]{2,1,0:T(8,128)(2,1)S(1)}, bf16[8,72,128]{2,1,0:T(8,128)(2,1)S(1)}, u32[]{:S(2)}, u32[]{:S(2)}) %collective-permute-start.16) | collective-permute-done | bytes 147488 | tf_op jit(solution)/shard_map/ppermute | solution.py:442
  54.6 1.9 %collective-permute-done.15 = bf16[8,72,128]{2,1,0:T(8,128)(2,1)S(1)} collective-permute-done((bf16[8,72,128]{2,1,0:T(8,128)(2,1)S(1)}, bf16[8,72,128]{2,1,0:T(8,128)(2,1)S(1)}, u32[]{:S(2)}, u32[]{:S(2)}) %collective-permute-start.15) | collective-permute-done | bytes 147488 | tf_op jit(solution)/shard_map/ppermute | solution.py:442
  60.8 14.6 %collective-permute-start.13 = (bf16[8,4,64,128]{3,2,1,0:T(8,128)(2,1)S(1)}, bf16[8,4,64,128]{3,2,1,0:T(8,128)(2,1)S(1)}, u32[]{:S(2)}, u32[]{:S(2)}) collective-permute-start(bf16[8,4,64,128]{3,2,1,0:T(8,128)(2,1)S(1)} %all-to-all-done.1.up_own.w_own), channel_id=1, source_target_pairs={{0,1},{1,0},{2,3},{3,2},{4,5},{5,4},{6,7},{7,6},{8,9},{9,8},{10,11... | collective-permute-start | bytes 1572872 | tf_op jit(solution)/shard_map/ppermute | solution.py:447
  75.5 1.6 %collective-permute-done.6 = bf16[64,128]{1,0:T(8,128)(2,1)S(1)} collective-permute-done((bf16[64,128]{1,0:T(8,128)(2,1)S(1)}, bf16[64,128]{1,0:T(8,128)(2,1)S(1)}, u32[]{:S(2)}, u32[]{:S(2)}) %collective-permute-start.6) | collective-permute-done | bytes 16416 | tf_op jit(solution)/shard_map/ppermute | solution.py:448
  77.0 2.3 %collective-permute-start.9 = (bf16[2,64,128]{2,1,0:T(8,128)(2,1)S(1)}, bf16[2,64,128]{2,1,0:T(8,128)(2,1)S(1)}, u32[]{:S(2)}, u32[]{:S(2)}) collective-permute-start(bf16[2,64,128]{2,1,0:T(8,128)(2,1)S(1)} %pad_maximum_fusion.2.q0), channel_id=1, source_target_pairs={{0,6},{2,0},{4,2},{6,4},{1,7},{3,1},{5,3},{7,5},{8,14},{10,8},{12,... | collective-permute-start | bytes 98312 | tf_op jit(solution)/shard_map/ppermute | solution.py:449
  79.3 7.2 %collective-permute-done.9.q3 = bf16[2,64,128]{2,1,0:T(8,128)(2,1)S(1)} collective-permute-done((bf16[2,64,128]{2,1,0:T(8,128)(2,1)S(1)}, bf16[2,64,128]{2,1,0:T(8,128)(2,1)S(1)}, u32[]{:S(2)}, u32[]{:S(2)}) %collective-permute-start.9) | collective-permute-done | bytes 32800 | tf_op jit(solution)/shard_map/ppermute | solution.py:449
  86.5 4.6 %collective-permute-done.8.q2 = bf16[2,64,128]{2,1,0:T(8,128)(2,1)S(1)} collective-permute-done((bf16[2,64,128]{2,1,0:T(8,128)(2,1)S(1)}, bf16[2,64,128]{2,1,0:T(8,128)(2,1)S(1)}, u32[]{:S(2)}, u32[]{:S(2)}) %collective-permute-start.8) | collective-permute-done | bytes 32800 | tf_op jit(solution)/shard_map/ppermute | solution.py:449
  91.9 3.7 %collective-permute-done.7.q1 = bf16[2,64,128]{2,1,0:T(8,128)(2,1)S(1)} collective-permute-done((bf16[2,64,128]{2,1,0:T(8,128)(2,1)S(1)}, bf16[2,64,128]{2,1,0:T(8,128)(2,1)S(1)}, u32[]{:S(2)}, u32[]{:S(2)}) %collective-permute-start.7) | collective-permute-done | bytes 32800 | tf_op jit(solution)/shard_map/ppermute | solution.py:449
  97.7 9.3 %shard_map.135 = (f32[256,128]{1,0:T(8,128)S(1)}, bf16[256,128]{1,0:T(8,128)(2,1)S(1)}, f32[8,256]{1,0:T(8,128)S(1)}) custom-call(s32[5]{0:T(128)S(1)} %stack.62.where, s32[256]{0:T(256)S(1)} %copy-done.1, bf16[4,256,256]{2,1,0:T(8,128)(2,1)S(1)} %get-tuple-element.23.q_ref, bf16[256,256]{1,0:T(8,128)(2,1)S(1)} %get-tuple-element.24.uk, ...), custom_call_target="tpu_custom_call" | custom-call | tf_op jit(solution)/shard_map/pallas_call | solution.py:465
  107.0 3.9 %collective-permute-start.20 = (bf16[256,128]{1,0:T(8,128)(2,1)S(1)}, bf16[256,128]{1,0:T(8,128)(2,1)S(1)}, u32[]{:S(2)}, u32[]{:S(2)}) collective-permute-start(bf16[256,128]{1,0:T(8,128)(2,1)S(1)} %get-tuple-element.31), channel_id=1, source_target_pairs={{0,1},{1,0},{2,3},{3,2},{4,5},{5,4},{6,7},{7,6},{8,9},{9,8},{10,11... | collective-permute-start | bytes 196616 | tf_op jit(solution)/shard_map/ppermute | solution.py:483
  113.1 2.9 %collective-permute-start.23 = (bf16[32,1024]{1,0:T(8,128)(2,1)S(1)}, bf16[32,1024]{1,0:T(8,128)(2,1)S(1)}, u32[]{:S(2)}, u32[]{:S(2)}) collective-permute-start(bf16[32,1024]{1,0:T(8,128)(2,1)S(1)} %get-tuple-element.35), channel_id=1, source_target_pairs={{0,4},{2,6},{4,0},{6,2},{1,5},{3,7},{5,1},{7,3},{8,12},{10,14},{12... | collective-permute-start | bytes 196616 | tf_op jit(solution)/shard_map/ppermute | solution.py:490
  117.8 1.7 %collective-permute-done.23.p2 = bf16[32,1024]{1,0:T(8,128)(2,1)S(1)} collective-permute-done((bf16[32,1024]{1,0:T(8,128)(2,1)S(1)}, bf16[32,1024]{1,0:T(8,128)(2,1)S(1)}, u32[]{:S(2)}, u32[]{:S(2)}) %collective-permute-start.23) | collective-permute-done | bytes 65568 | tf_op jit(solution)/shard_map/ppermute | solution.py:490
  (53 shorter events, 21.6 us)
Async XLA Ops:
  3.0 16.7 %all-to-all-start = ((bf16[8,40,128]{2,1,0:T(8,128)(2,1)}), bf16[8,40,128]{2,1,0:T(8,128)(2,1)S(1)}, u32[]{:S(2)}, u32[]{:S(2)}) async-start(bf16[8,40,128]{2,1,0:T(8,128)(2,1)} %shard_map.131), calls=%async_computation | async-start | bytes 163840 | tf_op jit(solution)/shard_map/all_to_all | solution.py:418
  12.1 12.4 %collective-permute-start.1 = (bf16[32,1024]{1,0:T(8,128)(2,1)S(1)}, bf16[32,1024]{1,0:T(8,128)(2,1)S(1)}, u32[]{:S(2)}, u32[]{:S(2)}) collective-permute-start(bf16[32,1024]{1,0:T(8,128)(2,1)S(1)} %copy-done), channel_id=1, source_target_pairs={{0,4},{2,6},{4,0},{6,2},{1,5},{3,7},{5,1},{7,3},{8,12},{10,14},{12... | collective-permute-start | bytes 196616 | tf_op jit(solution)/shard_map/ppermute | solution.py:421
  19.6 8.0 %collective-permute-start.5 = (bf16[8,40,128]{2,1,0:T(8,128)(2,1)S(1)}, bf16[8,40,128]{2,1,0:T(8,128)(2,1)S(1)}, u32[]{:S(2)}, u32[]{:S(2)}) collective-permute-start(bf16[8,40,128]{2,1,0:T(8,128)(2,1)S(1)} %all-to-all-done.g0), channel_id=1, source_target_pairs={{0,24},{8,0},{16,8},{24,16},{1,25},{9,1},{17,9},{25,17},{2,26},{10... | collective-permute-start | bytes 245768 | tf_op jit(solution)/shard_map/ppermute | solution.py:419
  22.1 5.5 %collective-permute-start.4 = (bf16[8,40,128]{2,1,0:T(8,128)(2,1)S(1)}, bf16[8,40,128]{2,1,0:T(8,128)(2,1)S(1)}, u32[]{:S(2)}, u32[]{:S(2)}) collective-permute-start(bf16[8,40,128]{2,1,0:T(8,128)(2,1)S(1)} %all-to-all-done.g0), channel_id=1, source_target_pairs={{0,16},{8,24},{16,0},{24,8},{1,17},{9,25},{17,1},{25,9},{2,18},{10... | collective-permute-start | bytes 245768 | tf_op jit(solution)/shard_map/ppermute | solution.py:419
  22.6 5.2 %collective-permute-start.3 = (bf16[8,40,128]{2,1,0:T(8,128)(2,1)S(1)}, bf16[8,40,128]{2,1,0:T(8,128)(2,1)S(1)}, u32[]{:S(2)}, u32[]{:S(2)}) collective-permute-start(bf16[8,40,128]{2,1,0:T(8,128)(2,1)S(1)} %all-to-all-done.g0), channel_id=1, source_target_pairs={{0,8},{8,16},{16,24},{24,0},{1,9},{9,17},{17,25},{25,1},{2,10},{10... | collective-permute-start | bytes 245768 | tf_op jit(solution)/shard_map/ppermute | solution.py:419
  23.2 4.4 %collective-permute-start = (bf16[32,1024]{1,0:T(8,128)(2,1)S(1)}, bf16[32,1024]{1,0:T(8,128)(2,1)S(1)}, u32[]{:S(2)}, u32[]{:S(2)}) collective-permute-start(bf16[32,1024]{1,0:T(8,128)(2,1)S(1)} %copy-done), channel_id=1, source_target_pairs={{0,2},{2,4},{4,6},{6,0},{1,3},{3,5},{5,7},{7,1},{8,10},{10,12},{12... | collective-permute-start | bytes 196616 | tf_op jit(solution)/shard_map/ppermute | solution.py:421
  29.3 11.8 %all-to-all-start.2 = ((bf16[8,72,128]{2,1,0:T(8,128)(2,1)}), bf16[8,72,128]{2,1,0:T(8,128)(2,1)S(1)}, u32[]{:S(2)}, u32[]{:S(2)}) async-start(bf16[8,72,128]{2,1,0:T(8,128)(2,1)} %get-tuple-element.29), calls=%async_computation.2 | async-start | bytes 294912 | tf_op jit(solution)/shard_map/all_to_all | solution.py:441
  36.1 4.1 %collective-permute-start.11 = (bf16[64,128]{1,0:T(8,128)(2,1)S(1)}, bf16[64,128]{1,0:T(8,128)(2,1)S(1)}, u32[]{:S(2)}, u32[]{:S(2)}) collective-permute-start(bf16[64,128]{1,0:T(8,128)(2,1)S(1)} %get-tuple-element.21), channel_id=1, source_target_pairs={{0,16},{8,24},{16,0},{24,8},{1,17},{9,25},{17,1},{25,9},{2,18},{10... | collective-permute-start | bytes 49160 | tf_op jit(solution)/shard_map/ppermute | solution.py:432
  37.3 3.8 %collective-permute-start.10 = (bf16[64,128]{1,0:T(8,128)(2,1)S(1)}, bf16[64,128]{1,0:T(8,128)(2,1)S(1)}, u32[]{:S(2)}, u32[]{:S(2)}) collective-permute-start(bf16[64,128]{1,0:T(8,128)(2,1)S(1)} %get-tuple-element.21), channel_id=1, source_target_pairs={{0,8},{8,16},{16,24},{24,0},{1,9},{9,17},{17,25},{25,1},{2,10},{10... | collective-permute-start | bytes 49160 | tf_op jit(solution)/shard_map/ppermute | solution.py:432
  42.0 18.8 %all-to-all-start.1 = ((bf16[8,4,64,128]{3,2,1,0:T(8,128)(2,1)}), bf16[8,4,64,128]{3,2,1,0:T(8,128)(2,1)S(1)}, u32[]{:S(2)}, u32[]{:S(2)}) async-start(bf16[8,4,64,128]{3,2,1,0:T(8,128)(2,1)} %broadcast_in_dim.2), calls=%async_computation.1 | async-start | bytes 1048576 | tf_op jit(solution)/shard_map/all_to_all | solution.py:446
  48.6 6.0 %collective-permute-start.16 = (bf16[8,72,128]{2,1,0:T(8,128)(2,1)S(1)}, bf16[8,72,128]{2,1,0:T(8,128)(2,1)S(1)}, u32[]{:S(2)}, u32[]{:S(2)}) collective-permute-start(bf16[8,72,128]{2,1,0:T(8,128)(2,1)S(1)} %all-to-all-done.2), channel_id=1, source_target_pairs={{0,24},{1,7},{2,26},{3,1},{4,28},{5,3},{6,30},{7,5},{8,0},{9,15},{... | collective-permute-start | bytes 442376 | tf_op jit(solution)/shard_map/ppermute | solution.py:442
  50.9 5.6 %collective-permute-start.15 = (bf16[8,72,128]{2,1,0:T(8,128)(2,1)S(1)}, bf16[8,72,128]{2,1,0:T(8,128)(2,1)S(1)}, u32[]{:S(2)}, u32[]{:S(2)}) collective-permute-start(bf16[8,72,128]{2,1,0:T(8,128)(2,1)S(1)} %all-to-all-done.2), channel_id=1, source_target_pairs={{0,16},{1,5},{2,18},{3,7},{4,20},{5,1},{6,22},{7,3},{8,24},{9,13},... | collective-permute-start | bytes 442376 | tf_op jit(solution)/shard_map/ppermute | solution.py:442
  51.7 6.4 %collective-permute-start.14 = (bf16[8,72,128]{2,1,0:T(8,128)(2,1)S(1)}, bf16[8,72,128]{2,1,0:T(8,128)(2,1)S(1)}, u32[]{:S(2)}, u32[]{:S(2)}) collective-permute-start(bf16[8,72,128]{2,1,0:T(8,128)(2,1)S(1)} %all-to-all-done.2), channel_id=1, source_target_pairs={{0,8},{1,3},{2,10},{3,5},{4,12},{5,7},{6,14},{7,1},{8,16},{9,11},{... | collective-permute-start | bytes 442376 | tf_op jit(solution)/shard_map/ppermute | solution.py:442
  58.1 38.8 %collective-permute-start.19 = (bf16[4,8,72,128]{3,2,1,0:T(8,128)(2,1)S(1)}, bf16[4,8,72,128]{3,2,1,0:T(8,128)(2,1)S(1)}, u32[]{:S(2)}, u32[]{:S(2)}) collective-permute-start(bf16[4,8,72,128]{3,2,1,0:T(8,128)(2,1)S(1)} %pad_maximum_fusion.b0), channel_id=1, source_target_pairs={{0,6},{1,25},{2,0},{3,27},{4,2},{5,29},{6,4},{7,31},{8,14},{9,1},{... | collective-permute-start | bytes 1769480 | tf_op jit(solution)/shard_map/ppermute | solution.py:444
  58.3 38.7 %collective-permute-start.18 = (bf16[4,8,72,128]{3,2,1,0:T(8,128)(2,1)S(1)}, bf16[4,8,72,128]{3,2,1,0:T(8,128)(2,1)S(1)}, u32[]{:S(2)}, u32[]{:S(2)}) collective-permute-start(bf16[4,8,72,128]{3,2,1,0:T(8,128)(2,1)S(1)} %pad_maximum_fusion.b0), channel_id=1, source_target_pairs={{0,4},{1,17},{2,6},{3,19},{4,0},{5,21},{6,2},{7,23},{8,12},{9,25},... | collective-permute-start | bytes 1769480 | tf_op jit(solution)/shard_map/ppermute | solution.py:444
  59.4 37.6 %collective-permute-start.17 = (bf16[4,8,72,128]{3,2,1,0:T(8,128)(2,1)S(1)}, bf16[4,8,72,128]{3,2,1,0:T(8,128)(2,1)S(1)}, u32[]{:S(2)}, u32[]{:S(2)}) collective-permute-start(bf16[4,8,72,128]{3,2,1,0:T(8,128)(2,1)S(1)} %pad_maximum_fusion.b0), channel_id=1, source_target_pairs={{0,2},{1,9},{2,4},{3,11},{4,6},{5,13},{6,0},{7,15},{8,10},{9,17},{... | collective-permute-start | bytes 1769480 | tf_op jit(solution)/shard_map/ppermute | solution.py:444
  60.8 34.8 %collective-permute-start.13 = (bf16[8,4,64,128]{3,2,1,0:T(8,128)(2,1)S(1)}, bf16[8,4,64,128]{3,2,1,0:T(8,128)(2,1)S(1)}, u32[]{:S(2)}, u32[]{:S(2)}) collective-permute-start(bf16[8,4,64,128]{3,2,1,0:T(8,128)(2,1)S(1)} %all-to-all-done.1.up_own.w_own), channel_id=1, source_target_pairs={{0,1},{1,0},{2,3},{3,2},{4,5},{5,4},{6,7},{7,6},{8,9},{9,8},{10,11... | collective-permute-start | bytes 1572872 | tf_op jit(solution)/shard_map/ppermute | solution.py:447
  77.0 9.5 %collective-permute-start.9 = (bf16[2,64,128]{2,1,0:T(8,128)(2,1)S(1)}, bf16[2,64,128]{2,1,0:T(8,128)(2,1)S(1)}, u32[]{:S(2)}, u32[]{:S(2)}) collective-permute-start(bf16[2,64,128]{2,1,0:T(8,128)(2,1)S(1)} %pad_maximum_fusion.2.q0), channel_id=1, source_target_pairs={{0,6},{2,0},{4,2},{6,4},{1,7},{3,1},{5,3},{7,5},{8,14},{10,8},{12,... | collective-permute-start | bytes 98312 | tf_op jit(solution)/shard_map/ppermute | solution.py:449
  86.5 4.6 %collective-permute-start.8 = (bf16[2,64,128]{2,1,0:T(8,128)(2,1)S(1)}, bf16[2,64,128]{2,1,0:T(8,128)(2,1)S(1)}, u32[]{:S(2)}, u32[]{:S(2)}) collective-permute-start(bf16[2,64,128]{2,1,0:T(8,128)(2,1)S(1)} %pad_maximum_fusion.2.q0), channel_id=1, source_target_pairs={{0,4},{2,6},{4,0},{6,2},{1,5},{3,7},{5,1},{7,3},{8,12},{10,14},{12... | collective-permute-start | bytes 98312 | tf_op jit(solution)/shard_map/ppermute | solution.py:449
  91.1 4.5 %collective-permute-start.7 = (bf16[2,64,128]{2,1,0:T(8,128)(2,1)S(1)}, bf16[2,64,128]{2,1,0:T(8,128)(2,1)S(1)}, u32[]{:S(2)}, u32[]{:S(2)}) collective-permute-start(bf16[2,64,128]{2,1,0:T(8,128)(2,1)S(1)} %pad_maximum_fusion.2.q0), channel_id=1, source_target_pairs={{0,2},{2,4},{4,6},{6,0},{1,3},{3,5},{5,7},{7,1},{8,10},{10,12},{12... | collective-permute-start | bytes 98312 | tf_op jit(solution)/shard_map/ppermute | solution.py:449
  107.0 5.1 %collective-permute-start.20 = (bf16[256,128]{1,0:T(8,128)(2,1)S(1)}, bf16[256,128]{1,0:T(8,128)(2,1)S(1)}, u32[]{:S(2)}, u32[]{:S(2)}) collective-permute-start(bf16[256,128]{1,0:T(8,128)(2,1)S(1)} %get-tuple-element.31), channel_id=1, source_target_pairs={{0,1},{1,0},{2,3},{3,2},{4,5},{5,4},{6,7},{7,6},{8,9},{9,8},{10,11... | collective-permute-start | bytes 196616 | tf_op jit(solution)/shard_map/ppermute | solution.py:483
  113.1 4.8 %collective-permute-start.22 = (bf16[32,1024]{1,0:T(8,128)(2,1)S(1)}, bf16[32,1024]{1,0:T(8,128)(2,1)S(1)}, u32[]{:S(2)}, u32[]{:S(2)}) collective-permute-start(bf16[32,1024]{1,0:T(8,128)(2,1)S(1)} %get-tuple-element.34), channel_id=1, source_target_pairs={{0,2},{2,4},{4,6},{6,0},{1,3},{3,5},{5,7},{7,1},{8,10},{10,12},{12... | collective-permute-start | bytes 196616 | tf_op jit(solution)/shard_map/ppermute | solution.py:490
  113.1 6.4 %collective-permute-start.23 = (bf16[32,1024]{1,0:T(8,128)(2,1)S(1)}, bf16[32,1024]{1,0:T(8,128)(2,1)S(1)}, u32[]{:S(2)}, u32[]{:S(2)}) collective-permute-start(bf16[32,1024]{1,0:T(8,128)(2,1)S(1)} %get-tuple-element.35), channel_id=1, source_target_pairs={{0,4},{2,6},{4,0},{6,2},{1,5},{3,7},{5,1},{7,3},{8,12},{10,14},{12... | collective-permute-start | bytes 196616 | tf_op jit(solution)/shard_map/ppermute | solution.py:490
  116.1 3.9 %collective-permute-start.24 = (bf16[32,1024]{1,0:T(8,128)(2,1)S(1)}, bf16[32,1024]{1,0:T(8,128)(2,1)S(1)}, u32[]{:S(2)}, u32[]{:S(2)}) collective-permute-start(bf16[32,1024]{1,0:T(8,128)(2,1)S(1)} %get-tuple-element.36), channel_id=1, source_target_pairs={{0,6},{2,0},{4,2},{6,4},{1,7},{3,1},{5,3},{7,5},{8,14},{10,8},{12,... | collective-permute-start | bytes 196616 | tf_op jit(solution)/shard_map/ppermute | solution.py:490
  (7 other events, 23.0 us)

commit v10 on v9

--- a/solution.py
+++ b/solution.py
@@ -54,6 +54,19 @@
 
 def column(row):
     return jnp.transpose(jnp.broadcast_to(row, (128, 128)))
+
+
+def by_twos(step, count):
+    def both(i, carry):
+        step(2 * i)
+        step(2 * i + 1)
+        return carry
+
+    lax.fori_loop(0, count // 2, both, 0)
+
+    @pl.when(lax.rem(count, 2) == 1)
+    def _():
+        step(count - 1)
 
 
 def frequency(index):
@@ -231,14 +244,14 @@
 
 
 def attend(
-    where, ids, q_ref, uk, uv, key_docs, gains, query_docs, b0, b1, b2, b3,
+    where, q_ref, uk, uv, key_docs, gains, query_docs, b0, b1, b2, b3,
     keep_ref, send_ref, ml_ref, kb, s_buf, v_buf, mx, total, acc,
 ):
     x0, y0, c = where[1], where[2], where[3]
     docs = key_docs[...]
     at = lanes((NS, 128))
-    before = (at == 127) & (docs < ids[0].astype(F32))
-    behind = (at == 0) & (docs > ids[255].astype(F32))
+    before = (at == 127) & (docs < query_docs[0:1, 0:1])
+    behind = (at == 0) & (docs > query_docs[1:2, 127:128])
     low = jnp.sum(before.astype(jnp.int32))
     high = NS - 1 - jnp.sum(behind.astype(jnp.int32))
     count = (high - low) // 2 + 1
@@ -256,7 +269,7 @@
     acc[...] = jnp.zeros(acc.shape, F32)
     wanted = jnp.concatenate([query_docs[0:1, :], query_docs[1:2, :]], axis=1)
 
-    def scores(tile, carry):
+    def scores(tile):
         latents, ropes, same = [], [], []
         for half in range(2):
             block = begin + 2 * tile + half
@@ -299,16 +312,15 @@
             )
             s_buf[tile, h] = got
             mx[h] = jnp.maximum(mx[h], jnp.max(got.reshape(32, 8, 256), axis=0))
-        return carry
-
-    lax.fori_loop(0, count, scores, 0)
+
+    by_twos(scores, count)
     tops = []
     for h in range(4):
         top = jnp.maximum(jnp.max(mx[h], axis=0, keepdims=True), FLOOR)
         mx[h] = jnp.broadcast_to(top, (8, 256))
         tops.append(top)
 
-    def weigh(tile, carry):
+    def weigh(tile):
         for h in range(4):
             own = slice(64 * h, 64 * (h + 1))
             weights = jnp.exp2(s_buf[tile, h].reshape(32, 8, 256) - mx[h][None])
@@ -317,9 +329,8 @@
             acc[own, :] = acc[own, :] + jnp.dot(
                 v_buf[tile, own, :], weights, preferred_element_type=F32
             )
-        return carry
-
-    lax.fori_loop(0, count, weigh, 0)
+
+    by_twos(weigh, count)
     for h in range(4):
         ml_ref[h : h + 1, :] = tops[h]
         ml_ref[4 + h : 5 + h, :] = jnp.sum(total[h], axis=0, keepdims=True)
@@ -469,7 +480,7 @@
             jax.ShapeDtypeStruct((256, 128), BF),
             jax.ShapeDtypeStruct((8, 256), F32),
         ),
-        2, 10, room=34,
+        1, 10, room=34,
         scratch=[
             VMEM((4, 4, NZ, 72, 128), BF),
             VMEM((16, 4, 256, 256), F32),
@@ -478,7 +489,7 @@
             VMEM((4, 8, 256), F32),
             VMEM((256, 256), F32),
         ],
-    )(here, doc_ids, queries, uk, uv, key_docs, gains, query_docs, held, *stage3)
+    )(here, queries, uk, uv, key_docs, gains, query_docs, held, *stage3)
 
     got = lax.ppermute(send, "c", swap)
     ml_got = lax.ppermute(ml, "c", swap)

time: 121 us -> 119 us (0.983)
  Pallas kernels: 17.1 us -> 15.3 us
    pallas_call x1, Pallas kernels: 9.3 us -> 7.44 us  [layer(): call(attend, (jax.ShapeDtypeStruct((256, 128), F32), jax.ShapeDtypeStruct...]
where the time goes in v10:
time: 119 us; the launch traced here: 118 us
  starting transfers between devices  62.4 us (52%)
  waiting for transfers between devices  37.9 us (32%)
  Pallas kernels  15.3 us (13%)
  local copies, waits for them, and re-layouts  1.76 us (1%)
    ppermute x3, waiting for transfers between devices, layer(): lax.ppermute(q_pair, 'y', ring(j))  15.5 us
    ppermute x1, starting transfers between devices, layer(): up_other = lax.ppermute(up_own, 'c', swap)  14.6 us
    all_to_all x1, starting transfers between devices, layer(): gathered = lax.all_to_all(message, 'z', 0, 0)  9.15 us
    pallas_call x1, Pallas kernels, layer(): call(attend, (jax.ShapeDtypeStruct((256, 128), F32), jax.ShapeDtypeStruct...  7.44 us
    all_to_all x1, starting transfers between devices, layer(): up_own = lax.all_to_all(later, 'z', 0, 0)  6.56 us
    ppermute x3, waiting for transfers between devices, layer(): lax.ppermute(stage1, AXES, shift_pairs(2, j))  5.95 us
    ppermute x3, starting transfers between devices, layer(): rows = [tokens] + [lax.ppermute(tokens, 'y', ring(j)) for j in range(1, NY)]  5.74 us
    all_to_all x1, waiting for transfers between devices, layer(): gathered = lax.all_to_all(message, 'z', 0, 0)  4.5 us
  transfers between devices with their start and end apart: 28, of which 17 were waited for; matrix products, arithmetic and copies ran while one was open for 1% of the time, Pallas kernels for 2%

profile of v10, /device:TPU:1, one launch (start us, length us, event | category | flops | bytes accessed | tf_op | source)
XLA Modules:
  0.0 118.2 jit_solution(8995452027782082062)
XLA Ops:
  0.7 2.2 %shard_map.131 = bf16[8,40,128]{2,1,0:T(8,128)(2,1)} custom-call(s32[5]{0:T(128)S(1)} %stack.62.where, bf16[32,256]{1,0:T(8,128)(2,1)} %dq_in.1, bf16[32,256]{1,0:T(8,128)(2,1)} %dk_in.1, bf16[32,32]{1,0:T(8,128)(2,1)} %dr_in.1), custom_call_target="tpu_custom_call" | custom-call | tf_op jit(solution)/shard_map/pallas_call | solution.py:423
  3.0 9.1 %all-to-all-start = ((bf16[8,40,128]{2,1,0:T(8,128)(2,1)}), bf16[8,40,128]{2,1,0:T(8,128)(2,1)S(1)}, u32[]{:S(2)}, u32[]{:S(2)}) async-start(bf16[8,40,128]{2,1,0:T(8,128)(2,1)} %shard_map.131), calls=%async_computation | async-start | bytes 163840 | tf_op jit(solution)/shard_map/all_to_all | solution.py:429
  12.1 3.0 %collective-permute-start.1 = (bf16[32,1024]{1,0:T(8,128)(2,1)S(1)}, bf16[32,1024]{1,0:T(8,128)(2,1)S(1)}, u32[]{:S(2)}, u32[]{:S(2)}) collective-permute-start(bf16[32,1024]{1,0:T(8,128)(2,1)S(1)} %copy-done), channel_id=1, source_target_pairs={{0,4},{2,6},{4,0},{6,2},{1,5},{3,7},{5,1},{7,3},{8,12},{10,14},{12... | collective-permute-start | bytes 196616 | tf_op jit(solution)/shard_map/ppermute | solution.py:432
  15.1 4.5 %all-to-all-done.g0 = bf16[8,40,128]{2,1,0:T(8,128)(2,1)S(1)} async-done(((bf16[8,40,128]{2,1,0:T(8,128)(2,1)}), bf16[8,40,128]{2,1,0:T(8,128)(2,1)S(1)}, u32[]{:S(2)}, u32[]{:S(2)}) %all-to-all-start) | async-done | bytes 81952 | tf_op jit(solution)/shard_map/all_to_all | solution.py:429
  19.6 2.5 %collective-permute-start.5 = (bf16[8,40,128]{2,1,0:T(8,128)(2,1)S(1)}, bf16[8,40,128]{2,1,0:T(8,128)(2,1)S(1)}, u32[]{:S(2)}, u32[]{:S(2)}) collective-permute-start(bf16[8,40,128]{2,1,0:T(8,128)(2,1)S(1)} %all-to-all-done.g0), channel_id=1, source_target_pairs={{0,24},{8,0},{16,8},{24,16},{1,25},{9,1},{17,9},{25,17},{2,26},{10... | collective-permute-start | bytes 245768 | tf_op jit(solution)/shard_map/ppermute | solution.py:430
  26.0 1.6 %collective-permute-done.t1 = bf16[32,1024]{1,0:T(8,128)(2,1)S(1)} collective-permute-done((bf16[32,1024]{1,0:T(8,128)(2,1)S(1)}, bf16[32,1024]{1,0:T(8,128)(2,1)S(1)}, u32[]{:S(2)}, u32[]{:S(2)}) %collective-permute-start) | collective-permute-done | bytes 65568 | tf_op jit(solution)/shard_map/ppermute | solution.py:432
  27.8 1.6 %shard_map.132 = (bf16[64,128]{1,0:T(8,128)(2,1)S(1)}, bf16[8,72,128]{2,1,0:T(8,128)(2,1)}) custom-call(s32[5]{0:T(128)S(1)} %stack.62.where, bf16[32,1024]{1,0:T(8,128)(2,1)S(1)} %copy-done, bf16[32,1024]{1,0:T(8,128)(2,1)S(1)} %collective-permute-done.t1, bf16[32,1024]{1,0:T(8,128)(2,1)S(1)} %collective-permute-done.1.t2, ...), custom_call_target="tpu_custom_call" | custom-call | tf_op jit(solution)/shard_map/pallas_call | solution.py:446
  29.3 3.4 %all-to-all-start.2 = ((bf16[8,72,128]{2,1,0:T(8,128)(2,1)}), bf16[8,72,128]{2,1,0:T(8,128)(2,1)S(1)}, u32[]{:S(2)}, u32[]{:S(2)}) async-start(bf16[8,72,128]{2,1,0:T(8,128)(2,1)} %get-tuple-element.29), calls=%async_computation.2 | async-start | bytes 294912 | tf_op jit(solution)/shard_map/all_to_all | solution.py:452
  33.7 2.3 %collective-permute-start.12 = (bf16[64,128]{1,0:T(8,128)(2,1)S(1)}, bf16[64,128]{1,0:T(8,128)(2,1)S(1)}, u32[]{:S(2)}, u32[]{:S(2)}) collective-permute-start(bf16[64,128]{1,0:T(8,128)(2,1)S(1)} %get-tuple-element.21), channel_id=1, source_target_pairs={{0,24},{8,0},{16,8},{24,16},{1,25},{9,1},{17,9},{25,17},{2,26},{10... | collective-permute-start | bytes 49160 | tf_op jit(solution)/shard_map/ppermute | solution.py:443
  37.3 2.8 %collective-permute-done.11 = bf16[64,128]{1,0:T(8,128)(2,1)S(1)} collective-permute-done((bf16[64,128]{1,0:T(8,128)(2,1)S(1)}, bf16[64,128]{1,0:T(8,128)(2,1)S(1)}, u32[]{:S(2)}, u32[]{:S(2)}) %collective-permute-start.11) | collective-permute-done | bytes 16416 | tf_op jit(solution)/shard_map/ppermute | solution.py:443
  42.0 6.6 %all-to-all-start.1 = ((bf16[8,4,64,128]{3,2,1,0:T(8,128)(2,1)}), bf16[8,4,64,128]{3,2,1,0:T(8,128)(2,1)S(1)}, u32[]{:S(2)}, u32[]{:S(2)}) async-start(bf16[8,4,64,128]{3,2,1,0:T(8,128)(2,1)} %broadcast_in_dim.2), calls=%async_computation.1 | async-start | bytes 1048576 | tf_op jit(solution)/shard_map/all_to_all | solution.py:457
  48.6 2.4 %collective-permute-start.16 = (bf16[8,72,128]{2,1,0:T(8,128)(2,1)S(1)}, bf16[8,72,128]{2,1,0:T(8,128)(2,1)S(1)}, u32[]{:S(2)}, u32[]{:S(2)}) collective-permute-start(bf16[8,72,128]{2,1,0:T(8,128)(2,1)S(1)} %all-to-all-done.2), channel_id=1, source_target_pairs={{0,24},{1,7},{2,26},{3,1},{4,28},{5,3},{6,30},{7,5},{8,0},{9,15},{... | collective-permute-start | bytes 442376 | tf_op jit(solution)/shard_map/ppermute | solution.py:453
  52.1 2.5 %collective-permute-done.16 = bf16[8,72,128]{2,1,0:T(8,128)(2,1)S(1)} collective-permute-done((bf16[8,72,128]{2,1,0:T(8,128)(2,1)S(1)}, bf16[8,72,128]{2,1,0:T(8,128)(2,1)S(1)}, u32[]{:S(2)}, u32[]{:S(2)}) %collective-permute-start.16) | collective-permute-done | bytes 147488 | tf_op jit(solution)/shard_map/ppermute | solution.py:453
  54.6 1.9 %collective-permute-done.15 = bf16[8,72,128]{2,1,0:T(8,128)(2,1)S(1)} collective-permute-done((bf16[8,72,128]{2,1,0:T(8,128)(2,1)S(1)}, bf16[8,72,128]{2,1,0:T(8,128)(2,1)S(1)}, u32[]{:S(2)}, u32[]{:S(2)}) %collective-permute-start.15) | collective-permute-done | bytes 147488 | tf_op jit(solution)/shard_map/ppermute | solution.py:453
  60.8 14.6 %collective-permute-start.13 = (bf16[8,4,64,128]{3,2,1,0:T(8,128)(2,1)S(1)}, bf16[8,4,64,128]{3,2,1,0:T(8,128)(2,1)S(1)}, u32[]{:S(2)}, u32[]{:S(2)}) collective-permute-start(bf16[8,4,64,128]{3,2,1,0:T(8,128)(2,1)S(1)} %all-to-all-done.1.up_own.w_own), channel_id=1, source_target_pairs={{0,1},{1,0},{2,3},{3,2},{4,5},{5,4},{6,7},{7,6},{8,9},{9,8},{10,11... | collective-permute-start | bytes 1572872 | tf_op jit(solution)/shard_map/ppermute | solution.py:458
  75.5 1.6 %collective-permute-done.6 = bf16[64,128]{1,0:T(8,128)(2,1)S(1)} collective-permute-done((bf16[64,128]{1,0:T(8,128)(2,1)S(1)}, bf16[64,128]{1,0:T(8,128)(2,1)S(1)}, u32[]{:S(2)}, u32[]{:S(2)}) %collective-permute-start.6) | collective-permute-done | bytes 16416 | tf_op jit(solution)/shard_map/ppermute | solution.py:459
  77.1 2.3 %collective-permute-start.9 = (bf16[2,64,128]{2,1,0:T(8,128)(2,1)S(1)}, bf16[2,64,128]{2,1,0:T(8,128)(2,1)S(1)}, u32[]{:S(2)}, u32[]{:S(2)}) collective-permute-start(bf16[2,64,128]{2,1,0:T(8,128)(2,1)S(1)} %pad_maximum_fusion.2.q0), channel_id=1, source_target_pairs={{0,6},{2,0},{4,2},{6,4},{1,7},{3,1},{5,3},{7,5},{8,14},{10,8},{12,... | collective-permute-start | bytes 98312 | tf_op jit(solution)/shard_map/ppermute | solution.py:460
  79.4 7.2 %collective-permute-done.9.q3 = bf16[2,64,128]{2,1,0:T(8,128)(2,1)S(1)} collective-permute-done((bf16[2,64,128]{2,1,0:T(8,128)(2,1)S(1)}, bf16[2,64,128]{2,1,0:T(8,128)(2,1)S(1)}, u32[]{:S(2)}, u32[]{:S(2)}) %collective-permute-start.9) | collective-permute-done | bytes 32800 | tf_op jit(solution)/shard_map/ppermute | solution.py:460
  86.5 4.6 %collective-permute-done.8.q2 = bf16[2,64,128]{2,1,0:T(8,128)(2,1)S(1)} collective-permute-done((bf16[2,64,128]{2,1,0:T(8,128)(2,1)S(1)}, bf16[2,64,128]{2,1,0:T(8,128)(2,1)S(1)}, u32[]{:S(2)}, u32[]{:S(2)}) %collective-permute-start.8) | collective-permute-done | bytes 32800 | tf_op jit(solution)/shard_map/ppermute | solution.py:460
  91.9 3.7 %collective-permute-done.7.q1 = bf16[2,64,128]{2,1,0:T(8,128)(2,1)S(1)} collective-permute-done((bf16[2,64,128]{2,1,0:T(8,128)(2,1)S(1)}, bf16[2,64,128]{2,1,0:T(8,128)(2,1)S(1)}, u32[]{:S(2)}, u32[]{:S(2)}) %collective-permute-start.7) | collective-permute-done | bytes 32800 | tf_op jit(solution)/shard_map/ppermute | solution.py:460
  97.0 7.4 %shard_map.135 = (f32[256,128]{1,0:T(8,128)S(1)}, bf16[256,128]{1,0:T(8,128)(2,1)S(1)}, f32[8,256]{1,0:T(8,128)S(1)}) custom-call(s32[5]{0:T(128)S(1)} %stack.62.where, bf16[4,256,256]{2,1,0:T(8,128)(2,1)S(1)} %get-tuple-element.23.q_ref, bf16[256,256]{1,0:T(8,128)(2,1)S(1)} %get-tuple-element.24.uk, bf16[256,256]{1,0:T(8,128)(2,1)S(1)} %get-tuple-element.25.uv, ...), custom_call_target="tpu_custom_call" | custom-call | tf_op jit(solution)/shard_map/pallas_call | solution.py:476
  104.4 4.0 %collective-permute-start.20 = (bf16[256,128]{1,0:T(8,128)(2,1)S(1)}, bf16[256,128]{1,0:T(8,128)(2,1)S(1)}, u32[]{:S(2)}, u32[]{:S(2)}) collective-permute-start(bf16[256,128]{1,0:T(8,128)(2,1)S(1)} %get-tuple-element.31), channel_id=1, source_target_pairs={{0,1},{1,0},{2,3},{3,2},{4,5},{5,4},{6,7},{7,6},{8,9},{9,8},{10,11... | collective-permute-start | bytes 196616 | tf_op jit(solution)/shard_map/ppermute | solution.py:494
  110.6 2.9 %collective-permute-start.23 = (bf16[32,1024]{1,0:T(8,128)(2,1)S(1)}, bf16[32,1024]{1,0:T(8,128)(2,1)S(1)}, u32[]{:S(2)}, u32[]{:S(2)}) collective-permute-start(bf16[32,1024]{1,0:T(8,128)(2,1)S(1)} %get-tuple-element.35), channel_id=1, source_target_pairs={{0,4},{2,6},{4,0},{6,2},{1,5},{3,7},{5,1},{7,3},{8,12},{10,14},{12... | collective-permute-start | bytes 196616 | tf_op jit(solution)/shard_map/ppermute | solution.py:501
  115.3 1.7 %collective-permute-done.23.p2 = bf16[32,1024]{1,0:T(8,128)(2,1)S(1)} collective-permute-done((bf16[32,1024]{1,0:T(8,128)(2,1)S(1)}, bf16[32,1024]{1,0:T(8,128)(2,1)S(1)}, u32[]{:S(2)}, u32[]{:S(2)}) %collective-permute-start.23) | collective-permute-done | bytes 65568 | tf_op jit(solution)/shard_map/ppermute | solution.py:501
  (51 shorter events, 21.0 us)
Async XLA Ops:
  3.0 16.7 %all-to-all-start = ((bf16[8,40,128]{2,1,0:T(8,128)(2,1)}), bf16[8,40,128]{2,1,0:T(8,128)(2,1)S(1)}, u32[]{:S(2)}, u32[]{:S(2)}) async-start(bf16[8,40,128]{2,1,0:T(8,128)(2,1)} %shard_map.131), calls=%async_computation | async-start | bytes 163840 | tf_op jit(solution)/shard_map/all_to_all | solution.py:429
  12.1 12.4 %collective-permute-start.1 = (bf16[32,1024]{1,0:T(8,128)(2,1)S(1)}, bf16[32,1024]{1,0:T(8,128)(2,1)S(1)}, u32[]{:S(2)}, u32[]{:S(2)}) collective-permute-start(bf16[32,1024]{1,0:T(8,128)(2,1)S(1)} %copy-done), channel_id=1, source_target_pairs={{0,4},{2,6},{4,0},{6,2},{1,5},{3,7},{5,1},{7,3},{8,12},{10,14},{12... | collective-permute-start | bytes 196616 | tf_op jit(solution)/shard_map/ppermute | solution.py:432
  19.6 8.0 %collective-permute-start.5 = (bf16[8,40,128]{2,1,0:T(8,128)(2,1)S(1)}, bf16[8,40,128]{2,1,0:T(8,128)(2,1)S(1)}, u32[]{:S(2)}, u32[]{:S(2)}) collective-permute-start(bf16[8,40,128]{2,1,0:T(8,128)(2,1)S(1)} %all-to-all-done.g0), channel_id=1, source_target_pairs={{0,24},{8,0},{16,8},{24,16},{1,25},{9,1},{17,9},{25,17},{2,26},{10... | collective-permute-start | bytes 245768 | tf_op jit(solution)/shard_map/ppermute | solution.py:430
  22.1 5.5 %collective-permute-start.4 = (bf16[8,40,128]{2,1,0:T(8,128)(2,1)S(1)}, bf16[8,40,128]{2,1,0:T(8,128)(2,1)S(1)}, u32[]{:S(2)}, u32[]{:S(2)}) collective-permute-start(bf16[8,40,128]{2,1,0:T(8,128)(2,1)S(1)} %all-to-all-done.g0), channel_id=1, source_target_pairs={{0,16},{8,24},{16,0},{24,8},{1,17},{9,25},{17,1},{25,9},{2,18},{10... | collective-permute-start | bytes 245768 | tf_op jit(solution)/shard_map/ppermute | solution.py:430
  22.6 5.2 %collective-permute-start.3 = (bf16[8,40,128]{2,1,0:T(8,128)(2,1)S(1)}, bf16[8,40,128]{2,1,0:T(8,128)(2,1)S(1)}, u32[]{:S(2)}, u32[]{:S(2)}) collective-permute-start(bf16[8,40,128]{2,1,0:T(8,128)(2,1)S(1)} %all-to-all-done.g0), channel_id=1, source_target_pairs={{0,8},{8,16},{16,24},{24,0},{1,9},{9,17},{17,25},{25,1},{2,10},{10... | collective-permute-start | bytes 245768 | tf_op jit(solution)/shard_map/ppermute | solution.py:430
  23.2 4.4 %collective-permute-start = (bf16[32,1024]{1,0:T(8,128)(2,1)S(1)}, bf16[32,1024]{1,0:T(8,128)(2,1)S(1)}, u32[]{:S(2)}, u32[]{:S(2)}) collective-permute-start(bf16[32,1024]{1,0:T(8,128)(2,1)S(1)} %copy-done), channel_id=1, source_target_pairs={{0,2},{2,4},{4,6},{6,0},{1,3},{3,5},{5,7},{7,1},{8,10},{10,12},{12... | collective-permute-start | bytes 196616 | tf_op jit(solution)/shard_map/ppermute | solution.py:432
  29.3 11.8 %all-to-all-start.2 = ((bf16[8,72,128]{2,1,0:T(8,128)(2,1)}), bf16[8,72,128]{2,1,0:T(8,128)(2,1)S(1)}, u32[]{:S(2)}, u32[]{:S(2)}) async-start(bf16[8,72,128]{2,1,0:T(8,128)(2,1)} %get-tuple-element.29), calls=%async_computation.2 | async-start | bytes 294912 | tf_op jit(solution)/shard_map/all_to_all | solution.py:452
  36.1 4.1 %collective-permute-start.11 = (bf16[64,128]{1,0:T(8,128)(2,1)S(1)}, bf16[64,128]{1,0:T(8,128)(2,1)S(1)}, u32[]{:S(2)}, u32[]{:S(2)}) collective-permute-start(bf16[64,128]{1,0:T(8,128)(2,1)S(1)} %get-tuple-element.21), channel_id=1, source_target_pairs={{0,16},{8,24},{16,0},{24,8},{1,17},{9,25},{17,1},{25,9},{2,18},{10... | collective-permute-start | bytes 49160 | tf_op jit(solution)/shard_map/ppermute | solution.py:443
  37.3 3.8 %collective-permute-start.10 = (bf16[64,128]{1,0:T(8,128)(2,1)S(1)}, bf16[64,128]{1,0:T(8,128)(2,1)S(1)}, u32[]{:S(2)}, u32[]{:S(2)}) collective-permute-start(bf16[64,128]{1,0:T(8,128)(2,1)S(1)} %get-tuple-element.21), channel_id=1, source_target_pairs={{0,8},{8,16},{16,24},{24,0},{1,9},{9,17},{17,25},{25,1},{2,10},{10... | collective-permute-start | bytes 49160 | tf_op jit(solution)/shard_map/ppermute | solution.py:443
  42.0 18.8 %all-to-all-start.1 = ((bf16[8,4,64,128]{3,2,1,0:T(8,128)(2,1)}), bf16[8,4,64,128]{3,2,1,0:T(8,128)(2,1)S(1)}, u32[]{:S(2)}, u32[]{:S(2)}) async-start(bf16[8,4,64,128]{3,2,1,0:T(8,128)(2,1)} %broadcast_in_dim.2), calls=%async_computation.1 | async-start | bytes 1048576 | tf_op jit(solution)/shard_map/all_to_all | solution.py:457
  48.6 6.0 %collective-permute-start.16 = (bf16[8,72,128]{2,1,0:T(8,128)(2,1)S(1)}, bf16[8,72,128]{2,1,0:T(8,128)(2,1)S(1)}, u32[]{:S(2)}, u32[]{:S(2)}) collective-permute-start(bf16[8,72,128]{2,1,0:T(8,128)(2,1)S(1)} %all-to-all-done.2), channel_id=1, source_target_pairs={{0,24},{1,7},{2,26},{3,1},{4,28},{5,3},{6,30},{7,5},{8,0},{9,15},{... | collective-permute-start | bytes 442376 | tf_op jit(solution)/shard_map/ppermute | solution.py:453
  51.0 5.6 %collective-permute-start.15 = (bf16[8,72,128]{2,1,0:T(8,128)(2,1)S(1)}, bf16[8,72,128]{2,1,0:T(8,128)(2,1)S(1)}, u32[]{:S(2)}, u32[]{:S(2)}) collective-permute-start(bf16[8,72,128]{2,1,0:T(8,128)(2,1)S(1)} %all-to-all-done.2), channel_id=1, source_target_pairs={{0,16},{1,5},{2,18},{3,7},{4,20},{5,1},{6,22},{7,3},{8,24},{9,13},... | collective-permute-start | bytes 442376 | tf_op jit(solution)/shard_map/ppermute | solution.py:453
  51.7 6.3 %collective-permute-start.14 = (bf16[8,72,128]{2,1,0:T(8,128)(2,1)S(1)}, bf16[8,72,128]{2,1,0:T(8,128)(2,1)S(1)}, u32[]{:S(2)}, u32[]{:S(2)}) collective-permute-start(bf16[8,72,128]{2,1,0:T(8,128)(2,1)S(1)} %all-to-all-done.2), channel_id=1, source_target_pairs={{0,8},{1,3},{2,10},{3,5},{4,12},{5,7},{6,14},{7,1},{8,16},{9,11},{... | collective-permute-start | bytes 442376 | tf_op jit(solution)/shard_map/ppermute | solution.py:453
  58.1 38.8 %collective-permute-start.19 = (bf16[4,8,72,128]{3,2,1,0:T(8,128)(2,1)S(1)}, bf16[4,8,72,128]{3,2,1,0:T(8,128)(2,1)S(1)}, u32[]{:S(2)}, u32[]{:S(2)}) collective-permute-start(bf16[4,8,72,128]{3,2,1,0:T(8,128)(2,1)S(1)} %pad_maximum_fusion.b0), channel_id=1, source_target_pairs={{0,6},{1,25},{2,0},{3,27},{4,2},{5,29},{6,4},{7,31},{8,14},{9,1},{... | collective-permute-start | bytes 1769480 | tf_op jit(solution)/shard_map/ppermute | solution.py:455
  58.3 38.7 %collective-permute-start.18 = (bf16[4,8,72,128]{3,2,1,0:T(8,128)(2,1)S(1)}, bf16[4,8,72,128]{3,2,1,0:T(8,128)(2,1)S(1)}, u32[]{:S(2)}, u32[]{:S(2)}) collective-permute-start(bf16[4,8,72,128]{3,2,1,0:T(8,128)(2,1)S(1)} %pad_maximum_fusion.b0), channel_id=1, source_target_pairs={{0,4},{1,17},{2,6},{3,19},{4,0},{5,21},{6,2},{7,23},{8,12},{9,25},... | collective-permute-start | bytes 1769480 | tf_op jit(solution)/shard_map/ppermute | solution.py:455
  59.4 37.6 %collective-permute-start.17 = (bf16[4,8,72,128]{3,2,1,0:T(8,128)(2,1)S(1)}, bf16[4,8,72,128]{3,2,1,0:T(8,128)(2,1)S(1)}, u32[]{:S(2)}, u32[]{:S(2)}) collective-permute-start(bf16[4,8,72,128]{3,2,1,0:T(8,128)(2,1)S(1)} %pad_maximum_fusion.b0), channel_id=1, source_target_pairs={{0,2},{1,9},{2,4},{3,11},{4,6},{5,13},{6,0},{7,15},{8,10},{9,17},{... | collective-permute-start | bytes 1769480 | tf_op jit(solution)/shard_map/ppermute | solution.py:455
  60.8 34.8 %collective-permute-start.13 = (bf16[8,4,64,128]{3,2,1,0:T(8,128)(2,1)S(1)}, bf16[8,4,64,128]{3,2,1,0:T(8,128)(2,1)S(1)}, u32[]{:S(2)}, u32[]{:S(2)}) collective-permute-start(bf16[8,4,64,128]{3,2,1,0:T(8,128)(2,1)S(1)} %all-to-all-done.1.up_own.w_own), channel_id=1, source_target_pairs={{0,1},{1,0},{2,3},{3,2},{4,5},{5,4},{6,7},{7,6},{8,9},{9,8},{10,11... | collective-permute-start | bytes 1572872 | tf_op jit(solution)/shard_map/ppermute | solution.py:458
  77.1 9.4 %collective-permute-start.9 = (bf16[2,64,128]{2,1,0:T(8,128)(2,1)S(1)}, bf16[2,64,128]{2,1,0:T(8,128)(2,1)S(1)}, u32[]{:S(2)}, u32[]{:S(2)}) collective-permute-start(bf16[2,64,128]{2,1,0:T(8,128)(2,1)S(1)} %pad_maximum_fusion.2.q0), channel_id=1, source_target_pairs={{0,6},{2,0},{4,2},{6,4},{1,7},{3,1},{5,3},{7,5},{8,14},{10,8},{12,... | collective-permute-start | bytes 98312 | tf_op jit(solution)/shard_map/ppermute | solution.py:460
  86.5 4.6 %collective-permute-start.8 = (bf16[2,64,128]{2,1,0:T(8,128)(2,1)S(1)}, bf16[2,64,128]{2,1,0:T(8,128)(2,1)S(1)}, u32[]{:S(2)}, u32[]{:S(2)}) collective-permute-start(bf16[2,64,128]{2,1,0:T(8,128)(2,1)S(1)} %pad_maximum_fusion.2.q0), channel_id=1, source_target_pairs={{0,4},{2,6},{4,0},{6,2},{1,5},{3,7},{5,1},{7,3},{8,12},{10,14},{12... | collective-permute-start | bytes 98312 | tf_op jit(solution)/shard_map/ppermute | solution.py:460
  91.1 4.5 %collective-permute-start.7 = (bf16[2,64,128]{2,1,0:T(8,128)(2,1)S(1)}, bf16[2,64,128]{2,1,0:T(8,128)(2,1)S(1)}, u32[]{:S(2)}, u32[]{:S(2)}) collective-permute-start(bf16[2,64,128]{2,1,0:T(8,128)(2,1)S(1)} %pad_maximum_fusion.2.q0), channel_id=1, source_target_pairs={{0,2},{2,4},{4,6},{6,0},{1,3},{3,5},{5,7},{7,1},{8,10},{10,12},{12... | collective-permute-start | bytes 98312 | tf_op jit(solution)/shard_map/ppermute | solution.py:460
  104.4 5.1 %collective-permute-start.20 = (bf16[256,128]{1,0:T(8,128)(2,1)S(1)}, bf16[256,128]{1,0:T(8,128)(2,1)S(1)}, u32[]{:S(2)}, u32[]{:S(2)}) collective-permute-start(bf16[256,128]{1,0:T(8,128)(2,1)S(1)} %get-tuple-element.31), channel_id=1, source_target_pairs={{0,1},{1,0},{2,3},{3,2},{4,5},{5,4},{6,7},{7,6},{8,9},{9,8},{10,11... | collective-permute-start | bytes 196616 | tf_op jit(solution)/shard_map/ppermute | solution.py:494
  110.5 4.8 %collective-permute-start.22 = (bf16[32,1024]{1,0:T(8,128)(2,1)S(1)}, bf16[32,1024]{1,0:T(8,128)(2,1)S(1)}, u32[]{:S(2)}, u32[]{:S(2)}) collective-permute-start(bf16[32,1024]{1,0:T(8,128)(2,1)S(1)} %get-tuple-element.34), channel_id=1, source_target_pairs={{0,2},{2,4},{4,6},{6,0},{1,3},{3,5},{5,7},{7,1},{8,10},{10,12},{12... | collective-permute-start | bytes 196616 | tf_op jit(solution)/shard_map/ppermute | solution.py:501
  110.6 6.3 %collective-permute-start.23 = (bf16[32,1024]{1,0:T(8,128)(2,1)S(1)}, bf16[32,1024]{1,0:T(8,128)(2,1)S(1)}, u32[]{:S(2)}, u32[]{:S(2)}) collective-permute-start(bf16[32,1024]{1,0:T(8,128)(2,1)S(1)} %get-tuple-element.35), channel_id=1, source_target_pairs={{0,4},{2,6},{4,0},{6,2},{1,5},{3,7},{5,1},{7,3},{8,12},{10,14},{12... | collective-permute-start | bytes 196616 | tf_op jit(solution)/shard_map/ppermute | solution.py:501
  113.5 3.9 %collective-permute-start.24 = (bf16[32,1024]{1,0:T(8,128)(2,1)S(1)}, bf16[32,1024]{1,0:T(8,128)(2,1)S(1)}, u32[]{:S(2)}, u32[]{:S(2)}) collective-permute-start(bf16[32,1024]{1,0:T(8,128)(2,1)S(1)} %get-tuple-element.36), channel_id=1, source_target_pairs={{0,6},{2,0},{4,2},{6,4},{1,7},{3,1},{5,3},{7,5},{8,14},{10,8},{12,... | collective-permute-start | bytes 196616 | tf_op jit(solution)/shard_map/ppermute | solution.py:501
  (6 other events, 22.3 us)

commit v11 on v10

--- a/solution.py
+++ b/solution.py
@@ -56,13 +56,19 @@
     return jnp.transpose(jnp.broadcast_to(row, (128, 128)))
 
 
-def by_twos(step, count):
-    def both(i, carry):
-        step(2 * i)
-        step(2 * i + 1)
+def by_fours(step, count):
+    def four(i, carry):
+        for k in range(4):
+            step(4 * i + k)
         return carry
 
-    lax.fori_loop(0, count // 2, both, 0)
+    lax.fori_loop(0, count // 4, four, 0)
+    done = count // 4 * 4
+
+    @pl.when(lax.rem(count, 4) >= 2)
+    def _():
+        step(done)
+        step(done + 1)
 
     @pl.when(lax.rem(count, 2) == 1)
     def _():
@@ -313,7 +319,7 @@
             s_buf[tile, h] = got
             mx[h] = jnp.maximum(mx[h], jnp.max(got.reshape(32, 8, 256), axis=0))
 
-    by_twos(scores, count)
+    by_fours(scores, count)
     tops = []
     for h in range(4):
         top = jnp.maximum(jnp.max(mx[h], axis=0, keepdims=True), FLOOR)
@@ -330,7 +336,7 @@
                 v_buf[tile, own, :], weights, preferred_element_type=F32
             )
 
-    by_twos(weigh, count)
+    by_fours(weigh, count)
     for h in range(4):
         ml_ref[h : h + 1, :] = tops[h]
         ml_ref[4 + h : 5 + h, :] = jnp.sum(total[h], axis=0, keepdims=True)

time: 119 us -> 118 us (level)
  no operation moved by 1% of the time
where the time goes in v11:
time: 118 us; the launch traced here: 117 us
  starting transfers between devices  62.4 us (53%)
  waiting for transfers between devices  37.9 us (32%)
  Pallas kernels  14.5 us (12%)
  local copies, waits for them, and re-layouts  1.76 us (1%)
    ppermute x3, waiting for transfers between devices, layer(): lax.ppermute(q_pair, 'y', ring(j))  15.5 us
    ppermute x1, starting transfers between devices, layer(): up_other = lax.ppermute(up_own, 'c', swap)  14.6 us
    all_to_all x1, starting transfers between devices, layer(): gathered = lax.all_to_all(message, 'z', 0, 0)  9.15 us
    pallas_call x1, Pallas kernels, layer(): call(attend, (jax.ShapeDtypeStruct((256, 128), F32), jax.ShapeDtypeStruct...  6.68 us
    all_to_all x1, starting transfers between devices, layer(): up_own = lax.all_to_all(later, 'z', 0, 0)  6.56 us
    ppermute x3, waiting for transfers between devices, layer(): lax.ppermute(stage1, AXES, shift_pairs(2, j))  5.95 us
    ppermute x3, starting transfers between devices, layer(): rows = [tokens] + [lax.ppermute(tokens, 'y', ring(j)) for j in range(1, NY)]  5.74 us
    all_to_all x1, waiting for transfers between devices, layer(): gathered = lax.all_to_all(message, 'z', 0, 0)  4.5 us
  transfers between devices with their start and end apart: 28, of which 17 were waited for; matrix products, arithmetic and copies ran while one was open for 1% of the time, Pallas kernels for 2%

profile of v11, /device:TPU:1, one launch (start us, length us, event | category | flops | bytes accessed | tf_op | source)
XLA Modules:
  0.0 117.4 jit_solution(16087712438192257079)
XLA Ops:
  0.7 2.2 %shard_map.131 = bf16[8,40,128]{2,1,0:T(8,128)(2,1)} custom-call(s32[5]{0:T(128)S(1)} %stack.62.where, bf16[32,256]{1,0:T(8,128)(2,1)} %dq_in.1, bf16[32,256]{1,0:T(8,128)(2,1)} %dk_in.1, bf16[32,32]{1,0:T(8,128)(2,1)} %dr_in.1), custom_call_target="tpu_custom_call" | custom-call | tf_op jit(solution)/shard_map/pallas_call | solution.py:429
  3.0 9.1 %all-to-all-start = ((bf16[8,40,128]{2,1,0:T(8,128)(2,1)}), bf16[8,40,128]{2,1,0:T(8,128)(2,1)S(1)}, u32[]{:S(2)}, u32[]{:S(2)}) async-start(bf16[8,40,128]{2,1,0:T(8,128)(2,1)} %shard_map.131), calls=%async_computation | async-start | bytes 163840 | tf_op jit(solution)/shard_map/all_to_all | solution.py:435
  12.1 3.0 %collective-permute-start.1 = (bf16[32,1024]{1,0:T(8,128)(2,1)S(1)}, bf16[32,1024]{1,0:T(8,128)(2,1)S(1)}, u32[]{:S(2)}, u32[]{:S(2)}) collective-permute-start(bf16[32,1024]{1,0:T(8,128)(2,1)S(1)} %copy-done), channel_id=1, source_target_pairs={{0,4},{2,6},{4,0},{6,2},{1,5},{3,7},{5,1},{7,3},{8,12},{10,14},{12... | collective-permute-start | bytes 196616 | tf_op jit(solution)/shard_map/ppermute | solution.py:438
  15.1 4.5 %all-to-all-done.g0 = bf16[8,40,128]{2,1,0:T(8,128)(2,1)S(1)} async-done(((bf16[8,40,128]{2,1,0:T(8,128)(2,1)}), bf16[8,40,128]{2,1,0:T(8,128)(2,1)S(1)}, u32[]{:S(2)}, u32[]{:S(2)}) %all-to-all-start) | async-done | bytes 81952 | tf_op jit(solution)/shard_map/all_to_all | solution.py:435
  19.6 2.5 %collective-permute-start.5 = (bf16[8,40,128]{2,1,0:T(8,128)(2,1)S(1)}, bf16[8,40,128]{2,1,0:T(8,128)(2,1)S(1)}, u32[]{:S(2)}, u32[]{:S(2)}) collective-permute-start(bf16[8,40,128]{2,1,0:T(8,128)(2,1)S(1)} %all-to-all-done.g0), channel_id=1, source_target_pairs={{0,24},{8,0},{16,8},{24,16},{1,25},{9,1},{17,9},{25,17},{2,26},{10... | collective-permute-start | bytes 245768 | tf_op jit(solution)/shard_map/ppermute | solution.py:436
  26.0 1.6 %collective-permute-done.t1 = bf16[32,1024]{1,0:T(8,128)(2,1)S(1)} collective-permute-done((bf16[32,1024]{1,0:T(8,128)(2,1)S(1)}, bf16[32,1024]{1,0:T(8,128)(2,1)S(1)}, u32[]{:S(2)}, u32[]{:S(2)}) %collective-permute-start) | collective-permute-done | bytes 65568 | tf_op jit(solution)/shard_map/ppermute | solution.py:438
  27.8 1.6 %shard_map.132 = (bf16[64,128]{1,0:T(8,128)(2,1)S(1)}, bf16[8,72,128]{2,1,0:T(8,128)(2,1)}) custom-call(s32[5]{0:T(128)S(1)} %stack.62.where, bf16[32,1024]{1,0:T(8,128)(2,1)S(1)} %copy-done, bf16[32,1024]{1,0:T(8,128)(2,1)S(1)} %collective-permute-done.t1, bf16[32,1024]{1,0:T(8,128)(2,1)S(1)} %collective-permute-done.1.t2, ...), custom_call_target="tpu_custom_call" | custom-call | tf_op jit(solution)/shard_map/pallas_call | solution.py:452
  29.3 3.4 %all-to-all-start.2 = ((bf16[8,72,128]{2,1,0:T(8,128)(2,1)}), bf16[8,72,128]{2,1,0:T(8,128)(2,1)S(1)}, u32[]{:S(2)}, u32[]{:S(2)}) async-start(bf16[8,72,128]{2,1,0:T(8,128)(2,1)} %get-tuple-element.29), calls=%async_computation.2 | async-start | bytes 294912 | tf_op jit(solution)/shard_map/all_to_all | solution.py:458
  33.7 2.3 %collective-permute-start.12 = (bf16[64,128]{1,0:T(8,128)(2,1)S(1)}, bf16[64,128]{1,0:T(8,128)(2,1)S(1)}, u32[]{:S(2)}, u32[]{:S(2)}) collective-permute-start(bf16[64,128]{1,0:T(8,128)(2,1)S(1)} %get-tuple-element.21), channel_id=1, source_target_pairs={{0,24},{8,0},{16,8},{24,16},{1,25},{9,1},{17,9},{25,17},{2,26},{10... | collective-permute-start | bytes 49160 | tf_op jit(solution)/shard_map/ppermute | solution.py:449
  37.3 2.8 %collective-permute-done.11 = bf16[64,128]{1,0:T(8,128)(2,1)S(1)} collective-permute-done((bf16[64,128]{1,0:T(8,128)(2,1)S(1)}, bf16[64,128]{1,0:T(8,128)(2,1)S(1)}, u32[]{:S(2)}, u32[]{:S(2)}) %collective-permute-start.11) | collective-permute-done | bytes 16416 | tf_op jit(solution)/shard_map/ppermute | solution.py:449
  42.0 6.6 %all-to-all-start.1 = ((bf16[8,4,64,128]{3,2,1,0:T(8,128)(2,1)}), bf16[8,4,64,128]{3,2,1,0:T(8,128)(2,1)S(1)}, u32[]{:S(2)}, u32[]{:S(2)}) async-start(bf16[8,4,64,128]{3,2,1,0:T(8,128)(2,1)} %broadcast_in_dim.2), calls=%async_computation.1 | async-start | bytes 1048576 | tf_op jit(solution)/shard_map/all_to_all | solution.py:463
  48.6 2.4 %collective-permute-start.16 = (bf16[8,72,128]{2,1,0:T(8,128)(2,1)S(1)}, bf16[8,72,128]{2,1,0:T(8,128)(2,1)S(1)}, u32[]{:S(2)}, u32[]{:S(2)}) collective-permute-start(bf16[8,72,128]{2,1,0:T(8,128)(2,1)S(1)} %all-to-all-done.2), channel_id=1, source_target_pairs={{0,24},{1,7},{2,26},{3,1},{4,28},{5,3},{6,30},{7,5},{8,0},{9,15},{... | collective-permute-start | bytes 442376 | tf_op jit(solution)/shard_map/ppermute | solution.py:459
  52.1 2.5 %collective-permute-done.16 = bf16[8,72,128]{2,1,0:T(8,128)(2,1)S(1)} collective-permute-done((bf16[8,72,128]{2,1,0:T(8,128)(2,1)S(1)}, bf16[8,72,128]{2,1,0:T(8,128)(2,1)S(1)}, u32[]{:S(2)}, u32[]{:S(2)}) %collective-permute-start.16) | collective-permute-done | bytes 147488 | tf_op jit(solution)/shard_map/ppermute | solution.py:459
  54.6 1.9 %collective-permute-done.15 = bf16[8,72,128]{2,1,0:T(8,128)(2,1)S(1)} collective-permute-done((bf16[8,72,128]{2,1,0:T(8,128)(2,1)S(1)}, bf16[8,72,128]{2,1,0:T(8,128)(2,1)S(1)}, u32[]{:S(2)}, u32[]{:S(2)}) %collective-permute-start.15) | collective-permute-done | bytes 147488 | tf_op jit(solution)/shard_map/ppermute | solution.py:459
  60.8 14.6 %collective-permute-start.13 = (bf16[8,4,64,128]{3,2,1,0:T(8,128)(2,1)S(1)}, bf16[8,4,64,128]{3,2,1,0:T(8,128)(2,1)S(1)}, u32[]{:S(2)}, u32[]{:S(2)}) collective-permute-start(bf16[8,4,64,128]{3,2,1,0:T(8,128)(2,1)S(1)} %all-to-all-done.1.up_own.w_own), channel_id=1, source_target_pairs={{0,1},{1,0},{2,3},{3,2},{4,5},{5,4},{6,7},{7,6},{8,9},{9,8},{10,11... | collective-permute-start | bytes 1572872 | tf_op jit(solution)/shard_map/ppermute | solution.py:464
  75.5 1.6 %collective-permute-done.6 = bf16[64,128]{1,0:T(8,128)(2,1)S(1)} collective-permute-done((bf16[64,128]{1,0:T(8,128)(2,1)S(1)}, bf16[64,128]{1,0:T(8,128)(2,1)S(1)}, u32[]{:S(2)}, u32[]{:S(2)}) %collective-permute-start.6) | collective-permute-done | bytes 16416 | tf_op jit(solution)/shard_map/ppermute | solution.py:465
  77.1 2.3 %collective-permute-start.9 = (bf16[2,64,128]{2,1,0:T(8,128)(2,1)S(1)}, bf16[2,64,128]{2,1,0:T(8,128)(2,1)S(1)}, u32[]{:S(2)}, u32[]{:S(2)}) collective-permute-start(bf16[2,64,128]{2,1,0:T(8,128)(2,1)S(1)} %pad_maximum_fusion.2.q0), channel_id=1, source_target_pairs={{0,6},{2,0},{4,2},{6,4},{1,7},{3,1},{5,3},{7,5},{8,14},{10,8},{12,... | collective-permute-start | bytes 98312 | tf_op jit(solution)/shard_map/ppermute | solution.py:466
  79.4 7.2 %collective-permute-done.9.q3 = bf16[2,64,128]{2,1,0:T(8,128)(2,1)S(1)} collective-permute-done((bf16[2,64,128]{2,1,0:T(8,128)(2,1)S(1)}, bf16[2,64,128]{2,1,0:T(8,128)(2,1)S(1)}, u32[]{:S(2)}, u32[]{:S(2)}) %collective-permute-start.9) | collective-permute-done | bytes 32800 | tf_op jit(solution)/shard_map/ppermute | solution.py:466
  86.5 4.6 %collective-permute-done.8.q2 = bf16[2,64,128]{2,1,0:T(8,128)(2,1)S(1)} collective-permute-done((bf16[2,64,128]{2,1,0:T(8,128)(2,1)S(1)}, bf16[2,64,128]{2,1,0:T(8,128)(2,1)S(1)}, u32[]{:S(2)}, u32[]{:S(2)}) %collective-permute-start.8) | collective-permute-done | bytes 32800 | tf_op jit(solution)/shard_map/ppermute | solution.py:466
  91.9 3.7 %collective-permute-done.7.q1 = bf16[2,64,128]{2,1,0:T(8,128)(2,1)S(1)} collective-permute-done((bf16[2,64,128]{2,1,0:T(8,128)(2,1)S(1)}, bf16[2,64,128]{2,1,0:T(8,128)(2,1)S(1)}, u32[]{:S(2)}, u32[]{:S(2)}) %collective-permute-start.7) | collective-permute-done | bytes 32800 | tf_op jit(solution)/shard_map/ppermute | solution.py:466
  97.0 6.7 %shard_map.135 = (f32[256,128]{1,0:T(8,128)S(1)}, bf16[256,128]{1,0:T(8,128)(2,1)S(1)}, f32[8,256]{1,0:T(8,128)S(1)}) custom-call(s32[5]{0:T(128)S(1)} %stack.62.where, bf16[4,256,256]{2,1,0:T(8,128)(2,1)S(1)} %get-tuple-element.23.q_ref, bf16[256,256]{1,0:T(8,128)(2,1)S(1)} %get-tuple-element.24.uk, bf16[256,256]{1,0:T(8,128)(2,1)S(1)} %get-tuple-element.25.uv, ...), custom_call_target="tpu_custom_call" | custom-call | tf_op jit(solution)/shard_map/pallas_call | solution.py:482
  103.7 4.0 %collective-permute-start.20 = (bf16[256,128]{1,0:T(8,128)(2,1)S(1)}, bf16[256,128]{1,0:T(8,128)(2,1)S(1)}, u32[]{:S(2)}, u32[]{:S(2)}) collective-permute-start(bf16[256,128]{1,0:T(8,128)(2,1)S(1)} %get-tuple-element.31), channel_id=1, source_target_pairs={{0,1},{1,0},{2,3},{3,2},{4,5},{5,4},{6,7},{7,6},{8,9},{9,8},{10,11... | collective-permute-start | bytes 196616 | tf_op jit(solution)/shard_map/ppermute | solution.py:500
  109.9 2.9 %collective-permute-start.23 = (bf16[32,1024]{1,0:T(8,128)(2,1)S(1)}, bf16[32,1024]{1,0:T(8,128)(2,1)S(1)}, u32[]{:S(2)}, u32[]{:S(2)}) collective-permute-start(bf16[32,1024]{1,0:T(8,128)(2,1)S(1)} %get-tuple-element.35), channel_id=1, source_target_pairs={{0,4},{2,6},{4,0},{6,2},{1,5},{3,7},{5,1},{7,3},{8,12},{10,14},{12... | collective-permute-start | bytes 196616 | tf_op jit(solution)/shard_map/ppermute | solution.py:507
  114.6 1.7 %collective-permute-done.23.p2 = bf16[32,1024]{1,0:T(8,128)(2,1)S(1)} collective-permute-done((bf16[32,1024]{1,0:T(8,128)(2,1)S(1)}, bf16[32,1024]{1,0:T(8,128)(2,1)S(1)}, u32[]{:S(2)}, u32[]{:S(2)}) %collective-permute-start.23) | collective-permute-done | bytes 65568 | tf_op jit(solution)/shard_map/ppermute | solution.py:507
  (51 shorter events, 21.0 us)
Async XLA Ops:
  3.0 16.7 %all-to-all-start = ((bf16[8,40,128]{2,1,0:T(8,128)(2,1)}), bf16[8,40,128]{2,1,0:T(8,128)(2,1)S(1)}, u32[]{:S(2)}, u32[]{:S(2)}) async-start(bf16[8,40,128]{2,1,0:T(8,128)(2,1)} %shard_map.131), calls=%async_computation | async-start | bytes 163840 | tf_op jit(solution)/shard_map/all_to_all | solution.py:435
  12.1 12.4 %collective-permute-start.1 = (bf16[32,1024]{1,0:T(8,128)(2,1)S(1)}, bf16[32,1024]{1,0:T(8,128)(2,1)S(1)}, u32[]{:S(2)}, u32[]{:S(2)}) collective-permute-start(bf16[32,1024]{1,0:T(8,128)(2,1)S(1)} %copy-done), channel_id=1, source_target_pairs={{0,4},{2,6},{4,0},{6,2},{1,5},{3,7},{5,1},{7,3},{8,12},{10,14},{12... | collective-permute-start | bytes 196616 | tf_op jit(solution)/shard_map/ppermute | solution.py:438
  19.6 8.0 %collective-permute-start.5 = (bf16[8,40,128]{2,1,0:T(8,128)(2,1)S(1)}, bf16[8,40,128]{2,1,0:T(8,128)(2,1)S(1)}, u32[]{:S(2)}, u32[]{:S(2)}) collective-permute-start(bf16[8,40,128]{2,1,0:T(8,128)(2,1)S(1)} %all-to-all-done.g0), channel_id=1, source_target_pairs={{0,24},{8,0},{16,8},{24,16},{1,25},{9,1},{17,9},{25,17},{2,26},{10... | collective-permute-start | bytes 245768 | tf_op jit(solution)/shard_map/ppermute | solution.py:436
  22.1 5.5 %collective-permute-start.4 = (bf16[8,40,128]{2,1,0:T(8,128)(2,1)S(1)}, bf16[8,40,128]{2,1,0:T(8,128)(2,1)S(1)}, u32[]{:S(2)}, u32[]{:S(2)}) collective-permute-start(bf16[8,40,128]{2,1,0:T(8,128)(2,1)S(1)} %all-to-all-done.g0), channel_id=1, source_target_pairs={{0,16},{8,24},{16,0},{24,8},{1,17},{9,25},{17,1},{25,9},{2,18},{10... | collective-permute-start | bytes 245768 | tf_op jit(solution)/shard_map/ppermute | solution.py:436
  22.6 5.2 %collective-permute-start.3 = (bf16[8,40,128]{2,1,0:T(8,128)(2,1)S(1)}, bf16[8,40,128]{2,1,0:T(8,128)(2,1)S(1)}, u32[]{:S(2)}, u32[]{:S(2)}) collective-permute-start(bf16[8,40,128]{2,1,0:T(8,128)(2,1)S(1)} %all-to-all-done.g0), channel_id=1, source_target_pairs={{0,8},{8,16},{16,24},{24,0},{1,9},{9,17},{17,25},{25,1},{2,10},{10... | collective-permute-start | bytes 245768 | tf_op jit(solution)/shard_map/ppermute | solution.py:436
  23.2 4.4 %collective-permute-start = (bf16[32,1024]{1,0:T(8,128)(2,1)S(1)}, bf16[32,1024]{1,0:T(8,128)(2,1)S(1)}, u32[]{:S(2)}, u32[]{:S(2)}) collective-permute-start(bf16[32,1024]{1,0:T(8,128)(2,1)S(1)} %copy-done), channel_id=1, source_target_pairs={{0,2},{2,4},{4,6},{6,0},{1,3},{3,5},{5,7},{7,1},{8,10},{10,12},{12... | collective-permute-start | bytes 196616 | tf_op jit(solution)/shard_map/ppermute | solution.py:438
  29.3 11.8 %all-to-all-start.2 = ((bf16[8,72,128]{2,1,0:T(8,128)(2,1)}), bf16[8,72,128]{2,1,0:T(8,128)(2,1)S(1)}, u32[]{:S(2)}, u32[]{:S(2)}) async-start(bf16[8,72,128]{2,1,0:T(8,128)(2,1)} %get-tuple-element.29), calls=%async_computation.2 | async-start | bytes 294912 | tf_op jit(solution)/shard_map/all_to_all | solution.py:458
  36.1 4.1 %collective-permute-start.11 = (bf16[64,128]{1,0:T(8,128)(2,1)S(1)}, bf16[64,128]{1,0:T(8,128)(2,1)S(1)}, u32[]{:S(2)}, u32[]{:S(2)}) collective-permute-start(bf16[64,128]{1,0:T(8,128)(2,1)S(1)} %get-tuple-element.21), channel_id=1, source_target_pairs={{0,16},{8,24},{16,0},{24,8},{1,17},{9,25},{17,1},{25,9},{2,18},{10... | collective-permute-start | bytes 49160 | tf_op jit(solution)/shard_map/ppermute | solution.py:449
  37.3 3.8 %collective-permute-start.10 = (bf16[64,128]{1,0:T(8,128)(2,1)S(1)}, bf16[64,128]{1,0:T(8,128)(2,1)S(1)}, u32[]{:S(2)}, u32[]{:S(2)}) collective-permute-start(bf16[64,128]{1,0:T(8,128)(2,1)S(1)} %get-tuple-element.21), channel_id=1, source_target_pairs={{0,8},{8,16},{16,24},{24,0},{1,9},{9,17},{17,25},{25,1},{2,10},{10... | collective-permute-start | bytes 49160 | tf_op jit(solution)/shard_map/ppermute | solution.py:449
  42.0 18.8 %all-to-all-start.1 = ((bf16[8,4,64,128]{3,2,1,0:T(8,128)(2,1)}), bf16[8,4,64,128]{3,2,1,0:T(8,128)(2,1)S(1)}, u32[]{:S(2)}, u32[]{:S(2)}) async-start(bf16[8,4,64,128]{3,2,1,0:T(8,128)(2,1)} %broadcast_in_dim.2), calls=%async_computation.1 | async-start | bytes 1048576 | tf_op jit(solution)/shard_map/all_to_all | solution.py:463
  48.6 6.0 %collective-permute-start.16 = (bf16[8,72,128]{2,1,0:T(8,128)(2,1)S(1)}, bf16[8,72,128]{2,1,0:T(8,128)(2,1)S(1)}, u32[]{:S(2)}, u32[]{:S(2)}) collective-permute-start(bf16[8,72,128]{2,1,0:T(8,128)(2,1)S(1)} %all-to-all-done.2), channel_id=1, source_target_pairs={{0,24},{1,7},{2,26},{3,1},{4,28},{5,3},{6,30},{7,5},{8,0},{9,15},{... | collective-permute-start | bytes 442376 | tf_op jit(solution)/shard_map/ppermute | solution.py:459
  51.0 5.6 %collective-permute-start.15 = (bf16[8,72,128]{2,1,0:T(8,128)(2,1)S(1)}, bf16[8,72,128]{2,1,0:T(8,128)(2,1)S(1)}, u32[]{:S(2)}, u32[]{:S(2)}) collective-permute-start(bf16[8,72,128]{2,1,0:T(8,128)(2,1)S(1)} %all-to-all-done.2), channel_id=1, source_target_pairs={{0,16},{1,5},{2,18},{3,7},{4,20},{5,1},{6,22},{7,3},{8,24},{9,13},... | collective-permute-start | bytes 442376 | tf_op jit(solution)/shard_map/ppermute | solution.py:459
  51.7 6.3 %collective-permute-start.14 = (bf16[8,72,128]{2,1,0:T(8,128)(2,1)S(1)}, bf16[8,72,128]{2,1,0:T(8,128)(2,1)S(1)}, u32[]{:S(2)}, u32[]{:S(2)}) collective-permute-start(bf16[8,72,128]{2,1,0:T(8,128)(2,1)S(1)} %all-to-all-done.2), channel_id=1, source_target_pairs={{0,8},{1,3},{2,10},{3,5},{4,12},{5,7},{6,14},{7,1},{8,16},{9,11},{... | collective-permute-start | bytes 442376 | tf_op jit(solution)/shard_map/ppermute | solution.py:459
  58.1 38.8 %collective-permute-start.19 = (bf16[4,8,72,128]{3,2,1,0:T(8,128)(2,1)S(1)}, bf16[4,8,72,128]{3,2,1,0:T(8,128)(2,1)S(1)}, u32[]{:S(2)}, u32[]{:S(2)}) collective-permute-start(bf16[4,8,72,128]{3,2,1,0:T(8,128)(2,1)S(1)} %pad_maximum_fusion.b0), channel_id=1, source_target_pairs={{0,6},{1,25},{2,0},{3,27},{4,2},{5,29},{6,4},{7,31},{8,14},{9,1},{... | collective-permute-start | bytes 1769480 | tf_op jit(solution)/shard_map/ppermute | solution.py:461
  58.3 38.7 %collective-permute-start.18 = (bf16[4,8,72,128]{3,2,1,0:T(8,128)(2,1)S(1)}, bf16[4,8,72,128]{3,2,1,0:T(8,128)(2,1)S(1)}, u32[]{:S(2)}, u32[]{:S(2)}) collective-permute-start(bf16[4,8,72,128]{3,2,1,0:T(8,128)(2,1)S(1)} %pad_maximum_fusion.b0), channel_id=1, source_target_pairs={{0,4},{1,17},{2,6},{3,19},{4,0},{5,21},{6,2},{7,23},{8,12},{9,25},... | collective-permute-start | bytes 1769480 | tf_op jit(solution)/shard_map/ppermute | solution.py:461
  59.4 37.6 %collective-permute-start.17 = (bf16[4,8,72,128]{3,2,1,0:T(8,128)(2,1)S(1)}, bf16[4,8,72,128]{3,2,1,0:T(8,128)(2,1)S(1)}, u32[]{:S(2)}, u32[]{:S(2)}) collective-permute-start(bf16[4,8,72,128]{3,2,1,0:T(8,128)(2,1)S(1)} %pad_maximum_fusion.b0), channel_id=1, source_target_pairs={{0,2},{1,9},{2,4},{3,11},{4,6},{5,13},{6,0},{7,15},{8,10},{9,17},{... | collective-permute-start | bytes 1769480 | tf_op jit(solution)/shard_map/ppermute | solution.py:461
  60.8 34.8 %collective-permute-start.13 = (bf16[8,4,64,128]{3,2,1,0:T(8,128)(2,1)S(1)}, bf16[8,4,64,128]{3,2,1,0:T(8,128)(2,1)S(1)}, u32[]{:S(2)}, u32[]{:S(2)}) collective-permute-start(bf16[8,4,64,128]{3,2,1,0:T(8,128)(2,1)S(1)} %all-to-all-done.1.up_own.w_own), channel_id=1, source_target_pairs={{0,1},{1,0},{2,3},{3,2},{4,5},{5,4},{6,7},{7,6},{8,9},{9,8},{10,11... | collective-permute-start | bytes 1572872 | tf_op jit(solution)/shard_map/ppermute | solution.py:464
  77.1 9.4 %collective-permute-start.9 = (bf16[2,64,128]{2,1,0:T(8,128)(2,1)S(1)}, bf16[2,64,128]{2,1,0:T(8,128)(2,1)S(1)}, u32[]{:S(2)}, u32[]{:S(2)}) collective-permute-start(bf16[2,64,128]{2,1,0:T(8,128)(2,1)S(1)} %pad_maximum_fusion.2.q0), channel_id=1, source_target_pairs={{0,6},{2,0},{4,2},{6,4},{1,7},{3,1},{5,3},{7,5},{8,14},{10,8},{12,... | collective-permute-start | bytes 98312 | tf_op jit(solution)/shard_map/ppermute | solution.py:466
  86.5 4.6 %collective-permute-start.8 = (bf16[2,64,128]{2,1,0:T(8,128)(2,1)S(1)}, bf16[2,64,128]{2,1,0:T(8,128)(2,1)S(1)}, u32[]{:S(2)}, u32[]{:S(2)}) collective-permute-start(bf16[2,64,128]{2,1,0:T(8,128)(2,1)S(1)} %pad_maximum_fusion.2.q0), channel_id=1, source_target_pairs={{0,4},{2,6},{4,0},{6,2},{1,5},{3,7},{5,1},{7,3},{8,12},{10,14},{12... | collective-permute-start | bytes 98312 | tf_op jit(solution)/shard_map/ppermute | solution.py:466
  91.1 4.5 %collective-permute-start.7 = (bf16[2,64,128]{2,1,0:T(8,128)(2,1)S(1)}, bf16[2,64,128]{2,1,0:T(8,128)(2,1)S(1)}, u32[]{:S(2)}, u32[]{:S(2)}) collective-permute-start(bf16[2,64,128]{2,1,0:T(8,128)(2,1)S(1)} %pad_maximum_fusion.2.q0), channel_id=1, source_target_pairs={{0,2},{2,4},{4,6},{6,0},{1,3},{3,5},{5,7},{7,1},{8,10},{10,12},{12... | collective-permute-start | bytes 98312 | tf_op jit(solution)/shard_map/ppermute | solution.py:466
  103.7 5.1 %collective-permute-start.20 = (bf16[256,128]{1,0:T(8,128)(2,1)S(1)}, bf16[256,128]{1,0:T(8,128)(2,1)S(1)}, u32[]{:S(2)}, u32[]{:S(2)}) collective-permute-start(bf16[256,128]{1,0:T(8,128)(2,1)S(1)} %get-tuple-element.31), channel_id=1, source_target_pairs={{0,1},{1,0},{2,3},{3,2},{4,5},{5,4},{6,7},{7,6},{8,9},{9,8},{10,11... | collective-permute-start | bytes 196616 | tf_op jit(solution)/shard_map/ppermute | solution.py:500
  109.8 4.8 %collective-permute-start.22 = (bf16[32,1024]{1,0:T(8,128)(2,1)S(1)}, bf16[32,1024]{1,0:T(8,128)(2,1)S(1)}, u32[]{:S(2)}, u32[]{:S(2)}) collective-permute-start(bf16[32,1024]{1,0:T(8,128)(2,1)S(1)} %get-tuple-element.34), channel_id=1, source_target_pairs={{0,2},{2,4},{4,6},{6,0},{1,3},{3,5},{5,7},{7,1},{8,10},{10,12},{12... | collective-permute-start | bytes 196616 | tf_op jit(solution)/shard_map/ppermute | solution.py:507
  109.9 6.3 %collective-permute-start.23 = (bf16[32,1024]{1,0:T(8,128)(2,1)S(1)}, bf16[32,1024]{1,0:T(8,128)(2,1)S(1)}, u32[]{:S(2)}, u32[]{:S(2)}) collective-permute-start(bf16[32,1024]{1,0:T(8,128)(2,1)S(1)} %get-tuple-element.35), channel_id=1, source_target_pairs={{0,4},{2,6},{4,0},{6,2},{1,5},{3,7},{5,1},{7,3},{8,12},{10,14},{12... | collective-permute-start | bytes 196616 | tf_op jit(solution)/shard_map/ppermute | solution.py:507
  112.8 3.9 %collective-permute-start.24 = (bf16[32,1024]{1,0:T(8,128)(2,1)S(1)}, bf16[32,1024]{1,0:T(8,128)(2,1)S(1)}, u32[]{:S(2)}, u32[]{:S(2)}) collective-permute-start(bf16[32,1024]{1,0:T(8,128)(2,1)S(1)} %get-tuple-element.36), channel_id=1, source_target_pairs={{0,6},{2,0},{4,2},{6,4},{1,7},{3,1},{5,3},{7,5},{8,14},{10,8},{12,... | collective-permute-start | bytes 196616 | tf_op jit(solution)/shard_map/ppermute | solution.py:507
  (6 other events, 22.4 us)

commit v12 on v11

--- a/solution.py
+++ b/solution.py
@@ -56,13 +56,20 @@
     return jnp.transpose(jnp.broadcast_to(row, (128, 128)))
 
 
-def by_fours(step, count):
-    def four(i, carry):
+def by_eights(step, count):
+    def eight(i, carry):
+        for k in range(8):
+            step(8 * i + k)
+        return carry
+
+    lax.fori_loop(0, count // 8, eight, 0)
+    most = count // 8 * 8
+
+    @pl.when(lax.rem(count, 8) >= 4)
+    def _():
         for k in range(4):
-            step(4 * i + k)
-        return carry
-
-    lax.fori_loop(0, count // 4, four, 0)
+            step(most + k)
+
     done = count // 4 * 4
 
     @pl.when(lax.rem(count, 4) >= 2)
@@ -319,7 +326,7 @@
             s_buf[tile, h] = got
             mx[h] = jnp.maximum(mx[h], jnp.max(got.reshape(32, 8, 256), axis=0))
 
-    by_fours(scores, count)
+    by_eights(scores, count)
     tops = []
     for h in range(4):
         top = jnp.maximum(jnp.max(mx[h], axis=0, keepdims=True), FLOOR)
@@ -336,7 +343,7 @@
                 v_buf[tile, own, :], weights, preferred_element_type=F32
             )
 
-    by_fours(weigh, count)
+    by_eights(weigh, count)
     for h in range(4):
         ml_ref[h : h + 1, :] = tops[h]
         ml_ref[4 + h : 5 + h, :] = jnp.sum(total[h], axis=0, keepdims=True)

time: 118 us -> 118 us (level)
  no operation moved by 1% of the time
where the time goes in v12:
time: 118 us; the launch traced here: 117 us
  starting transfers between devices  62.3 us (53%)
  waiting for transfers between devices  37.9 us (32%)
  Pallas kernels  14.4 us (12%)
  local copies, waits for them, and re-layouts  1.76 us (1%)
    ppermute x3, waiting for transfers between devices, layer(): lax.ppermute(q_pair, 'y', ring(j))  15.5 us
    ppermute x1, starting transfers between devices, layer(): up_other = lax.ppermute(up_own, 'c', swap)  14.6 us
    all_to_all x1, starting transfers between devices, layer(): gathered = lax.all_to_all(message, 'z', 0, 0)  9.15 us
    all_to_all x1, starting transfers between devices, layer(): up_own = lax.all_to_all(later, 'z', 0, 0)  6.56 us
    pallas_call x1, Pallas kernels, layer(): call(attend, (jax.ShapeDtypeStruct((256, 128), F32), jax.ShapeDtypeStruct...  6.52 us
    ppermute x3, waiting for transfers between devices, layer(): lax.ppermute(stage1, AXES, shift_pairs(2, j))  5.95 us
    ppermute x3, starting transfers between devices, layer(): rows = [tokens] + [lax.ppermute(tokens, 'y', ring(j)) for j in range(1, NY)]  5.74 us
    all_to_all x1, waiting for transfers between devices, layer(): gathered = lax.all_to_all(message, 'z', 0, 0)  4.5 us
  transfers between devices with their start and end apart: 28, of which 17 were waited for; matrix products, arithmetic and copies ran while one was open for 1% of the time, Pallas kernels for 2%

profile of v12, /device:TPU:1, one launch (start us, length us, event | category | flops | bytes accessed | tf_op | source)
XLA Modules:
  0.0 117.2 jit_solution(11199770538910439895)
XLA Ops:
  0.7 2.2 %shard_map.131 = bf16[8,40,128]{2,1,0:T(8,128)(2,1)} custom-call(s32[5]{0:T(128)S(1)} %stack.62.where, bf16[32,256]{1,0:T(8,128)(2,1)} %dq_in.1, bf16[32,256]{1,0:T(8,128)(2,1)} %dk_in.1, bf16[32,32]{1,0:T(8,128)(2,1)} %dr_in.1), custom_call_target="tpu_custom_call" | custom-call | tf_op jit(solution)/shard_map/pallas_call | solution.py:436
  3.0 9.1 %all-to-all-start = ((bf16[8,40,128]{2,1,0:T(8,128)(2,1)}), bf16[8,40,128]{2,1,0:T(8,128)(2,1)S(1)}, u32[]{:S(2)}, u32[]{:S(2)}) async-start(bf16[8,40,128]{2,1,0:T(8,128)(2,1)} %shard_map.131), calls=%async_computation | async-start | bytes 163840 | tf_op jit(solution)/shard_map/all_to_all | solution.py:442
  12.1 3.0 %collective-permute-start.1 = (bf16[32,1024]{1,0:T(8,128)(2,1)S(1)}, bf16[32,1024]{1,0:T(8,128)(2,1)S(1)}, u32[]{:S(2)}, u32[]{:S(2)}) collective-permute-start(bf16[32,1024]{1,0:T(8,128)(2,1)S(1)} %copy-done), channel_id=1, source_target_pairs={{0,4},{2,6},{4,0},{6,2},{1,5},{3,7},{5,1},{7,3},{8,12},{10,14},{12... | collective-permute-start | bytes 196616 | tf_op jit(solution)/shard_map/ppermute | solution.py:445
  15.1 4.5 %all-to-all-done.g0 = bf16[8,40,128]{2,1,0:T(8,128)(2,1)S(1)} async-done(((bf16[8,40,128]{2,1,0:T(8,128)(2,1)}), bf16[8,40,128]{2,1,0:T(8,128)(2,1)S(1)}, u32[]{:S(2)}, u32[]{:S(2)}) %all-to-all-start) | async-done | bytes 81952 | tf_op jit(solution)/shard_map/all_to_all | solution.py:442
  19.6 2.5 %collective-permute-start.5 = (bf16[8,40,128]{2,1,0:T(8,128)(2,1)S(1)}, bf16[8,40,128]{2,1,0:T(8,128)(2,1)S(1)}, u32[]{:S(2)}, u32[]{:S(2)}) collective-permute-start(bf16[8,40,128]{2,1,0:T(8,128)(2,1)S(1)} %all-to-all-done.g0), channel_id=1, source_target_pairs={{0,24},{8,0},{16,8},{24,16},{1,25},{9,1},{17,9},{25,17},{2,26},{10... | collective-permute-start | bytes 245768 | tf_op jit(solution)/shard_map/ppermute | solution.py:443
  26.0 1.6 %collective-permute-done.t1 = bf16[32,1024]{1,0:T(8,128)(2,1)S(1)} collective-permute-done((bf16[32,1024]{1,0:T(8,128)(2,1)S(1)}, bf16[32,1024]{1,0:T(8,128)(2,1)S(1)}, u32[]{:S(2)}, u32[]{:S(2)}) %collective-permute-start) | collective-permute-done | bytes 65568 | tf_op jit(solution)/shard_map/ppermute | solution.py:445
  27.8 1.6 %shard_map.132 = (bf16[64,128]{1,0:T(8,128)(2,1)S(1)}, bf16[8,72,128]{2,1,0:T(8,128)(2,1)}) custom-call(s32[5]{0:T(128)S(1)} %stack.62.where, bf16[32,1024]{1,0:T(8,128)(2,1)S(1)} %copy-done, bf16[32,1024]{1,0:T(8,128)(2,1)S(1)} %collective-permute-done.t1, bf16[32,1024]{1,0:T(8,128)(2,1)S(1)} %collective-permute-done.1.t2, ...), custom_call_target="tpu_custom_call" | custom-call | tf_op jit(solution)/shard_map/pallas_call | solution.py:459
  29.3 3.4 %all-to-all-start.2 = ((bf16[8,72,128]{2,1,0:T(8,128)(2,1)}), bf16[8,72,128]{2,1,0:T(8,128)(2,1)S(1)}, u32[]{:S(2)}, u32[]{:S(2)}) async-start(bf16[8,72,128]{2,1,0:T(8,128)(2,1)} %get-tuple-element.29), calls=%async_computation.2 | async-start | bytes 294912 | tf_op jit(solution)/shard_map/all_to_all | solution.py:465
  33.7 2.3 %collective-permute-start.12 = (bf16[64,128]{1,0:T(8,128)(2,1)S(1)}, bf16[64,128]{1,0:T(8,128)(2,1)S(1)}, u32[]{:S(2)}, u32[]{:S(2)}) collective-permute-start(bf16[64,128]{1,0:T(8,128)(2,1)S(1)} %get-tuple-element.21), channel_id=1, source_target_pairs={{0,24},{8,0},{16,8},{24,16},{1,25},{9,1},{17,9},{25,17},{2,26},{10... | collective-permute-start | bytes 49160 | tf_op jit(solution)/shard_map/ppermute | solution.py:456
  37.3 2.8 %collective-permute-done.11 = bf16[64,128]{1,0:T(8,128)(2,1)S(1)} collective-permute-done((bf16[64,128]{1,0:T(8,128)(2,1)S(1)}, bf16[64,128]{1,0:T(8,128)(2,1)S(1)}, u32[]{:S(2)}, u32[]{:S(2)}) %collective-permute-start.11) | collective-permute-done | bytes 16416 | tf_op jit(solution)/shard_map/ppermute | solution.py:456
  42.0 6.6 %all-to-all-start.1 = ((bf16[8,4,64,128]{3,2,1,0:T(8,128)(2,1)}), bf16[8,4,64,128]{3,2,1,0:T(8,128)(2,1)S(1)}, u32[]{:S(2)}, u32[]{:S(2)}) async-start(bf16[8,4,64,128]{3,2,1,0:T(8,128)(2,1)} %broadcast_in_dim.2), calls=%async_computation.1 | async-start | bytes 1048576 | tf_op jit(solution)/shard_map/all_to_all | solution.py:470
  48.6 2.4 %collective-permute-start.16 = (bf16[8,72,128]{2,1,0:T(8,128)(2,1)S(1)}, bf16[8,72,128]{2,1,0:T(8,128)(2,1)S(1)}, u32[]{:S(2)}, u32[]{:S(2)}) collective-permute-start(bf16[8,72,128]{2,1,0:T(8,128)(2,1)S(1)} %all-to-all-done.2), channel_id=1, source_target_pairs={{0,24},{1,7},{2,26},{3,1},{4,28},{5,3},{6,30},{7,5},{8,0},{9,15},{... | collective-permute-start | bytes 442376 | tf_op jit(solution)/shard_map/ppermute | solution.py:466
  52.1 2.5 %collective-permute-done.16 = bf16[8,72,128]{2,1,0:T(8,128)(2,1)S(1)} collective-permute-done((bf16[8,72,128]{2,1,0:T(8,128)(2,1)S(1)}, bf16[8,72,128]{2,1,0:T(8,128)(2,1)S(1)}, u32[]{:S(2)}, u32[]{:S(2)}) %collective-permute-start.16) | collective-permute-done | bytes 147488 | tf_op jit(solution)/shard_map/ppermute | solution.py:466
  54.6 1.9 %collective-permute-done.15 = bf16[8,72,128]{2,1,0:T(8,128)(2,1)S(1)} collective-permute-done((bf16[8,72,128]{2,1,0:T(8,128)(2,1)S(1)}, bf16[8,72,128]{2,1,0:T(8,128)(2,1)S(1)}, u32[]{:S(2)}, u32[]{:S(2)}) %collective-permute-start.15) | collective-permute-done | bytes 147488 | tf_op jit(solution)/shard_map/ppermute | solution.py:466
  60.8 14.6 %collective-permute-start.13 = (bf16[8,4,64,128]{3,2,1,0:T(8,128)(2,1)S(1)}, bf16[8,4,64,128]{3,2,1,0:T(8,128)(2,1)S(1)}, u32[]{:S(2)}, u32[]{:S(2)}) collective-permute-start(bf16[8,4,64,128]{3,2,1,0:T(8,128)(2,1)S(1)} %all-to-all-done.1.up_own.w_own), channel_id=1, source_target_pairs={{0,1},{1,0},{2,3},{3,2},{4,5},{5,4},{6,7},{7,6},{8,9},{9,8},{10,11... | collective-permute-start | bytes 1572872 | tf_op jit(solution)/shard_map/ppermute | solution.py:471
  75.5 1.6 %collective-permute-done.6 = bf16[64,128]{1,0:T(8,128)(2,1)S(1)} collective-permute-done((bf16[64,128]{1,0:T(8,128)(2,1)S(1)}, bf16[64,128]{1,0:T(8,128)(2,1)S(1)}, u32[]{:S(2)}, u32[]{:S(2)}) %collective-permute-start.6) | collective-permute-done | bytes 16416 | tf_op jit(solution)/shard_map/ppermute | solution.py:472
  77.1 2.3 %collective-permute-start.9 = (bf16[2,64,128]{2,1,0:T(8,128)(2,1)S(1)}, bf16[2,64,128]{2,1,0:T(8,128)(2,1)S(1)}, u32[]{:S(2)}, u32[]{:S(2)}) collective-permute-start(bf16[2,64,128]{2,1,0:T(8,128)(2,1)S(1)} %pad_maximum_fusion.2.q0), channel_id=1, source_target_pairs={{0,6},{2,0},{4,2},{6,4},{1,7},{3,1},{5,3},{7,5},{8,14},{10,8},{12,... | collective-permute-start | bytes 98312 | tf_op jit(solution)/shard_map/ppermute | solution.py:473
  79.4 7.2 %collective-permute-done.9.q3 = bf16[2,64,128]{2,1,0:T(8,128)(2,1)S(1)} collective-permute-done((bf16[2,64,128]{2,1,0:T(8,128)(2,1)S(1)}, bf16[2,64,128]{2,1,0:T(8,128)(2,1)S(1)}, u32[]{:S(2)}, u32[]{:S(2)}) %collective-permute-start.9) | collective-permute-done | bytes 32800 | tf_op jit(solution)/shard_map/ppermute | solution.py:473
  86.5 4.6 %collective-permute-done.8.q2 = bf16[2,64,128]{2,1,0:T(8,128)(2,1)S(1)} collective-permute-done((bf16[2,64,128]{2,1,0:T(8,128)(2,1)S(1)}, bf16[2,64,128]{2,1,0:T(8,128)(2,1)S(1)}, u32[]{:S(2)}, u32[]{:S(2)}) %collective-permute-start.8) | collective-permute-done | bytes 32800 | tf_op jit(solution)/shard_map/ppermute | solution.py:473
  91.9 3.7 %collective-permute-done.7.q1 = bf16[2,64,128]{2,1,0:T(8,128)(2,1)S(1)} collective-permute-done((bf16[2,64,128]{2,1,0:T(8,128)(2,1)S(1)}, bf16[2,64,128]{2,1,0:T(8,128)(2,1)S(1)}, u32[]{:S(2)}, u32[]{:S(2)}) %collective-permute-start.7) | collective-permute-done | bytes 32800 | tf_op jit(solution)/shard_map/ppermute | solution.py:473
  97.0 6.5 %shard_map.135 = (f32[256,128]{1,0:T(8,128)S(1)}, bf16[256,128]{1,0:T(8,128)(2,1)S(1)}, f32[8,256]{1,0:T(8,128)S(1)}) custom-call(s32[5]{0:T(128)S(1)} %stack.62.where, bf16[4,256,256]{2,1,0:T(8,128)(2,1)S(1)} %get-tuple-element.23.q_ref, bf16[256,256]{1,0:T(8,128)(2,1)S(1)} %get-tuple-element.24.uk, bf16[256,256]{1,0:T(8,128)(2,1)S(1)} %get-tuple-element.25.uv, ...), custom_call_target="tpu_custom_call" | custom-call | tf_op jit(solution)/shard_map/pallas_call | solution.py:489
  103.5 3.9 %collective-permute-start.20 = (bf16[256,128]{1,0:T(8,128)(2,1)S(1)}, bf16[256,128]{1,0:T(8,128)(2,1)S(1)}, u32[]{:S(2)}, u32[]{:S(2)}) collective-permute-start(bf16[256,128]{1,0:T(8,128)(2,1)S(1)} %get-tuple-element.31), channel_id=1, source_target_pairs={{0,1},{1,0},{2,3},{3,2},{4,5},{5,4},{6,7},{7,6},{8,9},{9,8},{10,11... | collective-permute-start | bytes 196616 | tf_op jit(solution)/shard_map/ppermute | solution.py:507
  109.7 2.9 %collective-permute-start.23 = (bf16[32,1024]{1,0:T(8,128)(2,1)S(1)}, bf16[32,1024]{1,0:T(8,128)(2,1)S(1)}, u32[]{:S(2)}, u32[]{:S(2)}) collective-permute-start(bf16[32,1024]{1,0:T(8,128)(2,1)S(1)} %get-tuple-element.35), channel_id=1, source_target_pairs={{0,4},{2,6},{4,0},{6,2},{1,5},{3,7},{5,1},{7,3},{8,12},{10,14},{12... | collective-permute-start | bytes 196616 | tf_op jit(solution)/shard_map/ppermute | solution.py:514
  114.4 1.7 %collective-permute-done.23.p2 = bf16[32,1024]{1,0:T(8,128)(2,1)S(1)} collective-permute-done((bf16[32,1024]{1,0:T(8,128)(2,1)S(1)}, bf16[32,1024]{1,0:T(8,128)(2,1)S(1)}, u32[]{:S(2)}, u32[]{:S(2)}) %collective-permute-start.23) | collective-permute-done | bytes 65568 | tf_op jit(solution)/shard_map/ppermute | solution.py:514
  (51 shorter events, 21.0 us)
Async XLA Ops:
  3.0 16.7 %all-to-all-start = ((bf16[8,40,128]{2,1,0:T(8,128)(2,1)}), bf16[8,40,128]{2,1,0:T(8,128)(2,1)S(1)}, u32[]{:S(2)}, u32[]{:S(2)}) async-start(bf16[8,40,128]{2,1,0:T(8,128)(2,1)} %shard_map.131), calls=%async_computation | async-start | bytes 163840 | tf_op jit(solution)/shard_map/all_to_all | solution.py:442
  12.1 12.4 %collective-permute-start.1 = (bf16[32,1024]{1,0:T(8,128)(2,1)S(1)}, bf16[32,1024]{1,0:T(8,128)(2,1)S(1)}, u32[]{:S(2)}, u32[]{:S(2)}) collective-permute-start(bf16[32,1024]{1,0:T(8,128)(2,1)S(1)} %copy-done), channel_id=1, source_target_pairs={{0,4},{2,6},{4,0},{6,2},{1,5},{3,7},{5,1},{7,3},{8,12},{10,14},{12... | collective-permute-start | bytes 196616 | tf_op jit(solution)/shard_map/ppermute | solution.py:445
  19.6 8.0 %collective-permute-start.5 = (bf16[8,40,128]{2,1,0:T(8,128)(2,1)S(1)}, bf16[8,40,128]{2,1,0:T(8,128)(2,1)S(1)}, u32[]{:S(2)}, u32[]{:S(2)}) collective-permute-start(bf16[8,40,128]{2,1,0:T(8,128)(2,1)S(1)} %all-to-all-done.g0), channel_id=1, source_target_pairs={{0,24},{8,0},{16,8},{24,16},{1,25},{9,1},{17,9},{25,17},{2,26},{10... | collective-permute-start | bytes 245768 | tf_op jit(solution)/shard_map/ppermute | solution.py:443
  22.1 5.5 %collective-permute-start.4 = (bf16[8,40,128]{2,1,0:T(8,128)(2,1)S(1)}, bf16[8,40,128]{2,1,0:T(8,128)(2,1)S(1)}, u32[]{:S(2)}, u32[]{:S(2)}) collective-permute-start(bf16[8,40,128]{2,1,0:T(8,128)(2,1)S(1)} %all-to-all-done.g0), channel_id=1, source_target_pairs={{0,16},{8,24},{16,0},{24,8},{1,17},{9,25},{17,1},{25,9},{2,18},{10... | collective-permute-start | bytes 245768 | tf_op jit(solution)/shard_map/ppermute | solution.py:443
  22.6 5.2 %collective-permute-start.3 = (bf16[8,40,128]{2,1,0:T(8,128)(2,1)S(1)}, bf16[8,40,128]{2,1,0:T(8,128)(2,1)S(1)}, u32[]{:S(2)}, u32[]{:S(2)}) collective-permute-start(bf16[8,40,128]{2,1,0:T(8,128)(2,1)S(1)} %all-to-all-done.g0), channel_id=1, source_target_pairs={{0,8},{8,16},{16,24},{24,0},{1,9},{9,17},{17,25},{25,1},{2,10},{10... | collective-permute-start | bytes 245768 | tf_op jit(solution)/shard_map/ppermute | solution.py:443
  23.2 4.4 %collective-permute-start = (bf16[32,1024]{1,0:T(8,128)(2,1)S(1)}, bf16[32,1024]{1,0:T(8,128)(2,1)S(1)}, u32[]{:S(2)}, u32[]{:S(2)}) collective-permute-start(bf16[32,1024]{1,0:T(8,128)(2,1)S(1)} %copy-done), channel_id=1, source_target_pairs={{0,2},{2,4},{4,6},{6,0},{1,3},{3,5},{5,7},{7,1},{8,10},{10,12},{12... | collective-permute-start | bytes 196616 | tf_op jit(solution)/shard_map/ppermute | solution.py:445
  29.3 11.8 %all-to-all-start.2 = ((bf16[8,72,128]{2,1,0:T(8,128)(2,1)}), bf16[8,72,128]{2,1,0:T(8,128)(2,1)S(1)}, u32[]{:S(2)}, u32[]{:S(2)}) async-start(bf16[8,72,128]{2,1,0:T(8,128)(2,1)} %get-tuple-element.29), calls=%async_computation.2 | async-start | bytes 294912 | tf_op jit(solution)/shard_map/all_to_all | solution.py:465
  36.1 4.1 %collective-permute-start.11 = (bf16[64,128]{1,0:T(8,128)(2,1)S(1)}, bf16[64,128]{1,0:T(8,128)(2,1)S(1)}, u32[]{:S(2)}, u32[]{:S(2)}) collective-permute-start(bf16[64,128]{1,0:T(8,128)(2,1)S(1)} %get-tuple-element.21), channel_id=1, source_target_pairs={{0,16},{8,24},{16,0},{24,8},{1,17},{9,25},{17,1},{25,9},{2,18},{10... | collective-permute-start | bytes 49160 | tf_op jit(solution)/shard_map/ppermute | solution.py:456
  37.3 3.8 %collective-permute-start.10 = (bf16[64,128]{1,0:T(8,128)(2,1)S(1)}, bf16[64,128]{1,0:T(8,128)(2,1)S(1)}, u32[]{:S(2)}, u32[]{:S(2)}) collective-permute-start(bf16[64,128]{1,0:T(8,128)(2,1)S(1)} %get-tuple-element.21), channel_id=1, source_target_pairs={{0,8},{8,16},{16,24},{24,0},{1,9},{9,17},{17,25},{25,1},{2,10},{10... | collective-permute-start | bytes 49160 | tf_op jit(solution)/shard_map/ppermute | solution.py:456
  42.0 18.8 %all-to-all-start.1 = ((bf16[8,4,64,128]{3,2,1,0:T(8,128)(2,1)}), bf16[8,4,64,128]{3,2,1,0:T(8,128)(2,1)S(1)}, u32[]{:S(2)}, u32[]{:S(2)}) async-start(bf16[8,4,64,128]{3,2,1,0:T(8,128)(2,1)} %broadcast_in_dim.2), calls=%async_computation.1 | async-start | bytes 1048576 | tf_op jit(solution)/shard_map/all_to_all | solution.py:470
  48.6 6.0 %collective-permute-start.16 = (bf16[8,72,128]{2,1,0:T(8,128)(2,1)S(1)}, bf16[8,72,128]{2,1,0:T(8,128)(2,1)S(1)}, u32[]{:S(2)}, u32[]{:S(2)}) collective-permute-start(bf16[8,72,128]{2,1,0:T(8,128)(2,1)S(1)} %all-to-all-done.2), channel_id=1, source_target_pairs={{0,24},{1,7},{2,26},{3,1},{4,28},{5,3},{6,30},{7,5},{8,0},{9,15},{... | collective-permute-start | bytes 442376 | tf_op jit(solution)/shard_map/ppermute | solution.py:466
  51.0 5.6 %collective-permute-start.15 = (bf16[8,72,128]{2,1,0:T(8,128)(2,1)S(1)}, bf16[8,72,128]{2,1,0:T(8,128)(2,1)S(1)}, u32[]{:S(2)}, u32[]{:S(2)}) collective-permute-start(bf16[8,72,128]{2,1,0:T(8,128)(2,1)S(1)} %all-to-all-done.2), channel_id=1, source_target_pairs={{0,16},{1,5},{2,18},{3,7},{4,20},{5,1},{6,22},{7,3},{8,24},{9,13},... | collective-permute-start | bytes 442376 | tf_op jit(solution)/shard_map/ppermute | solution.py:466
  51.7 6.3 %collective-permute-start.14 = (bf16[8,72,128]{2,1,0:T(8,128)(2,1)S(1)}, bf16[8,72,128]{2,1,0:T(8,128)(2,1)S(1)}, u32[]{:S(2)}, u32[]{:S(2)}) collective-permute-start(bf16[8,72,128]{2,1,0:T(8,128)(2,1)S(1)} %all-to-all-done.2), channel_id=1, source_target_pairs={{0,8},{1,3},{2,10},{3,5},{4,12},{5,7},{6,14},{7,1},{8,16},{9,11},{... | collective-permute-start | bytes 442376 | tf_op jit(solution)/shard_map/ppermute | solution.py:466
  58.1 38.8 %collective-permute-start.19 = (bf16[4,8,72,128]{3,2,1,0:T(8,128)(2,1)S(1)}, bf16[4,8,72,128]{3,2,1,0:T(8,128)(2,1)S(1)}, u32[]{:S(2)}, u32[]{:S(2)}) collective-permute-start(bf16[4,8,72,128]{3,2,1,0:T(8,128)(2,1)S(1)} %pad_maximum_fusion.b0), channel_id=1, source_target_pairs={{0,6},{1,25},{2,0},{3,27},{4,2},{5,29},{6,4},{7,31},{8,14},{9,1},{... | collective-permute-start | bytes 1769480 | tf_op jit(solution)/shard_map/ppermute | solution.py:468
  58.3 38.7 %collective-permute-start.18 = (bf16[4,8,72,128]{3,2,1,0:T(8,128)(2,1)S(1)}, bf16[4,8,72,128]{3,2,1,0:T(8,128)(2,1)S(1)}, u32[]{:S(2)}, u32[]{:S(2)}) collective-permute-start(bf16[4,8,72,128]{3,2,1,0:T(8,128)(2,1)S(1)} %pad_maximum_fusion.b0), channel_id=1, source_target_pairs={{0,4},{1,17},{2,6},{3,19},{4,0},{5,21},{6,2},{7,23},{8,12},{9,25},... | collective-permute-start | bytes 1769480 | tf_op jit(solution)/shard_map/ppermute | solution.py:468
  59.4 37.6 %collective-permute-start.17 = (bf16[4,8,72,128]{3,2,1,0:T(8,128)(2,1)S(1)}, bf16[4,8,72,128]{3,2,1,0:T(8,128)(2,1)S(1)}, u32[]{:S(2)}, u32[]{:S(2)}) collective-permute-start(bf16[4,8,72,128]{3,2,1,0:T(8,128)(2,1)S(1)} %pad_maximum_fusion.b0), channel_id=1, source_target_pairs={{0,2},{1,9},{2,4},{3,11},{4,6},{5,13},{6,0},{7,15},{8,10},{9,17},{... | collective-permute-start | bytes 1769480 | tf_op jit(solution)/shard_map/ppermute | solution.py:468
  60.8 34.8 %collective-permute-start.13 = (bf16[8,4,64,128]{3,2,1,0:T(8,128)(2,1)S(1)}, bf16[8,4,64,128]{3,2,1,0:T(8,128)(2,1)S(1)}, u32[]{:S(2)}, u32[]{:S(2)}) collective-permute-start(bf16[8,4,64,128]{3,2,1,0:T(8,128)(2,1)S(1)} %all-to-all-done.1.up_own.w_own), channel_id=1, source_target_pairs={{0,1},{1,0},{2,3},{3,2},{4,5},{5,4},{6,7},{7,6},{8,9},{9,8},{10,11... | collective-permute-start | bytes 1572872 | tf_op jit(solution)/shard_map/ppermute | solution.py:471
  77.1 9.4 %collective-permute-start.9 = (bf16[2,64,128]{2,1,0:T(8,128)(2,1)S(1)}, bf16[2,64,128]{2,1,0:T(8,128)(2,1)S(1)}, u32[]{:S(2)}, u32[]{:S(2)}) collective-permute-start(bf16[2,64,128]{2,1,0:T(8,128)(2,1)S(1)} %pad_maximum_fusion.2.q0), channel_id=1, source_target_pairs={{0,6},{2,0},{4,2},{6,4},{1,7},{3,1},{5,3},{7,5},{8,14},{10,8},{12,... | collective-permute-start | bytes 98312 | tf_op jit(solution)/shard_map/ppermute | solution.py:473
  86.5 4.6 %collective-permute-start.8 = (bf16[2,64,128]{2,1,0:T(8,128)(2,1)S(1)}, bf16[2,64,128]{2,1,0:T(8,128)(2,1)S(1)}, u32[]{:S(2)}, u32[]{:S(2)}) collective-permute-start(bf16[2,64,128]{2,1,0:T(8,128)(2,1)S(1)} %pad_maximum_fusion.2.q0), channel_id=1, source_target_pairs={{0,4},{2,6},{4,0},{6,2},{1,5},{3,7},{5,1},{7,3},{8,12},{10,14},{12... | collective-permute-start | bytes 98312 | tf_op jit(solution)/shard_map/ppermute | solution.py:473
  91.1 4.5 %collective-permute-start.7 = (bf16[2,64,128]{2,1,0:T(8,128)(2,1)S(1)}, bf16[2,64,128]{2,1,0:T(8,128)(2,1)S(1)}, u32[]{:S(2)}, u32[]{:S(2)}) collective-permute-start(bf16[2,64,128]{2,1,0:T(8,128)(2,1)S(1)} %pad_maximum_fusion.2.q0), channel_id=1, source_target_pairs={{0,2},{2,4},{4,6},{6,0},{1,3},{3,5},{5,7},{7,1},{8,10},{10,12},{12... | collective-permute-start | bytes 98312 | tf_op jit(solution)/shard_map/ppermute | solution.py:473
  103.5 5.1 %collective-permute-start.20 = (bf16[256,128]{1,0:T(8,128)(2,1)S(1)}, bf16[256,128]{1,0:T(8,128)(2,1)S(1)}, u32[]{:S(2)}, u32[]{:S(2)}) collective-permute-start(bf16[256,128]{1,0:T(8,128)(2,1)S(1)} %get-tuple-element.31), channel_id=1, source_target_pairs={{0,1},{1,0},{2,3},{3,2},{4,5},{5,4},{6,7},{7,6},{8,9},{9,8},{10,11... | collective-permute-start | bytes 196616 | tf_op jit(solution)/shard_map/ppermute | solution.py:507
  109.6 4.8 %collective-permute-start.22 = (bf16[32,1024]{1,0:T(8,128)(2,1)S(1)}, bf16[32,1024]{1,0:T(8,128)(2,1)S(1)}, u32[]{:S(2)}, u32[]{:S(2)}) collective-permute-start(bf16[32,1024]{1,0:T(8,128)(2,1)S(1)} %get-tuple-element.34), channel_id=1, source_target_pairs={{0,2},{2,4},{4,6},{6,0},{1,3},{3,5},{5,7},{7,1},{8,10},{10,12},{12... | collective-permute-start | bytes 196616 | tf_op jit(solution)/shard_map/ppermute | solution.py:514
  109.7 6.3 %collective-permute-start.23 = (bf16[32,1024]{1,0:T(8,128)(2,1)S(1)}, bf16[32,1024]{1,0:T(8,128)(2,1)S(1)}, u32[]{:S(2)}, u32[]{:S(2)}) collective-permute-start(bf16[32,1024]{1,0:T(8,128)(2,1)S(1)} %get-tuple-element.35), channel_id=1, source_target_pairs={{0,4},{2,6},{4,0},{6,2},{1,5},{3,7},{5,1},{7,3},{8,12},{10,14},{12... | collective-permute-start | bytes 196616 | tf_op jit(solution)/shard_map/ppermute | solution.py:514
  112.6 3.9 %collective-permute-start.24 = (bf16[32,1024]{1,0:T(8,128)(2,1)S(1)}, bf16[32,1024]{1,0:T(8,128)(2,1)S(1)}, u32[]{:S(2)}, u32[]{:S(2)}) collective-permute-start(bf16[32,1024]{1,0:T(8,128)(2,1)S(1)} %get-tuple-element.36), channel_id=1, source_target_pairs={{0,6},{2,0},{4,2},{6,4},{1,7},{3,1},{5,3},{7,5},{8,14},{10,8},{12,... | collective-permute-start | bytes 196616 | tf_op jit(solution)/shard_map/ppermute | solution.py:514
  (6 other events, 22.4 us)
